TPU v7x, 128 devices: a whole 4x4x4 slice. The times are simulated.
128 devices in a mesh: kv: 16 (over z, x), tp: 8 (over y, core).
Axes of the slice: x: 4, y: 4, z: 4, core: 2. Of those that a mesh axis runs over, the one named last changes fastest.
Arguments:
- tokens: bfloat16 [65536, 2048], P('kv'), may hold values from -6 to 6
- w_query: bfloat16 [2048, 2048], P(None, 'tp'), may hold values from -0.125 to 0.125
- w_key: bfloat16 [2048, 2048], P(None, 'tp'), may hold values from -0.125 to 0.125
- w_value: bfloat16 [2048, 2048], P(None, 'tp'), may hold values from -0.125 to 0.125
- w_out: bfloat16 [2048, 2048], P('tp'), may hold values from -1 to 1, as said below
- query_gain: float32 [128], replicated, may hold values from 0.5 to 1.5
- key_gain: float32 [128], replicated, may hold values from 0.5 to 1.5
- out_gain: float32 [2048], replicated, may hold values from 0.5 to 1.5
- chosen: int32 [1024, 8], P('kv'), may hold values from -1 to 1023, as said below
Outputs:
- layer_out: bfloat16 [65536, 2048], P('kv', 'tp')
Inputs may be any that keep to these rules, and one draw needn't show every extreme that they name: Row b of chosen lists min(8, b + 1) different key blocks, all at most b, with block b in the first slot, and -1 in the remaining slots. Split the blocks into groups of 64 consecutive blocks. The rows of one group other than the first name together at most 8 different blocks of the first group, and at most 2 different blocks of any other group but their own. Both bounds are reached. Entries of w_out have mean zero; the scale of a column grows smoothly with the feature index, by a factor of 8 from the first to the last feature.
All inputs are finite; a program needn't handle non-finite values.
Results may differ from a plain program's by a relative error of at most 0.025.
Values may be sent and summed in bfloat16 or wider, within the bound.
No kernel may reach another device: no remote copies, remote signals or barrier semaphores. Data moves between devices by JAX's collectives and lax.ppermute only.
A program may use at most 192 MiB of HBM per device.

v0:
```python
import jax
import jax.numpy as jnp
from jax import lax
from jax.experimental import pallas as pl
from jax.experimental.pallas import tpu as pltpu
from jax.sharding import Mesh
from jax.sharding import PartitionSpec as P

HEAD_DIM = 128
BLOCK = 64
HOT = 8
REACH = 2
KV = ("kv_0", "kv_1")
TP = ("tp_0", "tp_1")
WIDTH = 256
PAIR = 2
norm_eps = 1e-06
LOG2E = 1.4426950408889634
bf16 = jnp.bfloat16
f32 = jnp.float32
VMEM_LIMIT = 60 * 1024 * 1024


def head_norm(values, gain_row):
    factor = lax.rsqrt(jnp.mean(values * values, axis=-1, keepdims=True) + norm_eps)
    return (values * factor * gain_row).astype(bf16)


def share_kernel(rank, tok, out):
    rows = tok[...].astype(f32)
    devices = out.shape[0]
    part = BLOCK // devices
    for k in range(out.shape[1] // 16):
        parts = []
        for b in range(16 // part):
            first = (k * (16 // part) + b) * BLOCK
            parts.append(rows[first : first + BLOCK].reshape(devices, part, WIDTH))
        out[:, k * 16 : (k + 1) * 16, :] = jnp.concatenate(parts, axis=1).astype(bf16)


def token_shares(rank, tokens, devices):
    length = tokens.shape[0]
    tile = 1024
    small = tile // devices
    return pl.pallas_call(
        share_kernel,
        grid_spec=pltpu.PrefetchScalarGridSpec(
            num_scalar_prefetch=1,
            grid=(length // tile,),
            in_specs=[pl.BlockSpec((tile, WIDTH), lambda i, rank: (i, rank[0]))],
            out_specs=pl.BlockSpec((devices, small, WIDTH), lambda i, rank: (0, i, 0)),
        ),
        out_shape=jax.ShapeDtypeStruct((devices, length // devices, WIDTH), bf16),
        compiler_params=pltpu.CompilerParams(vmem_limit_bytes=VMEM_LIMIT),
        cost_estimate=pl.CostEstimate(flops=1 << 20, bytes_accessed=4 << 20, transcendentals=0),
        name="token_shares",
    )(rank, tokens)


def qkv_kernel(tok, wq, wk, wv, q_gain, k_gain, queries, pairs, weights, sems):
    @pl.when(pl.program_id(0) == 0)
    def _():
        copies = []
        for n, w in enumerate((wq, wk, wv)):
            span = weights.at[:, pl.ds(n * WIDTH, WIDTH)]
            copies.append(pltpu.make_async_copy(w, span, sems.at[n]))
        for copy in copies:
            copy.start()
        for copy in copies:
            copy.wait()

    sums = jnp.dot(tok[...], weights[...], preferred_element_type=f32)
    blocks = pairs.shape[0]
    for h in range(2):
        lanes = slice(h * HEAD_DIM, (h + 1) * HEAD_DIM)
        queries[:, lanes] = head_norm(sums[:, lanes], q_gain[...])
        key_lanes = slice(WIDTH + h * HEAD_DIM, WIDTH + (h + 1) * HEAD_DIM)
        normed = head_norm(sums[:, key_lanes], k_gain[...])
        pairs[:, 0, :, lanes] = normed.reshape(blocks, BLOCK, HEAD_DIM)
    pairs[:, 1, :, :] = sums[:, 2 * WIDTH :].astype(bf16).reshape(blocks, BLOCK, WIDTH)


def project_qkv(tokens, w_query, w_key, w_value, q_gain, k_gain):
    length, depth = tokens.shape
    tile = 512
    blocks = tile // BLOCK
    anywhere = pl.BlockSpec(memory_space=pl.ANY)
    gain_spec = pl.BlockSpec((1, HEAD_DIM), lambda i: (0, 0))
    return pl.pallas_call(
        qkv_kernel,
        grid=(length // tile,),
        in_specs=[
            pl.BlockSpec((tile, depth), lambda i: (i, 0)),
            anywhere,
            anywhere,
            anywhere,
            gain_spec,
            gain_spec,
        ],
        out_specs=[
            pl.BlockSpec((tile, WIDTH), lambda i: (i, 0)),
            pl.BlockSpec((blocks, PAIR, BLOCK, WIDTH), lambda i: (i, 0, 0, 0)),
        ],
        out_shape=[
            jax.ShapeDtypeStruct((length, WIDTH), bf16),
            jax.ShapeDtypeStruct((length // BLOCK, PAIR, BLOCK, WIDTH), bf16),
        ],
        scratch_shapes=[pltpu.VMEM((depth, 3 * WIDTH), bf16), pltpu.SemaphoreType.DMA((3,))],
        compiler_params=pltpu.CompilerParams(vmem_limit_bytes=VMEM_LIMIT),
        cost_estimate=pl.CostEstimate(
            flops=6 * length * depth * WIDTH, bytes_accessed=2 * length * depth, transcendentals=0
        ),
        name="project_qkv",
    )(tokens, w_query, w_key, w_value, q_gain, k_gain)


def hot_kernel(asked, order, same, other, wk, wv, gain, out, keep):
    keys = jnp.zeros((same.shape[1], WIDTH), f32)
    vals = jnp.zeros((same.shape[1], WIDTH), f32)
    count = same.shape[0]
    for k in range(2 * count):
        rows = same[k] if k < count else other[k - count]
        span = pl.ds(pl.multiple_of(order[k] * WIDTH, WIDTH), WIDTH)
        keys += jnp.dot(rows, wk[span, :], preferred_element_type=f32)
        vals += jnp.dot(rows, wv[span, :], preferred_element_type=f32)
    part = out.shape[1] // 2
    groups = keep.shape[0]
    for h in range(2):
        lanes = slice(h * HEAD_DIM, (h + 1) * HEAD_DIM)
        x = keys[:, lanes]
        factor = lax.rsqrt(jnp.mean(x * x, axis=-1, keepdims=True) + norm_eps)
        keep[:, :part, lanes] = (x * factor * gain[...]).reshape(groups, part, HEAD_DIM)
    keep[:, part:, :] = vals.reshape(groups, part, WIDTH)

    def one(m, carry):
        out[m] = keep[asked[m]].astype(bf16)
        return carry

    lax.fori_loop(0, out.shape[0], one, 0, unroll=8)


def project_hot(asked, order, same, other, w_key, w_value, gain):
    count, rows, _ = same.shape
    groups = 64
    part = rows // groups
    depth = w_key.shape[0]
    sends = asked.shape[0]
    whole = lambda *shape: pl.BlockSpec(shape, lambda i, a, o: (0,) * len(shape))
    return pl.pallas_call(
        hot_kernel,
        grid_spec=pltpu.PrefetchScalarGridSpec(
            num_scalar_prefetch=2,
            grid=(1,),
            in_specs=[
                whole(count, rows, WIDTH),
                whole(count, rows, WIDTH),
                whole(depth, WIDTH),
                whole(depth, WIDTH),
                whole(1, HEAD_DIM),
            ],
            out_specs=whole(sends, 2 * part, WIDTH),
            scratch_shapes=[pltpu.VMEM((groups, 2 * part, WIDTH), f32)],
        ),
        out_shape=jax.ShapeDtypeStruct((sends, 2 * part, WIDTH), bf16),
        compiler_params=pltpu.CompilerParams(vmem_limit_bytes=VMEM_LIMIT),
        cost_estimate=pl.CostEstimate(
            flops=4 * rows * depth * WIDTH, bytes_accessed=4 << 20, transcendentals=0
        ),
        name="project_hot",
    )(asked, order, same, other, w_key, w_value, gain)


def attention_kernel(at, where, q, mask, local, near, hot, out, table, sems):
    copies = []
    start = 0
    for n, part in enumerate((local, near, hot)):
        span = table.at[pl.ds(start, part.shape[0])]
        copies.append(pltpu.make_async_copy(part, span, sems.at[n]))
        start += part.shape[0]
    for copy in copies:
        copy.start()
    for copy in copies:
        copy.wait()

    count, rows_piece, _ = out.shape
    blocks = rows_piece // BLOCK
    slots = mask.shape[1] // BLOCK
    first = where[count]

    def one(n, carry):
        piece = where[n // blocks]
        inner = n % blocks
        block = piece * blocks + inner
        row = pl.multiple_of(block * BLOCK, BLOCK)
        to = pl.multiple_of(inner * BLOCK, BLOCK)
        rows = q[pl.ds(row, BLOCK), :]
        blank = jnp.zeros((BLOCK, HEAD_DIM), bf16)
        both = jnp.concatenate(
            [
                jnp.concatenate([rows[:, :HEAD_DIM], blank], axis=1),
                jnp.concatenate([blank, rows[:, HEAD_DIM:]], axis=1),
            ],
            axis=0,
        )
        base = (first + block) * slots
        picks = [at[base + j] for j in range(slots)]
        keys = jnp.concatenate([table[p, 0] for p in picks], axis=0)
        logits = lax.dot_general(both, keys, (((1,), (1,)), ((), ())), preferred_element_type=f32)
        weights = jnp.exp2(logits) * mask[pl.ds(block, 1), :]
        totals = jnp.sum(weights, axis=-1, keepdims=True)
        values = jnp.concatenate([table[p, 1] for p in picks], axis=0)
        sums = jnp.dot(weights.astype(bf16), values, preferred_element_type=f32)
        scale = 1.0 / totals
        out[n // blocks, pl.ds(to, BLOCK), :HEAD_DIM] = (
            sums[:BLOCK, :HEAD_DIM] * scale[:BLOCK]
        ).astype(bf16)
        out[n // blocks, pl.ds(to, BLOCK), HEAD_DIM:] = (
            sums[BLOCK:, HEAD_DIM:] * scale[BLOCK:]
        ).astype(bf16)
        return carry

    lax.fori_loop(0, count * blocks, one, 0, unroll=4)


def attend(chunk, chunks, ranks, at, where, queries, mask, local, near, hot):
    length = queries.shape[0] // chunks
    slots = mask.shape[1] // BLOCK
    blocks = length // BLOCK
    first = jnp.full((1,), chunk * blocks, jnp.int32)
    where = jnp.concatenate([where, first])
    anywhere = pl.BlockSpec(memory_space=pl.ANY)
    return pl.pallas_call(
        attention_kernel,
        grid_spec=pltpu.PrefetchScalarGridSpec(
            num_scalar_prefetch=2,
            grid=(1,),
            in_specs=[
                pl.BlockSpec((length, WIDTH), lambda i, at, where: (chunk, 0)),
                pl.BlockSpec((blocks, slots * BLOCK), lambda i, at, where: (chunk, 0)),
                anywhere,
                anywhere,
                anywhere,
            ],
            out_specs=pl.BlockSpec((ranks, length // ranks, WIDTH), lambda i, at, where: (0, 0, 0)),
            scratch_shapes=[
                pltpu.VMEM(
                    (local.shape[0] + near.shape[0] + hot.shape[0],) + local.shape[1:], bf16
                ),
                pltpu.SemaphoreType.DMA((3,)),
            ],
        ),
        out_shape=jax.ShapeDtypeStruct((ranks, length // ranks, WIDTH), bf16),
        compiler_params=pltpu.CompilerParams(vmem_limit_bytes=VMEM_LIMIT),
        cost_estimate=pl.CostEstimate(
            flops=8 * length * WIDTH * slots * BLOCK, bytes_accessed=16 << 20, transcendentals=0
        ),
        name="attend",
    )(at, where, queries, mask, local, near, hot)


def out_kernel(order, slot, pieces, w_same, w_other, gain, out, mixed, squares):
    n = pl.program_id(0)
    count = pieces.shape[0]
    half = count // 2
    rows = jnp.concatenate([pieces[order[k]] for k in range(count)], axis=1)
    weight = jnp.concatenate(
        [w_same[k] for k in range(half)] + [w_other[k] for k in range(half)], axis=0
    )
    sums = jnp.dot(rows, weight, preferred_element_type=f32)
    mixed[n] = sums
    tile = sums.shape[1]
    part = sum(sums[:, i : i + 128] * sums[:, i : i + 128] for i in range(0, tile, 128))

    @pl.when(n == 0)
    def _():
        squares[...] = part

    @pl.when(n > 0)
    def _():
        squares[...] += part

    @pl.when(n == pl.num_programs(0) - 1)
    def _():
        total = jnp.sum(squares[...], axis=-1, keepdims=True)
        factor = lax.rsqrt(total * (1.0 / (count * WIDTH)) + norm_eps)
        per = tile // WIDTH
        for j in range(count):
            lanes = slice((j % per) * WIDTH, (j % per + 1) * WIDTH)
            gains = gain[:, j * WIDTH : (j + 1) * WIDTH]
            out[slot[j]] = (mixed[j // per, :, lanes] * factor * gains).astype(bf16)


def project_out(order, slot, pieces, w_same, w_other, gain):
    count, rows, _ = pieces.shape
    half = count // 2
    width = w_same.shape[2]
    tile = 512
    return pl.pallas_call(
        out_kernel,
        grid_spec=pltpu.PrefetchScalarGridSpec(
            num_scalar_prefetch=2,
            grid=(width // tile,),
            in_specs=[
                pl.BlockSpec((count, rows, WIDTH), lambda n, order, slot: (0, 0, 0)),
                pl.BlockSpec((half, WIDTH, tile), lambda n, order, slot: (0, 0, n)),
                pl.BlockSpec((half, WIDTH, tile), lambda n, order, slot: (0, 0, n)),
                pl.BlockSpec((1, width), lambda n, order, slot: (0, 0)),
            ],
            out_specs=pl.BlockSpec((count, rows, WIDTH), lambda n, order, slot: (0, 0, 0)),
            scratch_shapes=[
                pltpu.VMEM((width // tile, rows, tile), f32),
                pltpu.VMEM((rows, 128), f32),
            ],
        ),
        out_shape=jax.ShapeDtypeStruct((count, rows, WIDTH), bf16),
        compiler_params=pltpu.CompilerParams(vmem_limit_bytes=VMEM_LIMIT),
        cost_estimate=pl.CostEstimate(
            flops=2 * rows * width * width, bytes_accessed=12 << 20, transcendentals=0
        ),
        name="project_out",
    )(order, slot, pieces, w_same, w_other, gain)


def place_kernel(order, whole, *rest):
    count = len(rest) - 2
    parts, out, sems = rest[:count], rest[count], rest[count + 1]
    copies = [pltpu.make_async_copy(whole, out.at[pl.ds(0, count)], sems.at[count])]
    for k in range(count):
        copies.append(pltpu.make_async_copy(parts[k], out.at[count + order[k]], sems.at[k]))
    for copy in copies:
        copy.start()
    for copy in copies:
        copy.wait()


def place(order, whole, parts):
    count = len(parts)
    shape = (2 * count,) + parts[0].shape
    anywhere = pl.BlockSpec(memory_space=pl.ANY)
    return pl.pallas_call(
        place_kernel,
        grid_spec=pltpu.PrefetchScalarGridSpec(
            num_scalar_prefetch=1,
            grid=(1,),
            in_specs=[anywhere] * (count + 1),
            out_specs=pl.BlockSpec(shape, lambda i, order: (0, 0, 0)),
            scratch_shapes=[pltpu.SemaphoreType.DMA((count + 1,))],
        ),
        out_shape=jax.ShapeDtypeStruct(shape, bf16),
        compiler_params=pltpu.CompilerParams(vmem_limit_bytes=VMEM_LIMIT),
        cost_estimate=pl.CostEstimate(flops=1 << 20, bytes_accessed=4 << 20, transcendentals=0),
        name="place",
    )(order, whole, *parts)


def exchange(pieces, axes):
    return lax.all_to_all(pieces, axes, split_axis=0, concat_axis=0, tiled=True)


def tied(*arrays):
    return lax.optimization_barrier(arrays)


def along_y(piece, shift):
    ring = lax.axis_size(TP[0])
    return lax.ppermute(piece, TP[0], [(i, (i + shift) % ring) for i in range(ring)])


def both_cores(parts):
    same = jnp.stack(parts)
    return same, lax.ppermute(same, TP[1], [(0, 1), (1, 0)])


OFFSETS = (0, -1, 1, 2)


def piece_order(sign):
    ring = lax.axis_size(TP[0])
    y = lax.axis_index(TP[0])
    c = lax.axis_index(TP[1])
    rows = jnp.stack([(y + ring + sign * d) % ring for d in OFFSETS])
    return jnp.concatenate([2 * rows + c, 2 * rows + 1 - c]).astype(jnp.int32)


def send_pieces(pieces):
    ring = lax.axis_size(TP[0])
    got = []
    for k in range(2 * ring):
        step, swap = OFFSETS[k % ring], k // ring
        pairs = [
            (2 * y + c, 2 * ((y - step) % ring) + (c + swap) % 2)
            for y in range(ring)
            for c in range(2)
        ]
        got.append(lax.ppermute(pieces[k], TP, pairs) if k else pieces[0])
    return got


def local(tokens, w_query, w_key, w_value, w_out, query_gain, key_gain, out_gain, chosen):
    length, _ = tokens.shape
    blocks_here = length // BLOCK
    devices = lax.axis_size(KV)
    position = lax.axis_index(KV)
    ranks = lax.axis_size(TP)
    part = BLOCK // devices
    key_row = key_gain[None, :]
    query_row = (query_gain * (HEAD_DIM ** (-0.5) * LOG2E))[None, :]

    usable = chosen >= 0
    pick = jnp.where(usable, chosen, 0)
    owner_of = pick // blocks_here
    all_blocks = jnp.arange(devices * blocks_here, dtype=jnp.int32)
    marked = jnp.where(usable & (owner_of != position), chosen, -1)
    wanted = jnp.any(marked[:, :, None] == all_blocks[None, None, :], axis=(0, 1)).reshape(
        devices, blocks_here
    )
    rank_of = jnp.cumsum(wanted.astype(jnp.int32), axis=1) - 1
    local_ids = jnp.arange(blocks_here, dtype=jnp.int32)
    places = wanted[:, :, None] & (
        rank_of[:, :, None] == jnp.arange(HOT, dtype=jnp.int32)[None, None, :]
    )
    named = jnp.sum(jnp.where(places, local_ids[None, :, None], 0), axis=1).astype(jnp.int32)
    requests = jnp.concatenate([named, jnp.broadcast_to(named[:1], named.shape)], axis=1)
    asked = exchange(requests, KV)
    asked_near = asked[:, :REACH].reshape(-1)
    asked_hot = asked[:, HOT:].reshape(-1)
    order = piece_order(1)
    toward = piece_order(-1)
    same_order = jnp.arange(ranks, dtype=jnp.int32)
    slot_for = jnp.sum(
        jnp.where(toward[None, :] == same_order[:, None], same_order[None, :], 0), axis=1
    ).astype(jnp.int32)

    rank = lax.axis_index(TP).astype(jnp.int32).reshape(1)
    shares = exchange(token_shares(rank, tokens, devices), KV)[0]
    w_after = along_y(w_out, 1)
    w_before = along_y(w_out, -1)

    queries, pairs = project_qkv(tokens, w_query, w_key, w_value, query_row, key_row)
    sent = pairs[asked_near].reshape(devices, REACH, PAIR, BLOCK, WIDTH)
    sent, w_after, w_before, shares = tied(sent, w_after, w_before, shares)
    near = exchange(sent, KV).reshape(devices * REACH, PAIR, BLOCK, WIDTH)
    parts = [shares] + [along_y(shares, shift) for shift in (1, -1, 2)]
    rows_same, rows_other = both_cores(parts)
    half = w_out.shape[0] // 2
    w_far = [along_y(w_after[:half], 1), along_y(w_before[half:], -1)]
    flat_rank = rank_of.reshape(-1)
    slot_rank = jnp.sum(
        jnp.where(pick[:, :, None] == all_blocks[None, None, :], flat_rank[None, None, :], 0), axis=-1
    )
    near_at = blocks_here + owner_of * REACH + slot_rank
    hot_at = blocks_here + devices * REACH + slot_rank
    at = jnp.where(
        owner_of == position, pick % blocks_here, jnp.where(owner_of == 0, hot_at, near_at)
    )
    at = jnp.where(usable, at, 0).astype(jnp.int32).reshape(-1)
    mask = jnp.repeat(usable.astype(f32), BLOCK, axis=1)

    asked_hot, at, mask, slot_for, toward = tied(asked_hot, at, mask, slot_for, toward)
    sent_hot = project_hot(asked_hot, order, rows_same, rows_other, w_key, w_value, key_row)
    w_same = jnp.concatenate([w_out, w_after, w_before, *w_far], axis=0)
    w_same = w_same.reshape((ranks // 2,) + w_out.shape)
    near, sent_hot, w_same = tied(near, sent_hot, w_same)
    hot = exchange(sent_hot.reshape(devices, HOT * 2 * part, WIDTH), KV)
    w_other = lax.ppermute(w_same, TP[1], [(0, 1), (1, 0)])
    hot = hot.reshape(devices, HOT, PAIR, part, WIDTH).transpose(1, 2, 0, 3, 4)
    hot = hot.reshape(HOT, PAIR, BLOCK, WIDTH)

    gain_row = out_gain[None, :]
    hot, w_same, w_other = tied(hot, w_same, w_other)
    first = attend(0, 2, ranks, at, same_order, queries, mask, pairs, near, hot)
    first = exchange(first, TP)
    second = attend(1, 2, ranks, at, toward, queries, mask, pairs, near, hot)
    second = send_pieces(second)
    first = project_out(order, same_order, first, w_same, w_other, gain_row)
    second = jnp.stack(tied(first, *second)[1:])
    first = exchange(first, TP)
    second = project_out(same_order, slot_for, second, w_same, w_other, gain_row)
    second = send_pieces(second)
    return place(order, first, second).reshape(length, WIDTH)


def solution(mesh):
    split = Mesh(mesh.devices.reshape(4, 4, 4, 2), KV + TP)
    return jax.shard_map(
        local,
        mesh=split,
        in_specs=(
            P(KV, None),
            P(None, TP),
            P(None, TP),
            P(None, TP),
            P(TP, None),
            P(),
            P(),
            P(),
            P(KV, None),
        ),
        out_specs=P(KV, TP),
        check_vma=False,
    )
```

profile of v0, /device:TPU:25, one launch (start us, length us, event | category | flops | bytes accessed | tf_op | source)
XLA Modules:
  0.0 208.2 jit_solution(11849723484991648736)
XLA Ops:
  0.0 1.5 collective-permute-start.1
  4.0 7.6 %all-to-all-start = ((s32[16,1,16]{2,1,0:T(1,128)}), s32[16,1,16]{2,1,0:T(1,128)S(1)}, u32[]{:S(2)}, u32[]{:S(2)}) async-start(s32[16,1,16]{2,1,0:T(1,128)} %bitcast.6), calls=%async_computation | async-start | bytes 16384 | tf_op jit(solution)/shard_map/all_to_all | solution.py:357
  11.7 1.2 multiply_bitcast_fusion.q_gain
  12.9 1.3 select_reduce_fusion
  14.3 4.0 %token_shares.1 = bf16[16,256,256]{2,1,0:T(8,128)(2,1)} custom-call(s32[1]{0:T(128)} %bitcast.13.rank, bf16[4096,2048]{1,0:T(8,128)(2,1)} %tok.3), custom_call_target="tpu_custom_call" | custom-call | flops 1048576 | bytes 4194304 | tf_op jit(solution)/shard_map/token_shares/pallas_call | solution.py:45
  18.3 6.6 %all-to-all-start.1 = ((bf16[16,256,256]{2,1,0:T(8,128)(2,1)}), bf16[16,256,256]{2,1,0:T(8,128)(2,1)S(1)}, u32[]{:S(2)}, u32[]{:S(2)}) async-start(bf16[16,256,256]{2,1,0:T(8,128)(2,1)} %token_shares.1), calls=%async_computation.1 | async-start | bytes 4194304 | tf_op jit(solution)/shard_map/all_to_all | solution.py:357
  24.9 19.7 %project_qkv.1 = (bf16[4096,256]{1,0:T(8,128)(2,1)}, bf16[64,2,64,256]{3,2,1,0:T(8,128)(2,1)}) custom-call(bf16[4096,2048]{1,0:T(8,128)(2,1)} %tok.3, bf16[2048,256]{1,0:T(8,128)(2,1)} %wq.1, bf16[2048,256]{1,0:T(8,128)(2,1)} %wk.3, bf16[2048,256]{1,0:T(8,128)(2,1)} %wv.3, f32[1,128]{1,0:T(1,128)} %multiply_bitcast_fusion.q_gain, f32[1,128]{1,0:T(1,128)} %bitcast.97), custom_call_target="tpu_custom_call" | custom-call | flops 12884901888 | bytes 16777216 | tf_op jit(solution)/shard_map/project_qkv/pallas_call | solution.py:89
  46.1 4.2 %gather_fusion = bf16[32,2,64,256]{3,2,1,0:T(8,128)(2,1)} fusion(bf16[64,2,64,256]{3,2,1,0:T(8,128)(2,1)} %get-tuple-element.33.local, s32[1024]{0:T(1024)S(1)} %pad_clamp_fusion), kind=kCustom, calls=%fused_computation | custom fusion | bytes 4194432 | tf_op jit(solution)/shard_map/gather | solution.py:440
  50.3 1.8 all-to-all-done.1
  52.2 6.4 %all-to-all-start.2 = ((bf16[16,2,2,64,256]{4,3,2,1,0:T(8,128)(2,1)}), bf16[16,2,2,64,256]{4,3,2,1,0:T(8,128)(2,1)S(1)}, u32[]{:S(2)}, u32[]{:S(2)}) async-start(bf16[16,2,2,64,256]{4,3,2,1,0:T(8,128)(2,1)} %bitcast.86), calls=%async_computation.2 | async-start | bytes 4194304 | tf_op jit(solution)/shard_map/all_to_all | solution.py:357
  59.9 0.9 broadcast_in_dim.76
  63.5 2.3 %constant_dynamic-update-slice_fusion.4 = bf16[1024,2048]{1,0:T(8,128)(2,1)} fusion(bf16[256,2048]{1,0:T(8,128)(2,1)} %param.13), kind=kLoop, calls=%fused_computation.48 | loop fusion | bytes 2097152
  66.6 1.3 collective-permute-start.2
  68.0 1.0 collective-permute-start.4
  69.0 1.1 slice.70
  70.1 1.9 collective-permute-start.6
  72.4 2.3 %constant_dynamic-update-slice_fusion.3 = bf16[1024,2048]{1,0:T(8,128)(2,1)} fusion(bf16[1024,2048]{1,0:T(8,128)(2,1)} %constant_dynamic-update-slice_fusion.4, bf16[256,2048]{1,0:T(8,128)(2,1)} %collective-permute-done), kind=kLoop, calls=%fused_computation.47 | loop fusion | bytes 2097152
  74.9 3.7 %collective-permute-start.5 = (bf16[4,256,256]{2,1,0:T(8,128)(2,1)S(1)}, bf16[4,256,256]{2,1,0:T(8,128)(2,1)}, u32[]{:S(2)}, u32[]{:S(2)}) collective-permute-start(bf16[4,256,256]{2,1,0:T(8,128)(2,1)S(1)} %pad_maximum_fusion.same), channel_id=1, source_target_pairs={{0,1},{1,0},{2,3},{3,2},{4,5},{5,4},{6,7},{7,6},{8,9},{9,8},{10,11... | collective-permute-start | bytes 1572872 | tf_op jit(solution)/shard_map/ppermute | solution.py:371
  78.5 1.0 constant_dynamic-update-slice_fusion.2
  79.6 5.1 %collective-permute-done.6 = bf16[128,2048]{1,0:T(8,128)(2,1)S(1)} collective-permute-done((bf16[128,2048]{1,0:T(8,128)(2,1)S(1)}, bf16[128,2048]{1,0:T(8,128)(2,1)S(1)}, u32[]{:S(2)}, u32[]{:S(2)}) %collective-permute-start.6) | collective-permute-done | bytes 524320 | tf_op jit(solution)/shard_map/ppermute | solution.py:366
  84.7 0.8 constant_dynamic-update-slice_fusion.1
  85.5 1.2 collective-permute-done.7
  86.7 0.9 constant_dynamic-update-slice_fusion
  87.5 4.4 %project_hot.1 = bf16[128,8,256]{2,1,0:T(8,128)(2,1)} custom-call(s32[128]{0:T(128)} %reshape.81.asked, s32[8]{0:T(128)} %pad_add_fusion.1.order, bf16[4,256,256]{2,1,0:T(8,128)(2,1)} %copy-done.3, bf16[4,256,256]{2,1,0:T(8,128)(2,1)} %collective-permute-done.5.other, bf16[2048,256]{1,0:T(8,128)(2,1)} %wk.3, bf16[2048,256]{1,0:T(8,128)(2,1)} %wv.3, ...), custom_call_target="tpu_custom_call" | custom-call | flops 536870912 | bytes 4194304 | tf_op jit(solution)/shard_map/project_hot/pallas_call | solution.py:149
  91.9 2.3 %collective-permute-start.8 = (bf16[4,256,2048]{2,1,0:T(8,128)(2,1)}, bf16[4,256,2048]{2,1,0:T(8,128)(2,1)}, u32[]{:S(2)}, u32[]{:S(2)}) collective-permute-start(bf16[4,256,2048]{2,1,0:T(8,128)(2,1)} %bitcast.81), channel_id=1, source_target_pairs={{0,1},{1,0},{2,3},{3,2},{4,5},{5,4},{6,7},{7,6},{8,9},{9,8},{10,11... | collective-permute-start | bytes 12582920 | tf_op jit(solution)/shard_map/ppermute | solution.py:465
  94.3 17.7 %all_to_all.37 = bf16[16,64,256]{2,1,0:T(8,128)(2,1)S(1)} all-to-all(bf16[16,64,256]{2,1,0:T(8,128)(2,1)} %bitcast.88), channel_id=1, replica_groups=mesh['kv_0'=4,'kv_1'=4,'tp_0'=4,'tp_1'=2] {'kv_0','kv_1'}, dimensions={0} | all-to-all | bytes 1048576 | tf_op jit(solution)/shard_map/all_to_all | solution.py:357
  112.5 0.9 reshape.91.hot
  113.5 14.0 %attend.2 = bf16[8,256,256]{2,1,0:T(8,128)(2,1)} custom-call(s32[512]{0:T(512)} %reshape.82.at, s32[9]{0:T(128)} %constant.108.clone.1.where, bf16[4096,256]{1,0:T(8,128)(2,1)} %get-tuple-element.31.q, f32[64,512]{1,0:T(8,128)} %reshape.83.mask, bf16[64,2,64,256]{3,2,1,0:T(8,128)(2,1)} %get-tuple-element.33.local, bf16[32,2,64,256]{3,2,1,0:T(8,128)(2,1)} %bitcast.84, ...), custom_call_target="tpu_custom_call" | custom-call | flops 2147483648 | bytes 16777216 | tf_op jit(solution)/shard_map/attend/pallas_call | solution.py:232
  127.5 6.6 %all-to-all-start.4 = ((bf16[8,256,256]{2,1,0:T(8,128)(2,1)}), bf16[8,256,256]{2,1,0:T(8,128)(2,1)S(1)}, u32[]{:S(2)}, u32[]{:S(2)}) async-start(bf16[8,256,256]{2,1,0:T(8,128)(2,1)} %attend.2), calls=%async_computation.4 | async-start | bytes 2097152 | tf_op jit(solution)/shard_map/all_to_all | solution.py:357
  134.7 13.9 %attend.3 = bf16[8,256,256]{2,1,0:T(8,128)(2,1)} custom-call(s32[512]{0:T(512)} %reshape.82.at, s32[9]{0:T(128)} %pad_add_fusion.3.where, bf16[4096,256]{1,0:T(8,128)(2,1)} %get-tuple-element.31.q, f32[64,512]{1,0:T(8,128)} %reshape.83.mask, bf16[64,2,64,256]{3,2,1,0:T(8,128)(2,1)} %get-tuple-element.33.local, bf16[32,2,64,256]{3,2,1,0:T(8,128)(2,1)} %bitcast.85, ...), custom_call_target="tpu_custom_call" | custom-call | flops 2147483648 | bytes 16777216 | tf_op jit(solution)/shard_map/attend/pallas_call | solution.py:232
  148.6 1.4 slice_bitcast_fusion.8
  152.1 2.1 %collective-permute-start.13 = (bf16[256,256]{1,0:T(8,128)(2,1)S(1)}, bf16[256,256]{1,0:T(8,128)(2,1)S(1)}, u32[]{:S(2)}, u32[]{:S(2)}) collective-permute-start(bf16[256,256]{1,0:T(8,128)(2,1)S(1)} %get-tuple-element.69), channel_id=1, source_target_pairs={{0,3},{1,2},{2,5},{3,4},{4,7},{5,6},{6,1},{7,0},{8,11},{9,10},{10,... | collective-permute-start | bytes 393224 | tf_op jit(solution)/shard_map/ppermute | solution.py:395
  154.3 4.5 %collective-permute-done.10 = bf16[256,256]{1,0:T(8,128)(2,1)S(1)} collective-permute-done((bf16[256,256]{1,0:T(8,128)(2,1)S(1)}, bf16[256,256]{1,0:T(8,128)(2,1)S(1)}, u32[]{:S(2)}, u32[]{:S(2)}) %collective-permute-start.10) | collective-permute-done | bytes 131104 | tf_op jit(solution)/shard_map/ppermute | solution.py:395
  158.8 1.0 collective-permute-start.9
  160.8 7.8 %project_out.2 = bf16[8,256,256]{2,1,0:T(8,128)(2,1)} custom-call(s32[8]{0:T(128)} %pad_add_fusion.1.order, s32[8]{0:T(128)} %iota.23.slot, bf16[8,256,256]{2,1,0:T(8,128)(2,1)} %copy-done.2, bf16[4,256,2048]{2,1,0:T(8,128)(2,1)} %bitcast.82, bf16[4,256,2048]{2,1,0:T(8,128)(2,1)} %collective-permute-done.8.w_other, f32[1,2048]{1,0:T(1,128)} %bitcast.95), custom_call_target="tpu_custom_call" | custom-call | flops 2147483648 | bytes 12582912 | tf_op jit(solution)/shard_map/project_out/pallas_call | solution.py:298
  168.5 6.8 %all-to-all-start.5 = ((bf16[8,256,256]{2,1,0:T(8,128)(2,1)}), bf16[8,256,256]{2,1,0:T(8,128)(2,1)S(1)}, u32[]{:S(2)}, u32[]{:S(2)}) async-start(bf16[8,256,256]{2,1,0:T(8,128)(2,1)} %project_out.2), calls=%async_computation.5 | async-start | bytes 2097152 | tf_op jit(solution)/shard_map/all_to_all | solution.py:357
  176.5 7.8 %project_out.3 = bf16[8,256,256]{2,1,0:T(8,128)(2,1)} custom-call(s32[8]{0:T(128)} %iota.24.order, s32[8]{0:T(128)} %select_reduce_fusion.2.slot, bf16[8,256,256]{2,1,0:T(8,128)(2,1)} %copy-done.4, bf16[4,256,2048]{2,1,0:T(8,128)(2,1)} %bitcast.83, bf16[4,256,2048]{2,1,0:T(8,128)(2,1)} %collective-permute-done.8.w_other, f32[1,2048]{1,0:T(1,128)} %bitcast.96), custom_call_target="tpu_custom_call" | custom-call | flops 2147483648 | bytes 12582912 | tf_op jit(solution)/shard_map/project_out/pallas_call | solution.py:298
  184.2 2.0 slice_bitcast_fusion
  186.2 1.1 collective-permute-start.16
  187.7 1.2 collective-permute-start.18
  188.9 1.2 collective-permute-start.19
  190.1 1.7 collective-permute-start.20
  191.8 0.8 collective-permute-start.21
  192.6 3.9 %collective-permute-done.17.rest_2_ = bf16[256,256]{1,0:T(8,128)(2,1)S(1)} collective-permute-done((bf16[256,256]{1,0:T(8,128)(2,1)S(1)}, bf16[256,256]{1,0:T(8,128)(2,1)S(1)}, u32[]{:S(2)}, u32[]{:S(2)}) %collective-permute-start.17) | collective-permute-done | bytes 131104 | tf_op jit(solution)/shard_map/ppermute | solution.py:395
  196.6 0.8 collective-permute-done.20.rest_5_
  197.4 1.8 collective-permute-done.21.rest_6_
  199.2 4.2 %collective-permute-done.22.rest_7_ = bf16[256,256]{1,0:T(8,128)(2,1)S(1)} collective-permute-done((bf16[256,256]{1,0:T(8,128)(2,1)S(1)}, bf16[256,256]{1,0:T(8,128)(2,1)S(1)}, u32[]{:S(2)}, u32[]{:S(2)}) %collective-permute-start.22) | collective-permute-done | bytes 131104 | tf_op jit(solution)/shard_map/ppermute | solution.py:395
  204.4 3.6 %place.1 = bf16[16,256,256]{2,1,0:T(8,128)(2,1)} custom-call(s32[8]{0:T(128)} %pad_add_fusion.1.order, bf16[8,256,256]{2,1,0:T(8,128)(2,1)} %copy-done.1, bf16[256,256]{1,0:T(8,128)(2,1)} %get-tuple-element.66.rest_0_, bf16[256,256]{1,0:T(8,128)(2,1)} %copy-done.5, bf16[256,256]{1,0:T(8,128)(2,1)} %copy-done.6, bf16[256,256]{1,0:T(8,128)(2,1)} %copy-done.7, ...), custom_call_target="tpu_custom_call" | custom-call | flops 1048576 | bytes 4194304 | tf_op jit(solution)/shard_map/place/pallas_call | solution.py:340
  (101 shorter events, 16.2 us)
Async XLA Ops:
  0.0 52.2 %collective-permute-start = (bf16[256,2048]{1,0:T(8,128)(2,1)}, bf16[256,2048]{1,0:T(8,128)(2,1)}, u32[]{:S(2)}, u32[]{:S(2)}) collective-permute-start(bf16[256,2048]{1,0:T(8,128)(2,1)} %param.13), channel_id=1, source_target_pairs={{0,2},{2,4},{4,6},{6,0},{1,3},{3,5},{5,7},{7,1},{8,10},{10,12},{12... | collective-permute-start | bytes 3145736 | tf_op jit(solution)/shard_map/ppermute | solution.py:366
  0.0 52.2 %collective-permute-start.1 = (bf16[256,2048]{1,0:T(8,128)(2,1)}, bf16[256,2048]{1,0:T(8,128)(2,1)S(1)}, u32[]{:S(2)}, u32[]{:S(2)}) collective-permute-start(bf16[256,2048]{1,0:T(8,128)(2,1)} %param.13), channel_id=1, source_target_pairs={{0,6},{2,0},{4,2},{6,4},{1,7},{3,1},{5,3},{7,5},{8,14},{10,8},{12,... | collective-permute-start | bytes 3145736 | tf_op jit(solution)/shard_map/ppermute | solution.py:366
  4.0 14.3 %all-to-all-start = ((s32[16,1,16]{2,1,0:T(1,128)}), s32[16,1,16]{2,1,0:T(1,128)S(1)}, u32[]{:S(2)}, u32[]{:S(2)}) async-start(s32[16,1,16]{2,1,0:T(1,128)} %bitcast.6), calls=%async_computation | async-start | bytes 16384 | tf_op jit(solution)/shard_map/all_to_all | solution.py:357
  18.3 33.8 %all-to-all-start.1 = ((bf16[16,256,256]{2,1,0:T(8,128)(2,1)}), bf16[16,256,256]{2,1,0:T(8,128)(2,1)S(1)}, u32[]{:S(2)}, u32[]{:S(2)}) async-start(bf16[16,256,256]{2,1,0:T(8,128)(2,1)} %token_shares.1), calls=%async_computation.1 | async-start | bytes 4194304 | tf_op jit(solution)/shard_map/all_to_all | solution.py:357
  52.2 39.7 %all-to-all-start.2 = ((bf16[16,2,2,64,256]{4,3,2,1,0:T(8,128)(2,1)}), bf16[16,2,2,64,256]{4,3,2,1,0:T(8,128)(2,1)S(1)}, u32[]{:S(2)}, u32[]{:S(2)}) async-start(bf16[16,2,2,64,256]{4,3,2,1,0:T(8,128)(2,1)} %bitcast.86), calls=%async_computation.2 | async-start | bytes 4194304 | tf_op jit(solution)/shard_map/all_to_all | solution.py:357
  62.3 1.2 copy-start.12
  66.6 8.1 %collective-permute-start.2 = (bf16[256,256]{1,0:T(8,128)(2,1)S(1)}, bf16[256,256]{1,0:T(8,128)(2,1)S(1)}, u32[]{:S(2)}, u32[]{:S(2)}) collective-permute-start(bf16[256,256]{1,0:T(8,128)(2,1)S(1)} %slice_bitcast_fusion.16), channel_id=1, source_target_pairs={{0,2},{2,4},{4,6},{6,0},{1,3},{3,5},{5,7},{7,1},{8,10},{10,12},{12... | collective-permute-start | bytes 393224 | tf_op jit(solution)/shard_map/ppermute | solution.py:366
  67.9 6.9 %collective-permute-start.3 = (bf16[256,256]{1,0:T(8,128)(2,1)S(1)}, bf16[256,256]{1,0:T(8,128)(2,1)S(1)}, u32[]{:S(2)}, u32[]{:S(2)}) collective-permute-start(bf16[256,256]{1,0:T(8,128)(2,1)S(1)} %slice_bitcast_fusion.16), channel_id=1, source_target_pairs={{0,6},{2,0},{4,2},{6,4},{1,7},{3,1},{5,3},{7,5},{8,14},{10,8},{12,... | collective-permute-start | bytes 393224 | tf_op jit(solution)/shard_map/ppermute | solution.py:366
  68.0 6.7 %collective-permute-start.4 = (bf16[256,256]{1,0:T(8,128)(2,1)S(1)}, bf16[256,256]{1,0:T(8,128)(2,1)S(1)}, u32[]{:S(2)}, u32[]{:S(2)}) collective-permute-start(bf16[256,256]{1,0:T(8,128)(2,1)S(1)} %slice_bitcast_fusion.16), channel_id=1, source_target_pairs={{0,4},{2,6},{4,0},{6,2},{1,5},{3,7},{5,1},{7,3},{8,12},{10,14},{12... | collective-permute-start | bytes 393224 | tf_op jit(solution)/shard_map/ppermute | solution.py:366
  70.1 14.6 %collective-permute-start.6 = (bf16[128,2048]{1,0:T(8,128)(2,1)S(1)}, bf16[128,2048]{1,0:T(8,128)(2,1)S(1)}, u32[]{:S(2)}, u32[]{:S(2)}) collective-permute-start(bf16[128,2048]{1,0:T(8,128)(2,1)S(1)} %slice.70), channel_id=1, source_target_pairs={{0,2},{2,4},{4,6},{6,0},{1,3},{3,5},{5,7},{7,1},{8,10},{10,12},{12... | collective-permute-start | bytes 1572872 | tf_op jit(solution)/shard_map/ppermute | solution.py:366
  72.1 14.6 %collective-permute-start.7 = (bf16[128,2048]{1,0:T(8,128)(2,1)S(1)}, bf16[128,2048]{1,0:T(8,128)(2,1)S(1)}, u32[]{:S(2)}, u32[]{:S(2)}) collective-permute-start(bf16[128,2048]{1,0:T(8,128)(2,1)S(1)} %slice.71), channel_id=1, source_target_pairs={{0,6},{2,0},{4,2},{6,4},{1,7},{3,1},{5,3},{7,5},{8,14},{10,8},{12,... | collective-permute-start | bytes 1572872 | tf_op jit(solution)/shard_map/ppermute | solution.py:366
  74.8 12.7 %copy-start.3 = (bf16[4,256,256]{2,1,0:T(8,128)(2,1)}, bf16[4,256,256]{2,1,0:T(8,128)(2,1)S(1)}, u32[]{:S(2)}) copy-start(bf16[4,256,256]{2,1,0:T(8,128)(2,1)S(1)} %pad_maximum_fusion.same) | copy-start | bytes 1572868
  74.9 12.7 %collective-permute-start.5 = (bf16[4,256,256]{2,1,0:T(8,128)(2,1)S(1)}, bf16[4,256,256]{2,1,0:T(8,128)(2,1)}, u32[]{:S(2)}, u32[]{:S(2)}) collective-permute-start(bf16[4,256,256]{2,1,0:T(8,128)(2,1)S(1)} %pad_maximum_fusion.same), channel_id=1, source_target_pairs={{0,1},{1,0},{2,3},{3,2},{4,5},{5,4},{6,7},{7,6},{8,9},{9,8},{10,11... | collective-permute-start | bytes 1572872 | tf_op jit(solution)/shard_map/ppermute | solution.py:371
  91.9 21.5 %copy-start = (bf16[16,2,2,64,256]{4,3,2,1,0:T(8,128)(2,1)}, bf16[16,2,2,64,256]{4,3,2,1,0:T(8,128)(2,1)S(1)}, u32[]{:S(2)}) copy-start(bf16[16,2,2,64,256]{4,3,2,1,0:T(8,128)(2,1)S(1)} %all-to-all-done.2) | copy-start | bytes 6291460
  91.9 21.5 %collective-permute-start.8 = (bf16[4,256,2048]{2,1,0:T(8,128)(2,1)}, bf16[4,256,2048]{2,1,0:T(8,128)(2,1)}, u32[]{:S(2)}, u32[]{:S(2)}) collective-permute-start(bf16[4,256,2048]{2,1,0:T(8,128)(2,1)} %bitcast.81), channel_id=1, source_target_pairs={{0,1},{1,0},{2,3},{3,2},{4,5},{5,4},{6,7},{7,6},{8,9},{9,8},{10,11... | collective-permute-start | bytes 12582920 | tf_op jit(solution)/shard_map/ppermute | solution.py:465
  113.5 20.6 %copy-start.13 = (s32[8]{0:T(128)S(1)}, s32[8]{0:T(128)}, u32[]{:S(2)}) copy-start(s32[8]{0:T(128)} %copy-done.12) | copy-start | bytes 100
  127.5 32.3 %all-to-all-start.4 = ((bf16[8,256,256]{2,1,0:T(8,128)(2,1)}), bf16[8,256,256]{2,1,0:T(8,128)(2,1)S(1)}, u32[]{:S(2)}, u32[]{:S(2)}) async-start(bf16[8,256,256]{2,1,0:T(8,128)(2,1)} %attend.2), calls=%async_computation.4 | async-start | bytes 2097152 | tf_op jit(solution)/shard_map/all_to_all | solution.py:357
  149.9 8.9 %collective-permute-start.10 = (bf16[256,256]{1,0:T(8,128)(2,1)S(1)}, bf16[256,256]{1,0:T(8,128)(2,1)S(1)}, u32[]{:S(2)}, u32[]{:S(2)}) collective-permute-start(bf16[256,256]{1,0:T(8,128)(2,1)S(1)} %get-tuple-element.72), channel_id=1, source_target_pairs={{0,6},{1,7},{2,0},{3,1},{4,2},{5,3},{6,4},{7,5},{8,14},{9,15},{10,... | collective-permute-start | bytes 393224 | tf_op jit(solution)/shard_map/ppermute | solution.py:395
  150.7 8.1 %collective-permute-start.11 = (bf16[256,256]{1,0:T(8,128)(2,1)S(1)}, bf16[256,256]{1,0:T(8,128)(2,1)S(1)}, u32[]{:S(2)}, u32[]{:S(2)}) collective-permute-start(bf16[256,256]{1,0:T(8,128)(2,1)S(1)} %get-tuple-element.71), channel_id=1, source_target_pairs={{0,4},{1,5},{2,6},{3,7},{4,0},{5,1},{6,2},{7,3},{8,12},{9,13},{10,... | collective-permute-start | bytes 393224 | tf_op jit(solution)/shard_map/ppermute | solution.py:395
  151.4 23.9 %collective-permute-start.12 = (bf16[256,256]{1,0:T(8,128)(2,1)S(1)}, bf16[256,256]{1,0:T(8,128)(2,1)S(1)}, u32[]{:S(2)}, u32[]{:S(2)}) collective-permute-start(bf16[256,256]{1,0:T(8,128)(2,1)S(1)} %get-tuple-element.70), channel_id=1, source_target_pairs={{0,1},{1,0},{2,3},{3,2},{4,5},{5,4},{6,7},{7,6},{8,9},{9,8},{10,11... | collective-permute-start | bytes 393224 | tf_op jit(solution)/shard_map/ppermute | solution.py:395
  152.1 23.2 %collective-permute-start.13 = (bf16[256,256]{1,0:T(8,128)(2,1)S(1)}, bf16[256,256]{1,0:T(8,128)(2,1)S(1)}, u32[]{:S(2)}, u32[]{:S(2)}) collective-permute-start(bf16[256,256]{1,0:T(8,128)(2,1)S(1)} %get-tuple-element.69), channel_id=1, source_target_pairs={{0,3},{1,2},{2,5},{3,4},{4,7},{5,6},{6,1},{7,0},{8,11},{9,10},{10,... | collective-permute-start | bytes 393224 | tf_op jit(solution)/shard_map/ppermute | solution.py:395
  154.2 21.1 %collective-permute-start.14 = (bf16[256,256]{1,0:T(8,128)(2,1)S(1)}, bf16[256,256]{1,0:T(8,128)(2,1)S(1)}, u32[]{:S(2)}, u32[]{:S(2)}) collective-permute-start(bf16[256,256]{1,0:T(8,128)(2,1)S(1)} %get-tuple-element.68), channel_id=1, source_target_pairs={{0,7},{1,6},{2,1},{3,0},{4,3},{5,2},{6,5},{7,4},{8,15},{9,14},{10,... | collective-permute-start | bytes 393224 | tf_op jit(solution)/shard_map/ppermute | solution.py:395
  158.8 16.5 %collective-permute-start.15 = (bf16[256,256]{1,0:T(8,128)(2,1)S(1)}, bf16[256,256]{1,0:T(8,128)(2,1)S(1)}, u32[]{:S(2)}, u32[]{:S(2)}) collective-permute-start(bf16[256,256]{1,0:T(8,128)(2,1)S(1)} %get-tuple-element.67), channel_id=1, source_target_pairs={{0,5},{1,4},{2,7},{3,6},{4,1},{5,0},{6,3},{7,2},{8,13},{9,12},{10,... | collective-permute-start | bytes 393224 | tf_op jit(solution)/shard_map/ppermute | solution.py:395
  158.8 16.5 %collective-permute-start.9 = (bf16[256,256]{1,0:T(8,128)(2,1)S(1)}, bf16[256,256]{1,0:T(8,128)(2,1)S(1)}, u32[]{:S(2)}, u32[]{:S(2)}) collective-permute-start(bf16[256,256]{1,0:T(8,128)(2,1)S(1)} %get-tuple-element.73), channel_id=1, source_target_pairs={{0,2},{1,3},{2,4},{3,5},{4,6},{5,7},{6,0},{7,1},{8,10},{9,11},{10,... | collective-permute-start | bytes 393224 | tf_op jit(solution)/shard_map/ppermute | solution.py:395
  159.8 1.0 copy-start.2
  168.5 34.9 %all-to-all-start.5 = ((bf16[8,256,256]{2,1,0:T(8,128)(2,1)}), bf16[8,256,256]{2,1,0:T(8,128)(2,1)S(1)}, u32[]{:S(2)}, u32[]{:S(2)}) async-start(bf16[8,256,256]{2,1,0:T(8,128)(2,1)} %project_out.2), calls=%async_computation.5 | async-start | bytes 2097152 | tf_op jit(solution)/shard_map/all_to_all | solution.py:357
  175.5 1.0 copy-start.4
  186.2 5.6 %collective-permute-start.16 = (bf16[256,256]{1,0:T(8,128)(2,1)S(1)}, bf16[256,256]{1,0:T(8,128)(2,1)S(1)}, u32[]{:S(2)}, u32[]{:S(2)}) collective-permute-start(bf16[256,256]{1,0:T(8,128)(2,1)S(1)} %get-tuple-element.65), channel_id=1, source_target_pairs={{0,2},{1,3},{2,4},{3,5},{4,6},{5,7},{6,0},{7,1},{8,10},{9,11},{10,... | collective-permute-start | bytes 393224 | tf_op jit(solution)/shard_map/ppermute | solution.py:395
  187.3 9.2 %collective-permute-start.17 = (bf16[256,256]{1,0:T(8,128)(2,1)S(1)}, bf16[256,256]{1,0:T(8,128)(2,1)S(1)}, u32[]{:S(2)}, u32[]{:S(2)}) collective-permute-start(bf16[256,256]{1,0:T(8,128)(2,1)S(1)} %get-tuple-element.64), channel_id=1, source_target_pairs={{0,6},{1,7},{2,0},{3,1},{4,2},{5,3},{6,4},{7,5},{8,14},{9,15},{10,... | collective-permute-start | bytes 393224 | tf_op jit(solution)/shard_map/ppermute | solution.py:395
  187.7 8.9 %collective-permute-start.18 = (bf16[256,256]{1,0:T(8,128)(2,1)S(1)}, bf16[256,256]{1,0:T(8,128)(2,1)S(1)}, u32[]{:S(2)}, u32[]{:S(2)}) collective-permute-start(bf16[256,256]{1,0:T(8,128)(2,1)S(1)} %get-tuple-element.63), channel_id=1, source_target_pairs={{0,4},{1,5},{2,6},{3,7},{4,0},{5,1},{6,2},{7,3},{8,12},{9,13},{10,... | collective-permute-start | bytes 393224 | tf_op jit(solution)/shard_map/ppermute | solution.py:395
  188.9 7.7 %collective-permute-start.19 = (bf16[256,256]{1,0:T(8,128)(2,1)S(1)}, bf16[256,256]{1,0:T(8,128)(2,1)S(1)}, u32[]{:S(2)}, u32[]{:S(2)}) collective-permute-start(bf16[256,256]{1,0:T(8,128)(2,1)S(1)} %get-tuple-element.62), channel_id=1, source_target_pairs={{0,1},{1,0},{2,3},{3,2},{4,5},{5,4},{6,7},{7,6},{8,9},{9,8},{10,11... | collective-permute-start | bytes 393224 | tf_op jit(solution)/shard_map/ppermute | solution.py:395
  190.1 7.3 %collective-permute-start.20 = (bf16[256,256]{1,0:T(8,128)(2,1)S(1)}, bf16[256,256]{1,0:T(8,128)(2,1)S(1)}, u32[]{:S(2)}, u32[]{:S(2)}) collective-permute-start(bf16[256,256]{1,0:T(8,128)(2,1)S(1)} %get-tuple-element.61), channel_id=1, source_target_pairs={{0,3},{1,2},{2,5},{3,4},{4,7},{5,6},{6,1},{7,0},{8,11},{9,10},{10,... | collective-permute-start | bytes 393224 | tf_op jit(solution)/shard_map/ppermute | solution.py:395
  191.8 11.6 %copy-start.5 = (bf16[256,256]{1,0:T(8,128)(2,1)}, bf16[256,256]{1,0:T(8,128)(2,1)S(1)}, u32[]{:S(2)}) copy-start(bf16[256,256]{1,0:T(8,128)(2,1)S(1)} %collective-permute-done.16.rest_1_) | copy-start | bytes 393220
  191.8 7.4 %collective-permute-start.21 = (bf16[256,256]{1,0:T(8,128)(2,1)S(1)}, bf16[256,256]{1,0:T(8,128)(2,1)S(1)}, u32[]{:S(2)}, u32[]{:S(2)}) collective-permute-start(bf16[256,256]{1,0:T(8,128)(2,1)S(1)} %get-tuple-element.60), channel_id=1, source_target_pairs={{0,7},{1,6},{2,1},{3,0},{4,3},{5,2},{6,5},{7,4},{8,15},{9,14},{10,... | collective-permute-start | bytes 393224 | tf_op jit(solution)/shard_map/ppermute | solution.py:395
  196.6 6.9 %copy-start.6 = (bf16[256,256]{1,0:T(8,128)(2,1)}, bf16[256,256]{1,0:T(8,128)(2,1)S(1)}, u32[]{:S(2)}) copy-start(bf16[256,256]{1,0:T(8,128)(2,1)S(1)} %collective-permute-done.17.rest_2_) | copy-start | bytes 393220
  196.6 6.9 %collective-permute-start.22 = (bf16[256,256]{1,0:T(8,128)(2,1)S(1)}, bf16[256,256]{1,0:T(8,128)(2,1)S(1)}, u32[]{:S(2)}, u32[]{:S(2)}) collective-permute-start(bf16[256,256]{1,0:T(8,128)(2,1)S(1)} %get-tuple-element.59), channel_id=1, source_target_pairs={{0,5},{1,4},{2,7},{3,6},{4,1},{5,0},{6,3},{7,2},{8,13},{9,12},{10,... | collective-permute-start | bytes 393224 | tf_op jit(solution)/shard_map/ppermute | solution.py:395
  196.6 6.9 %copy-start.7 = (bf16[256,256]{1,0:T(8,128)(2,1)}, bf16[256,256]{1,0:T(8,128)(2,1)S(1)}, u32[]{:S(2)}) copy-start(bf16[256,256]{1,0:T(8,128)(2,1)S(1)} %collective-permute-done.18.rest_3_) | copy-start | bytes 393220
  196.6 6.9 %copy-start.8 = (bf16[256,256]{1,0:T(8,128)(2,1)}, bf16[256,256]{1,0:T(8,128)(2,1)S(1)}, u32[]{:S(2)}) copy-start(bf16[256,256]{1,0:T(8,128)(2,1)S(1)} %collective-permute-done.19.rest_4_) | copy-start | bytes 393220
  197.4 6.0 %copy-start.9 = (bf16[256,256]{1,0:T(8,128)(2,1)}, bf16[256,256]{1,0:T(8,128)(2,1)S(1)}, u32[]{:S(2)}) copy-start(bf16[256,256]{1,0:T(8,128)(2,1)S(1)} %collective-permute-done.20.rest_5_) | copy-start | bytes 393220
  199.2 4.3 %copy-start.10 = (bf16[256,256]{1,0:T(8,128)(2,1)}, bf16[256,256]{1,0:T(8,128)(2,1)S(1)}, u32[]{:S(2)}) copy-start(bf16[256,256]{1,0:T(8,128)(2,1)S(1)} %collective-permute-done.21.rest_6_) | copy-start | bytes 393220
  203.4 0.6 copy-start.11
  203.4 1.0 copy-start.1
where the time goes:
time: 209 us; the launch traced here: 208 us
  Pallas kernels  75.1 us (36%)
  starting transfers between devices  57.9 us (28%)
  local copies, waits for them, and re-layouts  24.8 us (12%)
  waiting for transfers between devices  23.4 us (11%)
  blocking collectives  17.7 us (8%)
  other arithmetic  8.62 us (4%)
    all_to_all x5, starting transfers between devices, exchange(): return lax.all_to_all(pieces, axes, split_axis=0, concat_axis=0, tiled=True)  34 us
    pallas_call x2, Pallas kernels, attend(): pl.pallas_call(attention_kernel, grid_spec=pltpu.PrefetchScalarGridSpec(n...  27.9 us
    pallas_call x1, Pallas kernels, project_qkv(): pl.pallas_call(qkv_kernel, grid=(length // tile,), in_specs=[pl.BlockSpec...  19.7 us
    all_to_all x1, blocking collectives, exchange(): return lax.all_to_all(pieces, axes, split_axis=0, concat_axis=0, tiled=True)  17.7 us
    pallas_call x2, Pallas kernels, project_out(): pl.pallas_call(out_kernel, grid_spec=pltpu.PrefetchScalarGridSpec(num_sca...  15.5 us
    ppermute x14, waiting for transfers between devices, send_pieces(): got.append(lax.ppermute(pieces[k], TP, pairs) if k else pieces[0])  15.3 us
    ppermute x14, starting transfers between devices, send_pieces(): got.append(lax.ppermute(pieces[k], TP, pairs) if k else pieces[0])  11.7 us
    unnamed x40, local copies, waits for them, and re-layouts  9.13 us
  transfers between devices with their start and end apart: 28, of which 9 were waited for; matrix products, arithmetic and copies ran while one was open for 15% of the time, Pallas kernels for 28%

commit v1 on v0

--- a/solution.py
+++ b/solution.py
@@ -1,3 +1,5 @@
+import functools
+
 import jax
 import jax.numpy as jnp
 from jax import lax
@@ -57,61 +59,95 @@
     )(rank, tokens)
 
 
-def qkv_kernel(tok, wq, wk, wv, q_gain, k_gain, queries, pairs, weights, sems):
-    @pl.when(pl.program_id(0) == 0)
-    def _():
-        copies = []
-        for n, w in enumerate((wq, wk, wv)):
-            span = weights.at[:, pl.ds(n * WIDTH, WIDTH)]
-            copies.append(pltpu.make_async_copy(w, span, sems.at[n]))
-        for copy in copies:
-            copy.start()
-        for copy in copies:
-            copy.wait()
-
-    sums = jnp.dot(tok[...], weights[...], preferred_element_type=f32)
-    blocks = pairs.shape[0]
+def kv_kernel(asked, tok, wk, wv, gain, pairs, sent, keep, out_sem, sent_sem):
+    step = pl.program_id(0)
+    steps = pl.num_programs(0)
+    rows = tok[...]
+    blocks = keep.shape[0] // steps
+    first = pl.multiple_of(step * blocks, blocks)
+    here = pl.ds(first, blocks)
+    keys = jnp.dot(rows, wk[...], preferred_element_type=f32)
     for h in range(2):
         lanes = slice(h * HEAD_DIM, (h + 1) * HEAD_DIM)
-        queries[:, lanes] = head_norm(sums[:, lanes], q_gain[...])
-        key_lanes = slice(WIDTH + h * HEAD_DIM, WIDTH + (h + 1) * HEAD_DIM)
-        normed = head_norm(sums[:, key_lanes], k_gain[...])
-        pairs[:, 0, :, lanes] = normed.reshape(blocks, BLOCK, HEAD_DIM)
-    pairs[:, 1, :, :] = sums[:, 2 * WIDTH :].astype(bf16).reshape(blocks, BLOCK, WIDTH)
-
-
-def project_qkv(tokens, w_query, w_key, w_value, q_gain, k_gain):
+        normed = head_norm(keys[:, lanes], gain[...])
+        keep[here, 0, :, lanes] = normed.reshape(blocks, BLOCK, HEAD_DIM)
+    vals = jnp.dot(rows, wv[...], preferred_element_type=f32).astype(bf16)
+    keep[here, 1, :, :] = vals.reshape(blocks, BLOCK, WIDTH)
+    pltpu.make_async_copy(keep.at[here], pairs.at[here], out_sem).start()
+
+    @pl.when(step == steps - 1)
+    def _():
+        def begin(m, carry):
+            pltpu.make_async_copy(keep.at[asked[m]], sent.at[m], sent_sem).start()
+            return carry
+
+        lax.fori_loop(0, sent.shape[0], begin, 0)
+        pltpu.make_async_copy(keep.at[pl.ds(0, sent.shape[0])], sent, sent_sem).wait()
+        pltpu.make_async_copy(keep, pairs, out_sem).wait()
+
+
+def project_kv(asked, tokens, w_key, w_value, gain):
     length, depth = tokens.shape
-    tile = 512
-    blocks = tile // BLOCK
+    tile = 1024
+    sends = asked.shape[0]
+    shape = (PAIR, BLOCK, WIDTH)
     anywhere = pl.BlockSpec(memory_space=pl.ANY)
-    gain_spec = pl.BlockSpec((1, HEAD_DIM), lambda i: (0, 0))
     return pl.pallas_call(
-        qkv_kernel,
+        kv_kernel,
+        grid_spec=pltpu.PrefetchScalarGridSpec(
+            num_scalar_prefetch=1,
+            grid=(length // tile,),
+            in_specs=[
+                pl.BlockSpec((tile, depth), lambda i, asked: (i, 0)),
+                pl.BlockSpec((depth, WIDTH), lambda i, asked: (0, 0)),
+                pl.BlockSpec((depth, WIDTH), lambda i, asked: (0, 0)),
+                pl.BlockSpec((1, HEAD_DIM), lambda i, asked: (0, 0)),
+            ],
+            out_specs=[anywhere, anywhere],
+            scratch_shapes=[
+                pltpu.VMEM((length // BLOCK,) + shape, bf16),
+                pltpu.SemaphoreType.DMA,
+                pltpu.SemaphoreType.DMA,
+            ],
+        ),
+        out_shape=[
+            jax.ShapeDtypeStruct((length // BLOCK,) + shape, bf16),
+            jax.ShapeDtypeStruct((sends,) + shape, bf16),
+        ],
+        compiler_params=pltpu.CompilerParams(vmem_limit_bytes=VMEM_LIMIT),
+        cost_estimate=pl.CostEstimate(
+            flops=4 * length * depth * WIDTH, bytes_accessed=2 * length * depth, transcendentals=0
+        ),
+        name="project_kv",
+    )(asked, tokens, w_key, w_value, gain)
+
+
+def q_kernel(tok, wq, gain, out):
+    values = jnp.dot(tok[...], wq[...], preferred_element_type=f32)
+    for h in range(2):
+        lanes = slice(h * HEAD_DIM, (h + 1) * HEAD_DIM)
+        out[:, lanes] = head_norm(values[:, lanes], gain[...])
+
+
+def project_q(tokens, w_query, gain):
+    length, depth = tokens.shape
+    tile = 1024
+    return pl.pallas_call(
+        q_kernel,
         grid=(length // tile,),
         in_specs=[
             pl.BlockSpec((tile, depth), lambda i: (i, 0)),
-            anywhere,
-            anywhere,
-            anywhere,
-            gain_spec,
-            gain_spec,
+            pl.BlockSpec((depth, WIDTH), lambda i: (0, 0)),
+            pl.BlockSpec((1, HEAD_DIM), lambda i: (0, 0)),
         ],
-        out_specs=[
-            pl.BlockSpec((tile, WIDTH), lambda i: (i, 0)),
-            pl.BlockSpec((blocks, PAIR, BLOCK, WIDTH), lambda i: (i, 0, 0, 0)),
-        ],
-        out_shape=[
-            jax.ShapeDtypeStruct((length, WIDTH), bf16),
-            jax.ShapeDtypeStruct((length // BLOCK, PAIR, BLOCK, WIDTH), bf16),
-        ],
-        scratch_shapes=[pltpu.VMEM((depth, 3 * WIDTH), bf16), pltpu.SemaphoreType.DMA((3,))],
+        out_specs=pl.BlockSpec((tile, WIDTH), lambda i: (i, 0)),
+        out_shape=jax.ShapeDtypeStruct((length, WIDTH), bf16),
         compiler_params=pltpu.CompilerParams(vmem_limit_bytes=VMEM_LIMIT),
         cost_estimate=pl.CostEstimate(
-            flops=6 * length * depth * WIDTH, bytes_accessed=2 * length * depth, transcendentals=0
-        ),
-        name="project_qkv",
-    )(tokens, w_query, w_key, w_value, q_gain, k_gain)
+            flops=2 * length * depth * WIDTH, bytes_accessed=2 * length * depth, transcendentals=0
+        ),
+        name="project_q",
+    )(tokens, w_query, gain)
 
 
 def hot_kernel(asked, order, same, other, wk, wv, gain, out, keep):
@@ -170,7 +206,8 @@
     )(asked, order, same, other, w_key, w_value, gain)
 
 
-def attention_kernel(at, where, q, mask, local, near, hot, out, table, sems):
+def attention_kernel(first, at, where, q, mask, local, near, hot, *rest):
+    outs, (table, sems) = rest[:-2], rest[-2:]
     copies = []
     start = 0
     for n, part in enumerate((local, near, hot)):
@@ -181,20 +218,15 @@
         copy.start()
     for copy in copies:
         copy.wait()
-
-    count, rows_piece, _ = out.shape
-    blocks = rows_piece // BLOCK
     slots = mask.shape[1] // BLOCK
-    first = where[count]
-
-    def one(n, carry):
-        piece = where[n // blocks]
-        inner = n % blocks
-        block = piece * blocks + inner
+    count = where.shape[0]
+    whole = len(outs) == 1
+    per_piece = mask.shape[0] // count
+    blank = jnp.zeros((BLOCK, HEAD_DIM), bf16)
+
+    def load(block):
         row = pl.multiple_of(block * BLOCK, BLOCK)
-        to = pl.multiple_of(inner * BLOCK, BLOCK)
         rows = q[pl.ds(row, BLOCK), :]
-        blank = jnp.zeros((BLOCK, HEAD_DIM), bf16)
         both = jnp.concatenate(
             [
                 jnp.concatenate([rows[:, :HEAD_DIM], blank], axis=1),
@@ -203,72 +235,104 @@
             axis=0,
         )
         base = (first + block) * slots
-        picks = [at[base + j] for j in range(slots)]
-        keys = jnp.concatenate([table[p, 0] for p in picks], axis=0)
-        logits = lax.dot_general(both, keys, (((1,), (1,)), ((), ())), preferred_element_type=f32)
-        weights = jnp.exp2(logits) * mask[pl.ds(block, 1), :]
-        totals = jnp.sum(weights, axis=-1, keepdims=True)
-        values = jnp.concatenate([table[p, 1] for p in picks], axis=0)
-        sums = jnp.dot(weights.astype(bf16), values, preferred_element_type=f32)
-        scale = 1.0 / totals
-        out[n // blocks, pl.ds(to, BLOCK), :HEAD_DIM] = (
-            sums[:BLOCK, :HEAD_DIM] * scale[:BLOCK]
-        ).astype(bf16)
-        out[n // blocks, pl.ds(to, BLOCK), HEAD_DIM:] = (
-            sums[BLOCK:, HEAD_DIM:] * scale[BLOCK:]
-        ).astype(bf16)
-        return carry
-
-    lax.fori_loop(0, count * blocks, one, 0, unroll=4)
-
-
-def attend(chunk, chunks, ranks, at, where, queries, mask, local, near, hot):
+        return both, [at[base + j] for j in range(slots)]
+
+    def piece_of(n, put):
+        items = [load(where[n] * per_piece + i) for i in range(per_piece)]
+        logits = []
+        for both, picks in items:
+            keys = jnp.concatenate([table[p, 0] for p in picks], axis=0)
+            logits.append(
+                lax.dot_general(both, keys, (((1,), (1,)), ((), ())), preferred_element_type=f32)
+            )
+        weights = []
+        for i in range(per_piece):
+            block = where[n] * per_piece + i
+            weights.append(jnp.exp2(logits[i]) * mask[pl.ds(block, 1), :])
+        for i, (both, picks) in enumerate(items):
+            values = jnp.concatenate([table[p, 1] for p in picks], axis=0)
+            sums = jnp.dot(weights[i].astype(bf16), values, preferred_element_type=f32)
+            scale = 1.0 / jnp.sum(weights[i], axis=-1, keepdims=True)
+            to = slice(i * BLOCK, (i + 1) * BLOCK)
+            put(to, slice(0, HEAD_DIM), sums[:BLOCK, :HEAD_DIM] * scale[:BLOCK])
+            put(to, slice(HEAD_DIM, WIDTH), sums[BLOCK:, HEAD_DIM:] * scale[BLOCK:])
+
+    if whole:
+
+        def one(n, carry):
+            def put(rows, lanes, value):
+                outs[0][n, rows, lanes] = value.astype(bf16)
+
+            piece_of(n, put)
+            return carry
+
+        lax.fori_loop(0, count, one, 0)
+    else:
+        for n in range(count):
+
+            def put(rows, lanes, value, n=n):
+                outs[n][rows, lanes] = value.astype(bf16)
+
+            piece_of(n, put)
+
+
+def whole_block(*shape):
+    return pl.BlockSpec(shape, lambda i, *_: (0,) * len(shape))
+
+
+def attend(chunk, chunks, split, at, where, queries, mask, local, near, hot):
+    ranks = where.shape[0]
     length = queries.shape[0] // chunks
     slots = mask.shape[1] // BLOCK
     blocks = length // BLOCK
-    first = jnp.full((1,), chunk * blocks, jnp.int32)
-    where = jnp.concatenate([where, first])
+    rows = length // ranks
     anywhere = pl.BlockSpec(memory_space=pl.ANY)
-    return pl.pallas_call(
-        attention_kernel,
+    shape = (rows, WIDTH) if split else (ranks, rows, WIDTH)
+    count = ranks if split else 1
+    parts = (local, near, hot)
+    outs = pl.pallas_call(
+        functools.partial(attention_kernel, chunk * blocks),
         grid_spec=pltpu.PrefetchScalarGridSpec(
             num_scalar_prefetch=2,
             grid=(1,),
             in_specs=[
-                pl.BlockSpec((length, WIDTH), lambda i, at, where: (chunk, 0)),
-                pl.BlockSpec((blocks, slots * BLOCK), lambda i, at, where: (chunk, 0)),
+                pl.BlockSpec((length, WIDTH), lambda i, *_: (chunk, 0)),
+                pl.BlockSpec((blocks, slots * BLOCK), lambda i, *_: (chunk, 0)),
                 anywhere,
                 anywhere,
                 anywhere,
             ],
-            out_specs=pl.BlockSpec((ranks, length // ranks, WIDTH), lambda i, at, where: (0, 0, 0)),
+            out_specs=[whole_block(*shape)] * count,
             scratch_shapes=[
-                pltpu.VMEM(
-                    (local.shape[0] + near.shape[0] + hot.shape[0],) + local.shape[1:], bf16
-                ),
+                pltpu.VMEM((sum(p.shape[0] for p in parts),) + local.shape[1:], bf16),
                 pltpu.SemaphoreType.DMA((3,)),
             ],
         ),
-        out_shape=jax.ShapeDtypeStruct((ranks, length // ranks, WIDTH), bf16),
+        out_shape=[jax.ShapeDtypeStruct(shape, bf16)] * count,
         compiler_params=pltpu.CompilerParams(vmem_limit_bytes=VMEM_LIMIT),
         cost_estimate=pl.CostEstimate(
-            flops=8 * length * WIDTH * slots * BLOCK, bytes_accessed=16 << 20, transcendentals=0
+            flops=8 * length * WIDTH * slots * BLOCK, bytes_accessed=10 << 20, transcendentals=0
         ),
         name="attend",
-    )(at, where, queries, mask, local, near, hot)
-
-
-def out_kernel(order, slot, pieces, w_same, w_other, gain, out, mixed, squares):
+    )(at, where, queries, mask, *parts)
+    return list(outs) if split else outs[0]
+
+
+def out_kernel(order, slot, *refs):
+    count = order.shape[0]
     n = pl.program_id(0)
-    count = pieces.shape[0]
-    half = count // 2
-    rows = jnp.concatenate([pieces[order[k]] for k in range(count)], axis=1)
-    weight = jnp.concatenate(
-        [w_same[k] for k in range(half)] + [w_other[k] for k in range(half)], axis=0
-    )
+    if len(refs) > 2 * count + 4:
+        pieces, refs = refs[:count], refs[count:]
+    else:
+        pieces, refs = [refs[0].at[order[k]] for k in range(count)], refs[1:]
+    weights, gain, refs = refs[:count], refs[count], refs[count + 1 :]
+    outs, (mixed, squares) = refs[:-2], refs[-2:]
+    rows = jnp.concatenate([piece[...] for piece in pieces], axis=1)
+    weight = jnp.concatenate([w[...] for w in weights], axis=0)
     sums = jnp.dot(rows, weight, preferred_element_type=f32)
-    mixed[n] = sums
     tile = sums.shape[1]
+    mixed[2 * n] = sums[:, :WIDTH]
+    mixed[2 * n + 1] = sums[:, WIDTH:]
     part = sum(sums[:, i : i + 128] * sums[:, i : i + 128] for i in range(0, tile, 128))
 
     @pl.when(n == 0)
@@ -283,42 +347,43 @@
     def _():
         total = jnp.sum(squares[...], axis=-1, keepdims=True)
         factor = lax.rsqrt(total * (1.0 / (count * WIDTH)) + norm_eps)
-        per = tile // WIDTH
-        for j in range(count):
-            lanes = slice((j % per) * WIDTH, (j % per + 1) * WIDTH)
-            gains = gain[:, j * WIDTH : (j + 1) * WIDTH]
-            out[slot[j]] = (mixed[j // per, :, lanes] * factor * gains).astype(bf16)
-
-
-def project_out(order, slot, pieces, w_same, w_other, gain):
-    count, rows, _ = pieces.shape
-    half = count // 2
-    width = w_same.shape[2]
-    tile = 512
-    return pl.pallas_call(
+        for k in range(count):
+            value = (mixed[slot[k]] * factor * gain[slot[k]]).astype(bf16)
+            if len(outs) == 1:
+                outs[0][k] = value
+            else:
+                outs[k][...] = value
+
+
+def project_out(split, order, slot, pieces, weights, gain):
+    count = len(weights)
+    pieces = list(pieces) if split else [pieces]
+    rows = pieces[0].shape[-2]
+    depth, width = weights[0].shape
+    tile = 2 * WIDTH
+    shape = (rows, WIDTH) if split else (count, rows, WIDTH)
+    outs = pl.pallas_call(
         out_kernel,
         grid_spec=pltpu.PrefetchScalarGridSpec(
             num_scalar_prefetch=2,
             grid=(width // tile,),
-            in_specs=[
-                pl.BlockSpec((count, rows, WIDTH), lambda n, order, slot: (0, 0, 0)),
-                pl.BlockSpec((half, WIDTH, tile), lambda n, order, slot: (0, 0, n)),
-                pl.BlockSpec((half, WIDTH, tile), lambda n, order, slot: (0, 0, n)),
-                pl.BlockSpec((1, width), lambda n, order, slot: (0, 0)),
-            ],
-            out_specs=pl.BlockSpec((count, rows, WIDTH), lambda n, order, slot: (0, 0, 0)),
+            in_specs=[whole_block(*shape)] * len(pieces)
+            + [pl.BlockSpec((depth, tile), lambda n, *_: (0, n))] * count
+            + [whole_block(*gain.shape)],
+            out_specs=[whole_block(*shape)] * len(pieces),
             scratch_shapes=[
-                pltpu.VMEM((width // tile, rows, tile), f32),
+                pltpu.VMEM((count, rows, WIDTH), f32),
                 pltpu.VMEM((rows, 128), f32),
             ],
         ),
-        out_shape=jax.ShapeDtypeStruct((count, rows, WIDTH), bf16),
+        out_shape=[jax.ShapeDtypeStruct(shape, bf16)] * len(pieces),
         compiler_params=pltpu.CompilerParams(vmem_limit_bytes=VMEM_LIMIT),
         cost_estimate=pl.CostEstimate(
             flops=2 * rows * width * width, bytes_accessed=12 << 20, transcendentals=0
         ),
         name="project_out",
-    )(order, slot, pieces, w_same, w_other, gain)
+    )(order, slot, *pieces, *weights, gain)
+    return list(outs) if split else outs[0]
 
 
 def place_kernel(order, whole, *rest):
@@ -347,7 +412,7 @@
             scratch_shapes=[pltpu.SemaphoreType.DMA((count + 1,))],
         ),
         out_shape=jax.ShapeDtypeStruct(shape, bf16),
-        compiler_params=pltpu.CompilerParams(vmem_limit_bytes=VMEM_LIMIT),
+        compiler_params=pltpu.CompilerParams(vmem_limit_bytes=8 << 20),
         cost_estimate=pl.CostEstimate(flops=1 << 20, bytes_accessed=4 << 20, transcendentals=0),
         name="place",
     )(order, whole, *parts)
@@ -427,23 +492,25 @@
     order = piece_order(1)
     toward = piece_order(-1)
     same_order = jnp.arange(ranks, dtype=jnp.int32)
-    slot_for = jnp.sum(
-        jnp.where(toward[None, :] == same_order[:, None], same_order[None, :], 0), axis=1
-    ).astype(jnp.int32)
-
     rank = lax.axis_index(TP).astype(jnp.int32).reshape(1)
     shares = exchange(token_shares(rank, tokens, devices), KV)[0]
     w_after = along_y(w_out, 1)
     w_before = along_y(w_out, -1)
 
-    queries, pairs = project_qkv(tokens, w_query, w_key, w_value, query_row, key_row)
-    sent = pairs[asked_near].reshape(devices, REACH, PAIR, BLOCK, WIDTH)
-    sent, w_after, w_before, shares = tied(sent, w_after, w_before, shares)
+    pairs, sent = project_kv(asked_near, tokens, w_key, w_value, key_row)
+    sent, shares, w_after, w_before = tied(sent, shares, w_after, w_before)
+    sent = sent.reshape(devices, REACH, PAIR, BLOCK, WIDTH)
     near = exchange(sent, KV).reshape(devices * REACH, PAIR, BLOCK, WIDTH)
     parts = [shares] + [along_y(shares, shift) for shift in (1, -1, 2)]
+    again, sent = tied(tokens, sent)
+    queries = project_q(again, w_query, query_row)
+    queries, *parts = tied(queries, *parts)
     rows_same, rows_other = both_cores(parts)
-    half = w_out.shape[0] // 2
-    w_far = [along_y(w_after[:half], 1), along_y(w_before[half:], -1)]
+    sent_hot = project_hot(asked_hot, order, rows_same, rows_other, w_key, w_value, key_row)
+
+    pick, owner_of, rank_of, usable, sent_hot, w_after = tied(
+        pick, owner_of, rank_of, usable, sent_hot, w_after
+    )
     flat_rank = rank_of.reshape(-1)
     slot_rank = jnp.sum(
         jnp.where(pick[:, :, None] == all_blocks[None, None, :], flat_rank[None, None, :], 0), axis=-1
@@ -455,29 +522,27 @@
     )
     at = jnp.where(usable, at, 0).astype(jnp.int32).reshape(-1)
     mask = jnp.repeat(usable.astype(f32), BLOCK, axis=1)
-
-    asked_hot, at, mask, slot_for, toward = tied(asked_hot, at, mask, slot_for, toward)
-    sent_hot = project_hot(asked_hot, order, rows_same, rows_other, w_key, w_value, key_row)
-    w_same = jnp.concatenate([w_out, w_after, w_before, *w_far], axis=0)
-    w_same = w_same.reshape((ranks // 2,) + w_out.shape)
-    near, sent_hot, w_same = tied(near, sent_hot, w_same)
+    w_far = along_y(w_after, 1)
+
+    near, sent_hot = tied(near, sent_hot)
     hot = exchange(sent_hot.reshape(devices, HOT * 2 * part, WIDTH), KV)
-    w_other = lax.ppermute(w_same, TP[1], [(0, 1), (1, 0)])
+    w_same = [w_out, w_after, w_before, w_far]
+    w_other = [lax.ppermute(w, TP[1], [(0, 1), (1, 0)]) for w in w_same]
+    weights = w_same + w_other
     hot = hot.reshape(devices, HOT, PAIR, part, WIDTH).transpose(1, 2, 0, 3, 4)
     hot = hot.reshape(HOT, PAIR, BLOCK, WIDTH)
 
-    gain_row = out_gain[None, :]
-    hot, w_same, w_other = tied(hot, w_same, w_other)
-    first = attend(0, 2, ranks, at, same_order, queries, mask, pairs, near, hot)
+    gains = out_gain.reshape(ranks, 1, WIDTH)
+    first = attend(0, 2, False, at, same_order, queries, mask, pairs, near, hot)
     first = exchange(first, TP)
-    second = attend(1, 2, ranks, at, toward, queries, mask, pairs, near, hot)
+    second = attend(1, 2, True, at, toward, queries, mask, pairs, near, hot)
     second = send_pieces(second)
-    first = project_out(order, same_order, first, w_same, w_other, gain_row)
-    second = jnp.stack(tied(first, *second)[1:])
-    first = exchange(first, TP)
-    second = project_out(same_order, slot_for, second, w_same, w_other, gain_row)
+    first = project_out(False, order, same_order, first, weights, gains)
+    moved = exchange(first, TP)
+    second = tied(first, *second)[1:]
+    second = project_out(True, order, toward, second, weights, gains)
     second = send_pieces(second)
-    return place(order, first, second).reshape(length, WIDTH)
+    return place(order, moved, second).reshape(length, WIDTH)
 
 
 def solution(mesh):

time: 209 us -> 216 us (1.033)
  the two profiles are of different devices: /device:TPU:25 before, /device:TPU:32 now
where the time goes in v1:
time: 216 us; the launch traced here: 213 us
  Pallas kernels  73.3 us (34%)
  waiting for transfers between devices  64.5 us (30%)
  starting transfers between devices  55.7 us (26%)
  local copies, waits for them, and re-layouts  13.6 us (6%)
  other arithmetic  5.54 us (3%)
    all_to_all x6, starting transfers between devices, exchange(): return lax.all_to_all(pieces, axes, split_axis=0, concat_axis=0, tiled=True)  31.8 us
    all_to_all x6, waiting for transfers between devices, exchange(): return lax.all_to_all(pieces, axes, split_axis=0, concat_axis=0, tiled=True)  31 us
    pallas_call x2, Pallas kernels, attend(): pl.pallas_call(functools.partial(attention_kernel, chunk * blocks), grid_...  20.4 us
    ppermute x14, waiting for transfers between devices, send_pieces(): got.append(lax.ppermute(pieces[k], TP, pairs) if k else pieces[0])  20.3 us
    pallas_call x2, Pallas kernels, project_out(): pl.pallas_call(out_kernel, grid_spec=pltpu.PrefetchScalarGridSpec(num_sca...  16.1 us
    pallas_call x1, Pallas kernels, project_kv(): pl.pallas_call(kv_kernel, grid_spec=pltpu.PrefetchScalarGridSpec(num_scal...  15.1 us
    ppermute x14, starting transfers between devices, send_pieces(): got.append(lax.ppermute(pieces[k], TP, pairs) if k else pieces[0])  14.2 us
    ppermute x6, waiting for transfers between devices, along_y(): lax.ppermute(piece, TP[0], [(i, (i + shift) % ring) for i in range(ring)])  12.2 us
  transfers between devices with their start and end apart: 31, of which 16 were waited for; matrix products, arithmetic and copies ran while one was open for 6% of the time, Pallas kernels for 29%

profile of v1, /device:TPU:32, one launch (start us, length us, event | category | flops | bytes accessed | tf_op | source)
XLA Modules:
  0.0 213.1 jit_solution(4388660703876952706)
XLA Ops:
  2.5 7.9 %all-to-all-start = ((s32[16,1,16]{2,1,0:T(1,128)}), s32[16,1,16]{2,1,0:T(1,128)S(1)}, u32[]{:S(2)}, u32[]{:S(2)}) async-start(s32[16,1,16]{2,1,0:T(1,128)} %bitcast.6), calls=%async_computation | async-start | bytes 16384 | tf_op jit(solution)/shard_map/all_to_all | solution.py:422
  10.4 4.0 %token_shares.1 = bf16[16,256,256]{2,1,0:T(8,128)(2,1)} custom-call(s32[1]{0:T(128)} %bitcast.9.rank, bf16[4096,2048]{1,0:T(8,128)(2,1)} %tok.4), custom_call_target="tpu_custom_call" | custom-call | flops 1048576 | bytes 4194304 | tf_op jit(solution)/shard_map/token_shares/pallas_call | solution.py:47
  14.4 2.2 %all-to-all-done = s32[16,1,16]{2,1,0:T(1,128)S(1)} async-done(((s32[16,1,16]{2,1,0:T(1,128)}), s32[16,1,16]{2,1,0:T(1,128)S(1)}, u32[]{:S(2)}, u32[]{:S(2)}) %all-to-all-start) | async-done | bytes 1056 | tf_op jit(solution)/shard_map/all_to_all | solution.py:422
  16.6 5.5 %all-to-all-start.1 = ((bf16[16,256,256]{2,1,0:T(8,128)(2,1)}), bf16[16,256,256]{2,1,0:T(8,128)(2,1)}, u32[]{:S(2)}, u32[]{:S(2)}) async-start(bf16[16,256,256]{2,1,0:T(8,128)(2,1)} %token_shares.1), calls=%async_computation.1 | async-start | bytes 4194304 | tf_op jit(solution)/shard_map/all_to_all | solution.py:422
  22.1 1.6 collective-permute-start
  23.8 1.7 collective-permute-start.1
  26.0 15.1 %project_kv.1 = (bf16[64,2,64,256]{3,2,1,0:T(8,128)(2,1)}, bf16[32,2,64,256]{3,2,1,0:T(8,128)(2,1)}) custom-call(s32[32]{0:T(128)} %reshape.50.asked, bf16[4096,2048]{1,0:T(8,128)(2,1)} %tok.4, bf16[2048,256]{1,0:T(8,128)(2,1)} %wk.3, bf16[2048,256]{1,0:T(8,128)(2,1)} %wv.3, f32[1,128]{1,0:T(1,128)} %bitcast.43), custom_call_target="tpu_custom_call" | custom-call | flops 8589934592 | bytes 16777216 | tf_op jit(solution)/shard_map/project_kv/pallas_call | solution.py:95
  41.1 9.2 %all-to-all-done.1 = bf16[16,256,256]{2,1,0:T(8,128)(2,1)} async-done(((bf16[16,256,256]{2,1,0:T(8,128)(2,1)}), bf16[16,256,256]{2,1,0:T(8,128)(2,1)}, u32[]{:S(2)}, u32[]{:S(2)}) %all-to-all-start.1) | async-done | bytes 2097184 | tf_op jit(solution)/shard_map/all_to_all | solution.py:422
  50.3 0.9 slice_bitcast_fusion
  51.3 0.9 copy-done.5
  52.6 5.4 %all-to-all-start.2 = ((bf16[16,2,2,64,256]{4,3,2,1,0:T(8,128)(2,1)}), bf16[16,2,2,64,256]{4,3,2,1,0:T(8,128)(2,1)S(1)}, u32[]{:S(2)}, u32[]{:S(2)}) async-start(bf16[16,2,2,64,256]{4,3,2,1,0:T(8,128)(2,1)} %bitcast.32), calls=%async_computation.2 | async-start | bytes 4194304 | tf_op jit(solution)/shard_map/all_to_all | solution.py:422
  58.6 1.6 collective-permute-start.2
  60.1 1.7 collective-permute-start.3
  61.8 2.0 collective-permute-start.4
  63.8 10.1 %project_q.1.q = bf16[4096,256]{1,0:T(8,128)(2,1)} custom-call(bf16[4096,2048]{1,0:T(8,128)(2,1)} %tok.4, bf16[2048,256]{1,0:T(8,128)(2,1)} %wq.1, f32[1,128]{1,0:T(1,128)} %multiply_bitcast_fusion.gain), custom_call_target="tpu_custom_call" | custom-call | flops 4294967296 | bytes 16777216 | tf_op jit(solution)/shard_map/project_q/pallas_call | solution.py:135
  76.1 1.0 collective-permute-done.5.other
  77.0 4.4 %project_hot.1 = bf16[128,8,256]{2,1,0:T(8,128)(2,1)} custom-call(s32[128]{0:T(128)} %reshape.49.asked, s32[8]{0:T(128)} %pad_add_fusion.1.order, bf16[4,256,256]{2,1,0:T(8,128)(2,1)} %pad_maximum_fusion.same, bf16[4,256,256]{2,1,0:T(8,128)(2,1)} %collective-permute-done.5.other, bf16[2048,256]{1,0:T(8,128)(2,1)} %wk.3, bf16[2048,256]{1,0:T(8,128)(2,1)} %wv.3, ...), custom_call_target="tpu_custom_call" | custom-call | flops 536870912 | bytes 4194304 | tf_op jit(solution)/shard_map/project_hot/pallas_call | solution.py:185
  82.1 4.5 %all-to-all-done.2 = bf16[16,2,2,64,256]{4,3,2,1,0:T(8,128)(2,1)S(1)} async-done(((bf16[16,2,2,64,256]{4,3,2,1,0:T(8,128)(2,1)}), bf16[16,2,2,64,256]{4,3,2,1,0:T(8,128)(2,1)S(1)}, u32[]{:S(2)}, u32[]{:S(2)}) %all-to-all-start.2) | async-done | bytes 2097184 | tf_op jit(solution)/shard_map/all_to_all | solution.py:422
  86.6 5.7 %all-to-all-start.3 = ((bf16[16,64,256]{2,1,0:T(8,128)(2,1)}), bf16[16,64,256]{2,1,0:T(8,128)(2,1)}, u32[]{:S(2)}, u32[]{:S(2)}) async-start(bf16[16,64,256]{2,1,0:T(8,128)(2,1)} %bitcast.34), calls=%async_computation.3 | async-start | bytes 1048576 | tf_op jit(solution)/shard_map/all_to_all | solution.py:422
  93.9 1.3 select_reduce_fusion
  95.9 12.2 %collective-permute-done.6.refs_4_.refs_11_ = bf16[256,2048]{1,0:T(8,128)(2,1)} collective-permute-done((bf16[256,2048]{1,0:T(8,128)(2,1)}, bf16[256,2048]{1,0:T(8,128)(2,1)}, u32[]{:S(2)}, u32[]{:S(2)}) %collective-permute-start.6) | collective-permute-done | bytes 1048608 | tf_op jit(solution)/shard_map/ppermute | solution.py:431
  108.1 1.3 copy.29
  109.5 1.1 copy.30
  110.5 2.0 reshape.58.hot
  113.0 11.1 %attend.2 = bf16[8,256,256]{2,1,0:T(8,128)(2,1)} custom-call(s32[512]{0:T(512)} %reshape.53.at, s32[8]{0:T(128)} %iota.18.where, bf16[4096,256]{1,0:T(8,128)(2,1)} %project_q.1.q, f32[64,512]{1,0:T(8,128)} %reshape.54.mask, bf16[64,2,64,256]{3,2,1,0:T(8,128)(2,1)} %get-tuple-element.63.local, bf16[32,2,64,256]{3,2,1,0:T(8,128)(2,1)} %bitcast.30, ...), custom_call_target="tpu_custom_call" | custom-call | flops 2147483648 | bytes 10485760 | tf_op jit(solution)/shard_map/attend/pallas_call | solution.py:293
  124.1 3.7 %all-to-all-start.4 = ((bf16[8,256,256]{2,1,0:T(8,128)(2,1)}), bf16[8,256,256]{2,1,0:T(8,128)(2,1)S(1)}, u32[]{:S(2)}, u32[]{:S(2)}) async-start(bf16[8,256,256]{2,1,0:T(8,128)(2,1)} %attend.2), calls=%async_computation.4 | async-start | bytes 2097152 | tf_op jit(solution)/shard_map/all_to_all | solution.py:422
  128.5 15.0 %all-to-all-done.4.refs_0_ = bf16[8,256,256]{2,1,0:T(8,128)(2,1)S(1)} async-done(((bf16[8,256,256]{2,1,0:T(8,128)(2,1)}), bf16[8,256,256]{2,1,0:T(8,128)(2,1)S(1)}, u32[]{:S(2)}, u32[]{:S(2)}) %all-to-all-start.4) | async-done | bytes 1048608 | tf_op jit(solution)/shard_map/all_to_all | solution.py:422
  144.6 8.0 %project_out.2 = bf16[8,256,256]{2,1,0:T(8,128)(2,1)} custom-call(s32[8]{0:T(128)} %pad_add_fusion.1.order, s32[8]{0:T(128)} %iota.17.slot, bf16[8,256,256]{2,1,0:T(8,128)(2,1)} %copy-done.3, bf16[256,2048]{1,0:T(8,128)(2,1)} %refs_8_.1, bf16[256,2048]{1,0:T(8,128)(2,1)} %copy-done.5, bf16[256,2048]{1,0:T(8,128)(2,1)} %copy-done.6, ...), custom_call_target="tpu_custom_call" | custom-call | flops 2147483648 | bytes 12582912 | tf_op jit(solution)/shard_map/project_out/pallas_call | solution.py:365
  152.5 3.6 %all-to-all-start.5 = ((bf16[8,256,256]{2,1,0:T(8,128)(2,1)}), bf16[8,256,256]{2,1,0:T(8,128)(2,1)S(1)}, u32[]{:S(2)}, u32[]{:S(2)}) async-start(bf16[8,256,256]{2,1,0:T(8,128)(2,1)} %project_out.2), calls=%async_computation.5 | async-start | bytes 2097152 | tf_op jit(solution)/shard_map/all_to_all | solution.py:422
  156.1 9.3 %attend.3 = (bf16[256,256]{1,0:T(8,128)(2,1)}, bf16[256,256]{1,0:T(8,128)(2,1)}, bf16[256,256]{1,0:T(8,128)(2,1)}, bf16[256,256]{1,0:T(8,128)(2,1)}, bf16[256,25...) custom-call(s32[512]{0:T(512)} %reshape.53.at, ...), custom_call_target="tpu_custom_call" | custom-call | flops 2147483648 | bytes 10485760 | tf_op jit(solution)/shard_map/attend/pallas_call | solution.py:293
  165.4 2.0 collective-permute-start.11
  167.4 1.3 collective-permute-start.12
  168.7 2.2 %collective-permute-start.13 = (bf16[256,256]{1,0:T(8,128)(2,1)}, bf16[256,256]{1,0:T(8,128)(2,1)S(1)}, u32[]{:S(2)}, u32[]{:S(2)}) collective-permute-start(bf16[256,256]{1,0:T(8,128)(2,1)} %get-tuple-element.72), channel_id=1, source_target_pairs={{0,4},{1,5},{2,6},{3,7},{4,0},{5,1},{6,2},{7,3},{8,12},{9,13},{10,... | collective-permute-start | bytes 393224 | tf_op jit(solution)/shard_map/ppermute | solution.py:460
  171.6 3.7 %collective-permute-done.11.refs_1_ = bf16[256,256]{1,0:T(8,128)(2,1)S(1)} collective-permute-done((bf16[256,256]{1,0:T(8,128)(2,1)}, bf16[256,256]{1,0:T(8,128)(2,1)S(1)}, u32[]{:S(2)}, u32[]{:S(2)}) %collective-permute-start.11) | collective-permute-done | bytes 131104 | tf_op jit(solution)/shard_map/ppermute | solution.py:460
  175.7 2.4 %collective-permute-done.13.refs_3_ = bf16[256,256]{1,0:T(8,128)(2,1)S(1)} collective-permute-done((bf16[256,256]{1,0:T(8,128)(2,1)}, bf16[256,256]{1,0:T(8,128)(2,1)S(1)}, u32[]{:S(2)}, u32[]{:S(2)}) %collective-permute-start.13) | collective-permute-done | bytes 131104 | tf_op jit(solution)/shard_map/ppermute | solution.py:460
  178.2 2.2 %collective-permute-done.15.refs_5_ = bf16[256,256]{1,0:T(8,128)(2,1)S(1)} collective-permute-done((bf16[256,256]{1,0:T(8,128)(2,1)}, bf16[256,256]{1,0:T(8,128)(2,1)S(1)}, u32[]{:S(2)}, u32[]{:S(2)}) %collective-permute-start.15) | collective-permute-done | bytes 131104 | tf_op jit(solution)/shard_map/ppermute | solution.py:460
  181.1 1.6 collective-permute-done.17.refs_7_
  183.4 8.1 %project_out.3 = (bf16[256,256]{1,0:T(8,128)(2,1)}, bf16[256,256]{1,0:T(8,128)(2,1)}, bf16[256,256]{1,0:T(8,128)(2,1)}, bf16[256,256]{1,0:T(8,128)(2,1)}, bf16[2...) custom-call(s32[8]{0:T(128)} %pad_add_fusion.1.order, ...), custom_call_target="tpu_custom_call" | custom-call | flops 2147483648 | bytes 12582912 | tf_op jit(solution)/shard_map/project_out/pallas_call | solution.py:365
  191.5 1.1 collective-permute-start.18
  192.6 2.9 %collective-permute-start.19 = (bf16[256,256]{1,0:T(8,128)(2,1)}, bf16[256,256]{1,0:T(8,128)(2,1)S(1)}, u32[]{:S(2)}, u32[]{:S(2)}) collective-permute-start(bf16[256,256]{1,0:T(8,128)(2,1)} %get-tuple-element.87), channel_id=1, source_target_pairs={{0,6},{1,7},{2,0},{3,1},{4,2},{5,3},{6,4},{7,5},{8,14},{9,15},{10,... | collective-permute-start | bytes 393224 | tf_op jit(solution)/shard_map/ppermute | solution.py:460
  195.5 1.4 collective-permute-start.20
  196.9 1.5 collective-permute-start.22
  198.4 1.0 collective-permute-done.18.rest_1_
  200.0 1.7 collective-permute-done.19.rest_2_
  201.7 2.6 %collective-permute-done.20.rest_3_ = bf16[256,256]{1,0:T(8,128)(2,1)S(1)} collective-permute-done((bf16[256,256]{1,0:T(8,128)(2,1)}, bf16[256,256]{1,0:T(8,128)(2,1)S(1)}, u32[]{:S(2)}, u32[]{:S(2)}) %collective-permute-start.20) | collective-permute-done | bytes 131104 | tf_op jit(solution)/shard_map/ppermute | solution.py:460
  204.3 1.7 collective-permute-done.22.rest_5_
  206.0 2.6 %collective-permute-done.24.rest_7_ = bf16[256,256]{1,0:T(8,128)(2,1)S(1)} collective-permute-done((bf16[256,256]{1,0:T(8,128)(2,1)}, bf16[256,256]{1,0:T(8,128)(2,1)S(1)}, u32[]{:S(2)}, u32[]{:S(2)}) %collective-permute-start.24) | collective-permute-done | bytes 131104 | tf_op jit(solution)/shard_map/ppermute | solution.py:460
  209.5 3.4 %place.1 = bf16[16,256,256]{2,1,0:T(8,128)(2,1)} custom-call(s32[8]{0:T(128)S(1)} %copy-done.1, bf16[8,256,256]{2,1,0:T(8,128)(2,1)S(1)} %all-to-all-done.5.whole, bf16[256,256]{1,0:T(8,128)(2,1)S(1)} %copy-done, bf16[256,256]{1,0:T(8,128)(2,1)S(1)} %collective-permute-done.18.rest_1_, bf16[256,256]{1,0:T(8,128)(2,1)S(1)} %collective-permute-done.19.rest_2_, ...), custom_call_target="tpu_custom_call" | custom-call | flops 1048576 | bytes 4194304 | tf_op jit(solution)/shard_map/place/pallas_call | solution.py:405
  (88 shorter events, 15.3 us)
Async XLA Ops:
  2.5 14.1 %all-to-all-start = ((s32[16,1,16]{2,1,0:T(1,128)}), s32[16,1,16]{2,1,0:T(1,128)S(1)}, u32[]{:S(2)}, u32[]{:S(2)}) async-start(s32[16,1,16]{2,1,0:T(1,128)} %bitcast.6), calls=%async_computation | async-start | bytes 16384 | tf_op jit(solution)/shard_map/all_to_all | solution.py:422
  14.4 7.7 %copy-start.4 = (bf16[256,2048]{1,0:T(8,128)(2,1)S(1)}, bf16[256,2048]{1,0:T(8,128)(2,1)}, u32[]{:S(2)}) copy-start(bf16[256,2048]{1,0:T(8,128)(2,1)} %refs_8_.1) | copy-start | bytes 3145732
  16.6 33.7 %all-to-all-start.1 = ((bf16[16,256,256]{2,1,0:T(8,128)(2,1)}), bf16[16,256,256]{2,1,0:T(8,128)(2,1)}, u32[]{:S(2)}, u32[]{:S(2)}) async-start(bf16[16,256,256]{2,1,0:T(8,128)(2,1)} %token_shares.1), calls=%async_computation.1 | async-start | bytes 4194304 | tf_op jit(solution)/shard_map/all_to_all | solution.py:422
  22.1 29.1 %collective-permute-start = (bf16[256,2048]{1,0:T(8,128)(2,1)S(1)}, bf16[256,2048]{1,0:T(8,128)(2,1)S(1)}, u32[]{:S(2)}, u32[]{:S(2)}) collective-permute-start(bf16[256,2048]{1,0:T(8,128)(2,1)S(1)} %copy-done.4), channel_id=1, source_target_pairs={{0,2},{2,4},{4,6},{6,0},{1,3},{3,5},{5,7},{7,1},{8,10},{10,12},{12... | collective-permute-start | bytes 3145736 | tf_op jit(solution)/shard_map/ppermute | solution.py:431
  23.8 27.5 %collective-permute-start.1 = (bf16[256,2048]{1,0:T(8,128)(2,1)S(1)}, bf16[256,2048]{1,0:T(8,128)(2,1)S(1)}, u32[]{:S(2)}, u32[]{:S(2)}) collective-permute-start(bf16[256,2048]{1,0:T(8,128)(2,1)S(1)} %copy-done.4), channel_id=1, source_target_pairs={{0,6},{2,0},{4,2},{6,4},{1,7},{3,1},{5,3},{7,5},{8,14},{10,8},{12,... | collective-permute-start | bytes 3145736 | tf_op jit(solution)/shard_map/ppermute | solution.py:431
  51.2 1.0 copy-start.5
  51.3 1.4 copy-start.6
  51.3 6.8 %copy-start.14 = (f32[128]{0:T(128)S(1)}, f32[128]{0:T(128)}, u32[]{:S(2)}) copy-start(f32[128]{0:T(128)} %param.14) | copy-start | bytes 1540
  52.6 34.0 %all-to-all-start.2 = ((bf16[16,2,2,64,256]{4,3,2,1,0:T(8,128)(2,1)}), bf16[16,2,2,64,256]{4,3,2,1,0:T(8,128)(2,1)S(1)}, u32[]{:S(2)}, u32[]{:S(2)}) async-start(bf16[16,2,2,64,256]{4,3,2,1,0:T(8,128)(2,1)} %bitcast.32), calls=%async_computation.2 | async-start | bytes 4194304 | tf_op jit(solution)/shard_map/all_to_all | solution.py:422
  58.6 15.3 %collective-permute-start.2 = (bf16[256,256]{1,0:T(8,128)(2,1)S(1)}, bf16[256,256]{1,0:T(8,128)(2,1)S(1)}, u32[]{:S(2)}, u32[]{:S(2)}) collective-permute-start(bf16[256,256]{1,0:T(8,128)(2,1)S(1)} %slice_bitcast_fusion), channel_id=1, source_target_pairs={{0,2},{2,4},{4,6},{6,0},{1,3},{3,5},{5,7},{7,1},{8,10},{10,12},{12... | collective-permute-start | bytes 393224 | tf_op jit(solution)/shard_map/ppermute | solution.py:431
  60.1 13.7 %collective-permute-start.3 = (bf16[256,256]{1,0:T(8,128)(2,1)S(1)}, bf16[256,256]{1,0:T(8,128)(2,1)S(1)}, u32[]{:S(2)}, u32[]{:S(2)}) collective-permute-start(bf16[256,256]{1,0:T(8,128)(2,1)S(1)} %slice_bitcast_fusion), channel_id=1, source_target_pairs={{0,6},{2,0},{4,2},{6,4},{1,7},{3,1},{5,3},{7,5},{8,14},{10,8},{12,... | collective-permute-start | bytes 393224 | tf_op jit(solution)/shard_map/ppermute | solution.py:431
  61.8 12.1 %collective-permute-start.4 = (bf16[256,256]{1,0:T(8,128)(2,1)S(1)}, bf16[256,256]{1,0:T(8,128)(2,1)S(1)}, u32[]{:S(2)}, u32[]{:S(2)}) collective-permute-start(bf16[256,256]{1,0:T(8,128)(2,1)S(1)} %slice_bitcast_fusion), channel_id=1, source_target_pairs={{0,4},{2,6},{4,0},{6,2},{1,5},{3,7},{5,1},{7,3},{8,12},{10,14},{12... | collective-permute-start | bytes 393224 | tf_op jit(solution)/shard_map/ppermute | solution.py:431
  74.8 2.3 %collective-permute-start.5 = (bf16[4,256,256]{2,1,0:T(8,128)(2,1)}, bf16[4,256,256]{2,1,0:T(8,128)(2,1)}, u32[]{:S(2)}, u32[]{:S(2)}) collective-permute-start(bf16[4,256,256]{2,1,0:T(8,128)(2,1)} %pad_maximum_fusion.same), channel_id=1, source_target_pairs={{0,1},{1,0},{2,3},{3,2},{4,5},{5,4},{6,7},{7,6},{8,9},{9,8},{10,11... | collective-permute-start | bytes 1572872 | tf_op jit(solution)/shard_map/ppermute | solution.py:436
  81.4 26.7 %collective-permute-start.6 = (bf16[256,2048]{1,0:T(8,128)(2,1)}, bf16[256,2048]{1,0:T(8,128)(2,1)}, u32[]{:S(2)}, u32[]{:S(2)}) collective-permute-start(bf16[256,2048]{1,0:T(8,128)(2,1)} %copy-done.5), channel_id=1, source_target_pairs={{0,2},{2,4},{4,6},{6,0},{1,3},{3,5},{5,7},{7,1},{8,10},{10,12},{12... | collective-permute-start | bytes 3145736 | tf_op jit(solution)/shard_map/ppermute | solution.py:431
  86.6 25.9 %copy-start.2 = (bf16[16,2,2,64,256]{4,3,2,1,0:T(8,128)(2,1)}, bf16[16,2,2,64,256]{4,3,2,1,0:T(8,128)(2,1)S(1)}, u32[]{:S(2)}) copy-start(bf16[16,2,2,64,256]{4,3,2,1,0:T(8,128)(2,1)S(1)} %all-to-all-done.2) | copy-start | bytes 6291460
  86.6 21.5 %all-to-all-start.3 = ((bf16[16,64,256]{2,1,0:T(8,128)(2,1)}), bf16[16,64,256]{2,1,0:T(8,128)(2,1)}, u32[]{:S(2)}, u32[]{:S(2)}) async-start(bf16[16,64,256]{2,1,0:T(8,128)(2,1)} %bitcast.34), calls=%async_computation.3 | async-start | bytes 1048576 | tf_op jit(solution)/shard_map/all_to_all | solution.py:422
  92.3 36.1 %collective-permute-start.7 = (bf16[256,2048]{1,0:T(8,128)(2,1)S(1)}, bf16[256,2048]{1,0:T(8,128)(2,1)}, u32[]{:S(2)}, u32[]{:S(2)}) collective-permute-start(bf16[256,2048]{1,0:T(8,128)(2,1)S(1)} %copy-done.4), channel_id=1, source_target_pairs={{0,1},{1,0},{2,3},{3,2},{4,5},{5,4},{6,7},{7,6},{8,9},{9,8},{10,11... | collective-permute-start | bytes 3145736 | tf_op jit(solution)/shard_map/ppermute | solution.py:530
  92.4 36.1 %collective-permute-start.9 = (bf16[256,2048]{1,0:T(8,128)(2,1)}, bf16[256,2048]{1,0:T(8,128)(2,1)}, u32[]{:S(2)}, u32[]{:S(2)}) collective-permute-start(bf16[256,2048]{1,0:T(8,128)(2,1)} %copy-done.6), channel_id=1, source_target_pairs={{0,1},{1,0},{2,3},{3,2},{4,5},{5,4},{6,7},{7,6},{8,9},{9,8},{10,11... | collective-permute-start | bytes 3145736 | tf_op jit(solution)/shard_map/ppermute | solution.py:530
  92.9 35.6 %collective-permute-start.8 = (bf16[256,2048]{1,0:T(8,128)(2,1)}, bf16[256,2048]{1,0:T(8,128)(2,1)}, u32[]{:S(2)}, u32[]{:S(2)}) collective-permute-start(bf16[256,2048]{1,0:T(8,128)(2,1)} %copy-done.5), channel_id=1, source_target_pairs={{0,1},{1,0},{2,3},{3,2},{4,5},{5,4},{6,7},{7,6},{8,9},{9,8},{10,11... | collective-permute-start | bytes 3145736 | tf_op jit(solution)/shard_map/ppermute | solution.py:530
  108.1 20.4 %collective-permute-start.10 = (bf16[256,2048]{1,0:T(8,128)(2,1)}, bf16[256,2048]{1,0:T(8,128)(2,1)}, u32[]{:S(2)}, u32[]{:S(2)}) collective-permute-start(bf16[256,2048]{1,0:T(8,128)(2,1)} %collective-permute-done.6.refs_4_.refs_11_), channel_id=1, source_target_pairs={{0,1},{1,0},{2,3},{3,2},{4,5},{5,4},{6,7},{7,6},{8,9},{9,8},{10,11... | collective-permute-start | bytes 3145736 | tf_op jit(solution)/shard_map/ppermute | solution.py:530
  124.1 19.4 %all-to-all-start.4 = ((bf16[8,256,256]{2,1,0:T(8,128)(2,1)}), bf16[8,256,256]{2,1,0:T(8,128)(2,1)S(1)}, u32[]{:S(2)}, u32[]{:S(2)}) async-start(bf16[8,256,256]{2,1,0:T(8,128)(2,1)} %attend.2), calls=%async_computation.4 | async-start | bytes 2097152 | tf_op jit(solution)/shard_map/all_to_all | solution.py:422
  143.5 1.0 copy-start.3
  152.5 56.1 %all-to-all-start.5 = ((bf16[8,256,256]{2,1,0:T(8,128)(2,1)}), bf16[8,256,256]{2,1,0:T(8,128)(2,1)S(1)}, u32[]{:S(2)}, u32[]{:S(2)}) async-start(bf16[8,256,256]{2,1,0:T(8,128)(2,1)} %project_out.2), calls=%async_computation.5 | async-start | bytes 2097152 | tf_op jit(solution)/shard_map/all_to_all | solution.py:422
  165.4 10.0 %collective-permute-start.11 = (bf16[256,256]{1,0:T(8,128)(2,1)}, bf16[256,256]{1,0:T(8,128)(2,1)S(1)}, u32[]{:S(2)}, u32[]{:S(2)}) collective-permute-start(bf16[256,256]{1,0:T(8,128)(2,1)} %get-tuple-element.70), channel_id=1, source_target_pairs={{0,2},{1,3},{2,4},{3,5},{4,6},{5,7},{6,0},{7,1},{8,10},{9,11},{10,... | collective-permute-start | bytes 393224 | tf_op jit(solution)/shard_map/ppermute | solution.py:460
  167.4 8.0 %collective-permute-start.12 = (bf16[256,256]{1,0:T(8,128)(2,1)}, bf16[256,256]{1,0:T(8,128)(2,1)S(1)}, u32[]{:S(2)}, u32[]{:S(2)}) collective-permute-start(bf16[256,256]{1,0:T(8,128)(2,1)} %get-tuple-element.71), channel_id=1, source_target_pairs={{0,6},{1,7},{2,0},{3,1},{4,2},{5,3},{6,4},{7,5},{8,14},{9,15},{10,... | collective-permute-start | bytes 393224 | tf_op jit(solution)/shard_map/ppermute | solution.py:460
  168.7 9.5 %collective-permute-start.13 = (bf16[256,256]{1,0:T(8,128)(2,1)}, bf16[256,256]{1,0:T(8,128)(2,1)S(1)}, u32[]{:S(2)}, u32[]{:S(2)}) collective-permute-start(bf16[256,256]{1,0:T(8,128)(2,1)} %get-tuple-element.72), channel_id=1, source_target_pairs={{0,4},{1,5},{2,6},{3,7},{4,0},{5,1},{6,2},{7,3},{8,12},{9,13},{10,... | collective-permute-start | bytes 393224 | tf_op jit(solution)/shard_map/ppermute | solution.py:460
  170.9 7.3 %collective-permute-start.14 = (bf16[256,256]{1,0:T(8,128)(2,1)}, bf16[256,256]{1,0:T(8,128)(2,1)S(1)}, u32[]{:S(2)}, u32[]{:S(2)}) collective-permute-start(bf16[256,256]{1,0:T(8,128)(2,1)} %get-tuple-element.73), channel_id=1, source_target_pairs={{0,1},{1,0},{2,3},{3,2},{4,5},{5,4},{6,7},{7,6},{8,9},{9,8},{10,11... | collective-permute-start | bytes 393224 | tf_op jit(solution)/shard_map/ppermute | solution.py:460
  170.9 9.5 %collective-permute-start.15 = (bf16[256,256]{1,0:T(8,128)(2,1)}, bf16[256,256]{1,0:T(8,128)(2,1)S(1)}, u32[]{:S(2)}, u32[]{:S(2)}) collective-permute-start(bf16[256,256]{1,0:T(8,128)(2,1)} %get-tuple-element.74), channel_id=1, source_target_pairs={{0,3},{1,2},{2,5},{3,4},{4,7},{5,6},{6,1},{7,0},{8,11},{9,10},{10,... | collective-permute-start | bytes 393224 | tf_op jit(solution)/shard_map/ppermute | solution.py:460
  175.3 7.4 %copy-start.7 = (bf16[256,256]{1,0:T(8,128)(2,1)}, bf16[256,256]{1,0:T(8,128)(2,1)S(1)}, u32[]{:S(2)}) copy-start(bf16[256,256]{1,0:T(8,128)(2,1)S(1)} %collective-permute-done.11.refs_1_) | copy-start | bytes 393220
  175.3 5.8 %collective-permute-start.16 = (bf16[256,256]{1,0:T(8,128)(2,1)}, bf16[256,256]{1,0:T(8,128)(2,1)S(1)}, u32[]{:S(2)}, u32[]{:S(2)}) collective-permute-start(bf16[256,256]{1,0:T(8,128)(2,1)} %get-tuple-element.75), channel_id=1, source_target_pairs={{0,7},{1,6},{2,1},{3,0},{4,3},{5,2},{6,5},{7,4},{8,15},{9,14},{10,... | collective-permute-start | bytes 393224 | tf_op jit(solution)/shard_map/ppermute | solution.py:460
  175.3 7.4 %copy-start.8 = (bf16[256,256]{1,0:T(8,128)(2,1)}, bf16[256,256]{1,0:T(8,128)(2,1)S(1)}, u32[]{:S(2)}) copy-start(bf16[256,256]{1,0:T(8,128)(2,1)S(1)} %collective-permute-done.12.refs_2_) | copy-start | bytes 393220
  175.3 7.4 %collective-permute-start.17 = (bf16[256,256]{1,0:T(8,128)(2,1)}, bf16[256,256]{1,0:T(8,128)(2,1)S(1)}, u32[]{:S(2)}, u32[]{:S(2)}) collective-permute-start(bf16[256,256]{1,0:T(8,128)(2,1)} %get-tuple-element.76), channel_id=1, source_target_pairs={{0,5},{1,4},{2,7},{3,6},{4,1},{5,0},{6,3},{7,2},{8,13},{9,12},{10,... | collective-permute-start | bytes 393224 | tf_op jit(solution)/shard_map/ppermute | solution.py:460
  178.2 4.6 %copy-start.9 = (bf16[256,256]{1,0:T(8,128)(2,1)}, bf16[256,256]{1,0:T(8,128)(2,1)S(1)}, u32[]{:S(2)}) copy-start(bf16[256,256]{1,0:T(8,128)(2,1)S(1)} %collective-permute-done.13.refs_3_) | copy-start | bytes 393220
  178.2 4.6 %copy-start.10 = (bf16[256,256]{1,0:T(8,128)(2,1)}, bf16[256,256]{1,0:T(8,128)(2,1)S(1)}, u32[]{:S(2)}) copy-start(bf16[256,256]{1,0:T(8,128)(2,1)S(1)} %collective-permute-done.14.refs_4_) | copy-start | bytes 393220
  180.4 2.4 %copy-start.11 = (bf16[256,256]{1,0:T(8,128)(2,1)}, bf16[256,256]{1,0:T(8,128)(2,1)S(1)}, u32[]{:S(2)}) copy-start(bf16[256,256]{1,0:T(8,128)(2,1)S(1)} %collective-permute-done.15.refs_5_) | copy-start | bytes 393220
  181.1 1.6 copy-start.12
  182.8 0.6 copy-start.13
  183.4 25.2 %copy-start.1 = (s32[8]{0:T(128)S(1)}, s32[8]{0:T(128)}, u32[]{:S(2)}) copy-start(s32[8]{0:T(128)} %pad_add_fusion.1.order) | copy-start | bytes 100
  191.5 7.9 %collective-permute-start.18 = (bf16[256,256]{1,0:T(8,128)(2,1)}, bf16[256,256]{1,0:T(8,128)(2,1)S(1)}, u32[]{:S(2)}, u32[]{:S(2)}) collective-permute-start(bf16[256,256]{1,0:T(8,128)(2,1)} %get-tuple-element.86), channel_id=1, source_target_pairs={{0,2},{1,3},{2,4},{3,5},{4,6},{5,7},{6,0},{7,1},{8,10},{9,11},{10,... | collective-permute-start | bytes 393224 | tf_op jit(solution)/shard_map/ppermute | solution.py:460
  192.6 9.1 %collective-permute-start.19 = (bf16[256,256]{1,0:T(8,128)(2,1)}, bf16[256,256]{1,0:T(8,128)(2,1)S(1)}, u32[]{:S(2)}, u32[]{:S(2)}) collective-permute-start(bf16[256,256]{1,0:T(8,128)(2,1)} %get-tuple-element.87), channel_id=1, source_target_pairs={{0,6},{1,7},{2,0},{3,1},{4,2},{5,3},{6,4},{7,5},{8,14},{9,15},{10,... | collective-permute-start | bytes 393224 | tf_op jit(solution)/shard_map/ppermute | solution.py:460
  195.5 8.8 %collective-permute-start.20 = (bf16[256,256]{1,0:T(8,128)(2,1)}, bf16[256,256]{1,0:T(8,128)(2,1)S(1)}, u32[]{:S(2)}, u32[]{:S(2)}) collective-permute-start(bf16[256,256]{1,0:T(8,128)(2,1)} %get-tuple-element.88), channel_id=1, source_target_pairs={{0,4},{1,5},{2,6},{3,7},{4,0},{5,1},{6,2},{7,3},{8,12},{9,13},{10,... | collective-permute-start | bytes 393224 | tf_op jit(solution)/shard_map/ppermute | solution.py:460
  196.9 7.4 %collective-permute-start.21 = (bf16[256,256]{1,0:T(8,128)(2,1)}, bf16[256,256]{1,0:T(8,128)(2,1)S(1)}, u32[]{:S(2)}, u32[]{:S(2)}) collective-permute-start(bf16[256,256]{1,0:T(8,128)(2,1)} %get-tuple-element.89), channel_id=1, source_target_pairs={{0,1},{1,0},{2,3},{3,2},{4,5},{5,4},{6,7},{7,6},{8,9},{9,8},{10,11... | collective-permute-start | bytes 393224 | tf_op jit(solution)/shard_map/ppermute | solution.py:460
  196.9 9.1 %collective-permute-start.22 = (bf16[256,256]{1,0:T(8,128)(2,1)}, bf16[256,256]{1,0:T(8,128)(2,1)S(1)}, u32[]{:S(2)}, u32[]{:S(2)}) collective-permute-start(bf16[256,256]{1,0:T(8,128)(2,1)} %get-tuple-element.90), channel_id=1, source_target_pairs={{0,3},{1,2},{2,5},{3,4},{4,7},{5,6},{6,1},{7,0},{8,11},{9,10},{10,... | collective-permute-start | bytes 393224 | tf_op jit(solution)/shard_map/ppermute | solution.py:460
  199.4 6.6 %collective-permute-start.23 = (bf16[256,256]{1,0:T(8,128)(2,1)}, bf16[256,256]{1,0:T(8,128)(2,1)S(1)}, u32[]{:S(2)}, u32[]{:S(2)}) collective-permute-start(bf16[256,256]{1,0:T(8,128)(2,1)} %get-tuple-element.91), channel_id=1, source_target_pairs={{0,7},{1,6},{2,1},{3,0},{4,3},{5,2},{6,5},{7,4},{8,15},{9,14},{10,... | collective-permute-start | bytes 393224 | tf_op jit(solution)/shard_map/ppermute | solution.py:460
  201.7 6.9 %collective-permute-start.24 = (bf16[256,256]{1,0:T(8,128)(2,1)}, bf16[256,256]{1,0:T(8,128)(2,1)S(1)}, u32[]{:S(2)}, u32[]{:S(2)}) collective-permute-start(bf16[256,256]{1,0:T(8,128)(2,1)} %get-tuple-element.92), channel_id=1, source_target_pairs={{0,5},{1,4},{2,7},{3,6},{4,1},{5,0},{6,3},{7,2},{8,13},{9,12},{10,... | collective-permute-start | bytes 393224 | tf_op jit(solution)/shard_map/ppermute | solution.py:460
  208.6 0.9 copy-start

commit v2 on v1

--- a/solution.py
+++ b/solution.py
@@ -28,98 +28,81 @@
     return (values * factor * gain_row).astype(bf16)
 
 
-def share_kernel(rank, tok, out):
+def share_kernel(rank, tok, asks, out):
     rows = tok[...].astype(f32)
     devices = out.shape[0]
     part = BLOCK // devices
-    for k in range(out.shape[1] // 16):
+    small = rows.shape[0] // devices
+    step = pl.program_id(0)
+    for k in range(small // 16):
         parts = []
         for b in range(16 // part):
             first = (k * (16 // part) + b) * BLOCK
             parts.append(rows[first : first + BLOCK].reshape(devices, part, WIDTH))
-        out[:, k * 16 : (k + 1) * 16, :] = jnp.concatenate(parts, axis=1).astype(bf16)
-
-
-def token_shares(rank, tokens, devices):
+        at = pl.ds(pl.multiple_of(step * small + k * 16, 16), 16)
+        out[:, at, :] = jnp.concatenate(parts, axis=1).astype(bf16)
+
+    @pl.when(step == 0)
+    def _():
+        out[:, -16:, :] = asks[...]
+
+
+def token_shares(rank, tokens, asks):
     length = tokens.shape[0]
+    devices = asks.shape[0]
     tile = 1024
-    small = tile // devices
+    shape = (devices, length // devices + 16, WIDTH)
     return pl.pallas_call(
         share_kernel,
         grid_spec=pltpu.PrefetchScalarGridSpec(
             num_scalar_prefetch=1,
             grid=(length // tile,),
-            in_specs=[pl.BlockSpec((tile, WIDTH), lambda i, rank: (i, rank[0]))],
-            out_specs=pl.BlockSpec((devices, small, WIDTH), lambda i, rank: (0, i, 0)),
-        ),
-        out_shape=jax.ShapeDtypeStruct((devices, length // devices, WIDTH), bf16),
+            in_specs=[
+                pl.BlockSpec((tile, WIDTH), lambda i, rank: (i, rank[0])),
+                pl.BlockSpec(asks.shape, lambda i, rank: (0, 0, 0)),
+            ],
+            out_specs=pl.BlockSpec(shape, lambda i, rank: (0, 0, 0)),
+        ),
+        out_shape=jax.ShapeDtypeStruct(shape, bf16),
         compiler_params=pltpu.CompilerParams(vmem_limit_bytes=VMEM_LIMIT),
         cost_estimate=pl.CostEstimate(flops=1 << 20, bytes_accessed=4 << 20, transcendentals=0),
         name="token_shares",
-    )(rank, tokens)
-
-
-def kv_kernel(asked, tok, wk, wv, gain, pairs, sent, keep, out_sem, sent_sem):
-    step = pl.program_id(0)
-    steps = pl.num_programs(0)
+    )(rank, tokens, asks)
+
+
+def kv_kernel(tok, wk, wv, gain, out):
     rows = tok[...]
-    blocks = keep.shape[0] // steps
-    first = pl.multiple_of(step * blocks, blocks)
-    here = pl.ds(first, blocks)
     keys = jnp.dot(rows, wk[...], preferred_element_type=f32)
+    blocks = out.shape[0]
     for h in range(2):
         lanes = slice(h * HEAD_DIM, (h + 1) * HEAD_DIM)
         normed = head_norm(keys[:, lanes], gain[...])
-        keep[here, 0, :, lanes] = normed.reshape(blocks, BLOCK, HEAD_DIM)
+        out[:, 0, :, lanes] = normed.reshape(blocks, BLOCK, HEAD_DIM)
     vals = jnp.dot(rows, wv[...], preferred_element_type=f32).astype(bf16)
-    keep[here, 1, :, :] = vals.reshape(blocks, BLOCK, WIDTH)
-    pltpu.make_async_copy(keep.at[here], pairs.at[here], out_sem).start()
-
-    @pl.when(step == steps - 1)
-    def _():
-        def begin(m, carry):
-            pltpu.make_async_copy(keep.at[asked[m]], sent.at[m], sent_sem).start()
-            return carry
-
-        lax.fori_loop(0, sent.shape[0], begin, 0)
-        pltpu.make_async_copy(keep.at[pl.ds(0, sent.shape[0])], sent, sent_sem).wait()
-        pltpu.make_async_copy(keep, pairs, out_sem).wait()
-
-
-def project_kv(asked, tokens, w_key, w_value, gain):
+    out[:, 1, :, :] = vals.reshape(blocks, BLOCK, WIDTH)
+
+
+def project_kv(tokens, w_key, w_value, gain):
     length, depth = tokens.shape
     tile = 1024
-    sends = asked.shape[0]
-    shape = (PAIR, BLOCK, WIDTH)
-    anywhere = pl.BlockSpec(memory_space=pl.ANY)
+    blocks = tile // BLOCK
     return pl.pallas_call(
         kv_kernel,
-        grid_spec=pltpu.PrefetchScalarGridSpec(
-            num_scalar_prefetch=1,
-            grid=(length // tile,),
-            in_specs=[
-                pl.BlockSpec((tile, depth), lambda i, asked: (i, 0)),
-                pl.BlockSpec((depth, WIDTH), lambda i, asked: (0, 0)),
-                pl.BlockSpec((depth, WIDTH), lambda i, asked: (0, 0)),
-                pl.BlockSpec((1, HEAD_DIM), lambda i, asked: (0, 0)),
-            ],
-            out_specs=[anywhere, anywhere],
-            scratch_shapes=[
-                pltpu.VMEM((length // BLOCK,) + shape, bf16),
-                pltpu.SemaphoreType.DMA,
-                pltpu.SemaphoreType.DMA,
-            ],
-        ),
-        out_shape=[
-            jax.ShapeDtypeStruct((length // BLOCK,) + shape, bf16),
-            jax.ShapeDtypeStruct((sends,) + shape, bf16),
+        grid=(length // tile,),
+        in_specs=[
+            pl.BlockSpec((tile, depth), lambda i: (i, 0)),
+            pl.BlockSpec((depth, WIDTH), lambda i: (0, 0)),
+            pl.BlockSpec((depth, WIDTH), lambda i: (0, 0)),
+            pl.BlockSpec((1, HEAD_DIM), lambda i: (0, 0)),
         ],
+        out_specs=pl.BlockSpec((blocks, PAIR, BLOCK, WIDTH), lambda i: (i, 0, 0, 0)),
+        out_shape=jax.ShapeDtypeStruct((length // BLOCK, PAIR, BLOCK, WIDTH), bf16),
         compiler_params=pltpu.CompilerParams(vmem_limit_bytes=VMEM_LIMIT),
         cost_estimate=pl.CostEstimate(
             flops=4 * length * depth * WIDTH, bytes_accessed=2 * length * depth, transcendentals=0
         ),
         name="project_kv",
-    )(asked, tokens, w_key, w_value, gain)
+    )(tokens, w_key, w_value, gain)
 
 
 def q_kernel(tok, wq, gain, out):
@@ -150,17 +133,32 @@
     )(tokens, w_query, gain)
 
 
-def hot_kernel(asked, order, same, other, wk, wv, gain, out, keep):
+def send_kernel(near, asked, order, same, other, wk, wv, gain, pairs, out, keep, sems):
+    devices, rows, _ = out.shape
+    reach = near.shape[0] // devices
+    plain = reach * PAIR * BLOCK
+    copies = []
+    for m in range(near.shape[0]):
+        first = pl.multiple_of(near[m] * PAIR * BLOCK, PAIR * BLOCK)
+        to = pl.ds((m % reach) * PAIR * BLOCK, PAIR * BLOCK)
+        copies.append(
+            pltpu.make_async_copy(
+                pairs.at[pl.ds(first, PAIR * BLOCK)], out.at[m // reach, to], sems.at[m]
+            )
+        )
+    for copy in copies:
+        copy.start()
+
     keys = jnp.zeros((same.shape[1], WIDTH), f32)
     vals = jnp.zeros((same.shape[1], WIDTH), f32)
     count = same.shape[0]
     for k in range(2 * count):
-        rows = same[k] if k < count else other[k - count]
+        tokens = same[k] if k < count else other[k - count]
         span = pl.ds(pl.multiple_of(order[k] * WIDTH, WIDTH), WIDTH)
-        keys += jnp.dot(rows, wk[span, :], preferred_element_type=f32)
-        vals += jnp.dot(rows, wv[span, :], preferred_element_type=f32)
-    part = out.shape[1] // 2
-    groups = keep.shape[0]
+        keys += jnp.dot(tokens, wk[span, :], preferred_element_type=f32)
+        vals += jnp.dot(tokens, wv[span, :], preferred_element_type=f32)
+    groups, unit, _ = keep.shape
+    part = unit // 2
     for h in range(2):
         lanes = slice(h * HEAD_DIM, (h + 1) * HEAD_DIM)
         x = keys[:, lanes]
@@ -168,55 +166,84 @@
         keep[:, :part, lanes] = (x * factor * gain[...]).reshape(groups, part, HEAD_DIM)
     keep[:, part:, :] = vals.reshape(groups, part, WIDTH)
 
+    twos = (rows - plain) // (2 * unit)
+
     def one(m, carry):
-        out[m] = keep[asked[m]].astype(bf16)
+        both = jnp.concatenate([keep[asked[2 * m]], keep[asked[2 * m + 1]]], axis=0)
+        at = pl.multiple_of(plain + (m % twos) * 2 * unit, 2 * unit)
+        out[m // twos, pl.ds(at, 2 * unit), :] = both.astype(bf16)
         return carry
 
-    lax.fori_loop(0, out.shape[0], one, 0, unroll=8)
-
-
-def project_hot(asked, order, same, other, w_key, w_value, gain):
+    lax.fori_loop(0, devices * twos, one, 0, unroll=4)
+    for copy in copies:
+        copy.wait()
+
+
+def whole_block(*shape):
+    return pl.BlockSpec(shape, lambda i, *_: (0,) * len(shape))
+
+
+def project_sent(near, asked, order, same, other, w_key, w_value, gain, pairs, devices):
     count, rows, _ = same.shape
     groups = 64
-    part = rows // groups
+    unit = 2 * rows // groups
     depth = w_key.shape[0]
-    sends = asked.shape[0]
-    whole = lambda *shape: pl.BlockSpec(shape, lambda i, a, o: (0,) * len(shape))
+    length = (near.shape[0] // devices) * PAIR * BLOCK + (asked.shape[0] // devices) * unit
+    shape = (devices, length, WIDTH)
     return pl.pallas_call(
-        hot_kernel,
+        send_kernel,
         grid_spec=pltpu.PrefetchScalarGridSpec(
-            num_scalar_prefetch=2,
+            num_scalar_prefetch=3,
             grid=(1,),
             in_specs=[
-                whole(count, rows, WIDTH),
-                whole(count, rows, WIDTH),
-                whole(depth, WIDTH),
-                whole(depth, WIDTH),
-                whole(1, HEAD_DIM),
-            ],
-            out_specs=whole(sends, 2 * part, WIDTH),
-            scratch_shapes=[pltpu.VMEM((groups, 2 * part, WIDTH), f32)],
-        ),
-        out_shape=jax.ShapeDtypeStruct((sends, 2 * part, WIDTH), bf16),
+                whole_block(count, rows, WIDTH),
+                whole_block(count, rows, WIDTH),
+                whole_block(depth, WIDTH),
+                whole_block(depth, WIDTH),
+                whole_block(1, HEAD_DIM),
+                pl.BlockSpec(memory_space=pl.ANY),
+            ],
+            out_specs=whole_block(*shape),
+            scratch_shapes=[
+                pltpu.VMEM((groups, unit, WIDTH), f32),
+                pltpu.SemaphoreType.DMA((near.shape[0],)),
+            ],
+        ),
+        out_shape=jax.ShapeDtypeStruct(shape, bf16),
         compiler_params=pltpu.CompilerParams(vmem_limit_bytes=VMEM_LIMIT),
         cost_estimate=pl.CostEstimate(
-            flops=4 * rows * depth * WIDTH, bytes_accessed=4 << 20, transcendentals=0
-        ),
-        name="project_hot",
-    )(asked, order, same, other, w_key, w_value, gain)
-
-
-def attention_kernel(first, at, where, q, mask, local, near, hot, *rest):
-    outs, (table, sems) = rest[:-2], rest[-2:]
-    copies = []
-    start = 0
-    for n, part in enumerate((local, near, hot)):
-        span = table.at[pl.ds(start, part.shape[0])]
-        copies.append(pltpu.make_async_copy(part, span, sems.at[n]))
-        start += part.shape[0]
+            flops=4 * rows * depth * WIDTH, bytes_accessed=8 << 20, transcendentals=0
+        ),
+        name="project_sent",
+    )(near, asked, order, same, other, w_key, w_value, gain, pairs)
+
+
+def attention_kernel(first, at, where, q, mask, pairs, got, *rest):
+    outs, (table, raw, sems) = rest[:-3], rest[-3:]
+    devices, rows, _ = got.shape
+    here = pairs.shape[0]
+    hot_rows = raw.shape[1]
+    plain = rows - hot_rows
+    copies = [
+        pltpu.make_async_copy(got.at[:, pl.ds(plain, hot_rows)], raw, sems.at[devices]),
+        pltpu.make_async_copy(pairs, table.at[pl.ds(0, here)], sems.at[devices + 1]),
+    ]
+    for n in range(devices):
+        span = table.at[pl.ds(here + n * plain, plain)]
+        copies.append(pltpu.make_async_copy(got.at[n, pl.ds(0, plain)], span, sems.at[n]))
     for copy in copies:
         copy.start()
-    for copy in copies:
+    copies[0].wait()
+    part = BLOCK // devices
+    for n in range(hot_rows // 16):
+        both = raw[:, n * 16 : (n + 1) * 16, :].astype(f32)
+        for m in range(2):
+            start = here + devices * plain + (2 * n + m) * PAIR * BLOCK
+            for kind in range(PAIR):
+                low = m * 2 * part + kind * part
+                piece = both[:, low : low + part, :].reshape(BLOCK, WIDTH).astype(bf16)
+                table[start + kind * BLOCK : start + (kind + 1) * BLOCK, :] = piece
+    for copy in copies[1:]:
         copy.wait()
     slots = mask.shape[1] // BLOCK
     count = where.shape[0]
@@ -235,13 +262,15 @@
             axis=0,
         )
         base = (first + block) * slots
-        return both, [at[base + j] for j in range(slots)]
+        return both, [
+            pl.multiple_of(at[base + j] * PAIR * BLOCK, PAIR * BLOCK) for j in range(slots)
+        ]
 
     def piece_of(n, put):
         items = [load(where[n] * per_piece + i) for i in range(per_piece)]
         logits = []
         for both, picks in items:
-            keys = jnp.concatenate([table[p, 0] for p in picks], axis=0)
+            keys = jnp.concatenate([table[pl.ds(p, BLOCK), :] for p in picks], axis=0)
             logits.append(
                 lax.dot_general(both, keys, (((1,), (1,)), ((), ())), preferred_element_type=f32)
             )
@@ -250,7 +279,9 @@
             block = where[n] * per_piece + i
             weights.append(jnp.exp2(logits[i]) * mask[pl.ds(block, 1), :])
         for i, (both, picks) in enumerate(items):
-            values = jnp.concatenate([table[p, 1] for p in picks], axis=0)
+            values = jnp.concatenate(
+                [table[pl.ds(p + BLOCK, BLOCK), :] for p in picks], axis=0
+            )
             sums = jnp.dot(weights[i].astype(bf16), values, preferred_element_type=f32)
             scale = 1.0 / jnp.sum(weights[i], axis=-1, keepdims=True)
             to = slice(i * BLOCK, (i + 1) * BLOCK)
@@ -276,20 +307,18 @@
             piece_of(n, put)
 
 
-def whole_block(*shape):
-    return pl.BlockSpec(shape, lambda i, *_: (0,) * len(shape))
-
-
-def attend(chunk, chunks, split, at, where, queries, mask, local, near, hot):
+def attend(chunk, chunks, split, at, where, queries, mask, pairs, got):
     ranks = where.shape[0]
     length = queries.shape[0] // chunks
     slots = mask.shape[1] // BLOCK
     blocks = length // BLOCK
     rows = length // ranks
+    devices, arrived, _ = got.shape
+    plain = REACH * PAIR * BLOCK
     anywhere = pl.BlockSpec(memory_space=pl.ANY)
     shape = (rows, WIDTH) if split else (ranks, rows, WIDTH)
     count = ranks if split else 1
-    parts = (local, near, hot)
+    height = pairs.shape[0] + devices * plain + HOT * PAIR * BLOCK
     outs = pl.pallas_call(
         functools.partial(attention_kernel, chunk * blocks),
         grid_spec=pltpu.PrefetchScalarGridSpec(
@@ -300,12 +329,12 @@
                 pl.BlockSpec((blocks, slots * BLOCK), lambda i, *_: (chunk, 0)),
                 anywhere,
                 anywhere,
-                anywhere,
             ],
             out_specs=[whole_block(*shape)] * count,
             scratch_shapes=[
-                pltpu.VMEM((sum(p.shape[0] for p in parts),) + local.shape[1:], bf16),
-                pltpu.SemaphoreType.DMA((3,)),
+                pltpu.VMEM((height, WIDTH), bf16),
+                pltpu.VMEM((devices, arrived - plain, WIDTH), bf16),
+                pltpu.SemaphoreType.DMA((devices + 2,)),
             ],
         ),
         out_shape=[jax.ShapeDtypeStruct(shape, bf16)] * count,
@@ -314,7 +343,7 @@
             flops=8 * length * WIDTH * slots * BLOCK, bytes_accessed=10 << 20, transcendentals=0
         ),
         name="attend",
-    )(at, where, queries, mask, *parts)
+    )(at, where, queries, mask, pairs, got)
     return list(outs) if split else outs[0]
 
 
@@ -431,9 +460,13 @@
     return lax.ppermute(piece, TP[0], [(i, (i + shift) % ring) for i in range(ring)])
 
 
+def across(piece):
+    return lax.ppermute(piece, TP[1], [(0, 1), (1, 0)])
+
+
 def both_cores(parts):
     same = jnp.stack(parts)
-    return same, lax.ppermute(same, TP[1], [(0, 1), (1, 0)])
+    return same, across(same)
 
 
 OFFSETS = (0, -1, 1, 2)
@@ -467,7 +500,6 @@
     devices = lax.axis_size(KV)
     position = lax.axis_index(KV)
     ranks = lax.axis_size(TP)
-    part = BLOCK // devices
     key_row = key_gain[None, :]
     query_row = (query_gain * (HEAD_DIM ** (-0.5) * LOG2E))[None, :]
 
@@ -486,31 +518,24 @@
     )
     named = jnp.sum(jnp.where(places, local_ids[None, :, None], 0), axis=1).astype(jnp.int32)
     requests = jnp.concatenate([named, jnp.broadcast_to(named[:1], named.shape)], axis=1)
-    asked = exchange(requests, KV)
-    asked_near = asked[:, :REACH].reshape(-1)
-    asked_hot = asked[:, HOT:].reshape(-1)
+    asks = jnp.pad(requests.astype(bf16)[:, None, :], ((0, 0), (0, 15), (0, WIDTH - 2 * HOT)))
     order = piece_order(1)
     toward = piece_order(-1)
     same_order = jnp.arange(ranks, dtype=jnp.int32)
+
     rank = lax.axis_index(TP).astype(jnp.int32).reshape(1)
-    shares = exchange(token_shares(rank, tokens, devices), KV)[0]
+    arrived = exchange(token_shares(rank, tokens, asks), KV)
+    shares = arrived[0, :-16]
+    asked = arrived[:, -16, : 2 * HOT].astype(jnp.int32)
+    asked_near = asked[:, :REACH].reshape(-1)
+    asked_hot = asked[:, HOT:].reshape(-1)
     w_after = along_y(w_out, 1)
     w_before = along_y(w_out, -1)
-
-    pairs, sent = project_kv(asked_near, tokens, w_key, w_value, key_row)
-    sent, shares, w_after, w_before = tied(sent, shares, w_after, w_before)
-    sent = sent.reshape(devices, REACH, PAIR, BLOCK, WIDTH)
-    near = exchange(sent, KV).reshape(devices * REACH, PAIR, BLOCK, WIDTH)
-    parts = [shares] + [along_y(shares, shift) for shift in (1, -1, 2)]
-    again, sent = tied(tokens, sent)
+    w_own = across(w_out)
+
+    pairs = project_kv(tokens, w_key, w_value, key_row).reshape(-1, WIDTH)
+    again, pairs = tied(tokens, pairs)
     queries = project_q(again, w_query, query_row)
-    queries, *parts = tied(queries, *parts)
-    rows_same, rows_other = both_cores(parts)
-    sent_hot = project_hot(asked_hot, order, rows_same, rows_other, w_key, w_value, key_row)
-
-    pick, owner_of, rank_of, usable, sent_hot, w_after = tied(
-        pick, owner_of, rank_of, usable, sent_hot, w_after
-    )
     flat_rank = rank_of.reshape(-1)
     slot_rank = jnp.sum(
         jnp.where(pick[:, :, None] == all_blocks[None, None, :], flat_rank[None, None, :], 0), axis=-1
@@ -522,20 +547,25 @@
     )
     at = jnp.where(usable, at, 0).astype(jnp.int32).reshape(-1)
     mask = jnp.repeat(usable.astype(f32), BLOCK, axis=1)
+
+    shares, asked_near, asked_hot, queries, at, mask, order, w_after, w_before = tied(
+        shares, asked_near, asked_hot, queries, at, mask, order, w_after, w_before
+    )
+    parts = [shares] + [along_y(shares, shift) for shift in (1, -1, 2)]
     w_far = along_y(w_after, 1)
-
-    near, sent_hot = tied(near, sent_hot)
-    hot = exchange(sent_hot.reshape(devices, HOT * 2 * part, WIDTH), KV)
-    w_same = [w_out, w_after, w_before, w_far]
-    w_other = [lax.ppermute(w, TP[1], [(0, 1), (1, 0)]) for w in w_same]
-    weights = w_same + w_other
-    hot = hot.reshape(devices, HOT, PAIR, part, WIDTH).transpose(1, 2, 0, 3, 4)
-    hot = hot.reshape(HOT, PAIR, BLOCK, WIDTH)
+    w_swapped = [across(w_after), across(w_before)]
+    rows_same, rows_other = both_cores(parts)
+    sent = project_sent(
+        asked_near, asked_hot, order, rows_same, rows_other, w_key, w_value, key_row, pairs, devices
+    )
+    got = exchange(sent, KV)
+    w_swapped.append(across(w_far))
+    weights = [w_out, w_after, w_before, w_far, w_own] + w_swapped
 
     gains = out_gain.reshape(ranks, 1, WIDTH)
-    first = attend(0, 2, False, at, same_order, queries, mask, pairs, near, hot)
+    first = attend(0, 2, False, at, same_order, queries, mask, pairs, got)
     first = exchange(first, TP)
-    second = attend(1, 2, True, at, toward, queries, mask, pairs, near, hot)
+    second = attend(1, 2, True, at, toward, queries, mask, pairs, got)
     second = send_pieces(second)
     first = project_out(False, order, same_order, first, weights, gains)
     moved = exchange(first, TP)

time: 216 us -> 222 us (1.028)
  waiting for transfers between devices: 64.5 us -> 84.9 us
  starting transfers between devices: 55.7 us -> 43.1 us
  local copies, waits for them, and re-layouts: 13.6 us -> 10.4 us
    ppermute x6, waiting for transfers between devices: 12.2 us -> 31.3 us  [along_y(): lax.ppermute(piece, TP[0], [(i, (i + shift) % ring) for i in range(ring)])]
    all_to_all x6 -> x4, starting transfers between devices: 31.8 us -> 20.9 us  [exchange(): return lax.all_to_all(pieces, axes, split_axis=0, concat_axis=0, tiled=True)]
    all_to_all x6 -> x4, waiting for transfers between devices: 31 us -> 31.4 us  [exchange(): return lax.all_to_all(pieces, axes, split_axis=0, concat_axis=0, tiled=True)]
  transfers between devices with their start and end apart: 31 -> 29, of which waited for: 16 -> 17; matrix products, arithmetic and copies ran while one was open for 6% -> 5% of each run, Pallas kernels for 29% -> 26%
where the time goes in v2:
time: 222 us; the launch traced here: 218 us
  waiting for transfers between devices  84.9 us (38%)
  Pallas kernels  74.3 us (33%)
  starting transfers between devices  43.1 us (19%)
  local copies, waits for them, and re-layouts  10.4 us (5%)
  other arithmetic  4.9 us (2%)
    all_to_all x4, waiting for transfers between devices, exchange(): return lax.all_to_all(pieces, axes, split_axis=0, concat_axis=0, tiled=True)  31.4 us
    ppermute x6, waiting for transfers between devices, along_y(): lax.ppermute(piece, TP[0], [(i, (i + shift) % ring) for i in range(ring)])  31.3 us
    all_to_all x4, starting transfers between devices, exchange(): return lax.all_to_all(pieces, axes, split_axis=0, concat_axis=0, tiled=True)  20.9 us
    pallas_call x2, Pallas kernels, attend(): pl.pallas_call(functools.partial(attention_kernel, chunk * blocks), grid_...  20.5 us
    ppermute x14, waiting for transfers between devices, send_pieces(): got.append(lax.ppermute(pieces[k], TP, pairs) if k else pieces[0])  20.2 us
    pallas_call x2, Pallas kernels, project_out(): pl.pallas_call(out_kernel, grid_spec=pltpu.PrefetchScalarGridSpec(num_sca...  16.1 us
    ppermute x14, starting transfers between devices, send_pieces(): got.append(lax.ppermute(pieces[k], TP, pairs) if k else pieces[0])  14 us
    pallas_call x1, Pallas kernels, project_kv(): pl.pallas_call(kv_kernel, grid=(length // tile,), in_specs=[pl.BlockSpec(...  13.7 us
  transfers between devices with their start and end apart: 29, of which 17 were waited for; matrix products, arithmetic and copies ran while one was open for 5% of the time, Pallas kernels for 26%

profile of v2, /device:TPU:32, one launch (start us, length us, event | category | flops | bytes accessed | tf_op | source)
XLA Modules:
  0.0 218.0 jit_solution(2599898976586344778)
XLA Ops:
  0.0 1.6 collective-permute-start
  1.6 1.7 collective-permute-start.1
  3.2 0.8 copy.24
  6.0 4.1 %token_shares.1 = bf16[16,272,256]{2,1,0:T(8,128)(2,1)} custom-call(s32[1]{0:T(128)} %bitcast.rank, bf16[4096,2048]{1,0:T(8,128)(2,1)} %tok.4, bf16[16,16,256]{2,1,0:T(8,128)(2,1)} %pad.4.asks), custom_call_target="tpu_custom_call" | custom-call | flops 1048576 | bytes 4194304 | tf_op jit(solution)/shard_map/token_shares/pallas_call | solution.py:55
  10.1 7.9 %all-to-all-start = ((bf16[16,272,256]{2,1,0:T(8,128)(2,1)}), bf16[16,272,256]{2,1,0:T(8,128)(2,1)}, u32[]{:S(2)}, u32[]{:S(2)}) async-start(bf16[16,272,256]{2,1,0:T(8,128)(2,1)} %token_shares.1), calls=%async_computation | async-start | bytes 4456448 | tf_op jit(solution)/shard_map/all_to_all | solution.py:451
  18.1 1.3 select_reduce_fusion
  20.0 13.7 %project_kv.1 = bf16[64,2,64,256]{3,2,1,0:T(8,128)(2,1)} custom-call(bf16[4096,2048]{1,0:T(8,128)(2,1)} %tok.4, bf16[2048,256]{1,0:T(8,128)(2,1)} %wk.3, bf16[2048,256]{1,0:T(8,128)(2,1)} %wv.3, f32[1,128]{1,0:T(1,128)} %bitcast.35), custom_call_target="tpu_custom_call" | custom-call | flops 8589934592 | bytes 16777216 | tf_op jit(solution)/shard_map/project_kv/pallas_call | solution.py:89
  33.9 0.8 reshape.85.mask
  35.8 10.1 %project_q.1.q = bf16[4096,256]{1,0:T(8,128)(2,1)} custom-call(bf16[4096,2048]{1,0:T(8,128)(2,1)} %tok.4, bf16[2048,256]{1,0:T(8,128)(2,1)} %wq.1, f32[1,128]{1,0:T(1,128)} %multiply_bitcast_fusion.gain), custom_call_target="tpu_custom_call" | custom-call | flops 4294967296 | bytes 16777216 | tf_op jit(solution)/shard_map/project_q/pallas_call | solution.py:118
  45.9 2.8 %all-to-all-done = bf16[16,272,256]{2,1,0:T(8,128)(2,1)} async-done(((bf16[16,272,256]{2,1,0:T(8,128)(2,1)}), bf16[16,272,256]{2,1,0:T(8,128)(2,1)}, u32[]{:S(2)}, u32[]{:S(2)}) %all-to-all-start) | async-done | bytes 2228256 | tf_op jit(solution)/shard_map/all_to_all | solution.py:451
  48.7 0.8 slice_convert_fusion
  50.7 0.9 slice_bitcast_fusion
  51.8 3.1 %collective-permute-start.3 = (bf16[256,256]{1,0:T(8,128)(2,1)S(1)}, bf16[256,256]{1,0:T(8,128)(2,1)S(1)}, u32[]{:S(2)}, u32[]{:S(2)}) collective-permute-start(bf16[256,256]{1,0:T(8,128)(2,1)S(1)} %slice_bitcast_fusion), channel_id=1, source_target_pairs={{0,6},{2,0},{4,2},{6,4},{1,7},{3,1},{5,3},{7,5},{8,14},{10,8},{12,... | collective-permute-start | bytes 393224 | tf_op jit(solution)/shard_map/ppermute | solution.py:460
  55.5 3.8 %collective-permute-done.2 = bf16[256,256]{1,0:T(8,128)(2,1)S(1)} collective-permute-done((bf16[256,256]{1,0:T(8,128)(2,1)S(1)}, bf16[256,256]{1,0:T(8,128)(2,1)S(1)}, u32[]{:S(2)}, u32[]{:S(2)}) %collective-permute-start.2) | collective-permute-done | bytes 131104 | tf_op jit(solution)/shard_map/ppermute | solution.py:460
  59.3 2.2 collective-permute-done.4
  61.6 1.9 collective-permute-done.5.other
  63.5 0.8 copy-done.7
  64.3 6.6 %project_sent.1 = bf16[16,320,256]{2,1,0:T(8,128)(2,1)} custom-call(s32[32]{0:T(128)} %reshape.81.near, s32[128]{0:T(128)} %reshape.82.asked, s32[8]{0:T(128)} %pad_add_fusion.order, bf16[4,256,256]{2,1,0:T(8,128)(2,1)} %copy-done.6, bf16[4,256,256]{2,1,0:T(8,128)(2,1)} %copy-done.7, bf16[2048,256]{1,0:T(8,128)(2,1)} %wk.3, bf16[2048,256]{1,0:T(8,128)(2,1)} %wv.3, ...), custom_call_target="tpu_custom_call" | custom-call | flops 536870912 | bytes 8388608 | tf_op jit(solution)/shard_map/project_sent/pallas_call | solution.py:193
  70.9 5.7 %all-to-all-start.1 = ((bf16[16,320,256]{2,1,0:T(8,128)(2,1)}), bf16[16,320,256]{2,1,0:T(8,128)(2,1)S(1)}, u32[]{:S(2)}, u32[]{:S(2)}) async-start(bf16[16,320,256]{2,1,0:T(8,128)(2,1)} %project_sent.1), calls=%async_computation.1 | async-start | bytes 5242880 | tf_op jit(solution)/shard_map/all_to_all | solution.py:451
  77.7 25.4 %collective-permute-done.6.refs_4_.refs_11_ = bf16[256,2048]{1,0:T(8,128)(2,1)} collective-permute-done((bf16[256,2048]{1,0:T(8,128)(2,1)}, bf16[256,2048]{1,0:T(8,128)(2,1)}, u32[]{:S(2)}, u32[]{:S(2)}) %collective-permute-start.6) | collective-permute-done | bytes 1048608 | tf_op jit(solution)/shard_map/ppermute | solution.py:460
  103.0 13.4 %all-to-all-done.1.got = bf16[16,320,256]{2,1,0:T(8,128)(2,1)S(1)} async-done(((bf16[16,320,256]{2,1,0:T(8,128)(2,1)}), bf16[16,320,256]{2,1,0:T(8,128)(2,1)S(1)}, u32[]{:S(2)}, u32[]{:S(2)}) %all-to-all-start.1) | async-done | bytes 2621472 | tf_op jit(solution)/shard_map/all_to_all | solution.py:451
  117.0 0.9 copy-done.2
  117.9 11.1 %attend.2 = bf16[8,256,256]{2,1,0:T(8,128)(2,1)} custom-call(s32[512]{0:T(512)} %reshape.84.at, s32[8]{0:T(128)} %iota.18.where, bf16[4096,256]{1,0:T(8,128)(2,1)} %project_q.1.q, f32[64,512]{1,0:T(8,128)} %reshape.85.mask, bf16[8192,256]{1,0:T(8,128)(2,1)} %bitcast.25, bf16[16,320,256]{2,1,0:T(8,128)(2,1)} %copy-done.2), custom_call_target="tpu_custom_call" | custom-call | flops 2147483648 | bytes 10485760 | tf_op jit(solution)/shard_map/attend/pallas_call | solution.py:322
  129.0 3.6 %all-to-all-start.2 = ((bf16[8,256,256]{2,1,0:T(8,128)(2,1)}), bf16[8,256,256]{2,1,0:T(8,128)(2,1)S(1)}, u32[]{:S(2)}, u32[]{:S(2)}) async-start(bf16[8,256,256]{2,1,0:T(8,128)(2,1)} %attend.2), calls=%async_computation.2 | async-start | bytes 2097152 | tf_op jit(solution)/shard_map/all_to_all | solution.py:451
  133.2 15.2 %all-to-all-done.2.refs_0_ = bf16[8,256,256]{2,1,0:T(8,128)(2,1)S(1)} async-done(((bf16[8,256,256]{2,1,0:T(8,128)(2,1)}), bf16[8,256,256]{2,1,0:T(8,128)(2,1)S(1)}, u32[]{:S(2)}, u32[]{:S(2)}) %all-to-all-start.2) | async-done | bytes 1048608 | tf_op jit(solution)/shard_map/all_to_all | solution.py:451
  149.4 7.9 %project_out.2 = bf16[8,256,256]{2,1,0:T(8,128)(2,1)} custom-call(s32[8]{0:T(128)} %pad_add_fusion.order, s32[8]{0:T(128)} %iota.17.slot, bf16[8,256,256]{2,1,0:T(8,128)(2,1)} %copy-done.3, bf16[256,2048]{1,0:T(8,128)(2,1)} %refs_8_.1, bf16[256,2048]{1,0:T(8,128)(2,1)} %copy-done.4, bf16[256,2048]{1,0:T(8,128)(2,1)} %copy-done.5, ...), custom_call_target="tpu_custom_call" | custom-call | flops 2147483648 | bytes 12582912 | tf_op jit(solution)/shard_map/project_out/pallas_call | solution.py:394
  157.4 3.7 %all-to-all-start.3 = ((bf16[8,256,256]{2,1,0:T(8,128)(2,1)}), bf16[8,256,256]{2,1,0:T(8,128)(2,1)S(1)}, u32[]{:S(2)}, u32[]{:S(2)}) async-start(bf16[8,256,256]{2,1,0:T(8,128)(2,1)} %project_out.2), calls=%async_computation.3 | async-start | bytes 2097152 | tf_op jit(solution)/shard_map/all_to_all | solution.py:451
  161.1 9.4 %attend.3 = (bf16[256,256]{1,0:T(8,128)(2,1)}, bf16[256,256]{1,0:T(8,128)(2,1)}, bf16[256,256]{1,0:T(8,128)(2,1)}, bf16[256,256]{1,0:T(8,128)(2,1)}, bf16[256,25...) custom-call(s32[512]{0:T(512)} %reshape.84.at, ...), custom_call_target="tpu_custom_call" | custom-call | flops 2147483648 | bytes 10485760 | tf_op jit(solution)/shard_map/attend/pallas_call | solution.py:322
  170.5 1.8 collective-permute-start.11
  172.3 1.5 collective-permute-start.12
  173.8 2.0 collective-permute-start.13
  175.8 0.7 collective-permute-start.15
  176.5 3.6 %collective-permute-done.11.refs_1_ = bf16[256,256]{1,0:T(8,128)(2,1)S(1)} collective-permute-done((bf16[256,256]{1,0:T(8,128)(2,1)}, bf16[256,256]{1,0:T(8,128)(2,1)S(1)}, u32[]{:S(2)}, u32[]{:S(2)}) %collective-permute-start.11) | collective-permute-done | bytes 131104 | tf_op jit(solution)/shard_map/ppermute | solution.py:493
  180.5 2.5 %collective-permute-done.13.refs_3_ = bf16[256,256]{1,0:T(8,128)(2,1)S(1)} collective-permute-done((bf16[256,256]{1,0:T(8,128)(2,1)}, bf16[256,256]{1,0:T(8,128)(2,1)S(1)}, u32[]{:S(2)}, u32[]{:S(2)}) %collective-permute-start.13) | collective-permute-done | bytes 131104 | tf_op jit(solution)/shard_map/ppermute | solution.py:493
  183.0 2.3 %collective-permute-done.15.refs_5_ = bf16[256,256]{1,0:T(8,128)(2,1)S(1)} collective-permute-done((bf16[256,256]{1,0:T(8,128)(2,1)}, bf16[256,256]{1,0:T(8,128)(2,1)S(1)}, u32[]{:S(2)}, u32[]{:S(2)}) %collective-permute-start.15) | collective-permute-done | bytes 131104 | tf_op jit(solution)/shard_map/ppermute | solution.py:493
  186.0 1.5 collective-permute-done.17.refs_7_
  188.2 8.1 %project_out.3 = (bf16[256,256]{1,0:T(8,128)(2,1)}, bf16[256,256]{1,0:T(8,128)(2,1)}, bf16[256,256]{1,0:T(8,128)(2,1)}, bf16[256,256]{1,0:T(8,128)(2,1)}, bf16[2...) custom-call(s32[8]{0:T(128)} %pad_add_fusion.order, ...), custom_call_target="tpu_custom_call" | custom-call | flops 2147483648 | bytes 12582912 | tf_op jit(solution)/shard_map/project_out/pallas_call | solution.py:394
  196.3 1.2 collective-permute-start.18
  197.5 2.9 %collective-permute-start.19 = (bf16[256,256]{1,0:T(8,128)(2,1)}, bf16[256,256]{1,0:T(8,128)(2,1)S(1)}, u32[]{:S(2)}, u32[]{:S(2)}) collective-permute-start(bf16[256,256]{1,0:T(8,128)(2,1)} %get-tuple-element.69), channel_id=1, source_target_pairs={{0,6},{1,7},{2,0},{3,1},{4,2},{5,3},{6,4},{7,5},{8,14},{9,15},{10,... | collective-permute-start | bytes 393224 | tf_op jit(solution)/shard_map/ppermute | solution.py:493
  200.4 1.4 collective-permute-start.20
  201.8 1.5 collective-permute-start.22
  203.3 1.0 collective-permute-done.18.rest_1_
  204.9 1.7 collective-permute-done.19.rest_2_
  206.6 2.6 %collective-permute-done.20.rest_3_ = bf16[256,256]{1,0:T(8,128)(2,1)S(1)} collective-permute-done((bf16[256,256]{1,0:T(8,128)(2,1)}, bf16[256,256]{1,0:T(8,128)(2,1)S(1)}, u32[]{:S(2)}, u32[]{:S(2)}) %collective-permute-start.20) | collective-permute-done | bytes 131104 | tf_op jit(solution)/shard_map/ppermute | solution.py:493
  209.2 1.7 collective-permute-done.22.rest_5_
  210.9 2.6 %collective-permute-done.24.rest_7_ = bf16[256,256]{1,0:T(8,128)(2,1)S(1)} collective-permute-done((bf16[256,256]{1,0:T(8,128)(2,1)}, bf16[256,256]{1,0:T(8,128)(2,1)S(1)}, u32[]{:S(2)}, u32[]{:S(2)}) %collective-permute-start.24) | collective-permute-done | bytes 131104 | tf_op jit(solution)/shard_map/ppermute | solution.py:493
  213.5 0.9 copy-done
  214.4 3.4 %place.1 = bf16[16,256,256]{2,1,0:T(8,128)(2,1)} custom-call(s32[8]{0:T(128)S(1)} %copy-done.1, bf16[8,256,256]{2,1,0:T(8,128)(2,1)S(1)} %all-to-all-done.3.whole, bf16[256,256]{1,0:T(8,128)(2,1)S(1)} %copy-done, bf16[256,256]{1,0:T(8,128)(2,1)S(1)} %collective-permute-done.18.rest_1_, bf16[256,256]{1,0:T(8,128)(2,1)S(1)} %collective-permute-done.19.rest_2_, ...), custom_call_target="tpu_custom_call" | custom-call | flops 1048576 | bytes 4194304 | tf_op jit(solution)/shard_map/place/pallas_call | solution.py:434
  (87 shorter events, 11.7 us)
Async XLA Ops:
  0.0 51.6 %collective-permute-start = (bf16[256,2048]{1,0:T(8,128)(2,1)}, bf16[256,2048]{1,0:T(8,128)(2,1)S(1)}, u32[]{:S(2)}, u32[]{:S(2)}) collective-permute-start(bf16[256,2048]{1,0:T(8,128)(2,1)} %refs_8_.1), channel_id=1, source_target_pairs={{0,2},{2,4},{4,6},{6,0},{1,3},{3,5},{5,7},{7,1},{8,10},{10,12},{12... | collective-permute-start | bytes 3145736 | tf_op jit(solution)/shard_map/ppermute | solution.py:460
  1.6 50.1 %collective-permute-start.1 = (bf16[256,2048]{1,0:T(8,128)(2,1)}, bf16[256,2048]{1,0:T(8,128)(2,1)S(1)}, u32[]{:S(2)}, u32[]{:S(2)}) collective-permute-start(bf16[256,2048]{1,0:T(8,128)(2,1)} %refs_8_.1), channel_id=1, source_target_pairs={{0,6},{2,0},{4,2},{6,4},{1,7},{3,1},{5,3},{7,5},{8,14},{10,8},{12,... | collective-permute-start | bytes 3145736 | tf_op jit(solution)/shard_map/ppermute | solution.py:460
  10.1 38.6 %all-to-all-start = ((bf16[16,272,256]{2,1,0:T(8,128)(2,1)}), bf16[16,272,256]{2,1,0:T(8,128)(2,1)}, u32[]{:S(2)}, u32[]{:S(2)}) async-start(bf16[16,272,256]{2,1,0:T(8,128)(2,1)} %token_shares.1), calls=%async_computation | async-start | bytes 4456448 | tf_op jit(solution)/shard_map/all_to_all | solution.py:451
  20.0 15.3 %copy-start.15 = (f32[128]{0:T(128)S(1)}, f32[128]{0:T(128)}, u32[]{:S(2)}) copy-start(f32[128]{0:T(128)} %param.14) | copy-start | bytes 1540
  51.6 19.2 %copy-start.4 = (bf16[256,2048]{1,0:T(8,128)(2,1)}, bf16[256,2048]{1,0:T(8,128)(2,1)S(1)}, u32[]{:S(2)}) copy-start(bf16[256,2048]{1,0:T(8,128)(2,1)S(1)} %collective-permute-done.refs_2_.refs_9_) | copy-start | bytes 3145732
  51.7 19.2 %copy-start.5 = (bf16[256,2048]{1,0:T(8,128)(2,1)}, bf16[256,2048]{1,0:T(8,128)(2,1)S(1)}, u32[]{:S(2)}) copy-start(bf16[256,2048]{1,0:T(8,128)(2,1)S(1)} %collective-permute-done.1.refs_3_.refs_10_) | copy-start | bytes 3145732
  51.7 7.6 %collective-permute-start.2 = (bf16[256,256]{1,0:T(8,128)(2,1)S(1)}, bf16[256,256]{1,0:T(8,128)(2,1)S(1)}, u32[]{:S(2)}, u32[]{:S(2)}) collective-permute-start(bf16[256,256]{1,0:T(8,128)(2,1)S(1)} %slice_bitcast_fusion), channel_id=1, source_target_pairs={{0,2},{2,4},{4,6},{6,0},{1,3},{3,5},{5,7},{7,1},{8,10},{10,12},{12... | collective-permute-start | bytes 393224 | tf_op jit(solution)/shard_map/ppermute | solution.py:460
  51.8 7.4 %collective-permute-start.3 = (bf16[256,256]{1,0:T(8,128)(2,1)S(1)}, bf16[256,256]{1,0:T(8,128)(2,1)S(1)}, u32[]{:S(2)}, u32[]{:S(2)}) collective-permute-start(bf16[256,256]{1,0:T(8,128)(2,1)S(1)} %slice_bitcast_fusion), channel_id=1, source_target_pairs={{0,6},{2,0},{4,2},{6,4},{1,7},{3,1},{5,3},{7,5},{8,14},{10,8},{12,... | collective-permute-start | bytes 393224 | tf_op jit(solution)/shard_map/ppermute | solution.py:460
  55.0 6.5 %collective-permute-start.4 = (bf16[256,256]{1,0:T(8,128)(2,1)S(1)}, bf16[256,256]{1,0:T(8,128)(2,1)S(1)}, u32[]{:S(2)}, u32[]{:S(2)}) collective-permute-start(bf16[256,256]{1,0:T(8,128)(2,1)S(1)} %slice_bitcast_fusion), channel_id=1, source_target_pairs={{0,4},{2,6},{4,0},{6,2},{1,5},{3,7},{5,1},{7,3},{8,12},{10,14},{12... | collective-permute-start | bytes 393224 | tf_op jit(solution)/shard_map/ppermute | solution.py:460
  61.5 2.0 copy-start.6
  61.5 2.0 collective-permute-start.5
  63.5 0.8 copy-start.7
  70.9 45.5 %all-to-all-start.1 = ((bf16[16,320,256]{2,1,0:T(8,128)(2,1)}), bf16[16,320,256]{2,1,0:T(8,128)(2,1)S(1)}, u32[]{:S(2)}, u32[]{:S(2)}) async-start(bf16[16,320,256]{2,1,0:T(8,128)(2,1)} %project_sent.1), calls=%async_computation.1 | async-start | bytes 5242880 | tf_op jit(solution)/shard_map/all_to_all | solution.py:451
  76.6 26.4 %collective-permute-start.6 = (bf16[256,2048]{1,0:T(8,128)(2,1)}, bf16[256,2048]{1,0:T(8,128)(2,1)}, u32[]{:S(2)}, u32[]{:S(2)}) collective-permute-start(bf16[256,2048]{1,0:T(8,128)(2,1)} %copy-done.4), channel_id=1, source_target_pairs={{0,2},{2,4},{4,6},{6,0},{1,3},{3,5},{5,7},{7,1},{8,10},{10,12},{12... | collective-permute-start | bytes 3145736 | tf_op jit(solution)/shard_map/ppermute | solution.py:460
  77.1 56.1 %collective-permute-start.7 = (bf16[256,2048]{1,0:T(8,128)(2,1)}, bf16[256,2048]{1,0:T(8,128)(2,1)}, u32[]{:S(2)}, u32[]{:S(2)}) collective-permute-start(bf16[256,2048]{1,0:T(8,128)(2,1)} %refs_8_.1), channel_id=1, source_target_pairs={{0,1},{1,0},{2,3},{3,2},{4,5},{5,4},{6,7},{7,6},{8,9},{9,8},{10,11... | collective-permute-start | bytes 3145736 | tf_op jit(solution)/shard_map/ppermute | solution.py:464
  77.1 56.1 %collective-permute-start.8 = (bf16[256,2048]{1,0:T(8,128)(2,1)}, bf16[256,2048]{1,0:T(8,128)(2,1)}, u32[]{:S(2)}, u32[]{:S(2)}) collective-permute-start(bf16[256,2048]{1,0:T(8,128)(2,1)} %copy-done.4), channel_id=1, source_target_pairs={{0,1},{1,0},{2,3},{3,2},{4,5},{5,4},{6,7},{7,6},{8,9},{9,8},{10,11... | collective-permute-start | bytes 3145736 | tf_op jit(solution)/shard_map/ppermute | solution.py:464
  77.6 55.5 %collective-permute-start.9 = (bf16[256,2048]{1,0:T(8,128)(2,1)}, bf16[256,2048]{1,0:T(8,128)(2,1)}, u32[]{:S(2)}, u32[]{:S(2)}) collective-permute-start(bf16[256,2048]{1,0:T(8,128)(2,1)} %copy-done.5), channel_id=1, source_target_pairs={{0,1},{1,0},{2,3},{3,2},{4,5},{5,4},{6,7},{7,6},{8,9},{9,8},{10,11... | collective-permute-start | bytes 3145736 | tf_op jit(solution)/shard_map/ppermute | solution.py:464
  103.0 30.2 %collective-permute-start.10 = (bf16[256,2048]{1,0:T(8,128)(2,1)}, bf16[256,2048]{1,0:T(8,128)(2,1)}, u32[]{:S(2)}, u32[]{:S(2)}) collective-permute-start(bf16[256,2048]{1,0:T(8,128)(2,1)} %collective-permute-done.6.refs_4_.refs_11_), channel_id=1, source_target_pairs={{0,1},{1,0},{2,3},{3,2},{4,5},{5,4},{6,7},{7,6},{8,9},{9,8},{10,11... | collective-permute-start | bytes 3145736 | tf_op jit(solution)/shard_map/ppermute | solution.py:464
  116.4 1.5 copy-start.2
  129.0 19.4 %all-to-all-start.2 = ((bf16[8,256,256]{2,1,0:T(8,128)(2,1)}), bf16[8,256,256]{2,1,0:T(8,128)(2,1)S(1)}, u32[]{:S(2)}, u32[]{:S(2)}) async-start(bf16[8,256,256]{2,1,0:T(8,128)(2,1)} %attend.2), calls=%async_computation.2 | async-start | bytes 2097152 | tf_op jit(solution)/shard_map/all_to_all | solution.py:451
  148.4 1.0 copy-start.3
  157.4 56.2 %all-to-all-start.3 = ((bf16[8,256,256]{2,1,0:T(8,128)(2,1)}), bf16[8,256,256]{2,1,0:T(8,128)(2,1)S(1)}, u32[]{:S(2)}, u32[]{:S(2)}) async-start(bf16[8,256,256]{2,1,0:T(8,128)(2,1)} %project_out.2), calls=%async_computation.3 | async-start | bytes 2097152 | tf_op jit(solution)/shard_map/all_to_all | solution.py:451
  170.5 9.7 %collective-permute-start.11 = (bf16[256,256]{1,0:T(8,128)(2,1)}, bf16[256,256]{1,0:T(8,128)(2,1)S(1)}, u32[]{:S(2)}, u32[]{:S(2)}) collective-permute-start(bf16[256,256]{1,0:T(8,128)(2,1)} %get-tuple-element.52), channel_id=1, source_target_pairs={{0,2},{1,3},{2,4},{3,5},{4,6},{5,7},{6,0},{7,1},{8,10},{9,11},{10,... | collective-permute-start | bytes 393224 | tf_op jit(solution)/shard_map/ppermute | solution.py:493
  172.3 7.9 %collective-permute-start.12 = (bf16[256,256]{1,0:T(8,128)(2,1)}, bf16[256,256]{1,0:T(8,128)(2,1)S(1)}, u32[]{:S(2)}, u32[]{:S(2)}) collective-permute-start(bf16[256,256]{1,0:T(8,128)(2,1)} %get-tuple-element.53), channel_id=1, source_target_pairs={{0,6},{1,7},{2,0},{3,1},{4,2},{5,3},{6,4},{7,5},{8,14},{9,15},{10,... | collective-permute-start | bytes 393224 | tf_op jit(solution)/shard_map/ppermute | solution.py:493
  173.8 9.2 %collective-permute-start.13 = (bf16[256,256]{1,0:T(8,128)(2,1)}, bf16[256,256]{1,0:T(8,128)(2,1)S(1)}, u32[]{:S(2)}, u32[]{:S(2)}) collective-permute-start(bf16[256,256]{1,0:T(8,128)(2,1)} %get-tuple-element.54), channel_id=1, source_target_pairs={{0,4},{1,5},{2,6},{3,7},{4,0},{5,1},{6,2},{7,3},{8,12},{9,13},{10,... | collective-permute-start | bytes 393224 | tf_op jit(solution)/shard_map/ppermute | solution.py:493
  175.8 7.1 %collective-permute-start.14 = (bf16[256,256]{1,0:T(8,128)(2,1)}, bf16[256,256]{1,0:T(8,128)(2,1)S(1)}, u32[]{:S(2)}, u32[]{:S(2)}) collective-permute-start(bf16[256,256]{1,0:T(8,128)(2,1)} %get-tuple-element.55), channel_id=1, source_target_pairs={{0,1},{1,0},{2,3},{3,2},{4,5},{5,4},{6,7},{7,6},{8,9},{9,8},{10,11... | collective-permute-start | bytes 393224 | tf_op jit(solution)/shard_map/ppermute | solution.py:493
  175.8 9.5 %collective-permute-start.15 = (bf16[256,256]{1,0:T(8,128)(2,1)}, bf16[256,256]{1,0:T(8,128)(2,1)S(1)}, u32[]{:S(2)}, u32[]{:S(2)}) collective-permute-start(bf16[256,256]{1,0:T(8,128)(2,1)} %get-tuple-element.56), channel_id=1, source_target_pairs={{0,3},{1,2},{2,5},{3,4},{4,7},{5,6},{6,1},{7,0},{8,11},{9,10},{10,... | collective-permute-start | bytes 393224 | tf_op jit(solution)/shard_map/ppermute | solution.py:493
  180.2 7.4 %copy-start.8 = (bf16[256,256]{1,0:T(8,128)(2,1)}, bf16[256,256]{1,0:T(8,128)(2,1)S(1)}, u32[]{:S(2)}) copy-start(bf16[256,256]{1,0:T(8,128)(2,1)S(1)} %collective-permute-done.11.refs_1_) | copy-start | bytes 393220
  180.2 5.9 %collective-permute-start.16 = (bf16[256,256]{1,0:T(8,128)(2,1)}, bf16[256,256]{1,0:T(8,128)(2,1)S(1)}, u32[]{:S(2)}, u32[]{:S(2)}) collective-permute-start(bf16[256,256]{1,0:T(8,128)(2,1)} %get-tuple-element.57), channel_id=1, source_target_pairs={{0,7},{1,6},{2,1},{3,0},{4,3},{5,2},{6,5},{7,4},{8,15},{9,14},{10,... | collective-permute-start | bytes 393224 | tf_op jit(solution)/shard_map/ppermute | solution.py:493
  180.2 7.4 %copy-start.9 = (bf16[256,256]{1,0:T(8,128)(2,1)}, bf16[256,256]{1,0:T(8,128)(2,1)S(1)}, u32[]{:S(2)}) copy-start(bf16[256,256]{1,0:T(8,128)(2,1)S(1)} %collective-permute-done.12.refs_2_) | copy-start | bytes 393220
  180.2 7.3 %collective-permute-start.17 = (bf16[256,256]{1,0:T(8,128)(2,1)}, bf16[256,256]{1,0:T(8,128)(2,1)S(1)}, u32[]{:S(2)}, u32[]{:S(2)}) collective-permute-start(bf16[256,256]{1,0:T(8,128)(2,1)} %get-tuple-element.58), channel_id=1, source_target_pairs={{0,5},{1,4},{2,7},{3,6},{4,1},{5,0},{6,3},{7,2},{8,13},{9,12},{10,... | collective-permute-start | bytes 393224 | tf_op jit(solution)/shard_map/ppermute | solution.py:493
  183.0 4.6 %copy-start.10 = (bf16[256,256]{1,0:T(8,128)(2,1)}, bf16[256,256]{1,0:T(8,128)(2,1)S(1)}, u32[]{:S(2)}) copy-start(bf16[256,256]{1,0:T(8,128)(2,1)S(1)} %collective-permute-done.13.refs_3_) | copy-start | bytes 393220
  183.0 4.6 %copy-start.11 = (bf16[256,256]{1,0:T(8,128)(2,1)}, bf16[256,256]{1,0:T(8,128)(2,1)S(1)}, u32[]{:S(2)}) copy-start(bf16[256,256]{1,0:T(8,128)(2,1)S(1)} %collective-permute-done.14.refs_4_) | copy-start | bytes 393220
  185.3 2.2 %copy-start.12 = (bf16[256,256]{1,0:T(8,128)(2,1)}, bf16[256,256]{1,0:T(8,128)(2,1)S(1)}, u32[]{:S(2)}) copy-start(bf16[256,256]{1,0:T(8,128)(2,1)S(1)} %collective-permute-done.15.refs_5_) | copy-start | bytes 393220
  186.0 1.5 copy-start.13
  187.5 0.6 copy-start.14
  188.2 25.4 %copy-start.1 = (s32[8]{0:T(128)S(1)}, s32[8]{0:T(128)}, u32[]{:S(2)}) copy-start(s32[8]{0:T(128)} %pad_add_fusion.order) | copy-start | bytes 100
  196.3 8.0 %collective-permute-start.18 = (bf16[256,256]{1,0:T(8,128)(2,1)}, bf16[256,256]{1,0:T(8,128)(2,1)S(1)}, u32[]{:S(2)}, u32[]{:S(2)}) collective-permute-start(bf16[256,256]{1,0:T(8,128)(2,1)} %get-tuple-element.68), channel_id=1, source_target_pairs={{0,2},{1,3},{2,4},{3,5},{4,6},{5,7},{6,0},{7,1},{8,10},{9,11},{10,... | collective-permute-start | bytes 393224 | tf_op jit(solution)/shard_map/ppermute | solution.py:493
  197.5 9.1 %collective-permute-start.19 = (bf16[256,256]{1,0:T(8,128)(2,1)}, bf16[256,256]{1,0:T(8,128)(2,1)S(1)}, u32[]{:S(2)}, u32[]{:S(2)}) collective-permute-start(bf16[256,256]{1,0:T(8,128)(2,1)} %get-tuple-element.69), channel_id=1, source_target_pairs={{0,6},{1,7},{2,0},{3,1},{4,2},{5,3},{6,4},{7,5},{8,14},{9,15},{10,... | collective-permute-start | bytes 393224 | tf_op jit(solution)/shard_map/ppermute | solution.py:493
  200.4 8.8 %collective-permute-start.20 = (bf16[256,256]{1,0:T(8,128)(2,1)}, bf16[256,256]{1,0:T(8,128)(2,1)S(1)}, u32[]{:S(2)}, u32[]{:S(2)}) collective-permute-start(bf16[256,256]{1,0:T(8,128)(2,1)} %get-tuple-element.70), channel_id=1, source_target_pairs={{0,4},{1,5},{2,6},{3,7},{4,0},{5,1},{6,2},{7,3},{8,12},{9,13},{10,... | collective-permute-start | bytes 393224 | tf_op jit(solution)/shard_map/ppermute | solution.py:493
  201.8 7.4 %collective-permute-start.21 = (bf16[256,256]{1,0:T(8,128)(2,1)}, bf16[256,256]{1,0:T(8,128)(2,1)S(1)}, u32[]{:S(2)}, u32[]{:S(2)}) collective-permute-start(bf16[256,256]{1,0:T(8,128)(2,1)} %get-tuple-element.71), channel_id=1, source_target_pairs={{0,1},{1,0},{2,3},{3,2},{4,5},{5,4},{6,7},{7,6},{8,9},{9,8},{10,11... | collective-permute-start | bytes 393224 | tf_op jit(solution)/shard_map/ppermute | solution.py:493
  201.8 9.1 %collective-permute-start.22 = (bf16[256,256]{1,0:T(8,128)(2,1)}, bf16[256,256]{1,0:T(8,128)(2,1)S(1)}, u32[]{:S(2)}, u32[]{:S(2)}) collective-permute-start(bf16[256,256]{1,0:T(8,128)(2,1)} %get-tuple-element.72), channel_id=1, source_target_pairs={{0,3},{1,2},{2,5},{3,4},{4,7},{5,6},{6,1},{7,0},{8,11},{9,10},{10,... | collective-permute-start | bytes 393224 | tf_op jit(solution)/shard_map/ppermute | solution.py:493
  204.3 6.6 %collective-permute-start.23 = (bf16[256,256]{1,0:T(8,128)(2,1)}, bf16[256,256]{1,0:T(8,128)(2,1)S(1)}, u32[]{:S(2)}, u32[]{:S(2)}) collective-permute-start(bf16[256,256]{1,0:T(8,128)(2,1)} %get-tuple-element.73), channel_id=1, source_target_pairs={{0,7},{1,6},{2,1},{3,0},{4,3},{5,2},{6,5},{7,4},{8,15},{9,14},{10,... | collective-permute-start | bytes 393224 | tf_op jit(solution)/shard_map/ppermute | solution.py:493
  206.6 6.9 %collective-permute-start.24 = (bf16[256,256]{1,0:T(8,128)(2,1)}, bf16[256,256]{1,0:T(8,128)(2,1)S(1)}, u32[]{:S(2)}, u32[]{:S(2)}) collective-permute-start(bf16[256,256]{1,0:T(8,128)(2,1)} %get-tuple-element.74), channel_id=1, source_target_pairs={{0,5},{1,4},{2,7},{3,6},{4,1},{5,0},{6,3},{7,2},{8,13},{9,12},{10,... | collective-permute-start | bytes 393224 | tf_op jit(solution)/shard_map/ppermute | solution.py:493
  213.5 0.9 copy-start

commit v3 on v2

--- a/solution.py
+++ b/solution.py
@@ -133,22 +133,52 @@
     )(tokens, w_query, gain)
 
 
-def send_kernel(near, asked, order, same, other, wk, wv, gain, pairs, out, keep, sems):
+def near_kernel(near, pairs, out, room, in_sems, out_sems):
+    devices = out.shape[0]
+    reach = near.shape[0] // devices
+    unit = PAIR * BLOCK
+    coming, going = [], []
+    for m in range(near.shape[0]):
+        first = pl.multiple_of(near[m] * unit, unit)
+        coming.append(
+            pltpu.make_async_copy(pairs.at[pl.ds(first, unit)], room.at[m], in_sems.at[m])
+        )
+        to = out.at[m // reach, pl.ds((m % reach) * unit, unit)]
+        going.append(pltpu.make_async_copy(room.at[m], to, out_sems.at[m]))
+    for copy in coming:
+        copy.start()
+    for n, copy in enumerate(coming):
+        copy.wait()
+        going[n].start()
+    for copy in going:
+        copy.wait()
+
+
+def gather_near(near, pairs, devices, length):
+    anywhere = pl.BlockSpec(memory_space=pl.ANY)
+    sends = near.shape[0]
+    return pl.pallas_call(
+        near_kernel,
+        grid_spec=pltpu.PrefetchScalarGridSpec(
+            num_scalar_prefetch=1,
+            grid=(1,),
+            in_specs=[anywhere],
+            out_specs=anywhere,
+            scratch_shapes=[
+                pltpu.VMEM((sends, PAIR * BLOCK, WIDTH), bf16),
+                pltpu.SemaphoreType.DMA((sends,)),
+                pltpu.SemaphoreType.DMA((sends,)),
+            ],
+        ),
+        out_shape=jax.ShapeDtypeStruct((devices, length, WIDTH), bf16),
+        compiler_params=pltpu.CompilerParams(vmem_limit_bytes=VMEM_LIMIT),
+        cost_estimate=pl.CostEstimate(flops=1 << 20, bytes_accessed=4 << 20, transcendentals=0),
+        name="gather_near",
+    )(near, pairs)
+
+
+def send_kernel(asked, order, same, other, wk, wv, gain, _, out, keep):
     devices, rows, _ = out.shape
-    reach = near.shape[0] // devices
-    plain = reach * PAIR * BLOCK
-    copies = []
-    for m in range(near.shape[0]):
-        first = pl.multiple_of(near[m] * PAIR * BLOCK, PAIR * BLOCK)
-        to = pl.ds((m % reach) * PAIR * BLOCK, PAIR * BLOCK)
-        copies.append(
-            pltpu.make_async_copy(
-                pairs.at[pl.ds(first, PAIR * BLOCK)], out.at[m // reach, to], sems.at[m]
-            )
-        )
-    for copy in copies:
-        copy.start()
-
     keys = jnp.zeros((same.shape[1], WIDTH), f32)
     vals = jnp.zeros((same.shape[1], WIDTH), f32)
     count = same.shape[0]
@@ -166,34 +196,33 @@
         keep[:, :part, lanes] = (x * factor * gain[...]).reshape(groups, part, HEAD_DIM)
     keep[:, part:, :] = vals.reshape(groups, part, WIDTH)
 
-    twos = (rows - plain) // (2 * unit)
+    twos = rows // (2 * unit)
 
     def one(m, carry):
         both = jnp.concatenate([keep[asked[2 * m]], keep[asked[2 * m + 1]]], axis=0)
-        at = pl.multiple_of(plain + (m % twos) * 2 * unit, 2 * unit)
+        at = pl.multiple_of((m % twos) * 2 * unit, 2 * unit)
         out[m // twos, pl.ds(at, 2 * unit), :] = both.astype(bf16)
         return carry
 
     lax.fori_loop(0, devices * twos, one, 0, unroll=4)
-    for copy in copies:
-        copy.wait()
 
 
 def whole_block(*shape):
     return pl.BlockSpec(shape, lambda i, *_: (0,) * len(shape))
 
 
-def project_sent(near, asked, order, same, other, w_key, w_value, gain, pairs, devices):
+def project_sent(asked, order, same, other, w_key, w_value, gain, sent):
     count, rows, _ = same.shape
     groups = 64
     unit = 2 * rows // groups
     depth = w_key.shape[0]
-    length = (near.shape[0] // devices) * PAIR * BLOCK + (asked.shape[0] // devices) * unit
-    shape = (devices, length, WIDTH)
+    devices, length, _ = sent.shape
+    hot_rows = (asked.shape[0] // devices) * unit
+    last = length // hot_rows - 1
     return pl.pallas_call(
         send_kernel,
         grid_spec=pltpu.PrefetchScalarGridSpec(
-            num_scalar_prefetch=3,
+            num_scalar_prefetch=2,
             grid=(1,),
             in_specs=[
                 whole_block(count, rows, WIDTH),
@@ -203,19 +232,17 @@
                 whole_block(1, HEAD_DIM),
                 pl.BlockSpec(memory_space=pl.ANY),
             ],
-            out_specs=whole_block(*shape),
-            scratch_shapes=[
-                pltpu.VMEM((groups, unit, WIDTH), f32),
-                pltpu.SemaphoreType.DMA((near.shape[0],)),
-            ],
-        ),
-        out_shape=jax.ShapeDtypeStruct(shape, bf16),
+            out_specs=pl.BlockSpec((devices, hot_rows, WIDTH), lambda i, *_: (0, last, 0)),
+            scratch_shapes=[pltpu.VMEM((groups, unit, WIDTH), f32)],
+        ),
+        out_shape=jax.ShapeDtypeStruct(sent.shape, bf16),
+        input_output_aliases={7: 0},
         compiler_params=pltpu.CompilerParams(vmem_limit_bytes=VMEM_LIMIT),
         cost_estimate=pl.CostEstimate(
             flops=4 * rows * depth * WIDTH, bytes_accessed=8 << 20, transcendentals=0
         ),
         name="project_sent",
-    )(near, asked, order, same, other, w_key, w_value, gain, pairs)
+    )(asked, order, same, other, w_key, w_value, gain, sent)
 
 
 def attention_kernel(first, at, where, q, mask, pairs, got, *rest):
@@ -437,7 +464,7 @@
             num_scalar_prefetch=1,
             grid=(1,),
             in_specs=[anywhere] * (count + 1),
-            out_specs=pl.BlockSpec(shape, lambda i, order: (0, 0, 0)),
+            out_specs=anywhere,
             scratch_shapes=[pltpu.SemaphoreType.DMA((count + 1,))],
         ),
         out_shape=jax.ShapeDtypeStruct(shape, bf16),
@@ -500,6 +527,7 @@
     devices = lax.axis_size(KV)
     position = lax.axis_index(KV)
     ranks = lax.axis_size(TP)
+    part = BLOCK // devices
     key_row = key_gain[None, :]
     query_row = (query_gain * (HEAD_DIM ** (-0.5) * LOG2E))[None, :]
 
@@ -525,10 +553,6 @@
 
     rank = lax.axis_index(TP).astype(jnp.int32).reshape(1)
     arrived = exchange(token_shares(rank, tokens, asks), KV)
-    shares = arrived[0, :-16]
-    asked = arrived[:, -16, : 2 * HOT].astype(jnp.int32)
-    asked_near = asked[:, :REACH].reshape(-1)
-    asked_hot = asked[:, HOT:].reshape(-1)
     w_after = along_y(w_out, 1)
     w_before = along_y(w_out, -1)
     w_own = across(w_out)
@@ -548,16 +572,21 @@
     at = jnp.where(usable, at, 0).astype(jnp.int32).reshape(-1)
     mask = jnp.repeat(usable.astype(f32), BLOCK, axis=1)
 
-    shares, asked_near, asked_hot, queries, at, mask, order, w_after, w_before = tied(
-        shares, asked_near, asked_hot, queries, at, mask, order, w_after, w_before
+    arrived, queries, at, mask, order, w_after, w_before = tied(
+        arrived, queries, at, mask, order, w_after, w_before
     )
+    shares = arrived[0, :-16]
     parts = [shares] + [along_y(shares, shift) for shift in (1, -1, 2)]
     w_far = along_y(w_after, 1)
     w_swapped = [across(w_after), across(w_before)]
+    asked = arrived[:, -16, : 2 * HOT].astype(jnp.int32)
+    asked_near = asked[:, :REACH].reshape(-1)
+    asked_hot = asked[:, HOT:].reshape(-1)
+    length_sent = REACH * PAIR * BLOCK + HOT * 2 * part
+    sent = gather_near(asked_near, pairs, devices, length_sent)
+    asked_hot, sent, *parts = tied(asked_hot, sent, *parts)
     rows_same, rows_other = both_cores(parts)
-    sent = project_sent(
-        asked_near, asked_hot, order, rows_same, rows_other, w_key, w_value, key_row, pairs, devices
-    )
+    sent = project_sent(asked_hot, order, rows_same, rows_other, w_key, w_value, key_row, sent)
     got = exchange(sent, KV)
     w_swapped.append(across(w_far))
     weights = [w_out, w_after, w_before, w_far, w_own] + w_swapped

time: 222 us -> 218 us (0.982)
  waiting for transfers between devices: 84.9 us -> 78.4 us
    ppermute x6, waiting for transfers between devices: 31.3 us -> 25.1 us  [along_y(): lax.ppermute(piece, TP[0], [(i, (i + shift) % ring) for i in range(ring)])]
    pallas_call x0 -> x1, Pallas kernels: none -> 4.35 us  [gather_near(): pl.pallas_call(near_kernel, grid_spec=pltpu.PrefetchScalarGridSpec(num_sc...]
  transfers between devices with their start and end apart: 29 -> 29, of which waited for: 17 -> 15; matrix products, arithmetic and copies ran while one was open for 5% -> 5% of each run, Pallas kernels for 26% -> 29%
where the time goes in v3:
time: 218 us; the launch traced here: 214 us
  waiting for transfers between devices  78.4 us (36%)
  Pallas kernels  75.6 us (35%)
  starting transfers between devices  43.8 us (20%)
  local copies, waits for them, and re-layouts  10.5 us (5%)
  other arithmetic  4.99 us (2%)
    all_to_all x4, waiting for transfers between devices, exchange(): return lax.all_to_all(pieces, axes, split_axis=0, concat_axis=0, tiled=True)  31.2 us
    ppermute x6, waiting for transfers between devices, along_y(): lax.ppermute(piece, TP[0], [(i, (i + shift) % ring) for i in range(ring)])  25.1 us
    all_to_all x4, starting transfers between devices, exchange(): return lax.all_to_all(pieces, axes, split_axis=0, concat_axis=0, tiled=True)  21.3 us
    pallas_call x2, Pallas kernels, attend(): pl.pallas_call(functools.partial(attention_kernel, chunk * blocks), grid_...  20.5 us
    ppermute x14, waiting for transfers between devices, send_pieces(): got.append(lax.ppermute(pieces[k], TP, pairs) if k else pieces[0])  20.2 us
    pallas_call x2, Pallas kernels, project_out(): pl.pallas_call(out_kernel, grid_spec=pltpu.PrefetchScalarGridSpec(num_sca...  16.2 us
    ppermute x14, starting transfers between devices, send_pieces(): got.append(lax.ppermute(pieces[k], TP, pairs) if k else pieces[0])  14.1 us
    pallas_call x1, Pallas kernels, project_kv(): pl.pallas_call(kv_kernel, grid=(length // tile,), in_specs=[pl.BlockSpec(...  13.7 us
  transfers between devices with their start and end apart: 29, of which 15 were waited for; matrix products, arithmetic and copies ran while one was open for 5% of the time, Pallas kernels for 29%

profile of v3, /device:TPU:32, one launch (start us, length us, event | category | flops | bytes accessed | tf_op | source)
XLA Modules:
  0.0 213.8 jit_solution(14186791792824722024)
XLA Ops:
  0.0 1.6 collective-permute-start
  1.6 1.7 collective-permute-start.1
  3.2 0.8 copy.25
  6.0 4.1 %token_shares.1 = bf16[16,272,256]{2,1,0:T(8,128)(2,1)} custom-call(s32[1]{0:T(128)} %bitcast.rank, bf16[4096,2048]{1,0:T(8,128)(2,1)} %tok.4, bf16[16,16,256]{2,1,0:T(8,128)(2,1)} %pad.4.asks), custom_call_target="tpu_custom_call" | custom-call | flops 1048576 | bytes 4194304 | tf_op jit(solution)/shard_map/token_shares/pallas_call | solution.py:55
  10.1 7.9 %all-to-all-start = ((bf16[16,272,256]{2,1,0:T(8,128)(2,1)}), bf16[16,272,256]{2,1,0:T(8,128)(2,1)}, u32[]{:S(2)}, u32[]{:S(2)}) async-start(bf16[16,272,256]{2,1,0:T(8,128)(2,1)} %token_shares.1), calls=%async_computation | async-start | bytes 4456448 | tf_op jit(solution)/shard_map/all_to_all | solution.py:478
  18.1 1.3 select_reduce_fusion
  19.4 0.7 reshape.82.at
  20.1 13.7 %project_kv.1 = bf16[64,2,64,256]{3,2,1,0:T(8,128)(2,1)} custom-call(bf16[4096,2048]{1,0:T(8,128)(2,1)} %tok.4, bf16[2048,256]{1,0:T(8,128)(2,1)} %wk.3, bf16[2048,256]{1,0:T(8,128)(2,1)} %wv.3, f32[1,128]{1,0:T(1,128)} %bitcast.35), custom_call_target="tpu_custom_call" | custom-call | flops 8589934592 | bytes 16777216 | tf_op jit(solution)/shard_map/project_kv/pallas_call | solution.py:89
  33.9 0.8 reshape.83.mask
  35.9 10.1 %project_q.1.q = bf16[4096,256]{1,0:T(8,128)(2,1)} custom-call(bf16[4096,2048]{1,0:T(8,128)(2,1)} %tok.4, bf16[2048,256]{1,0:T(8,128)(2,1)} %wq.1, f32[1,128]{1,0:T(1,128)} %multiply_bitcast_fusion.gain), custom_call_target="tpu_custom_call" | custom-call | flops 4294967296 | bytes 16777216 | tf_op jit(solution)/shard_map/project_q/pallas_call | solution.py:118
  46.0 2.7 %all-to-all-done = bf16[16,272,256]{2,1,0:T(8,128)(2,1)} async-done(((bf16[16,272,256]{2,1,0:T(8,128)(2,1)}), bf16[16,272,256]{2,1,0:T(8,128)(2,1)}, u32[]{:S(2)}, u32[]{:S(2)}) %all-to-all-start) | async-done | bytes 2228256 | tf_op jit(solution)/shard_map/all_to_all | solution.py:478
  48.7 0.9 slice_bitcast_fusion
  49.8 3.1 %collective-permute-start.3 = (bf16[256,256]{1,0:T(8,128)(2,1)S(1)}, bf16[256,256]{1,0:T(8,128)(2,1)S(1)}, u32[]{:S(2)}, u32[]{:S(2)}) collective-permute-start(bf16[256,256]{1,0:T(8,128)(2,1)S(1)} %slice_bitcast_fusion), channel_id=1, source_target_pairs={{0,6},{2,0},{4,2},{6,4},{1,7},{3,1},{5,3},{7,5},{8,14},{10,8},{12,... | collective-permute-start | bytes 393224 | tf_op jit(solution)/shard_map/ppermute | solution.py:487
  53.4 0.8 slice_convert_fusion
  55.5 4.4 %gather_near.1._ = bf16[16,320,256]{2,1,0:T(8,128)(2,1)} custom-call(s32[32]{0:T(128)} %reshape.85.near, bf16[8192,256]{1,0:T(8,128)(2,1)} %bitcast.24), custom_call_target="tpu_custom_call" | custom-call | flops 1048576 | bytes 4194304 | tf_op jit(solution)/shard_map/gather_near/pallas_call | solution.py:160
  60.1 1.9 collective-permute-done.5.other
  62.0 0.8 copy-done.7
  62.9 4.8 %project_sent.1 = bf16[16,320,256]{2,1,0:T(8,128)(2,1)} custom-call(s32[128]{0:T(128)} %reshape.84.asked, s32[8]{0:T(128)} %pad_add_fusion.order, bf16[4,256,256]{2,1,0:T(8,128)(2,1)} %copy-done.6, bf16[4,256,256]{2,1,0:T(8,128)(2,1)} %copy-done.7, bf16[2048,256]{1,0:T(8,128)(2,1)} %wk.3, bf16[2048,256]{1,0:T(8,128)(2,1)} %wv.3, ...), custom_call_target="tpu_custom_call", output_to_operand_aliasing={{}: (7, {})} | custom-call | flops 536870912 | bytes 8388608 | tf_op jit(solution)/shard_map/project_sent/pallas_call | solution.py:222
  67.6 5.7 %all-to-all-start.1 = ((bf16[16,320,256]{2,1,0:T(8,128)(2,1)}), bf16[16,320,256]{2,1,0:T(8,128)(2,1)S(1)}, u32[]{:S(2)}, u32[]{:S(2)}) async-start(bf16[16,320,256]{2,1,0:T(8,128)(2,1)} %project_sent.1), calls=%async_computation.1 | async-start | bytes 5242880 | tf_op jit(solution)/shard_map/all_to_all | solution.py:478
  74.5 25.1 %collective-permute-done.6.refs_4_.refs_11_ = bf16[256,2048]{1,0:T(8,128)(2,1)} collective-permute-done((bf16[256,2048]{1,0:T(8,128)(2,1)}, bf16[256,2048]{1,0:T(8,128)(2,1)}, u32[]{:S(2)}, u32[]{:S(2)}) %collective-permute-start.6) | collective-permute-done | bytes 1048608 | tf_op jit(solution)/shard_map/ppermute | solution.py:487
  99.6 13.2 %all-to-all-done.1.got = bf16[16,320,256]{2,1,0:T(8,128)(2,1)S(1)} async-done(((bf16[16,320,256]{2,1,0:T(8,128)(2,1)}), bf16[16,320,256]{2,1,0:T(8,128)(2,1)S(1)}, u32[]{:S(2)}, u32[]{:S(2)}) %all-to-all-start.1) | async-done | bytes 2621472 | tf_op jit(solution)/shard_map/all_to_all | solution.py:478
  113.4 0.9 copy-done.2
  114.3 11.1 %attend.2 = bf16[8,256,256]{2,1,0:T(8,128)(2,1)} custom-call(s32[512]{0:T(512)} %reshape.82.at, s32[8]{0:T(128)} %iota.18.where, bf16[4096,256]{1,0:T(8,128)(2,1)} %project_q.1.q, f32[64,512]{1,0:T(8,128)} %reshape.83.mask, bf16[8192,256]{1,0:T(8,128)(2,1)} %bitcast.25, bf16[16,320,256]{2,1,0:T(8,128)(2,1)} %copy-done.2), custom_call_target="tpu_custom_call" | custom-call | flops 2147483648 | bytes 10485760 | tf_op jit(solution)/shard_map/attend/pallas_call | solution.py:349
  125.4 4.2 %all-to-all-start.2 = ((bf16[8,256,256]{2,1,0:T(8,128)(2,1)}), bf16[8,256,256]{2,1,0:T(8,128)(2,1)S(1)}, u32[]{:S(2)}, u32[]{:S(2)}) async-start(bf16[8,256,256]{2,1,0:T(8,128)(2,1)} %attend.2), calls=%async_computation.2 | async-start | bytes 2097152 | tf_op jit(solution)/shard_map/all_to_all | solution.py:478
  130.3 15.3 %all-to-all-done.2.refs_0_ = bf16[8,256,256]{2,1,0:T(8,128)(2,1)S(1)} async-done(((bf16[8,256,256]{2,1,0:T(8,128)(2,1)}), bf16[8,256,256]{2,1,0:T(8,128)(2,1)S(1)}, u32[]{:S(2)}, u32[]{:S(2)}) %all-to-all-start.2) | async-done | bytes 1048608 | tf_op jit(solution)/shard_map/all_to_all | solution.py:478
  146.6 8.0 %project_out.2 = bf16[8,256,256]{2,1,0:T(8,128)(2,1)} custom-call(s32[8]{0:T(128)} %pad_add_fusion.order, s32[8]{0:T(128)} %iota.17.slot, bf16[8,256,256]{2,1,0:T(8,128)(2,1)} %copy-done.3, bf16[256,2048]{1,0:T(8,128)(2,1)} %refs_8_.1, bf16[256,2048]{1,0:T(8,128)(2,1)} %copy-done.4, bf16[256,2048]{1,0:T(8,128)(2,1)} %copy-done.5, ...), custom_call_target="tpu_custom_call" | custom-call | flops 2147483648 | bytes 12582912 | tf_op jit(solution)/shard_map/project_out/pallas_call | solution.py:421
  154.5 3.6 %all-to-all-start.3 = ((bf16[8,256,256]{2,1,0:T(8,128)(2,1)}), bf16[8,256,256]{2,1,0:T(8,128)(2,1)S(1)}, u32[]{:S(2)}, u32[]{:S(2)}) async-start(bf16[8,256,256]{2,1,0:T(8,128)(2,1)} %project_out.2), calls=%async_computation.3 | async-start | bytes 2097152 | tf_op jit(solution)/shard_map/all_to_all | solution.py:478
  158.1 9.4 %attend.3 = (bf16[256,256]{1,0:T(8,128)(2,1)}, bf16[256,256]{1,0:T(8,128)(2,1)}, bf16[256,256]{1,0:T(8,128)(2,1)}, bf16[256,256]{1,0:T(8,128)(2,1)}, bf16[256,25...) custom-call(s32[512]{0:T(512)} %reshape.82.at, ...), custom_call_target="tpu_custom_call" | custom-call | flops 2147483648 | bytes 10485760 | tf_op jit(solution)/shard_map/attend/pallas_call | solution.py:349
  167.5 2.0 collective-permute-start.11
  169.5 1.3 collective-permute-start.12
  170.8 2.2 %collective-permute-start.13 = (bf16[256,256]{1,0:T(8,128)(2,1)}, bf16[256,256]{1,0:T(8,128)(2,1)S(1)}, u32[]{:S(2)}, u32[]{:S(2)}) collective-permute-start(bf16[256,256]{1,0:T(8,128)(2,1)} %get-tuple-element.62), channel_id=1, source_target_pairs={{0,4},{1,5},{2,6},{3,7},{4,0},{5,1},{6,2},{7,3},{8,12},{9,13},{10,... | collective-permute-start | bytes 393224 | tf_op jit(solution)/shard_map/ppermute | solution.py:520
  173.1 0.7 collective-permute-start.15
  173.8 3.6 %collective-permute-done.11.refs_1_ = bf16[256,256]{1,0:T(8,128)(2,1)S(1)} collective-permute-done((bf16[256,256]{1,0:T(8,128)(2,1)}, bf16[256,256]{1,0:T(8,128)(2,1)S(1)}, u32[]{:S(2)}, u32[]{:S(2)}) %collective-permute-start.11) | collective-permute-done | bytes 131104 | tf_op jit(solution)/shard_map/ppermute | solution.py:520
  177.6 2.5 %collective-permute-done.13.refs_3_ = bf16[256,256]{1,0:T(8,128)(2,1)S(1)} collective-permute-done((bf16[256,256]{1,0:T(8,128)(2,1)}, bf16[256,256]{1,0:T(8,128)(2,1)S(1)}, u32[]{:S(2)}, u32[]{:S(2)}) %collective-permute-start.13) | collective-permute-done | bytes 131104 | tf_op jit(solution)/shard_map/ppermute | solution.py:520
  180.2 2.3 %collective-permute-done.15.refs_5_ = bf16[256,256]{1,0:T(8,128)(2,1)S(1)} collective-permute-done((bf16[256,256]{1,0:T(8,128)(2,1)}, bf16[256,256]{1,0:T(8,128)(2,1)S(1)}, u32[]{:S(2)}, u32[]{:S(2)}) %collective-permute-start.15) | collective-permute-done | bytes 131104 | tf_op jit(solution)/shard_map/ppermute | solution.py:520
  183.2 1.5 collective-permute-done.17.refs_7_
  185.4 8.2 %project_out.3 = (bf16[256,256]{1,0:T(8,128)(2,1)}, bf16[256,256]{1,0:T(8,128)(2,1)}, bf16[256,256]{1,0:T(8,128)(2,1)}, bf16[256,256]{1,0:T(8,128)(2,1)}, bf16[2...) custom-call(s32[8]{0:T(128)} %pad_add_fusion.order, ...), custom_call_target="tpu_custom_call" | custom-call | flops 2147483648 | bytes 12582912 | tf_op jit(solution)/shard_map/project_out/pallas_call | solution.py:421
  193.5 1.2 collective-permute-start.18
  194.7 2.9 %collective-permute-start.19 = (bf16[256,256]{1,0:T(8,128)(2,1)}, bf16[256,256]{1,0:T(8,128)(2,1)S(1)}, u32[]{:S(2)}, u32[]{:S(2)}) collective-permute-start(bf16[256,256]{1,0:T(8,128)(2,1)} %get-tuple-element.77), channel_id=1, source_target_pairs={{0,6},{1,7},{2,0},{3,1},{4,2},{5,3},{6,4},{7,5},{8,14},{9,15},{10,... | collective-permute-start | bytes 393224 | tf_op jit(solution)/shard_map/ppermute | solution.py:520
  197.7 1.4 collective-permute-start.20
  199.0 1.5 collective-permute-start.22
  200.6 1.0 collective-permute-done.18.rest_1_
  202.2 1.7 collective-permute-done.19.rest_2_
  203.9 2.6 %collective-permute-done.20.rest_3_ = bf16[256,256]{1,0:T(8,128)(2,1)S(1)} collective-permute-done((bf16[256,256]{1,0:T(8,128)(2,1)}, bf16[256,256]{1,0:T(8,128)(2,1)S(1)}, u32[]{:S(2)}, u32[]{:S(2)}) %collective-permute-start.20) | collective-permute-done | bytes 131104 | tf_op jit(solution)/shard_map/ppermute | solution.py:520
  206.4 1.7 collective-permute-done.22.rest_5_
  208.1 2.6 %collective-permute-done.24.rest_7_ = bf16[256,256]{1,0:T(8,128)(2,1)S(1)} collective-permute-done((bf16[256,256]{1,0:T(8,128)(2,1)}, bf16[256,256]{1,0:T(8,128)(2,1)S(1)}, u32[]{:S(2)}, u32[]{:S(2)}) %collective-permute-start.24) | collective-permute-done | bytes 131104 | tf_op jit(solution)/shard_map/ppermute | solution.py:520
  210.8 0.9 copy-done
  211.7 1.9 place.1
  (88 shorter events, 11.3 us)
Async XLA Ops:
  0.0 46.0 %collective-permute-start = (bf16[256,2048]{1,0:T(8,128)(2,1)}, bf16[256,2048]{1,0:T(8,128)(2,1)S(1)}, u32[]{:S(2)}, u32[]{:S(2)}) collective-permute-start(bf16[256,2048]{1,0:T(8,128)(2,1)} %refs_8_.1), channel_id=1, source_target_pairs={{0,2},{2,4},{4,6},{6,0},{1,3},{3,5},{5,7},{7,1},{8,10},{10,12},{12... | collective-permute-start | bytes 3145736 | tf_op jit(solution)/shard_map/ppermute | solution.py:487
  1.6 44.4 %collective-permute-start.1 = (bf16[256,2048]{1,0:T(8,128)(2,1)}, bf16[256,2048]{1,0:T(8,128)(2,1)S(1)}, u32[]{:S(2)}, u32[]{:S(2)}) collective-permute-start(bf16[256,2048]{1,0:T(8,128)(2,1)} %refs_8_.1), channel_id=1, source_target_pairs={{0,6},{2,0},{4,2},{6,4},{1,7},{3,1},{5,3},{7,5},{8,14},{10,8},{12,... | collective-permute-start | bytes 3145736 | tf_op jit(solution)/shard_map/ppermute | solution.py:487
  10.1 38.6 %all-to-all-start = ((bf16[16,272,256]{2,1,0:T(8,128)(2,1)}), bf16[16,272,256]{2,1,0:T(8,128)(2,1)}, u32[]{:S(2)}, u32[]{:S(2)}) async-start(bf16[16,272,256]{2,1,0:T(8,128)(2,1)} %token_shares.1), calls=%async_computation | async-start | bytes 4456448 | tf_op jit(solution)/shard_map/all_to_all | solution.py:478
  20.1 15.3 %copy-start.15 = (f32[128]{0:T(128)S(1)}, f32[128]{0:T(128)}, u32[]{:S(2)}) copy-start(f32[128]{0:T(128)} %param.14) | copy-start | bytes 1540
  46.0 13.9 %copy-start.4 = (bf16[256,2048]{1,0:T(8,128)(2,1)}, bf16[256,2048]{1,0:T(8,128)(2,1)S(1)}, u32[]{:S(2)}) copy-start(bf16[256,2048]{1,0:T(8,128)(2,1)S(1)} %collective-permute-done.refs_2_.refs_9_) | copy-start | bytes 3145732
  46.0 13.9 %copy-start.5 = (bf16[256,2048]{1,0:T(8,128)(2,1)}, bf16[256,2048]{1,0:T(8,128)(2,1)S(1)}, u32[]{:S(2)}) copy-start(bf16[256,2048]{1,0:T(8,128)(2,1)S(1)} %collective-permute-done.1.refs_3_.refs_10_) | copy-start | bytes 3145732
  49.6 10.3 %collective-permute-start.2 = (bf16[256,256]{1,0:T(8,128)(2,1)S(1)}, bf16[256,256]{1,0:T(8,128)(2,1)S(1)}, u32[]{:S(2)}, u32[]{:S(2)}) collective-permute-start(bf16[256,256]{1,0:T(8,128)(2,1)S(1)} %slice_bitcast_fusion), channel_id=1, source_target_pairs={{0,2},{2,4},{4,6},{6,0},{1,3},{3,5},{5,7},{7,1},{8,10},{10,12},{12... | collective-permute-start | bytes 393224 | tf_op jit(solution)/shard_map/ppermute | solution.py:487
  49.8 10.1 %collective-permute-start.3 = (bf16[256,256]{1,0:T(8,128)(2,1)S(1)}, bf16[256,256]{1,0:T(8,128)(2,1)S(1)}, u32[]{:S(2)}, u32[]{:S(2)}) collective-permute-start(bf16[256,256]{1,0:T(8,128)(2,1)S(1)} %slice_bitcast_fusion), channel_id=1, source_target_pairs={{0,6},{2,0},{4,2},{6,4},{1,7},{3,1},{5,3},{7,5},{8,14},{10,8},{12,... | collective-permute-start | bytes 393224 | tf_op jit(solution)/shard_map/ppermute | solution.py:487
  52.9 7.0 %collective-permute-start.4 = (bf16[256,256]{1,0:T(8,128)(2,1)S(1)}, bf16[256,256]{1,0:T(8,128)(2,1)S(1)}, u32[]{:S(2)}, u32[]{:S(2)}) collective-permute-start(bf16[256,256]{1,0:T(8,128)(2,1)S(1)} %slice_bitcast_fusion), channel_id=1, source_target_pairs={{0,4},{2,6},{4,0},{6,2},{1,5},{3,7},{5,1},{7,3},{8,12},{10,14},{12... | collective-permute-start | bytes 393224 | tf_op jit(solution)/shard_map/ppermute | solution.py:487
  60.0 2.0 copy-start.6
  60.0 2.0 collective-permute-start.5
  62.0 0.8 copy-start.7
  67.6 45.1 %all-to-all-start.1 = ((bf16[16,320,256]{2,1,0:T(8,128)(2,1)}), bf16[16,320,256]{2,1,0:T(8,128)(2,1)S(1)}, u32[]{:S(2)}, u32[]{:S(2)}) async-start(bf16[16,320,256]{2,1,0:T(8,128)(2,1)} %project_sent.1), calls=%async_computation.1 | async-start | bytes 5242880 | tf_op jit(solution)/shard_map/all_to_all | solution.py:478
  73.3 26.3 %collective-permute-start.6 = (bf16[256,2048]{1,0:T(8,128)(2,1)}, bf16[256,2048]{1,0:T(8,128)(2,1)}, u32[]{:S(2)}, u32[]{:S(2)}) collective-permute-start(bf16[256,2048]{1,0:T(8,128)(2,1)} %copy-done.4), channel_id=1, source_target_pairs={{0,2},{2,4},{4,6},{6,0},{1,3},{3,5},{5,7},{7,1},{8,10},{10,12},{12... | collective-permute-start | bytes 3145736 | tf_op jit(solution)/shard_map/ppermute | solution.py:487
  74.0 56.3 %collective-permute-start.7 = (bf16[256,2048]{1,0:T(8,128)(2,1)}, bf16[256,2048]{1,0:T(8,128)(2,1)}, u32[]{:S(2)}, u32[]{:S(2)}) collective-permute-start(bf16[256,2048]{1,0:T(8,128)(2,1)} %refs_8_.1), channel_id=1, source_target_pairs={{0,1},{1,0},{2,3},{3,2},{4,5},{5,4},{6,7},{7,6},{8,9},{9,8},{10,11... | collective-permute-start | bytes 3145736 | tf_op jit(solution)/shard_map/ppermute | solution.py:491
  74.0 56.3 %collective-permute-start.8 = (bf16[256,2048]{1,0:T(8,128)(2,1)}, bf16[256,2048]{1,0:T(8,128)(2,1)}, u32[]{:S(2)}, u32[]{:S(2)}) collective-permute-start(bf16[256,2048]{1,0:T(8,128)(2,1)} %copy-done.4), channel_id=1, source_target_pairs={{0,1},{1,0},{2,3},{3,2},{4,5},{5,4},{6,7},{7,6},{8,9},{9,8},{10,11... | collective-permute-start | bytes 3145736 | tf_op jit(solution)/shard_map/ppermute | solution.py:491
  74.5 55.8 %collective-permute-start.9 = (bf16[256,2048]{1,0:T(8,128)(2,1)}, bf16[256,2048]{1,0:T(8,128)(2,1)}, u32[]{:S(2)}, u32[]{:S(2)}) collective-permute-start(bf16[256,2048]{1,0:T(8,128)(2,1)} %copy-done.5), channel_id=1, source_target_pairs={{0,1},{1,0},{2,3},{3,2},{4,5},{5,4},{6,7},{7,6},{8,9},{9,8},{10,11... | collective-permute-start | bytes 3145736 | tf_op jit(solution)/shard_map/ppermute | solution.py:491
  99.6 30.7 %collective-permute-start.10 = (bf16[256,2048]{1,0:T(8,128)(2,1)}, bf16[256,2048]{1,0:T(8,128)(2,1)}, u32[]{:S(2)}, u32[]{:S(2)}) collective-permute-start(bf16[256,2048]{1,0:T(8,128)(2,1)} %collective-permute-done.6.refs_4_.refs_11_), channel_id=1, source_target_pairs={{0,1},{1,0},{2,3},{3,2},{4,5},{5,4},{6,7},{7,6},{8,9},{9,8},{10,11... | collective-permute-start | bytes 3145736 | tf_op jit(solution)/shard_map/ppermute | solution.py:491
  112.8 1.5 copy-start.2
  125.4 20.2 %all-to-all-start.2 = ((bf16[8,256,256]{2,1,0:T(8,128)(2,1)}), bf16[8,256,256]{2,1,0:T(8,128)(2,1)S(1)}, u32[]{:S(2)}, u32[]{:S(2)}) async-start(bf16[8,256,256]{2,1,0:T(8,128)(2,1)} %attend.2), calls=%async_computation.2 | async-start | bytes 2097152 | tf_op jit(solution)/shard_map/all_to_all | solution.py:478
  145.6 1.0 copy-start.3
  154.5 56.2 %all-to-all-start.3 = ((bf16[8,256,256]{2,1,0:T(8,128)(2,1)}), bf16[8,256,256]{2,1,0:T(8,128)(2,1)S(1)}, u32[]{:S(2)}, u32[]{:S(2)}) async-start(bf16[8,256,256]{2,1,0:T(8,128)(2,1)} %project_out.2), calls=%async_computation.3 | async-start | bytes 2097152 | tf_op jit(solution)/shard_map/all_to_all | solution.py:478
  167.5 9.8 %collective-permute-start.11 = (bf16[256,256]{1,0:T(8,128)(2,1)}, bf16[256,256]{1,0:T(8,128)(2,1)S(1)}, u32[]{:S(2)}, u32[]{:S(2)}) collective-permute-start(bf16[256,256]{1,0:T(8,128)(2,1)} %get-tuple-element.60), channel_id=1, source_target_pairs={{0,2},{1,3},{2,4},{3,5},{4,6},{5,7},{6,0},{7,1},{8,10},{9,11},{10,... | collective-permute-start | bytes 393224 | tf_op jit(solution)/shard_map/ppermute | solution.py:520
  169.5 7.8 %collective-permute-start.12 = (bf16[256,256]{1,0:T(8,128)(2,1)}, bf16[256,256]{1,0:T(8,128)(2,1)S(1)}, u32[]{:S(2)}, u32[]{:S(2)}) collective-permute-start(bf16[256,256]{1,0:T(8,128)(2,1)} %get-tuple-element.61), channel_id=1, source_target_pairs={{0,6},{1,7},{2,0},{3,1},{4,2},{5,3},{6,4},{7,5},{8,14},{9,15},{10,... | collective-permute-start | bytes 393224 | tf_op jit(solution)/shard_map/ppermute | solution.py:520
  170.8 9.3 %collective-permute-start.13 = (bf16[256,256]{1,0:T(8,128)(2,1)}, bf16[256,256]{1,0:T(8,128)(2,1)S(1)}, u32[]{:S(2)}, u32[]{:S(2)}) collective-permute-start(bf16[256,256]{1,0:T(8,128)(2,1)} %get-tuple-element.62), channel_id=1, source_target_pairs={{0,4},{1,5},{2,6},{3,7},{4,0},{5,1},{6,2},{7,3},{8,12},{9,13},{10,... | collective-permute-start | bytes 393224 | tf_op jit(solution)/shard_map/ppermute | solution.py:520
  173.1 7.1 %collective-permute-start.14 = (bf16[256,256]{1,0:T(8,128)(2,1)}, bf16[256,256]{1,0:T(8,128)(2,1)S(1)}, u32[]{:S(2)}, u32[]{:S(2)}) collective-permute-start(bf16[256,256]{1,0:T(8,128)(2,1)} %get-tuple-element.63), channel_id=1, source_target_pairs={{0,1},{1,0},{2,3},{3,2},{4,5},{5,4},{6,7},{7,6},{8,9},{9,8},{10,11... | collective-permute-start | bytes 393224 | tf_op jit(solution)/shard_map/ppermute | solution.py:520
  173.1 9.4 %collective-permute-start.15 = (bf16[256,256]{1,0:T(8,128)(2,1)}, bf16[256,256]{1,0:T(8,128)(2,1)S(1)}, u32[]{:S(2)}, u32[]{:S(2)}) collective-permute-start(bf16[256,256]{1,0:T(8,128)(2,1)} %get-tuple-element.64), channel_id=1, source_target_pairs={{0,3},{1,2},{2,5},{3,4},{4,7},{5,6},{6,1},{7,0},{8,11},{9,10},{10,... | collective-permute-start | bytes 393224 | tf_op jit(solution)/shard_map/ppermute | solution.py:520
  177.3 7.4 %copy-start.8 = (bf16[256,256]{1,0:T(8,128)(2,1)}, bf16[256,256]{1,0:T(8,128)(2,1)S(1)}, u32[]{:S(2)}) copy-start(bf16[256,256]{1,0:T(8,128)(2,1)S(1)} %collective-permute-done.11.refs_1_) | copy-start | bytes 393220
  177.3 5.8 %collective-permute-start.16 = (bf16[256,256]{1,0:T(8,128)(2,1)}, bf16[256,256]{1,0:T(8,128)(2,1)S(1)}, u32[]{:S(2)}, u32[]{:S(2)}) collective-permute-start(bf16[256,256]{1,0:T(8,128)(2,1)} %get-tuple-element.65), channel_id=1, source_target_pairs={{0,7},{1,6},{2,1},{3,0},{4,3},{5,2},{6,5},{7,4},{8,15},{9,14},{10,... | collective-permute-start | bytes 393224 | tf_op jit(solution)/shard_map/ppermute | solution.py:520
  177.4 7.3 %copy-start.9 = (bf16[256,256]{1,0:T(8,128)(2,1)}, bf16[256,256]{1,0:T(8,128)(2,1)S(1)}, u32[]{:S(2)}) copy-start(bf16[256,256]{1,0:T(8,128)(2,1)S(1)} %collective-permute-done.12.refs_2_) | copy-start | bytes 393220
  177.4 7.3 %collective-permute-start.17 = (bf16[256,256]{1,0:T(8,128)(2,1)}, bf16[256,256]{1,0:T(8,128)(2,1)S(1)}, u32[]{:S(2)}, u32[]{:S(2)}) collective-permute-start(bf16[256,256]{1,0:T(8,128)(2,1)} %get-tuple-element.66), channel_id=1, source_target_pairs={{0,5},{1,4},{2,7},{3,6},{4,1},{5,0},{6,3},{7,2},{8,13},{9,12},{10,... | collective-permute-start | bytes 393224 | tf_op jit(solution)/shard_map/ppermute | solution.py:520
  180.2 4.5 %copy-start.10 = (bf16[256,256]{1,0:T(8,128)(2,1)}, bf16[256,256]{1,0:T(8,128)(2,1)S(1)}, u32[]{:S(2)}) copy-start(bf16[256,256]{1,0:T(8,128)(2,1)S(1)} %collective-permute-done.13.refs_3_) | copy-start | bytes 393220
  180.2 4.5 %copy-start.11 = (bf16[256,256]{1,0:T(8,128)(2,1)}, bf16[256,256]{1,0:T(8,128)(2,1)S(1)}, u32[]{:S(2)}) copy-start(bf16[256,256]{1,0:T(8,128)(2,1)S(1)} %collective-permute-done.14.refs_4_) | copy-start | bytes 393220
  182.5 2.2 %copy-start.12 = (bf16[256,256]{1,0:T(8,128)(2,1)}, bf16[256,256]{1,0:T(8,128)(2,1)S(1)}, u32[]{:S(2)}) copy-start(bf16[256,256]{1,0:T(8,128)(2,1)S(1)} %collective-permute-done.15.refs_5_) | copy-start | bytes 393220
  183.2 1.6 copy-start.13
  184.7 0.7 copy-start.14
  185.3 25.4 %copy-start.1 = (s32[8]{0:T(128)S(1)}, s32[8]{0:T(128)}, u32[]{:S(2)}) copy-start(s32[8]{0:T(128)} %pad_add_fusion.order) | copy-start | bytes 100
  193.5 8.0 %collective-permute-start.18 = (bf16[256,256]{1,0:T(8,128)(2,1)}, bf16[256,256]{1,0:T(8,128)(2,1)S(1)}, u32[]{:S(2)}, u32[]{:S(2)}) collective-permute-start(bf16[256,256]{1,0:T(8,128)(2,1)} %get-tuple-element.76), channel_id=1, source_target_pairs={{0,2},{1,3},{2,4},{3,5},{4,6},{5,7},{6,0},{7,1},{8,10},{9,11},{10,... | collective-permute-start | bytes 393224 | tf_op jit(solution)/shard_map/ppermute | solution.py:520
  194.7 9.1 %collective-permute-start.19 = (bf16[256,256]{1,0:T(8,128)(2,1)}, bf16[256,256]{1,0:T(8,128)(2,1)S(1)}, u32[]{:S(2)}, u32[]{:S(2)}) collective-permute-start(bf16[256,256]{1,0:T(8,128)(2,1)} %get-tuple-element.77), channel_id=1, source_target_pairs={{0,6},{1,7},{2,0},{3,1},{4,2},{5,3},{6,4},{7,5},{8,14},{9,15},{10,... | collective-permute-start | bytes 393224 | tf_op jit(solution)/shard_map/ppermute | solution.py:520
  197.7 8.8 %collective-permute-start.20 = (bf16[256,256]{1,0:T(8,128)(2,1)}, bf16[256,256]{1,0:T(8,128)(2,1)S(1)}, u32[]{:S(2)}, u32[]{:S(2)}) collective-permute-start(bf16[256,256]{1,0:T(8,128)(2,1)} %get-tuple-element.78), channel_id=1, source_target_pairs={{0,4},{1,5},{2,6},{3,7},{4,0},{5,1},{6,2},{7,3},{8,12},{9,13},{10,... | collective-permute-start | bytes 393224 | tf_op jit(solution)/shard_map/ppermute | solution.py:520
  199.0 7.4 %collective-permute-start.21 = (bf16[256,256]{1,0:T(8,128)(2,1)}, bf16[256,256]{1,0:T(8,128)(2,1)S(1)}, u32[]{:S(2)}, u32[]{:S(2)}) collective-permute-start(bf16[256,256]{1,0:T(8,128)(2,1)} %get-tuple-element.79), channel_id=1, source_target_pairs={{0,1},{1,0},{2,3},{3,2},{4,5},{5,4},{6,7},{7,6},{8,9},{9,8},{10,11... | collective-permute-start | bytes 393224 | tf_op jit(solution)/shard_map/ppermute | solution.py:520
  199.0 9.1 %collective-permute-start.22 = (bf16[256,256]{1,0:T(8,128)(2,1)}, bf16[256,256]{1,0:T(8,128)(2,1)S(1)}, u32[]{:S(2)}, u32[]{:S(2)}) collective-permute-start(bf16[256,256]{1,0:T(8,128)(2,1)} %get-tuple-element.80), channel_id=1, source_target_pairs={{0,3},{1,2},{2,5},{3,4},{4,7},{5,6},{6,1},{7,0},{8,11},{9,10},{10,... | collective-permute-start | bytes 393224 | tf_op jit(solution)/shard_map/ppermute | solution.py:520
  201.6 6.6 %collective-permute-start.23 = (bf16[256,256]{1,0:T(8,128)(2,1)}, bf16[256,256]{1,0:T(8,128)(2,1)S(1)}, u32[]{:S(2)}, u32[]{:S(2)}) collective-permute-start(bf16[256,256]{1,0:T(8,128)(2,1)} %get-tuple-element.81), channel_id=1, source_target_pairs={{0,7},{1,6},{2,1},{3,0},{4,3},{5,2},{6,5},{7,4},{8,15},{9,14},{10,... | collective-permute-start | bytes 393224 | tf_op jit(solution)/shard_map/ppermute | solution.py:520
  203.9 6.9 %collective-permute-start.24 = (bf16[256,256]{1,0:T(8,128)(2,1)}, bf16[256,256]{1,0:T(8,128)(2,1)S(1)}, u32[]{:S(2)}, u32[]{:S(2)}) collective-permute-start(bf16[256,256]{1,0:T(8,128)(2,1)} %get-tuple-element.82), channel_id=1, source_target_pairs={{0,5},{1,4},{2,7},{3,6},{4,1},{5,0},{6,3},{7,2},{8,13},{9,12},{10,... | collective-permute-start | bytes 393224 | tf_op jit(solution)/shard_map/ppermute | solution.py:520
  210.8 0.9 copy-start

commit v4 on v3

--- a/solution.py
+++ b/solution.py
@@ -28,46 +28,35 @@
     return (values * factor * gain_row).astype(bf16)
 
 
-def share_kernel(rank, tok, asks, out):
+def share_kernel(rank, tok, out):
     rows = tok[...].astype(f32)
     devices = out.shape[0]
     part = BLOCK // devices
-    small = rows.shape[0] // devices
-    step = pl.program_id(0)
-    for k in range(small // 16):
+    for k in range(out.shape[1] // 16):
         parts = []
         for b in range(16 // part):
             first = (k * (16 // part) + b) * BLOCK
             parts.append(rows[first : first + BLOCK].reshape(devices, part, WIDTH))
-        at = pl.ds(pl.multiple_of(step * small + k * 16, 16), 16)
-        out[:, at, :] = jnp.concatenate(parts, axis=1).astype(bf16)
-
-    @pl.when(step == 0)
-    def _():
-        out[:, -16:, :] = asks[...]
-
-
-def token_shares(rank, tokens, asks):
+        out[:, k * 16 : (k + 1) * 16, :] = jnp.concatenate(parts, axis=1).astype(bf16)
+
+
+def token_shares(rank, tokens, devices):
     length = tokens.shape[0]
-    devices = asks.shape[0]
     tile = 1024
-    shape = (devices, length // devices + 16, WIDTH)
+    small = tile // devices
     return pl.pallas_call(
         share_kernel,
         grid_spec=pltpu.PrefetchScalarGridSpec(
             num_scalar_prefetch=1,
             grid=(length // tile,),
-            in_specs=[
-                pl.BlockSpec((tile, WIDTH), lambda i, rank: (i, rank[0])),
-                pl.BlockSpec(asks.shape, lambda i, rank: (0, 0, 0)),
-            ],
-            out_specs=pl.BlockSpec(shape, lambda i, rank: (0, 0, 0)),
-        ),
-        out_shape=jax.ShapeDtypeStruct(shape, bf16),
+            in_specs=[pl.BlockSpec((tile, WIDTH), lambda i, rank: (i, rank[0]))],
+            out_specs=pl.BlockSpec((devices, small, WIDTH), lambda i, rank: (0, i, 0)),
+        ),
+        out_shape=jax.ShapeDtypeStruct((devices, length // devices, WIDTH), bf16),
         compiler_params=pltpu.CompilerParams(vmem_limit_bytes=VMEM_LIMIT),
         cost_estimate=pl.CostEstimate(flops=1 << 20, bytes_accessed=4 << 20, transcendentals=0),
         name="token_shares",
-    )(rank, tokens, asks)
+    )(rank, tokens)
 
 
 def kv_kernel(tok, wk, wv, gain, out):
@@ -134,8 +123,6 @@
 
 
 def near_kernel(near, pairs, out, room, in_sems, out_sems):
-    devices = out.shape[0]
-    reach = near.shape[0] // devices
     unit = PAIR * BLOCK
     coming, going = [], []
     for m in range(near.shape[0]):
@@ -143,8 +130,7 @@
         coming.append(
             pltpu.make_async_copy(pairs.at[pl.ds(first, unit)], room.at[m], in_sems.at[m])
         )
-        to = out.at[m // reach, pl.ds((m % reach) * unit, unit)]
-        going.append(pltpu.make_async_copy(room.at[m], to, out_sems.at[m]))
+        going.append(pltpu.make_async_copy(room.at[m], out.at[m], out_sems.at[m]))
     for copy in coming:
         copy.start()
     for n, copy in enumerate(coming):
@@ -154,7 +140,7 @@
         copy.wait()
 
 
-def gather_near(near, pairs, devices, length):
+def gather_near(near, pairs):
     anywhere = pl.BlockSpec(memory_space=pl.ANY)
     sends = near.shape[0]
     return pl.pallas_call(
@@ -170,14 +156,14 @@
                 pltpu.SemaphoreType.DMA((sends,)),
             ],
         ),
-        out_shape=jax.ShapeDtypeStruct((devices, length, WIDTH), bf16),
+        out_shape=jax.ShapeDtypeStruct((sends, PAIR * BLOCK, WIDTH), bf16),
         compiler_params=pltpu.CompilerParams(vmem_limit_bytes=VMEM_LIMIT),
         cost_estimate=pl.CostEstimate(flops=1 << 20, bytes_accessed=4 << 20, transcendentals=0),
         name="gather_near",
     )(near, pairs)
 
 
-def send_kernel(asked, order, same, other, wk, wv, gain, _, out, keep):
+def send_kernel(asked, order, same, other, wk, wv, gain, out, keep):
     devices, rows, _ = out.shape
     keys = jnp.zeros((same.shape[1], WIDTH), f32)
     vals = jnp.zeros((same.shape[1], WIDTH), f32)
@@ -211,14 +197,12 @@
     return pl.BlockSpec(shape, lambda i, *_: (0,) * len(shape))
 
 
-def project_sent(asked, order, same, other, w_key, w_value, gain, sent):
+def project_sent(asked, order, same, other, w_key, w_value, gain, devices):
     count, rows, _ = same.shape
     groups = 64
     unit = 2 * rows // groups
     depth = w_key.shape[0]
-    devices, length, _ = sent.shape
-    hot_rows = (asked.shape[0] // devices) * unit
-    last = length // hot_rows - 1
+    shape = (devices, (asked.shape[0] // devices) * unit, WIDTH)
     return pl.pallas_call(
         send_kernel,
         grid_spec=pltpu.PrefetchScalarGridSpec(
@@ -230,34 +214,29 @@
                 whole_block(depth, WIDTH),
                 whole_block(depth, WIDTH),
                 whole_block(1, HEAD_DIM),
-                pl.BlockSpec(memory_space=pl.ANY),
             ],
-            out_specs=pl.BlockSpec((devices, hot_rows, WIDTH), lambda i, *_: (0, last, 0)),
+            out_specs=whole_block(*shape),
             scratch_shapes=[pltpu.VMEM((groups, unit, WIDTH), f32)],
         ),
-        out_shape=jax.ShapeDtypeStruct(sent.shape, bf16),
-        input_output_aliases={7: 0},
+        out_shape=jax.ShapeDtypeStruct(shape, bf16),
         compiler_params=pltpu.CompilerParams(vmem_limit_bytes=VMEM_LIMIT),
         cost_estimate=pl.CostEstimate(
             flops=4 * rows * depth * WIDTH, bytes_accessed=8 << 20, transcendentals=0
         ),
         name="project_sent",
-    )(asked, order, same, other, w_key, w_value, gain, sent)
-
-
-def attention_kernel(first, at, where, q, mask, pairs, got, *rest):
+    )(asked, order, same, other, w_key, w_value, gain)
+
+
+def attention_kernel(first, at, where, q, mask, pairs, near, hot, *rest):
     outs, (table, raw, sems) = rest[:-3], rest[-3:]
-    devices, rows, _ = got.shape
+    devices, hot_rows, _ = hot.shape
     here = pairs.shape[0]
-    hot_rows = raw.shape[1]
-    plain = rows - hot_rows
+    plain = near.shape[0]
     copies = [
-        pltpu.make_async_copy(got.at[:, pl.ds(plain, hot_rows)], raw, sems.at[devices]),
-        pltpu.make_async_copy(pairs, table.at[pl.ds(0, here)], sems.at[devices + 1]),
+        pltpu.make_async_copy(hot, raw, sems.at[0]),
+        pltpu.make_async_copy(pairs, table.at[pl.ds(0, here)], sems.at[1]),
+        pltpu.make_async_copy(near, table.at[pl.ds(here, plain)], sems.at[2]),
     ]
-    for n in range(devices):
-        span = table.at[pl.ds(here + n * plain, plain)]
-        copies.append(pltpu.make_async_copy(got.at[n, pl.ds(0, plain)], span, sems.at[n]))
     for copy in copies:
         copy.start()
     copies[0].wait()
@@ -265,7 +244,7 @@
     for n in range(hot_rows // 16):
         both = raw[:, n * 16 : (n + 1) * 16, :].astype(f32)
         for m in range(2):
-            start = here + devices * plain + (2 * n + m) * PAIR * BLOCK
+            start = here + plain + (2 * n + m) * PAIR * BLOCK
             for kind in range(PAIR):
                 low = m * 2 * part + kind * part
                 piece = both[:, low : low + part, :].reshape(BLOCK, WIDTH).astype(bf16)
@@ -334,18 +313,16 @@
             piece_of(n, put)
 
 
-def attend(chunk, chunks, split, at, where, queries, mask, pairs, got):
+def attend(chunk, chunks, split, at, where, queries, mask, pairs, near, hot):
     ranks = where.shape[0]
     length = queries.shape[0] // chunks
     slots = mask.shape[1] // BLOCK
     blocks = length // BLOCK
     rows = length // ranks
-    devices, arrived, _ = got.shape
-    plain = REACH * PAIR * BLOCK
     anywhere = pl.BlockSpec(memory_space=pl.ANY)
     shape = (rows, WIDTH) if split else (ranks, rows, WIDTH)
     count = ranks if split else 1
-    height = pairs.shape[0] + devices * plain + HOT * PAIR * BLOCK
+    height = pairs.shape[0] + near.shape[0] + HOT * PAIR * BLOCK
     outs = pl.pallas_call(
         functools.partial(attention_kernel, chunk * blocks),
         grid_spec=pltpu.PrefetchScalarGridSpec(
@@ -356,12 +333,13 @@
                 pl.BlockSpec((blocks, slots * BLOCK), lambda i, *_: (chunk, 0)),
                 anywhere,
                 anywhere,
+                anywhere,
             ],
             out_specs=[whole_block(*shape)] * count,
             scratch_shapes=[
                 pltpu.VMEM((height, WIDTH), bf16),
-                pltpu.VMEM((devices, arrived - plain, WIDTH), bf16),
-                pltpu.SemaphoreType.DMA((devices + 2,)),
+                pltpu.VMEM(hot.shape, bf16),
+                pltpu.SemaphoreType.DMA((3,)),
             ],
         ),
         out_shape=[jax.ShapeDtypeStruct(shape, bf16)] * count,
@@ -370,7 +348,7 @@
             flops=8 * length * WIDTH * slots * BLOCK, bytes_accessed=10 << 20, transcendentals=0
         ),
         name="attend",
-    )(at, where, queries, mask, pairs, got)
+    )(at, where, queries, mask, pairs, near, hot)
     return list(outs) if split else outs[0]
 
 
@@ -491,6 +469,14 @@
     return lax.ppermute(piece, TP[1], [(0, 1), (1, 0)])
 
 
+def turned(blocks, here, step, axis):
+    size = lax.axis_size(axis)
+    mine = lax.dynamic_index_in_dim(blocks, (here + step) % size, 0, keepdims=False)
+    if step == 0:
+        return mine
+    return lax.ppermute(mine, axis, [(i, (i + step) % size) for i in range(size)])
+
+
 def both_cores(parts):
     same = jnp.stack(parts)
     return same, across(same)
@@ -527,9 +513,13 @@
     devices = lax.axis_size(KV)
     position = lax.axis_index(KV)
     ranks = lax.axis_size(TP)
-    part = BLOCK // devices
     key_row = key_gain[None, :]
     query_row = (query_gain * (HEAD_DIM ** (-0.5) * LOG2E))[None, :]
+
+    rank = lax.axis_index(TP).astype(jnp.int32).reshape(1)
+    shares = token_shares(rank, tokens, devices)
+    chosen, shares = tied(chosen, shares)
+    shares = exchange(shares, KV)[0]
 
     usable = chosen >= 0
     pick = jnp.where(usable, chosen, 0)
@@ -546,20 +536,42 @@
     )
     named = jnp.sum(jnp.where(places, local_ids[None, :, None], 0), axis=1).astype(jnp.int32)
     requests = jnp.concatenate([named, jnp.broadcast_to(named[:1], named.shape)], axis=1)
-    asks = jnp.pad(requests.astype(bf16)[:, None, :], ((0, 0), (0, 15), (0, WIDTH - 2 * HOT)))
     order = piece_order(1)
     toward = piece_order(-1)
     same_order = jnp.arange(ranks, dtype=jnp.int32)
 
-    rank = lax.axis_index(TP).astype(jnp.int32).reshape(1)
-    arrived = exchange(token_shares(rank, tokens, asks), KV)
+    long, side = lax.axis_size(KV[0]), lax.axis_size(KV[1])
+    z, x = lax.axis_index(KV[0]), lax.axis_index(KV[1])
+    by_row = requests.reshape(long, side, -1)
+    rows_in = [turned(by_row, z, step, KV[0]) for step in range(long)]
+    pairs = project_kv(tokens, w_key, w_value, key_row).reshape(-1, WIDTH)
+    pairs, *rows_in = tied(pairs, *rows_in)
+    by_side = jnp.stack(rows_in, axis=1)
+    sides_in = [turned(by_side, x, step, KV[1]) for step in range(side)]
+    asked = jnp.stack(sides_in, axis=1).reshape(devices, -1)
+    sources = jnp.stack(
+        [((z + long - s) % long) * side + (x + side - t) % side for s in range(long) for t in range(side)]
+    )
+    wheres = sources[None, :] == jnp.arange(devices, dtype=jnp.int32)[:, None]
+    asked = jnp.sum(jnp.where(wheres[:, :, None], asked[None], 0), axis=1).astype(jnp.int32)
+    asked_near = asked[:, :REACH].reshape(-1)
+    asked_hot = asked[:, HOT:].reshape(-1)
+
+    sent = gather_near(asked_near, pairs)
+    sent, shares = tied(sent, shares)
+    near = exchange(sent.reshape(devices, -1, WIDTH), KV).reshape(-1, WIDTH)
+    parts = [shares] + [along_y(shares, shift) for shift in (1, -1, 2)]
     w_after = along_y(w_out, 1)
     w_before = along_y(w_out, -1)
     w_own = across(w_out)
-
-    pairs = project_kv(tokens, w_key, w_value, key_row).reshape(-1, WIDTH)
-    again, pairs = tied(tokens, pairs)
+    again, sent = tied(tokens, sent)
     queries = project_q(again, w_query, query_row)
+    queries, *parts = tied(queries, *parts)
+    rows_same, rows_other = both_cores(parts)
+    sent_hot = project_sent(
+        asked_hot, order, rows_same, rows_other, w_key, w_value, key_row, devices
+    )
+    pick, owner_of, rank_of, usable, sent_hot = tied(pick, owner_of, rank_of, usable, sent_hot)
     flat_rank = rank_of.reshape(-1)
     slot_rank = jnp.sum(
         jnp.where(pick[:, :, None] == all_blocks[None, None, :], flat_rank[None, None, :], 0), axis=-1
@@ -572,29 +584,17 @@
     at = jnp.where(usable, at, 0).astype(jnp.int32).reshape(-1)
     mask = jnp.repeat(usable.astype(f32), BLOCK, axis=1)
 
-    arrived, queries, at, mask, order, w_after, w_before = tied(
-        arrived, queries, at, mask, order, w_after, w_before
-    )
-    shares = arrived[0, :-16]
-    parts = [shares] + [along_y(shares, shift) for shift in (1, -1, 2)]
+    near, sent_hot = tied(near, sent_hot)
+    hot = exchange(sent_hot, KV)
     w_far = along_y(w_after, 1)
     w_swapped = [across(w_after), across(w_before)]
-    asked = arrived[:, -16, : 2 * HOT].astype(jnp.int32)
-    asked_near = asked[:, :REACH].reshape(-1)
-    asked_hot = asked[:, HOT:].reshape(-1)
-    length_sent = REACH * PAIR * BLOCK + HOT * 2 * part
-    sent = gather_near(asked_near, pairs, devices, length_sent)
-    asked_hot, sent, *parts = tied(asked_hot, sent, *parts)
-    rows_same, rows_other = both_cores(parts)
-    sent = project_sent(asked_hot, order, rows_same, rows_other, w_key, w_value, key_row, sent)
-    got = exchange(sent, KV)
     w_swapped.append(across(w_far))
     weights = [w_out, w_after, w_before, w_far, w_own] + w_swapped
 
     gains = out_gain.reshape(ranks, 1, WIDTH)
-    first = attend(0, 2, False, at, same_order, queries, mask, pairs, got)
+    first = attend(0, 2, False, at, same_order, queries, mask, pairs, near, hot)
     first = exchange(first, TP)
-    second = attend(1, 2, True, at, toward, queries, mask, pairs, got)
+    second = attend(1, 2, True, at, toward, queries, mask, pairs, near, hot)
     second = send_pieces(second)
     first = project_out(False, order, same_order, first, weights, gains)
     moved = exchange(first, TP)

time: 218 us -> 219 us (level)
  the two profiles are of different devices: /device:TPU:32 before, /device:TPU:1 now
where the time goes in v4:
time: 219 us; the launch traced here: 218 us
  starting transfers between devices  79.4 us (36%)
  Pallas kernels  75.5 us (34%)
  waiting for transfers between devices  51.2 us (23%)
  local copies, waits for them, and re-layouts  7.47 us (3%)
  other arithmetic  4.36 us (2%)
    all_to_all x5, starting transfers between devices, exchange(): return lax.all_to_all(pieces, axes, split_axis=0, concat_axis=0, tiled=True)  31.1 us
    all_to_all x5, waiting for transfers between devices, exchange(): return lax.all_to_all(pieces, axes, split_axis=0, concat_axis=0, tiled=True)  20.6 us
    pallas_call x2, Pallas kernels, attend(): pl.pallas_call(functools.partial(attention_kernel, chunk * blocks), grid_...  20.5 us
    ppermute x14, starting transfers between devices, send_pieces(): got.append(lax.ppermute(pieces[k], TP, pairs) if k else pieces[0])  18.7 us
    pallas_call x2, Pallas kernels, project_out(): pl.pallas_call(out_kernel, grid_spec=pltpu.PrefetchScalarGridSpec(num_sca...  16.1 us
    ppermute x14, waiting for transfers between devices, send_pieces(): got.append(lax.ppermute(pieces[k], TP, pairs) if k else pieces[0])  15.7 us
    ppermute x6, starting transfers between devices, turned(): lax.ppermute(mine, axis, [(i, (i + step) % size) for i in range(size)])  15.2 us
    ppermute x6, waiting for transfers between devices, along_y(): lax.ppermute(piece, TP[0], [(i, (i + shift) % ring) for i in range(ring)])  13.8 us
  transfers between devices with their start and end apart: 36, of which 14 were waited for; matrix products, arithmetic and copies ran while one was open for 4% of the time, Pallas kernels for 28%

profile of v4, /device:TPU:1, one launch (start us, length us, event | category | flops | bytes accessed | tf_op | source)
XLA Modules:
  0.0 218.4 jit_solution(17547875022857446023)
XLA Ops:
  0.0 4.0 %token_shares.1 = bf16[16,256,256]{2,1,0:T(8,128)(2,1)} custom-call(s32[1]{0:T(128)} %bitcast.4.rank, bf16[4096,2048]{1,0:T(8,128)(2,1)} %tok.4), custom_call_target="tpu_custom_call" | custom-call | flops 1048576 | bytes 4194304 | tf_op jit(solution)/shard_map/token_shares/pallas_call | solution.py:47
  4.0 8.5 %all-to-all-start = ((bf16[16,256,256]{2,1,0:T(8,128)(2,1)}), bf16[16,256,256]{2,1,0:T(8,128)(2,1)S(1)}, u32[]{:S(2)}, u32[]{:S(2)}) async-start(bf16[16,256,256]{2,1,0:T(8,128)(2,1)} %token_shares.1), calls=%async_computation | async-start | bytes 4194304 | tf_op jit(solution)/shard_map/all_to_all | solution.py:456
  13.9 1.4 collective-permute-start
  15.3 2.4 %collective-permute-start.1 = (s32[4,16]{1,0:T(4,128)S(1)}, s32[4,16]{1,0:T(4,128)S(1)}, u32[]{:S(2)}, u32[]{:S(2)}) collective-permute-start(s32[4,16]{1,0:T(4,128)S(1)} %get-tuple-element.109), channel_id=1, source_target_pairs={{0,64},{32,96},{64,0},{96,32},{1,65},{33,97},{65,1},{97,33},{2,66}... | collective-permute-start | bytes 776 | tf_op jit(solution)/shard_map/ppermute | solution.py:477
  17.7 1.2 collective-permute-start.2
  18.8 1.3 collective-permute-start.10
  20.1 13.7 %project_kv.1 = bf16[64,2,64,256]{3,2,1,0:T(8,128)(2,1)} custom-call(bf16[4096,2048]{1,0:T(8,128)(2,1)} %tok.4, bf16[2048,256]{1,0:T(8,128)(2,1)} %wk.3, bf16[2048,256]{1,0:T(8,128)(2,1)} %wv.3, f32[1,128]{1,0:T(1,128)} %bitcast.86), custom_call_target="tpu_custom_call" | custom-call | flops 8589934592 | bytes 16777216 | tf_op jit(solution)/shard_map/project_kv/pallas_call | solution.py:78
  34.0 1.3 collective-permute-start.3
  35.2 7.0 %collective-permute-start.4 = (s32[4,16]{1,0:T(4,128)S(1)}, s32[4,16]{1,0:T(4,128)S(1)}, u32[]{:S(2)}, u32[]{:S(2)}) collective-permute-start(s32[4,16]{1,0:T(4,128)S(1)} %bitcast.78), channel_id=1, source_target_pairs={{0,16},{8,24},{16,0},{24,8},{1,17},{9,25},{17,1},{25,9},{2,18},{10... | collective-permute-start | bytes 776 | tf_op jit(solution)/shard_map/ppermute | solution.py:477
  42.2 2.0 collective-permute-start.5
  45.8 4.4 %gather_near.1 = bf16[32,128,256]{2,1,0:T(8,128)(2,1)} custom-call(s32[32]{0:T(128)} %reshape.68.near, bf16[8192,256]{1,0:T(8,128)(2,1)} %bitcast.60), custom_call_target="tpu_custom_call" | custom-call | flops 1048576 | bytes 4194304 | tf_op jit(solution)/shard_map/gather_near/pallas_call | solution.py:146
  50.2 6.4 %all-to-all-start.1 = ((bf16[16,256,256]{2,1,0:T(8,128)(2,1)}), bf16[16,256,256]{2,1,0:T(8,128)(2,1)S(1)}, u32[]{:S(2)}, u32[]{:S(2)}) async-start(bf16[16,256,256]{2,1,0:T(8,128)(2,1)} %bitcast.65), calls=%async_computation.1 | async-start | bytes 4194304 | tf_op jit(solution)/shard_map/all_to_all | solution.py:456
  56.6 2.8 %collective-permute-start.11 = (bf16[256,2048]{1,0:T(8,128)(2,1)}, bf16[256,2048]{1,0:T(8,128)(2,1)}, u32[]{:S(2)}, u32[]{:S(2)}) collective-permute-start(bf16[256,2048]{1,0:T(8,128)(2,1)} %refs_8_.1), channel_id=1, source_target_pairs={{0,6},{2,0},{4,2},{6,4},{1,7},{3,1},{5,3},{7,5},{8,14},{10,8},{12,... | collective-permute-start | bytes 3145736 | tf_op jit(solution)/shard_map/ppermute | solution.py:465
  60.1 2.7 %collective-permute-start.7 = (bf16[256,256]{1,0:T(8,128)(2,1)S(1)}, bf16[256,256]{1,0:T(8,128)(2,1)S(1)}, u32[]{:S(2)}, u32[]{:S(2)}) collective-permute-start(bf16[256,256]{1,0:T(8,128)(2,1)S(1)} %slice_bitcast_fusion), channel_id=1, source_target_pairs={{0,6},{2,0},{4,2},{6,4},{1,7},{3,1},{5,3},{7,5},{8,14},{10,8},{12,... | collective-permute-start | bytes 393224 | tf_op jit(solution)/shard_map/ppermute | solution.py:465
  62.7 1.2 collective-permute-start.8
  63.9 10.1 %project_q.1.q = bf16[4096,256]{1,0:T(8,128)(2,1)} custom-call(bf16[4096,2048]{1,0:T(8,128)(2,1)} %tok.4, bf16[2048,256]{1,0:T(8,128)(2,1)} %wq.1, f32[1,128]{1,0:T(1,128)} %multiply_bitcast_fusion.gain), custom_call_target="tpu_custom_call" | custom-call | flops 4294967296 | bytes 16777216 | tf_op jit(solution)/shard_map/project_q/pallas_call | solution.py:107
  74.0 13.5 %collective-permute-done.6 = bf16[256,256]{1,0:T(8,128)(2,1)S(1)} collective-permute-done((bf16[256,256]{1,0:T(8,128)(2,1)S(1)}, bf16[256,256]{1,0:T(8,128)(2,1)S(1)}, u32[]{:S(2)}, u32[]{:S(2)}) %collective-permute-start.6) | collective-permute-done | bytes 131104 | tf_op jit(solution)/shard_map/ppermute | solution.py:465
  87.9 4.9 %collective-permute-start.9 = (bf16[4,256,256]{2,1,0:T(8,128)(2,1)S(1)}, bf16[4,256,256]{2,1,0:T(8,128)(2,1)S(1)}, u32[]{:S(2)}, u32[]{:S(2)}) collective-permute-start(bf16[4,256,256]{2,1,0:T(8,128)(2,1)S(1)} %pad_maximum_fusion.same), channel_id=1, source_target_pairs={{0,1},{1,0},{2,3},{3,2},{4,5},{5,4},{6,7},{7,6},{8,9},{9,8},{10,11... | collective-permute-start | bytes 1572872 | tf_op jit(solution)/shard_map/ppermute | solution.py:469
  95.2 4.8 %project_sent.1 = bf16[16,64,256]{2,1,0:T(8,128)(2,1)} custom-call(s32[128]{0:T(128)} %reshape.67.asked, s32[8]{0:T(128)} %pad_add_fusion.3.order, bf16[4,256,256]{2,1,0:T(8,128)(2,1)} %copy-done.5, bf16[4,256,256]{2,1,0:T(8,128)(2,1)} %copy-done.6, bf16[2048,256]{1,0:T(8,128)(2,1)} %wk.3, bf16[2048,256]{1,0:T(8,128)(2,1)} %wv.3, f32[1,128]{1,0:T(1,128)} %bitcast.87), custom_call_target="tpu_custom_call" | custom-call | flops 536870912 | bytes 8388608 | tf_op jit(solution)/shard_map/project_sent/pallas_call | solution.py:206
  100.0 6.6 %all-to-all-start.2 = ((bf16[16,64,256]{2,1,0:T(8,128)(2,1)}), bf16[16,64,256]{2,1,0:T(8,128)(2,1)S(1)}, u32[]{:S(2)}, u32[]{:S(2)}) async-start(bf16[16,64,256]{2,1,0:T(8,128)(2,1)} %project_sent.1), calls=%async_computation.2 | async-start | bytes 1048576 | tf_op jit(solution)/shard_map/all_to_all | solution.py:456
  109.1 1.3 select_reduce_fusion
  111.0 6.3 %all-to-all-done.2.hot = bf16[16,64,256]{2,1,0:T(8,128)(2,1)S(1)} async-done(((bf16[16,64,256]{2,1,0:T(8,128)(2,1)}), bf16[16,64,256]{2,1,0:T(8,128)(2,1)S(1)}, u32[]{:S(2)}, u32[]{:S(2)}) %all-to-all-start.2) | async-done | bytes 524320 | tf_op jit(solution)/shard_map/all_to_all | solution.py:456
  118.1 11.1 %attend.2 = bf16[8,256,256]{2,1,0:T(8,128)(2,1)} custom-call(s32[512]{0:T(512)} %reshape.69.at, s32[8]{0:T(128)} %iota.26.where, bf16[4096,256]{1,0:T(8,128)(2,1)} %project_q.1.q, f32[64,512]{1,0:T(8,128)} %reshape.70.mask, bf16[8192,256]{1,0:T(8,128)(2,1)} %bitcast.61, bf16[4096,256]{1,0:T(8,128)(2,1)} %bitcast.63, bf16[16,64,256]{2,1,0:T(8,128)(2,1)} %copy-done.3), custom_call_target="tpu_custom_call" | custom-call | flops 2147483648 | bytes 10485760 | tf_op jit(solution)/shard_map/attend/pallas_call | solution.py:326
  129.2 5.2 %all-to-all-start.3 = ((bf16[8,256,256]{2,1,0:T(8,128)(2,1)}), bf16[8,256,256]{2,1,0:T(8,128)(2,1)S(1)}, u32[]{:S(2)}, u32[]{:S(2)}) async-start(bf16[8,256,256]{2,1,0:T(8,128)(2,1)} %attend.2), calls=%async_computation.3 | async-start | bytes 2097152 | tf_op jit(solution)/shard_map/all_to_all | solution.py:456
  135.1 14.3 %all-to-all-done.3.refs_0_ = bf16[8,256,256]{2,1,0:T(8,128)(2,1)S(1)} async-done(((bf16[8,256,256]{2,1,0:T(8,128)(2,1)}), bf16[8,256,256]{2,1,0:T(8,128)(2,1)S(1)}, u32[]{:S(2)}, u32[]{:S(2)}) %all-to-all-start.3) | async-done | bytes 1048608 | tf_op jit(solution)/shard_map/all_to_all | solution.py:456
  150.5 8.0 %project_out.2 = bf16[8,256,256]{2,1,0:T(8,128)(2,1)} custom-call(s32[8]{0:T(128)} %pad_add_fusion.3.order, s32[8]{0:T(128)} %iota.25.slot, bf16[8,256,256]{2,1,0:T(8,128)(2,1)} %copy-done.4, bf16[256,2048]{1,0:T(8,128)(2,1)} %refs_8_.1, bf16[256,2048]{1,0:T(8,128)(2,1)} %collective-permute-done.10.refs_2_.refs_9_, ...), custom_call_target="tpu_custom_call" | custom-call | flops 2147483648 | bytes 12582912 | tf_op jit(solution)/shard_map/project_out/pallas_call | solution.py:399
  158.4 4.4 %all-to-all-start.4 = ((bf16[8,256,256]{2,1,0:T(8,128)(2,1)}), bf16[8,256,256]{2,1,0:T(8,128)(2,1)S(1)}, u32[]{:S(2)}, u32[]{:S(2)}) async-start(bf16[8,256,256]{2,1,0:T(8,128)(2,1)} %project_out.2), calls=%async_computation.4 | async-start | bytes 2097152 | tf_op jit(solution)/shard_map/all_to_all | solution.py:456
  162.8 9.4 %attend.3 = (bf16[256,256]{1,0:T(8,128)(2,1)}, bf16[256,256]{1,0:T(8,128)(2,1)}, bf16[256,256]{1,0:T(8,128)(2,1)}, bf16[256,256]{1,0:T(8,128)(2,1)}, bf16[256,25...) custom-call(s32[512]{0:T(512)} %reshape.69.at, ...), custom_call_target="tpu_custom_call" | custom-call | flops 2147483648 | bytes 10485760 | tf_op jit(solution)/shard_map/attend/pallas_call | solution.py:326
  172.2 1.4 collective-permute-start.17
  173.7 1.3 collective-permute-start.18
  175.0 1.7 collective-permute-start.19
  176.7 1.2 collective-permute-start.20
  178.1 3.6 %collective-permute-done.17.refs_1_ = bf16[256,256]{1,0:T(8,128)(2,1)S(1)} collective-permute-done((bf16[256,256]{1,0:T(8,128)(2,1)}, bf16[256,256]{1,0:T(8,128)(2,1)S(1)}, u32[]{:S(2)}, u32[]{:S(2)}) %collective-permute-start.17) | collective-permute-done | bytes 131104 | tf_op jit(solution)/shard_map/ppermute | solution.py:506
  183.5 3.6 %collective-permute-done.21.refs_5_ = bf16[256,256]{1,0:T(8,128)(2,1)S(1)} collective-permute-done((bf16[256,256]{1,0:T(8,128)(2,1)}, bf16[256,256]{1,0:T(8,128)(2,1)S(1)}, u32[]{:S(2)}, u32[]{:S(2)}) %collective-permute-start.21) | collective-permute-done | bytes 131104 | tf_op jit(solution)/shard_map/ppermute | solution.py:506
  187.1 0.9 collective-permute-done.22.refs_6_
  188.0 1.4 collective-permute-done.23.refs_7_
  190.0 8.1 %project_out.3 = (bf16[256,256]{1,0:T(8,128)(2,1)}, bf16[256,256]{1,0:T(8,128)(2,1)}, bf16[256,256]{1,0:T(8,128)(2,1)}, bf16[256,256]{1,0:T(8,128)(2,1)}, bf16[2...) custom-call(s32[8]{0:T(128)} %pad_add_fusion.3.order, ...), custom_call_target="tpu_custom_call" | custom-call | flops 2147483648 | bytes 12582912 | tf_op jit(solution)/shard_map/project_out/pallas_call | solution.py:399
  198.1 1.1 collective-permute-start.24
  199.2 2.5 %collective-permute-start.25 = (bf16[256,256]{1,0:T(8,128)(2,1)}, bf16[256,256]{1,0:T(8,128)(2,1)S(1)}, u32[]{:S(2)}, u32[]{:S(2)}) collective-permute-start(bf16[256,256]{1,0:T(8,128)(2,1)} %get-tuple-element.91), channel_id=1, source_target_pairs={{0,6},{1,7},{2,0},{3,1},{4,2},{5,3},{6,4},{7,5},{8,14},{9,15},{10,... | collective-permute-start | bytes 393224 | tf_op jit(solution)/shard_map/ppermute | solution.py:506
  201.8 1.1 collective-permute-start.26
  202.9 1.0 collective-permute-start.27
  203.8 1.0 collective-permute-start.28
  205.4 3.2 %collective-permute-start.29 = (bf16[256,256]{1,0:T(8,128)(2,1)}, bf16[256,256]{1,0:T(8,128)(2,1)S(1)}, u32[]{:S(2)}, u32[]{:S(2)}) collective-permute-start(bf16[256,256]{1,0:T(8,128)(2,1)} %get-tuple-element.95), channel_id=1, source_target_pairs={{0,7},{1,6},{2,1},{3,0},{4,3},{5,2},{6,5},{7,4},{8,15},{9,14},{10,... | collective-permute-start | bytes 393224 | tf_op jit(solution)/shard_map/ppermute | solution.py:506
  208.5 1.5 collective-permute-start.30
  210.0 2.5 %collective-permute-done.28.rest_5_ = bf16[256,256]{1,0:T(8,128)(2,1)S(1)} collective-permute-done((bf16[256,256]{1,0:T(8,128)(2,1)}, bf16[256,256]{1,0:T(8,128)(2,1)S(1)}, u32[]{:S(2)}, u32[]{:S(2)}) %collective-permute-start.28) | collective-permute-done | bytes 131104 | tf_op jit(solution)/shard_map/ppermute | solution.py:506
  212.5 2.9 %collective-permute-done.30.rest_7_ = bf16[256,256]{1,0:T(8,128)(2,1)S(1)} collective-permute-done((bf16[256,256]{1,0:T(8,128)(2,1)}, bf16[256,256]{1,0:T(8,128)(2,1)S(1)}, u32[]{:S(2)}, u32[]{:S(2)}) %collective-permute-start.30) | collective-permute-done | bytes 131104 | tf_op jit(solution)/shard_map/ppermute | solution.py:506
  215.5 0.9 copy-done
  216.4 1.9 place.1
  (106 shorter events, 15.2 us)
Async XLA Ops:
  4.0 8.6 %copy-start.14 = (s32[64,8]{0,1:T(8,128)S(1)}, s32[64,8]{0,1:T(8,128)}, u32[]{:S(2)}) copy-start(s32[64,8]{0,1:T(8,128)} %param.17) | copy-start | bytes 6148
  4.0 46.2 %all-to-all-start = ((bf16[16,256,256]{2,1,0:T(8,128)(2,1)}), bf16[16,256,256]{2,1,0:T(8,128)(2,1)S(1)}, u32[]{:S(2)}, u32[]{:S(2)}) async-start(bf16[16,256,256]{2,1,0:T(8,128)(2,1)} %token_shares.1), calls=%async_computation | async-start | bytes 4194304 | tf_op jit(solution)/shard_map/all_to_all | solution.py:456
  13.9 20.0 %collective-permute-start = (s32[4,16]{1,0:T(4,128)S(1)}, s32[4,16]{1,0:T(4,128)S(1)}, u32[]{:S(2)}, u32[]{:S(2)}) collective-permute-start(s32[4,16]{1,0:T(4,128)S(1)} %get-tuple-element.110), channel_id=1, source_target_pairs={{0,32},{32,64},{64,96},{96,0},{1,33},{33,65},{65,97},{97,1},{2,34}... | collective-permute-start | bytes 776 | tf_op jit(solution)/shard_map/ppermute | solution.py:477
  15.3 18.6 %collective-permute-start.1 = (s32[4,16]{1,0:T(4,128)S(1)}, s32[4,16]{1,0:T(4,128)S(1)}, u32[]{:S(2)}, u32[]{:S(2)}) collective-permute-start(s32[4,16]{1,0:T(4,128)S(1)} %get-tuple-element.109), channel_id=1, source_target_pairs={{0,64},{32,96},{64,0},{96,32},{1,65},{33,97},{65,1},{97,33},{2,66}... | collective-permute-start | bytes 776 | tf_op jit(solution)/shard_map/ppermute | solution.py:477
  17.7 16.3 %collective-permute-start.2 = (s32[4,16]{1,0:T(4,128)S(1)}, s32[4,16]{1,0:T(4,128)S(1)}, u32[]{:S(2)}, u32[]{:S(2)}) collective-permute-start(s32[4,16]{1,0:T(4,128)S(1)} %get-tuple-element.108), channel_id=1, source_target_pairs={{0,96},{32,0},{64,32},{96,64},{1,97},{33,1},{65,33},{97,65},{2,98}... | collective-permute-start | bytes 776 | tf_op jit(solution)/shard_map/ppermute | solution.py:477
  18.8 41.2 %collective-permute-start.10 = (bf16[256,2048]{1,0:T(8,128)(2,1)}, bf16[256,2048]{1,0:T(8,128)(2,1)}, u32[]{:S(2)}, u32[]{:S(2)}) collective-permute-start(bf16[256,2048]{1,0:T(8,128)(2,1)} %refs_8_.1), channel_id=1, source_target_pairs={{0,2},{2,4},{4,6},{6,0},{1,3},{3,5},{5,7},{7,1},{8,10},{10,12},{12... | collective-permute-start | bytes 3145736 | tf_op jit(solution)/shard_map/ppermute | solution.py:465
  34.0 10.3 %collective-permute-start.3 = (s32[4,16]{1,0:T(4,128)S(1)}, s32[4,16]{1,0:T(4,128)S(1)}, u32[]{:S(2)}, u32[]{:S(2)}) collective-permute-start(s32[4,16]{1,0:T(4,128)S(1)} %bitcast.79), channel_id=1, source_target_pairs={{0,8},{8,16},{16,24},{24,0},{1,9},{9,17},{17,25},{25,1},{2,10},{10... | collective-permute-start | bytes 776 | tf_op jit(solution)/shard_map/ppermute | solution.py:477
  35.2 9.0 %collective-permute-start.4 = (s32[4,16]{1,0:T(4,128)S(1)}, s32[4,16]{1,0:T(4,128)S(1)}, u32[]{:S(2)}, u32[]{:S(2)}) collective-permute-start(s32[4,16]{1,0:T(4,128)S(1)} %bitcast.78), channel_id=1, source_target_pairs={{0,16},{8,24},{16,0},{24,8},{1,17},{9,25},{17,1},{25,9},{2,18},{10... | collective-permute-start | bytes 776 | tf_op jit(solution)/shard_map/ppermute | solution.py:477
  42.2 2.8 %collective-permute-start.5 = (s32[4,16]{1,0:T(4,128)S(1)}, s32[4,16]{1,0:T(4,128)S(1)}, u32[]{:S(2)}, u32[]{:S(2)}) collective-permute-start(s32[4,16]{1,0:T(4,128)S(1)} %bitcast.77), channel_id=1, source_target_pairs={{0,24},{8,0},{16,8},{24,16},{1,25},{9,1},{17,9},{25,17},{2,26},{10... | collective-permute-start | bytes 776 | tf_op jit(solution)/shard_map/ppermute | solution.py:477
  50.2 9.3 %copy-start.15 = (f32[128]{0:T(128)S(1)}, f32[128]{0:T(128)}, u32[]{:S(2)}) copy-start(f32[128]{0:T(128)} %param.14) | copy-start | bytes 1540
  50.2 49.7 %all-to-all-start.1 = ((bf16[16,256,256]{2,1,0:T(8,128)(2,1)}), bf16[16,256,256]{2,1,0:T(8,128)(2,1)S(1)}, u32[]{:S(2)}, u32[]{:S(2)}) async-start(bf16[16,256,256]{2,1,0:T(8,128)(2,1)} %bitcast.65), calls=%async_computation.1 | async-start | bytes 4194304 | tf_op jit(solution)/shard_map/all_to_all | solution.py:456
  56.6 50.8 %collective-permute-start.11 = (bf16[256,2048]{1,0:T(8,128)(2,1)}, bf16[256,2048]{1,0:T(8,128)(2,1)}, u32[]{:S(2)}, u32[]{:S(2)}) collective-permute-start(bf16[256,2048]{1,0:T(8,128)(2,1)} %refs_8_.1), channel_id=1, source_target_pairs={{0,6},{2,0},{4,2},{6,4},{1,7},{3,1},{5,3},{7,5},{8,14},{10,8},{12,... | collective-permute-start | bytes 3145736 | tf_op jit(solution)/shard_map/ppermute | solution.py:465
  60.0 47.8 %collective-permute-start.12 = (bf16[256,2048]{1,0:T(8,128)(2,1)}, bf16[256,2048]{1,0:T(8,128)(2,1)}, u32[]{:S(2)}, u32[]{:S(2)}) collective-permute-start(bf16[256,2048]{1,0:T(8,128)(2,1)} %collective-permute-done.10.refs_2_.refs_9_), channel_id=1, source_target_pairs={{0,2},{2,4},{4,6},{6,0},{1,3},{3,5},{5,7},{7,1},{8,10},{10,12},{12... | collective-permute-start | bytes 3145736 | tf_op jit(solution)/shard_map/ppermute | solution.py:465
  60.0 27.4 %collective-permute-start.6 = (bf16[256,256]{1,0:T(8,128)(2,1)S(1)}, bf16[256,256]{1,0:T(8,128)(2,1)S(1)}, u32[]{:S(2)}, u32[]{:S(2)}) collective-permute-start(bf16[256,256]{1,0:T(8,128)(2,1)S(1)} %slice_bitcast_fusion), channel_id=1, source_target_pairs={{0,2},{2,4},{4,6},{6,0},{1,3},{3,5},{5,7},{7,1},{8,10},{10,12},{12... | collective-permute-start | bytes 393224 | tf_op jit(solution)/shard_map/ppermute | solution.py:465
  60.1 27.4 %collective-permute-start.7 = (bf16[256,256]{1,0:T(8,128)(2,1)S(1)}, bf16[256,256]{1,0:T(8,128)(2,1)S(1)}, u32[]{:S(2)}, u32[]{:S(2)}) collective-permute-start(bf16[256,256]{1,0:T(8,128)(2,1)S(1)} %slice_bitcast_fusion), channel_id=1, source_target_pairs={{0,6},{2,0},{4,2},{6,4},{1,7},{3,1},{5,3},{7,5},{8,14},{10,8},{12,... | collective-permute-start | bytes 393224 | tf_op jit(solution)/shard_map/ppermute | solution.py:465
  62.7 25.1 %collective-permute-start.8 = (bf16[256,256]{1,0:T(8,128)(2,1)S(1)}, bf16[256,256]{1,0:T(8,128)(2,1)S(1)}, u32[]{:S(2)}, u32[]{:S(2)}) collective-permute-start(bf16[256,256]{1,0:T(8,128)(2,1)S(1)} %slice_bitcast_fusion), channel_id=1, source_target_pairs={{0,4},{2,6},{4,0},{6,2},{1,5},{3,7},{5,1},{7,3},{8,12},{10,14},{12... | collective-permute-start | bytes 393224 | tf_op jit(solution)/shard_map/ppermute | solution.py:465
  87.9 6.5 %copy-start.5 = (bf16[4,256,256]{2,1,0:T(8,128)(2,1)}, bf16[4,256,256]{2,1,0:T(8,128)(2,1)S(1)}, u32[]{:S(2)}) copy-start(bf16[4,256,256]{2,1,0:T(8,128)(2,1)S(1)} %pad_maximum_fusion.same) | copy-start | bytes 1572868
  87.9 6.5 %collective-permute-start.9 = (bf16[4,256,256]{2,1,0:T(8,128)(2,1)S(1)}, bf16[4,256,256]{2,1,0:T(8,128)(2,1)S(1)}, u32[]{:S(2)}, u32[]{:S(2)}) collective-permute-start(bf16[4,256,256]{2,1,0:T(8,128)(2,1)S(1)} %pad_maximum_fusion.same), channel_id=1, source_target_pairs={{0,1},{1,0},{2,3},{3,2},{4,5},{5,4},{6,7},{7,6},{8,9},{9,8},{10,11... | collective-permute-start | bytes 1572872 | tf_op jit(solution)/shard_map/ppermute | solution.py:469
  100.0 17.9 %copy-start.2 = (bf16[16,256,256]{2,1,0:T(8,128)(2,1)}, bf16[16,256,256]{2,1,0:T(8,128)(2,1)S(1)}, u32[]{:S(2)}) copy-start(bf16[16,256,256]{2,1,0:T(8,128)(2,1)S(1)} %all-to-all-done.1) | copy-start | bytes 6291460
  100.0 17.3 %all-to-all-start.2 = ((bf16[16,64,256]{2,1,0:T(8,128)(2,1)}), bf16[16,64,256]{2,1,0:T(8,128)(2,1)S(1)}, u32[]{:S(2)}, u32[]{:S(2)}) async-start(bf16[16,64,256]{2,1,0:T(8,128)(2,1)} %project_sent.1), calls=%async_computation.2 | async-start | bytes 1048576 | tf_op jit(solution)/shard_map/all_to_all | solution.py:456
  106.6 28.6 %collective-permute-start.13 = (bf16[256,2048]{1,0:T(8,128)(2,1)}, bf16[256,2048]{1,0:T(8,128)(2,1)}, u32[]{:S(2)}, u32[]{:S(2)}) collective-permute-start(bf16[256,2048]{1,0:T(8,128)(2,1)} %refs_8_.1), channel_id=1, source_target_pairs={{0,1},{1,0},{2,3},{3,2},{4,5},{5,4},{6,7},{7,6},{8,9},{9,8},{10,11... | collective-permute-start | bytes 3145736 | tf_op jit(solution)/shard_map/ppermute | solution.py:469
  107.3 27.8 %collective-permute-start.14 = (bf16[256,2048]{1,0:T(8,128)(2,1)}, bf16[256,2048]{1,0:T(8,128)(2,1)}, u32[]{:S(2)}, u32[]{:S(2)}) collective-permute-start(bf16[256,2048]{1,0:T(8,128)(2,1)} %collective-permute-done.10.refs_2_.refs_9_), channel_id=1, source_target_pairs={{0,1},{1,0},{2,3},{3,2},{4,5},{5,4},{6,7},{7,6},{8,9},{9,8},{10,11... | collective-permute-start | bytes 3145736 | tf_op jit(solution)/shard_map/ppermute | solution.py:469
  107.4 27.7 %collective-permute-start.15 = (bf16[256,2048]{1,0:T(8,128)(2,1)}, bf16[256,2048]{1,0:T(8,128)(2,1)}, u32[]{:S(2)}, u32[]{:S(2)}) collective-permute-start(bf16[256,2048]{1,0:T(8,128)(2,1)} %collective-permute-done.11.refs_3_.refs_10_), channel_id=1, source_target_pairs={{0,1},{1,0},{2,3},{3,2},{4,5},{5,4},{6,7},{7,6},{8,9},{9,8},{10,11... | collective-permute-start | bytes 3145736 | tf_op jit(solution)/shard_map/ppermute | solution.py:469
  107.8 27.3 %collective-permute-start.16 = (bf16[256,2048]{1,0:T(8,128)(2,1)}, bf16[256,2048]{1,0:T(8,128)(2,1)}, u32[]{:S(2)}, u32[]{:S(2)}) collective-permute-start(bf16[256,2048]{1,0:T(8,128)(2,1)} %collective-permute-done.12.refs_4_.refs_11_), channel_id=1, source_target_pairs={{0,1},{1,0},{2,3},{3,2},{4,5},{5,4},{6,7},{7,6},{8,9},{9,8},{10,11... | collective-permute-start | bytes 3145736 | tf_op jit(solution)/shard_map/ppermute | solution.py:469
  129.2 20.2 %all-to-all-start.3 = ((bf16[8,256,256]{2,1,0:T(8,128)(2,1)}), bf16[8,256,256]{2,1,0:T(8,128)(2,1)S(1)}, u32[]{:S(2)}, u32[]{:S(2)}) async-start(bf16[8,256,256]{2,1,0:T(8,128)(2,1)} %attend.2), calls=%async_computation.3 | async-start | bytes 2097152 | tf_op jit(solution)/shard_map/all_to_all | solution.py:456
  149.5 1.0 copy-start.4
  158.4 57.0 %all-to-all-start.4 = ((bf16[8,256,256]{2,1,0:T(8,128)(2,1)}), bf16[8,256,256]{2,1,0:T(8,128)(2,1)S(1)}, u32[]{:S(2)}, u32[]{:S(2)}) async-start(bf16[8,256,256]{2,1,0:T(8,128)(2,1)} %project_out.2), calls=%async_computation.4 | async-start | bytes 2097152 | tf_op jit(solution)/shard_map/all_to_all | solution.py:456
  172.2 9.4 %collective-permute-start.17 = (bf16[256,256]{1,0:T(8,128)(2,1)}, bf16[256,256]{1,0:T(8,128)(2,1)S(1)}, u32[]{:S(2)}, u32[]{:S(2)}) collective-permute-start(bf16[256,256]{1,0:T(8,128)(2,1)} %get-tuple-element.74), channel_id=1, source_target_pairs={{0,2},{1,3},{2,4},{3,5},{4,6},{5,7},{6,0},{7,1},{8,10},{9,11},{10,... | collective-permute-start | bytes 393224 | tf_op jit(solution)/shard_map/ppermute | solution.py:506
  173.7 8.7 %collective-permute-start.18 = (bf16[256,256]{1,0:T(8,128)(2,1)}, bf16[256,256]{1,0:T(8,128)(2,1)S(1)}, u32[]{:S(2)}, u32[]{:S(2)}) collective-permute-start(bf16[256,256]{1,0:T(8,128)(2,1)} %get-tuple-element.75), channel_id=1, source_target_pairs={{0,6},{1,7},{2,0},{3,1},{4,2},{5,3},{6,4},{7,5},{8,14},{9,15},{10,... | collective-permute-start | bytes 393224 | tf_op jit(solution)/shard_map/ppermute | solution.py:506
  175.0 8.5 %collective-permute-start.19 = (bf16[256,256]{1,0:T(8,128)(2,1)}, bf16[256,256]{1,0:T(8,128)(2,1)S(1)}, u32[]{:S(2)}, u32[]{:S(2)}) collective-permute-start(bf16[256,256]{1,0:T(8,128)(2,1)} %get-tuple-element.76), channel_id=1, source_target_pairs={{0,4},{1,5},{2,6},{3,7},{4,0},{5,1},{6,2},{7,3},{8,12},{9,13},{10,... | collective-permute-start | bytes 393224 | tf_op jit(solution)/shard_map/ppermute | solution.py:506
  176.7 6.8 %collective-permute-start.20 = (bf16[256,256]{1,0:T(8,128)(2,1)}, bf16[256,256]{1,0:T(8,128)(2,1)S(1)}, u32[]{:S(2)}, u32[]{:S(2)}) collective-permute-start(bf16[256,256]{1,0:T(8,128)(2,1)} %get-tuple-element.77), channel_id=1, source_target_pairs={{0,1},{1,0},{2,3},{3,2},{4,5},{5,4},{6,7},{7,6},{8,9},{9,8},{10,11... | collective-permute-start | bytes 393224 | tf_op jit(solution)/shard_map/ppermute | solution.py:506
  177.9 9.2 %collective-permute-start.21 = (bf16[256,256]{1,0:T(8,128)(2,1)}, bf16[256,256]{1,0:T(8,128)(2,1)S(1)}, u32[]{:S(2)}, u32[]{:S(2)}) collective-permute-start(bf16[256,256]{1,0:T(8,128)(2,1)} %get-tuple-element.78), channel_id=1, source_target_pairs={{0,3},{1,2},{2,5},{3,4},{4,7},{5,6},{6,1},{7,0},{8,11},{9,10},{10,... | collective-permute-start | bytes 393224 | tf_op jit(solution)/shard_map/ppermute | solution.py:506
  181.7 7.7 %copy-start.7 = (bf16[256,256]{1,0:T(8,128)(2,1)}, bf16[256,256]{1,0:T(8,128)(2,1)S(1)}, u32[]{:S(2)}) copy-start(bf16[256,256]{1,0:T(8,128)(2,1)S(1)} %collective-permute-done.17.refs_1_) | copy-start | bytes 393220
  181.7 6.3 %collective-permute-start.22 = (bf16[256,256]{1,0:T(8,128)(2,1)}, bf16[256,256]{1,0:T(8,128)(2,1)S(1)}, u32[]{:S(2)}, u32[]{:S(2)}) collective-permute-start(bf16[256,256]{1,0:T(8,128)(2,1)} %get-tuple-element.79), channel_id=1, source_target_pairs={{0,7},{1,6},{2,1},{3,0},{4,3},{5,2},{6,5},{7,4},{8,15},{9,14},{10,... | collective-permute-start | bytes 393224 | tf_op jit(solution)/shard_map/ppermute | solution.py:506
  182.3 7.0 %copy-start.8 = (bf16[256,256]{1,0:T(8,128)(2,1)}, bf16[256,256]{1,0:T(8,128)(2,1)S(1)}, u32[]{:S(2)}) copy-start(bf16[256,256]{1,0:T(8,128)(2,1)S(1)} %collective-permute-done.18.refs_2_) | copy-start | bytes 393220
  182.3 7.0 %collective-permute-start.23 = (bf16[256,256]{1,0:T(8,128)(2,1)}, bf16[256,256]{1,0:T(8,128)(2,1)S(1)}, u32[]{:S(2)}, u32[]{:S(2)}) collective-permute-start(bf16[256,256]{1,0:T(8,128)(2,1)} %get-tuple-element.80), channel_id=1, source_target_pairs={{0,5},{1,4},{2,7},{3,6},{4,1},{5,0},{6,3},{7,2},{8,13},{9,12},{10,... | collective-permute-start | bytes 393224 | tf_op jit(solution)/shard_map/ppermute | solution.py:506
  183.5 5.9 %copy-start.9 = (bf16[256,256]{1,0:T(8,128)(2,1)}, bf16[256,256]{1,0:T(8,128)(2,1)S(1)}, u32[]{:S(2)}) copy-start(bf16[256,256]{1,0:T(8,128)(2,1)S(1)} %collective-permute-done.19.refs_3_) | copy-start | bytes 393220
  183.5 5.9 %copy-start.10 = (bf16[256,256]{1,0:T(8,128)(2,1)}, bf16[256,256]{1,0:T(8,128)(2,1)S(1)}, u32[]{:S(2)}) copy-start(bf16[256,256]{1,0:T(8,128)(2,1)S(1)} %collective-permute-done.20.refs_4_) | copy-start | bytes 393220
  187.1 2.3 %copy-start.11 = (bf16[256,256]{1,0:T(8,128)(2,1)}, bf16[256,256]{1,0:T(8,128)(2,1)S(1)}, u32[]{:S(2)}) copy-start(bf16[256,256]{1,0:T(8,128)(2,1)S(1)} %collective-permute-done.21.refs_5_) | copy-start | bytes 393220
  188.0 1.4 copy-start.12
  190.0 25.4 %copy-start.1 = (s32[8]{0:T(128)S(1)}, s32[8]{0:T(128)}, u32[]{:S(2)}) copy-start(s32[8]{0:T(128)} %pad_add_fusion.3.order) | copy-start | bytes 100
  198.1 7.2 %collective-permute-start.24 = (bf16[256,256]{1,0:T(8,128)(2,1)}, bf16[256,256]{1,0:T(8,128)(2,1)S(1)}, u32[]{:S(2)}, u32[]{:S(2)}) collective-permute-start(bf16[256,256]{1,0:T(8,128)(2,1)} %get-tuple-element.90), channel_id=1, source_target_pairs={{0,2},{1,3},{2,4},{3,5},{4,6},{5,7},{6,0},{7,1},{8,10},{9,11},{10,... | collective-permute-start | bytes 393224 | tf_op jit(solution)/shard_map/ppermute | solution.py:506
  199.2 9.3 %collective-permute-start.25 = (bf16[256,256]{1,0:T(8,128)(2,1)}, bf16[256,256]{1,0:T(8,128)(2,1)S(1)}, u32[]{:S(2)}, u32[]{:S(2)}) collective-permute-start(bf16[256,256]{1,0:T(8,128)(2,1)} %get-tuple-element.91), channel_id=1, source_target_pairs={{0,6},{1,7},{2,0},{3,1},{4,2},{5,3},{6,4},{7,5},{8,14},{9,15},{10,... | collective-permute-start | bytes 393224 | tf_op jit(solution)/shard_map/ppermute | solution.py:506
  201.8 8.2 %collective-permute-start.26 = (bf16[256,256]{1,0:T(8,128)(2,1)}, bf16[256,256]{1,0:T(8,128)(2,1)S(1)}, u32[]{:S(2)}, u32[]{:S(2)}) collective-permute-start(bf16[256,256]{1,0:T(8,128)(2,1)} %get-tuple-element.92), channel_id=1, source_target_pairs={{0,4},{1,5},{2,6},{3,7},{4,0},{5,1},{6,2},{7,3},{8,12},{9,13},{10,... | collective-permute-start | bytes 393224 | tf_op jit(solution)/shard_map/ppermute | solution.py:506
  202.9 7.1 %collective-permute-start.27 = (bf16[256,256]{1,0:T(8,128)(2,1)}, bf16[256,256]{1,0:T(8,128)(2,1)S(1)}, u32[]{:S(2)}, u32[]{:S(2)}) collective-permute-start(bf16[256,256]{1,0:T(8,128)(2,1)} %get-tuple-element.93), channel_id=1, source_target_pairs={{0,1},{1,0},{2,3},{3,2},{4,5},{5,4},{6,7},{7,6},{8,9},{9,8},{10,11... | collective-permute-start | bytes 393224 | tf_op jit(solution)/shard_map/ppermute | solution.py:506
  203.8 8.7 %collective-permute-start.28 = (bf16[256,256]{1,0:T(8,128)(2,1)}, bf16[256,256]{1,0:T(8,128)(2,1)S(1)}, u32[]{:S(2)}, u32[]{:S(2)}) collective-permute-start(bf16[256,256]{1,0:T(8,128)(2,1)} %get-tuple-element.94), channel_id=1, source_target_pairs={{0,3},{1,2},{2,5},{3,4},{4,7},{5,6},{6,1},{7,0},{8,11},{9,10},{10,... | collective-permute-start | bytes 393224 | tf_op jit(solution)/shard_map/ppermute | solution.py:506
  205.4 7.1 %collective-permute-start.29 = (bf16[256,256]{1,0:T(8,128)(2,1)}, bf16[256,256]{1,0:T(8,128)(2,1)S(1)}, u32[]{:S(2)}, u32[]{:S(2)}) collective-permute-start(bf16[256,256]{1,0:T(8,128)(2,1)} %get-tuple-element.95), channel_id=1, source_target_pairs={{0,7},{1,6},{2,1},{3,0},{4,3},{5,2},{6,5},{7,4},{8,15},{9,14},{10,... | collective-permute-start | bytes 393224 | tf_op jit(solution)/shard_map/ppermute | solution.py:506
  208.5 6.9 %collective-permute-start.30 = (bf16[256,256]{1,0:T(8,128)(2,1)}, bf16[256,256]{1,0:T(8,128)(2,1)S(1)}, u32[]{:S(2)}, u32[]{:S(2)}) collective-permute-start(bf16[256,256]{1,0:T(8,128)(2,1)} %get-tuple-element.96), channel_id=1, source_target_pairs={{0,5},{1,4},{2,7},{3,6},{4,1},{5,0},{6,3},{7,2},{8,13},{9,12},{10,... | collective-permute-start | bytes 393224 | tf_op jit(solution)/shard_map/ppermute | solution.py:506
  (4 other events, 3.2 us)

commit v5 on v4

--- a/solution.py
+++ b/solution.py
@@ -12,6 +12,7 @@
 BLOCK = 64
 HOT = 8
 REACH = 2
+FIRST_BLOCKS = 5
 KV = ("kv_0", "kv_1")
 TP = ("tp_0", "tp_1")
 WIDTH = 256
@@ -227,8 +228,8 @@
     )(asked, order, same, other, w_key, w_value, gain)
 
 
-def attention_kernel(first, at, where, q, mask, pairs, near, hot, *rest):
-    outs, (table, raw, sems) = rest[:-3], rest[-3:]
+def attention_kernel(first, at, where, queries, masks, pairs, near, hot, *rest):
+    outs, (q, mask, table, raw, sems) = rest[:-5], rest[-5:]
     devices, hot_rows, _ = hot.shape
     here = pairs.shape[0]
     plain = near.shape[0]
@@ -236,6 +237,8 @@
         pltpu.make_async_copy(hot, raw, sems.at[0]),
         pltpu.make_async_copy(pairs, table.at[pl.ds(0, here)], sems.at[1]),
         pltpu.make_async_copy(near, table.at[pl.ds(here, plain)], sems.at[2]),
+        pltpu.make_async_copy(queries.at[pl.ds(first * BLOCK, q.shape[0])], q, sems.at[3]),
+        pltpu.make_async_copy(masks.at[pl.ds(first, mask.shape[0])], mask, sems.at[4]),
     ]
     for copy in copies:
         copy.start()
@@ -313,33 +316,34 @@
             piece_of(n, put)
 
 
-def attend(chunk, chunks, split, at, where, queries, mask, pairs, near, hot):
+def attend(first, blocks, split, at, where, queries, mask, pairs, near, hot):
     ranks = where.shape[0]
-    length = queries.shape[0] // chunks
+    length = blocks * BLOCK
     slots = mask.shape[1] // BLOCK
-    blocks = length // BLOCK
     rows = length // ranks
     anywhere = pl.BlockSpec(memory_space=pl.ANY)
     shape = (rows, WIDTH) if split else (ranks, rows, WIDTH)
     count = ranks if split else 1
     height = pairs.shape[0] + near.shape[0] + HOT * PAIR * BLOCK
     outs = pl.pallas_call(
-        functools.partial(attention_kernel, chunk * blocks),
+        functools.partial(attention_kernel, first),
         grid_spec=pltpu.PrefetchScalarGridSpec(
             num_scalar_prefetch=2,
             grid=(1,),
             in_specs=[
-                pl.BlockSpec((length, WIDTH), lambda i, *_: (chunk, 0)),
-                pl.BlockSpec((blocks, slots * BLOCK), lambda i, *_: (chunk, 0)),
+                anywhere,
+                anywhere,
                 anywhere,
                 anywhere,
                 anywhere,
             ],
             out_specs=[whole_block(*shape)] * count,
             scratch_shapes=[
+                pltpu.VMEM((length, WIDTH), bf16),
+                pltpu.VMEM((blocks, slots * BLOCK), f32),
                 pltpu.VMEM((height, WIDTH), bf16),
                 pltpu.VMEM(hot.shape, bf16),
-                pltpu.SemaphoreType.DMA((3,)),
+                pltpu.SemaphoreType.DMA((5,)),
             ],
         ),
         out_shape=[jax.ShapeDtypeStruct(shape, bf16)] * count,
@@ -365,8 +369,8 @@
     weight = jnp.concatenate([w[...] for w in weights], axis=0)
     sums = jnp.dot(rows, weight, preferred_element_type=f32)
     tile = sums.shape[1]
-    mixed[2 * n] = sums[:, :WIDTH]
-    mixed[2 * n + 1] = sums[:, WIDTH:]
+    for i in range(tile // WIDTH):
+        mixed[(tile // WIDTH) * n + i] = sums[:, i * WIDTH : (i + 1) * WIDTH]
     part = sum(sums[:, i : i + 128] * sums[:, i : i + 128] for i in range(0, tile, 128))
 
     @pl.when(n == 0)
@@ -394,7 +398,7 @@
     pieces = list(pieces) if split else [pieces]
     rows = pieces[0].shape[-2]
     depth, width = weights[0].shape
-    tile = 2 * WIDTH
+    tile = 4 * WIDTH
     shape = (rows, WIDTH) if split else (count, rows, WIDTH)
     outs = pl.pallas_call(
         out_kernel,
@@ -423,9 +427,12 @@
 def place_kernel(order, whole, *rest):
     count = len(rest) - 2
     parts, out, sems = rest[:count], rest[count], rest[count + 1]
-    copies = [pltpu.make_async_copy(whole, out.at[pl.ds(0, count)], sems.at[count])]
+    rows = parts[0].shape[0]
+    base = whole.shape[0]
+    copies = [pltpu.make_async_copy(whole, out.at[pl.ds(0, base)], sems.at[count])]
     for k in range(count):
-        copies.append(pltpu.make_async_copy(parts[k], out.at[count + order[k]], sems.at[k]))
+        to = pl.multiple_of(base + order[k] * rows, BLOCK)
+        copies.append(pltpu.make_async_copy(parts[k], out.at[pl.ds(to, rows)], sems.at[k]))
     for copy in copies:
         copy.start()
     for copy in copies:
@@ -434,7 +441,7 @@
 
 def place(order, whole, parts):
     count = len(parts)
-    shape = (2 * count,) + parts[0].shape
+    length = whole.shape[0] + count * parts[0].shape[0]
     anywhere = pl.BlockSpec(memory_space=pl.ANY)
     return pl.pallas_call(
         place_kernel,
@@ -445,7 +452,7 @@
             out_specs=anywhere,
             scratch_shapes=[pltpu.SemaphoreType.DMA((count + 1,))],
         ),
-        out_shape=jax.ShapeDtypeStruct(shape, bf16),
+        out_shape=jax.ShapeDtypeStruct((length, WIDTH), bf16),
         compiler_params=pltpu.CompilerParams(vmem_limit_bytes=8 << 20),
         cost_estimate=pl.CostEstimate(flops=1 << 20, bytes_accessed=4 << 20, transcendentals=0),
         name="place",
@@ -544,10 +551,10 @@
     z, x = lax.axis_index(KV[0]), lax.axis_index(KV[1])
     by_row = requests.reshape(long, side, -1)
     rows_in = [turned(by_row, z, step, KV[0]) for step in range(long)]
-    pairs = project_kv(tokens, w_key, w_value, key_row).reshape(-1, WIDTH)
-    pairs, *rows_in = tied(pairs, *rows_in)
     by_side = jnp.stack(rows_in, axis=1)
     sides_in = [turned(by_side, x, step, KV[1]) for step in range(side)]
+    pairs = project_kv(tokens, w_key, w_value, key_row).reshape(-1, WIDTH)
+    pairs, *sides_in = tied(pairs, *sides_in)
     asked = jnp.stack(sides_in, axis=1).reshape(devices, -1)
     sources = jnp.stack(
         [((z + long - s) % long) * side + (x + side - t) % side for s in range(long) for t in range(side)]
@@ -584,6 +591,9 @@
     at = jnp.where(usable, at, 0).astype(jnp.int32).reshape(-1)
     mask = jnp.repeat(usable.astype(f32), BLOCK, axis=1)
 
+    at, mask, order, toward, same_order, sent_hot = tied(
+        at, mask, order, toward, same_order, sent_hot
+    )
     near, sent_hot = tied(near, sent_hot)
     hot = exchange(sent_hot, KV)
     w_far = along_y(w_after, 1)
@@ -592,16 +602,17 @@
     weights = [w_out, w_after, w_before, w_far, w_own] + w_swapped
 
     gains = out_gain.reshape(ranks, 1, WIDTH)
-    first = attend(0, 2, False, at, same_order, queries, mask, pairs, near, hot)
+    early = (FIRST_BLOCKS * blocks_here) // 8
+    first = attend(0, early, False, at, same_order, queries, mask, pairs, near, hot)
     first = exchange(first, TP)
-    second = attend(1, 2, True, at, toward, queries, mask, pairs, near, hot)
+    second = attend(early, blocks_here - early, True, at, toward, queries, mask, pairs, near, hot)
     second = send_pieces(second)
     first = project_out(False, order, same_order, first, weights, gains)
     moved = exchange(first, TP)
     second = tied(first, *second)[1:]
     second = project_out(True, order, toward, second, weights, gains)
     second = send_pieces(second)
-    return place(order, moved, second).reshape(length, WIDTH)
+    return place(order, moved.reshape(-1, WIDTH), second)
 
 
 def solution(mesh):

time: 219 us -> 207 us (0.945)
  waiting for transfers between devices: 51.2 us -> 32.7 us
  blocking collectives: 0 us -> 17.9 us
  starting transfers between devices: 79.4 us -> 69.4 us
  Pallas kernels: 75.5 us -> 72.8 us
    all_to_all x0 -> x1, blocking collectives: none -> 17.9 us  [exchange(): return lax.all_to_all(pieces, axes, split_axis=0, concat_axis=0, tiled=True)]
    ppermute x6, waiting for transfers between devices: 13.8 us -> 0.02 us  [along_y(): lax.ppermute(piece, TP[0], [(i, (i + shift) % ring) for i in range(ring)])]
    all_to_all x5 -> x4, waiting for transfers between devices: 20.6 us -> 10.4 us  [exchange(): return lax.all_to_all(pieces, axes, split_axis=0, concat_axis=0, tiled=True)]
    all_to_all x5 -> x4, starting transfers between devices: 31.1 us -> 22.7 us  [exchange(): return lax.all_to_all(pieces, axes, split_axis=0, concat_axis=0, tiled=True)]
    ppermute x5, waiting for transfers between devices: 0.24 us -> 5.32 us  [across(): return lax.ppermute(piece, TP[1], [(0, 1), (1, 0)])]
  transfers between devices with their start and end apart: 36 -> 35, of which waited for: 14 -> 11; matrix products, arithmetic and copies ran while one was open for 4% -> 4% of each run, Pallas kernels for 28% -> 30%
where the time goes in v5:
time: 207 us; the launch traced here: 206 us
  Pallas kernels  72.8 us (35%)
  starting transfers between devices  69.4 us (34%)
  waiting for transfers between devices  32.7 us (16%)
  blocking collectives  17.9 us (9%)
  local copies, waits for them, and re-layouts  7.5 us (4%)
  other arithmetic  5.24 us (3%)
    all_to_all x4, starting transfers between devices, exchange(): return lax.all_to_all(pieces, axes, split_axis=0, concat_axis=0, tiled=True)  22.7 us
    ppermute x14, starting transfers between devices, send_pieces(): got.append(lax.ppermute(pieces[k], TP, pairs) if k else pieces[0])  19.4 us
    pallas_call x2, Pallas kernels, attend(): pl.pallas_call(functools.partial(attention_kernel, first), grid_spec=pltp...  18.9 us
    all_to_all x1, blocking collectives, exchange(): return lax.all_to_all(pieces, axes, split_axis=0, concat_axis=0, tiled=True)  17.9 us
    ppermute x6, starting transfers between devices, turned(): lax.ppermute(mine, axis, [(i, (i + step) % size) for i in range(size)])  15.9 us
    ppermute x14, waiting for transfers between devices, send_pieces(): got.append(lax.ppermute(pieces[k], TP, pairs) if k else pieces[0])  15.9 us
    pallas_call x2, Pallas kernels, project_out(): pl.pallas_call(out_kernel, grid_spec=pltpu.PrefetchScalarGridSpec(num_sca...  15.1 us
    pallas_call x1, Pallas kernels, project_kv(): pl.pallas_call(kv_kernel, grid=(length // tile,), in_specs=[pl.BlockSpec(...  13.7 us
  transfers between devices with their start and end apart: 35, of which 11 were waited for; matrix products, arithmetic and copies ran while one was open for 4% of the time, Pallas kernels for 30%

profile of v5, /device:TPU:1, one launch (start us, length us, event | category | flops | bytes accessed | tf_op | source)
XLA Modules:
  0.0 206.0 jit_solution(10824576663371251782)
XLA Ops:
  0.0 2.1 %collective-permute-start.10 = (bf16[256,2048]{1,0:T(8,128)(2,1)}, bf16[256,2048]{1,0:T(8,128)(2,1)S(1)}, u32[]{:S(2)}, u32[]{:S(2)}) collective-permute-start(bf16[256,2048]{1,0:T(8,128)(2,1)} %refs_8_.1), channel_id=1, source_target_pairs={{0,2},{2,4},{4,6},{6,0},{1,3},{3,5},{5,7},{7,1},{8,10},{10,12},{12... | collective-permute-start | bytes 3145736 | tf_op jit(solution)/shard_map/ppermute | solution.py:472
  2.1 1.4 collective-permute-start.11
  3.6 4.0 %token_shares.1 = bf16[16,256,256]{2,1,0:T(8,128)(2,1)} custom-call(s32[1]{0:T(128)} %bitcast.rank, bf16[4096,2048]{1,0:T(8,128)(2,1)} %tok.4), custom_call_target="tpu_custom_call" | custom-call | flops 1048576 | bytes 4194304 | tf_op jit(solution)/shard_map/token_shares/pallas_call | solution.py:48
  7.6 7.7 %all-to-all-start = ((bf16[16,256,256]{2,1,0:T(8,128)(2,1)}), bf16[16,256,256]{2,1,0:T(8,128)(2,1)S(1)}, u32[]{:S(2)}, u32[]{:S(2)}) async-start(bf16[16,256,256]{2,1,0:T(8,128)(2,1)} %token_shares.1), calls=%async_computation | async-start | bytes 4194304 | tf_op jit(solution)/shard_map/all_to_all | solution.py:463
  16.6 1.4 collective-permute-start
  18.0 2.4 %collective-permute-start.1 = (s32[4,16]{1,0:T(4,128)S(1)}, s32[4,16]{1,0:T(4,128)S(1)}, u32[]{:S(2)}, u32[]{:S(2)}) collective-permute-start(s32[4,16]{1,0:T(4,128)S(1)} %get-tuple-element.122), channel_id=1, source_target_pairs={{0,64},{32,96},{64,0},{96,32},{1,65},{33,97},{65,1},{97,33},{2,66}... | collective-permute-start | bytes 776 | tf_op jit(solution)/shard_map/ppermute | solution.py:484
  20.4 1.2 collective-permute-start.2
  22.3 13.7 %project_kv.1 = bf16[64,2,64,256]{3,2,1,0:T(8,128)(2,1)} custom-call(bf16[4096,2048]{1,0:T(8,128)(2,1)} %tok.4, bf16[2048,256]{1,0:T(8,128)(2,1)} %wk.3, bf16[2048,256]{1,0:T(8,128)(2,1)} %wv.3, f32[1,128]{1,0:T(1,128)} %bitcast.86), custom_call_target="tpu_custom_call" | custom-call | flops 8589934592 | bytes 16777216 | tf_op jit(solution)/shard_map/project_kv/pallas_call | solution.py:79
  36.0 1.3 collective-permute-start.3
  37.3 8.0 %collective-permute-start.4 = (s32[4,16]{1,0:T(4,128)S(1)}, s32[4,16]{1,0:T(4,128)S(1)}, u32[]{:S(2)}, u32[]{:S(2)}) collective-permute-start(s32[4,16]{1,0:T(4,128)S(1)} %bitcast.78), channel_id=1, source_target_pairs={{0,16},{8,24},{16,0},{24,8},{1,17},{9,25},{17,1},{25,9},{2,18},{10... | collective-permute-start | bytes 776 | tf_op jit(solution)/shard_map/ppermute | solution.py:484
  45.3 1.7 collective-permute-start.5
  47.0 1.1 collective-permute-done.5
  48.7 4.4 %gather_near.1 = bf16[32,128,256]{2,1,0:T(8,128)(2,1)} custom-call(s32[32]{0:T(128)} %reshape.68.near, bf16[8192,256]{1,0:T(8,128)(2,1)} %bitcast.61), custom_call_target="tpu_custom_call" | custom-call | flops 1048576 | bytes 4194304 | tf_op jit(solution)/shard_map/gather_near/pallas_call | solution.py:147
  53.2 4.9 %all-to-all-start.1 = ((bf16[16,256,256]{2,1,0:T(8,128)(2,1)}), bf16[16,256,256]{2,1,0:T(8,128)(2,1)S(1)}, u32[]{:S(2)}, u32[]{:S(2)}) async-start(bf16[16,256,256]{2,1,0:T(8,128)(2,1)} %bitcast.66), calls=%async_computation.1 | async-start | bytes 4194304 | tf_op jit(solution)/shard_map/all_to_all | solution.py:463
  58.3 2.7 %collective-permute-start.7 = (bf16[256,256]{1,0:T(8,128)(2,1)S(1)}, bf16[256,256]{1,0:T(8,128)(2,1)S(1)}, u32[]{:S(2)}, u32[]{:S(2)}) collective-permute-start(bf16[256,256]{1,0:T(8,128)(2,1)S(1)} %slice_bitcast_fusion), channel_id=1, source_target_pairs={{0,6},{2,0},{4,2},{6,4},{1,7},{3,1},{5,3},{7,5},{8,14},{10,8},{12,... | collective-permute-start | bytes 393224 | tf_op jit(solution)/shard_map/ppermute | solution.py:472
  61.4 10.1 %project_q.1.queries = bf16[4096,256]{1,0:T(8,128)(2,1)} custom-call(bf16[4096,2048]{1,0:T(8,128)(2,1)} %tok.4, bf16[2048,256]{1,0:T(8,128)(2,1)} %wq.1, f32[1,128]{1,0:T(1,128)} %multiply_bitcast_fusion.gain), custom_call_target="tpu_custom_call" | custom-call | flops 4294967296 | bytes 16777216 | tf_op jit(solution)/shard_map/project_q/pallas_call | solution.py:108
  72.3 3.3 %collective-permute-start.9 = (bf16[4,256,256]{2,1,0:T(8,128)(2,1)}, bf16[4,256,256]{2,1,0:T(8,128)(2,1)}, u32[]{:S(2)}, u32[]{:S(2)}) collective-permute-start(bf16[4,256,256]{2,1,0:T(8,128)(2,1)} %pad_maximum_fusion.same), channel_id=1, source_target_pairs={{0,1},{1,0},{2,3},{3,2},{4,5},{5,4},{6,7},{7,6},{8,9},{9,8},{10,11... | collective-permute-start | bytes 1572872 | tf_op jit(solution)/shard_map/ppermute | solution.py:476
  78.0 4.8 %project_sent.1 = bf16[16,64,256]{2,1,0:T(8,128)(2,1)} custom-call(s32[128]{0:T(128)} %reshape.67.asked, s32[8]{0:T(128)} %pad_add_fusion.3.order, bf16[4,256,256]{2,1,0:T(8,128)(2,1)} %pad_maximum_fusion.same, bf16[4,256,256]{2,1,0:T(8,128)(2,1)} %collective-permute-done.9.other, bf16[2048,256]{1,0:T(8,128)(2,1)} %wk.3, bf16[2048,256]{1,0:T(8,128)(2,1)} %wv.3, ...), custom_call_target="tpu_custom_call" | custom-call | flops 536870912 | bytes 8388608 | tf_op jit(solution)/shard_map/project_sent/pallas_call | solution.py:207
  83.7 1.3 select_reduce_fusion
  86.3 17.9 %all_to_all.25.hot = bf16[16,64,256]{2,1,0:T(8,128)(2,1)} all-to-all(bf16[16,64,256]{2,1,0:T(8,128)(2,1)} %project_sent.1), channel_id=1, replica_groups=mesh['kv_0'=4,'kv_1'=4,'tp_0'=4,'tp_1'=2] {'kv_0','kv_1'}, dimensions={0} | all-to-all | bytes 1048576 | tf_op jit(solution)/shard_map/all_to_all | solution.py:463
  104.1 11.2 %attend.2 = bf16[8,320,256]{2,1,0:T(8,128)(2,1)} custom-call(s32[512]{0:T(512)} %reshape.69.at, s32[8]{0:T(128)} %iota.23.where.slot, bf16[4096,256]{1,0:T(8,128)(2,1)} %project_q.1.queries, f32[64,512]{1,0:T(8,128)} %reshape.70.masks, bf16[8192,256]{1,0:T(8,128)(2,1)} %bitcast.62, bf16[4096,256]{1,0:T(8,128)(2,1)} %bitcast.64, ...), custom_call_target="tpu_custom_call" | custom-call | flops 2684354560 | bytes 10485760 | tf_op jit(solution)/shard_map/attend/pallas_call | solution.py:328
  115.4 5.6 %all-to-all-start.3 = ((bf16[8,320,256]{2,1,0:T(8,128)(2,1)}), bf16[8,320,256]{2,1,0:T(8,128)(2,1)S(1)}, u32[]{:S(2)}, u32[]{:S(2)}) async-start(bf16[8,320,256]{2,1,0:T(8,128)(2,1)} %attend.2), calls=%async_computation.3 | async-start | bytes 2621440 | tf_op jit(solution)/shard_map/all_to_all | solution.py:463
  122.0 1.7 collective-permute-done.13.refs_5_.refs_12_
  123.7 1.5 collective-permute-done.14.refs_6_.refs_13_
  125.2 1.5 collective-permute-done.15.refs_7_.refs_14_
  128.4 10.4 %all-to-all-done.3.refs_0_ = bf16[8,320,256]{2,1,0:T(8,128)(2,1)S(1)} async-done(((bf16[8,320,256]{2,1,0:T(8,128)(2,1)}), bf16[8,320,256]{2,1,0:T(8,128)(2,1)S(1)}, u32[]{:S(2)}, u32[]{:S(2)}) %all-to-all-start.3) | async-done | bytes 1310752 | tf_op jit(solution)/shard_map/all_to_all | solution.py:463
  138.8 1.1 copy-done.3
  139.9 8.3 %project_out.2 = bf16[8,320,256]{2,1,0:T(8,128)(2,1)} custom-call(s32[8]{0:T(128)} %pad_add_fusion.3.order, s32[8]{0:T(128)} %iota.23.where.slot, bf16[8,320,256]{2,1,0:T(8,128)(2,1)} %copy-done.3, bf16[256,2048]{1,0:T(8,128)(2,1)} %refs_8_.1, bf16[256,2048]{1,0:T(8,128)(2,1)} %copy-done.5, bf16[256,2048]{1,0:T(8,128)(2,1)} %collective-permute-done.11.refs_3_.refs_10_, ...), custom_call_target="tpu_custom_call" | custom-call | flops 2684354560 | bytes 12582912 | tf_op jit(solution)/shard_map/project_out/pallas_call | solution.py:403
  148.2 4.4 %all-to-all-start.4 = ((bf16[8,320,256]{2,1,0:T(8,128)(2,1)}), bf16[8,320,256]{2,1,0:T(8,128)(2,1)S(1)}, u32[]{:S(2)}, u32[]{:S(2)}) async-start(bf16[8,320,256]{2,1,0:T(8,128)(2,1)} %project_out.2), calls=%async_computation.4 | async-start | bytes 2621440 | tf_op jit(solution)/shard_map/all_to_all | solution.py:463
  152.6 7.7 %attend.3 = (bf16[192,256]{1,0:T(8,128)(2,1)}, bf16[192,256]{1,0:T(8,128)(2,1)}, bf16[192,256]{1,0:T(8,128)(2,1)}, bf16[192,256]{1,0:T(8,128)(2,1)}, bf16[192,25...) custom-call(s32[512]{0:T(512)} %reshape.69.at, ...), custom_call_target="tpu_custom_call" | custom-call | flops 1610612736 | bytes 10485760 | tf_op jit(solution)/shard_map/attend/pallas_call | solution.py:328
  160.3 1.4 collective-permute-start.17
  161.7 1.3 collective-permute-start.18
  163.0 1.7 collective-permute-start.19
  164.7 1.2 collective-permute-start.20
  166.1 6.3 %collective-permute-done.17.refs_1_ = bf16[192,256]{1,0:T(8,128)(2,1)S(1)} collective-permute-done((bf16[192,256]{1,0:T(8,128)(2,1)}, bf16[192,256]{1,0:T(8,128)(2,1)S(1)}, u32[]{:S(2)}, u32[]{:S(2)}) %collective-permute-start.17) | collective-permute-done | bytes 98336 | tf_op jit(solution)/shard_map/ppermute | solution.py:513
  172.4 1.8 collective-permute-start.22
  174.3 1.6 collective-permute-start.23
  176.7 4.3 %collective-permute-done.23.refs_7_ = bf16[192,256]{1,0:T(8,128)(2,1)S(1)} collective-permute-done((bf16[192,256]{1,0:T(8,128)(2,1)}, bf16[192,256]{1,0:T(8,128)(2,1)S(1)}, u32[]{:S(2)}, u32[]{:S(2)}) %collective-permute-start.23) | collective-permute-done | bytes 98336 | tf_op jit(solution)/shard_map/ppermute | solution.py:513
  181.7 6.9 %project_out.3 = (bf16[192,256]{1,0:T(8,128)(2,1)}, bf16[192,256]{1,0:T(8,128)(2,1)}, bf16[192,256]{1,0:T(8,128)(2,1)}, bf16[192,256]{1,0:T(8,128)(2,1)}, bf16[1...) custom-call(s32[8]{0:T(128)} %pad_add_fusion.3.order, ...), custom_call_target="tpu_custom_call" | custom-call | flops 1610612736 | bytes 12582912 | tf_op jit(solution)/shard_map/project_out/pallas_call | solution.py:403
  188.6 1.3 collective-permute-start.24
  189.9 1.5 collective-permute-start.25
  191.9 1.3 collective-permute-start.27
  193.3 1.0 collective-permute-start.28
  194.3 1.9 collective-permute-start.29
  196.2 2.5 %collective-permute-start.30 = (bf16[192,256]{1,0:T(8,128)(2,1)}, bf16[192,256]{1,0:T(8,128)(2,1)S(1)}, u32[]{:S(2)}, u32[]{:S(2)}) collective-permute-start(bf16[192,256]{1,0:T(8,128)(2,1)} %get-tuple-element.108), channel_id=1, source_target_pairs={{0,5},{1,4},{2,7},{3,6},{4,1},{5,0},{6,3},{7,2},{8,13},{9,12},{10,... | collective-permute-start | bytes 294920 | tf_op jit(solution)/shard_map/ppermute | solution.py:513
  198.7 1.4 collective-permute-done.28.rest_5_
  200.1 2.9 %collective-permute-done.30.rest_7_ = bf16[192,256]{1,0:T(8,128)(2,1)S(1)} collective-permute-done((bf16[192,256]{1,0:T(8,128)(2,1)}, bf16[192,256]{1,0:T(8,128)(2,1)S(1)}, u32[]{:S(2)}, u32[]{:S(2)}) %collective-permute-start.30) | collective-permute-done | bytes 98336 | tf_op jit(solution)/shard_map/ppermute | solution.py:513
  203.9 1.9 place.1
  (108 shorter events, 14.6 us)
Async XLA Ops:
  0.0 77.6 %collective-permute-start.10 = (bf16[256,2048]{1,0:T(8,128)(2,1)}, bf16[256,2048]{1,0:T(8,128)(2,1)S(1)}, u32[]{:S(2)}, u32[]{:S(2)}) collective-permute-start(bf16[256,2048]{1,0:T(8,128)(2,1)} %refs_8_.1), channel_id=1, source_target_pairs={{0,2},{2,4},{4,6},{6,0},{1,3},{3,5},{5,7},{7,1},{8,10},{10,12},{12... | collective-permute-start | bytes 3145736 | tf_op jit(solution)/shard_map/ppermute | solution.py:472
  2.1 119.4 %collective-permute-start.11 = (bf16[256,2048]{1,0:T(8,128)(2,1)}, bf16[256,2048]{1,0:T(8,128)(2,1)}, u32[]{:S(2)}, u32[]{:S(2)}) collective-permute-start(bf16[256,2048]{1,0:T(8,128)(2,1)} %refs_8_.1), channel_id=1, source_target_pairs={{0,6},{2,0},{4,2},{6,4},{1,7},{3,1},{5,3},{7,5},{8,14},{10,8},{12,... | collective-permute-start | bytes 3145736 | tf_op jit(solution)/shard_map/ppermute | solution.py:472
  7.6 7.8 %copy-start.16 = (s32[64,8]{0,1:T(8,128)S(1)}, s32[64,8]{0,1:T(8,128)}, u32[]{:S(2)}) copy-start(s32[64,8]{0,1:T(8,128)} %param.17) | copy-start | bytes 6148
  7.6 14.1 %copy-start.17 = (f32[128]{0:T(128)S(1)}, f32[128]{0:T(128)}, u32[]{:S(2)}) copy-start(f32[128]{0:T(128)} %param.14) | copy-start | bytes 1540
  7.6 45.6 %all-to-all-start = ((bf16[16,256,256]{2,1,0:T(8,128)(2,1)}), bf16[16,256,256]{2,1,0:T(8,128)(2,1)S(1)}, u32[]{:S(2)}, u32[]{:S(2)}) async-start(bf16[16,256,256]{2,1,0:T(8,128)(2,1)} %token_shares.1), calls=%async_computation | async-start | bytes 4194304 | tf_op jit(solution)/shard_map/all_to_all | solution.py:463
  16.6 19.3 %collective-permute-start = (s32[4,16]{1,0:T(4,128)S(1)}, s32[4,16]{1,0:T(4,128)S(1)}, u32[]{:S(2)}, u32[]{:S(2)}) collective-permute-start(s32[4,16]{1,0:T(4,128)S(1)} %get-tuple-element.123), channel_id=1, source_target_pairs={{0,32},{32,64},{64,96},{96,0},{1,33},{33,65},{65,97},{97,1},{2,34}... | collective-permute-start | bytes 776 | tf_op jit(solution)/shard_map/ppermute | solution.py:484
  18.0 18.0 %collective-permute-start.1 = (s32[4,16]{1,0:T(4,128)S(1)}, s32[4,16]{1,0:T(4,128)S(1)}, u32[]{:S(2)}, u32[]{:S(2)}) collective-permute-start(s32[4,16]{1,0:T(4,128)S(1)} %get-tuple-element.122), channel_id=1, source_target_pairs={{0,64},{32,96},{64,0},{96,32},{1,65},{33,97},{65,1},{97,33},{2,66}... | collective-permute-start | bytes 776 | tf_op jit(solution)/shard_map/ppermute | solution.py:484
  20.4 15.6 %collective-permute-start.2 = (s32[4,16]{1,0:T(4,128)S(1)}, s32[4,16]{1,0:T(4,128)S(1)}, u32[]{:S(2)}, u32[]{:S(2)}) collective-permute-start(s32[4,16]{1,0:T(4,128)S(1)} %get-tuple-element.121), channel_id=1, source_target_pairs={{0,96},{32,0},{64,32},{96,64},{1,97},{33,1},{65,33},{97,65},{2,98}... | collective-permute-start | bytes 776 | tf_op jit(solution)/shard_map/ppermute | solution.py:484
  36.0 10.9 %collective-permute-start.3 = (s32[4,16]{1,0:T(4,128)S(1)}, s32[4,16]{1,0:T(4,128)S(1)}, u32[]{:S(2)}, u32[]{:S(2)}) collective-permute-start(s32[4,16]{1,0:T(4,128)S(1)} %bitcast.79), channel_id=1, source_target_pairs={{0,8},{8,16},{16,24},{24,0},{1,9},{9,17},{17,25},{25,1},{2,10},{10... | collective-permute-start | bytes 776 | tf_op jit(solution)/shard_map/ppermute | solution.py:484
  37.3 9.7 %collective-permute-start.4 = (s32[4,16]{1,0:T(4,128)S(1)}, s32[4,16]{1,0:T(4,128)S(1)}, u32[]{:S(2)}, u32[]{:S(2)}) collective-permute-start(s32[4,16]{1,0:T(4,128)S(1)} %bitcast.78), channel_id=1, source_target_pairs={{0,16},{8,24},{16,0},{24,8},{1,17},{9,25},{17,1},{25,9},{2,18},{10... | collective-permute-start | bytes 776 | tf_op jit(solution)/shard_map/ppermute | solution.py:484
  45.3 2.7 %collective-permute-start.5 = (s32[4,16]{1,0:T(4,128)S(1)}, s32[4,16]{1,0:T(4,128)S(1)}, u32[]{:S(2)}, u32[]{:S(2)}) collective-permute-start(s32[4,16]{1,0:T(4,128)S(1)} %bitcast.77), channel_id=1, source_target_pairs={{0,24},{8,0},{16,8},{24,16},{1,25},{9,1},{17,9},{25,17},{2,26},{10... | collective-permute-start | bytes 776 | tf_op jit(solution)/shard_map/ppermute | solution.py:484
  53.2 33.1 %all-to-all-start.1 = ((bf16[16,256,256]{2,1,0:T(8,128)(2,1)}), bf16[16,256,256]{2,1,0:T(8,128)(2,1)S(1)}, u32[]{:S(2)}, u32[]{:S(2)}) async-start(bf16[16,256,256]{2,1,0:T(8,128)(2,1)} %bitcast.66), calls=%async_computation.1 | async-start | bytes 4194304 | tf_op jit(solution)/shard_map/all_to_all | solution.py:463
  58.3 13.2 %collective-permute-start.6 = (bf16[256,256]{1,0:T(8,128)(2,1)S(1)}, bf16[256,256]{1,0:T(8,128)(2,1)S(1)}, u32[]{:S(2)}, u32[]{:S(2)}) collective-permute-start(bf16[256,256]{1,0:T(8,128)(2,1)S(1)} %slice_bitcast_fusion), channel_id=1, source_target_pairs={{0,2},{2,4},{4,6},{6,0},{1,3},{3,5},{5,7},{7,1},{8,10},{10,12},{12... | collective-permute-start | bytes 393224 | tf_op jit(solution)/shard_map/ppermute | solution.py:472
  58.3 13.2 %collective-permute-start.7 = (bf16[256,256]{1,0:T(8,128)(2,1)S(1)}, bf16[256,256]{1,0:T(8,128)(2,1)S(1)}, u32[]{:S(2)}, u32[]{:S(2)}) collective-permute-start(bf16[256,256]{1,0:T(8,128)(2,1)S(1)} %slice_bitcast_fusion), channel_id=1, source_target_pairs={{0,6},{2,0},{4,2},{6,4},{1,7},{3,1},{5,3},{7,5},{8,14},{10,8},{12,... | collective-permute-start | bytes 393224 | tf_op jit(solution)/shard_map/ppermute | solution.py:472
  60.9 10.5 %collective-permute-start.8 = (bf16[256,256]{1,0:T(8,128)(2,1)S(1)}, bf16[256,256]{1,0:T(8,128)(2,1)S(1)}, u32[]{:S(2)}, u32[]{:S(2)}) collective-permute-start(bf16[256,256]{1,0:T(8,128)(2,1)S(1)} %slice_bitcast_fusion), channel_id=1, source_target_pairs={{0,4},{2,6},{4,0},{6,2},{1,5},{3,7},{5,1},{7,3},{8,12},{10,14},{12... | collective-permute-start | bytes 393224 | tf_op jit(solution)/shard_map/ppermute | solution.py:472
  72.3 5.7 %collective-permute-start.9 = (bf16[4,256,256]{2,1,0:T(8,128)(2,1)}, bf16[4,256,256]{2,1,0:T(8,128)(2,1)}, u32[]{:S(2)}, u32[]{:S(2)}) collective-permute-start(bf16[4,256,256]{2,1,0:T(8,128)(2,1)} %pad_maximum_fusion.same), channel_id=1, source_target_pairs={{0,1},{1,0},{2,3},{3,2},{4,5},{5,4},{6,7},{7,6},{8,9},{9,8},{10,11... | collective-permute-start | bytes 1572872 | tf_op jit(solution)/shard_map/ppermute | solution.py:476
  77.6 43.5 %copy-start.5 = (bf16[256,2048]{1,0:T(8,128)(2,1)}, bf16[256,2048]{1,0:T(8,128)(2,1)S(1)}, u32[]{:S(2)}) copy-start(bf16[256,2048]{1,0:T(8,128)(2,1)S(1)} %collective-permute-done.10.refs_2_.refs_9_) | copy-start | bytes 3145732
  77.6 44.0 %collective-permute-start.12 = (bf16[256,2048]{1,0:T(8,128)(2,1)S(1)}, bf16[256,2048]{1,0:T(8,128)(2,1)}, u32[]{:S(2)}, u32[]{:S(2)}) collective-permute-start(bf16[256,2048]{1,0:T(8,128)(2,1)S(1)} %collective-permute-done.10.refs_2_.refs_9_), channel_id=1, source_target_pairs={{0,2},{2,4},{4,6},{6,0},{1,3},{3,5},{5,7},{7,1},{8,10},{10,12},{12... | collective-permute-start | bytes 3145736 | tf_op jit(solution)/shard_map/ppermute | solution.py:472
  86.3 17.9 %copy-start.2 = (bf16[16,256,256]{2,1,0:T(8,128)(2,1)}, bf16[16,256,256]{2,1,0:T(8,128)(2,1)S(1)}, u32[]{:S(2)}) copy-start(bf16[16,256,256]{2,1,0:T(8,128)(2,1)S(1)} %all-to-all-done.1) | copy-start | bytes 6291460
  115.3 5.7 %copy-start.4 = (bf16[256,2048]{1,0:T(8,128)(2,1)S(1)}, bf16[256,2048]{1,0:T(8,128)(2,1)}, u32[]{:S(2)}) copy-start(bf16[256,2048]{1,0:T(8,128)(2,1)} %refs_8_.1) | copy-start | bytes 3145732
  115.4 23.4 %all-to-all-start.3 = ((bf16[8,320,256]{2,1,0:T(8,128)(2,1)}), bf16[8,320,256]{2,1,0:T(8,128)(2,1)S(1)}, u32[]{:S(2)}, u32[]{:S(2)}) async-start(bf16[8,320,256]{2,1,0:T(8,128)(2,1)} %attend.2), calls=%async_computation.3 | async-start | bytes 2621440 | tf_op jit(solution)/shard_map/all_to_all | solution.py:463
  121.0 2.7 %collective-permute-start.13 = (bf16[256,2048]{1,0:T(8,128)(2,1)S(1)}, bf16[256,2048]{1,0:T(8,128)(2,1)S(1)}, u32[]{:S(2)}, u32[]{:S(2)}) collective-permute-start(bf16[256,2048]{1,0:T(8,128)(2,1)S(1)} %copy-done.4), channel_id=1, source_target_pairs={{0,1},{1,0},{2,3},{3,2},{4,5},{5,4},{6,7},{7,6},{8,9},{9,8},{10,11... | collective-permute-start | bytes 3145736 | tf_op jit(solution)/shard_map/ppermute | solution.py:476
  121.1 4.1 %collective-permute-start.14 = (bf16[256,2048]{1,0:T(8,128)(2,1)S(1)}, bf16[256,2048]{1,0:T(8,128)(2,1)S(1)}, u32[]{:S(2)}, u32[]{:S(2)}) collective-permute-start(bf16[256,2048]{1,0:T(8,128)(2,1)S(1)} %collective-permute-done.10.refs_2_.refs_9_), channel_id=1, source_target_pairs={{0,1},{1,0},{2,3},{3,2},{4,5},{5,4},{6,7},{7,6},{8,9},{9,8},{10,11... | collective-permute-start | bytes 3145736 | tf_op jit(solution)/shard_map/ppermute | solution.py:476
  121.5 5.2 %collective-permute-start.15 = (bf16[256,2048]{1,0:T(8,128)(2,1)}, bf16[256,2048]{1,0:T(8,128)(2,1)S(1)}, u32[]{:S(2)}, u32[]{:S(2)}) collective-permute-start(bf16[256,2048]{1,0:T(8,128)(2,1)} %collective-permute-done.11.refs_3_.refs_10_), channel_id=1, source_target_pairs={{0,1},{1,0},{2,3},{3,2},{4,5},{5,4},{6,7},{7,6},{8,9},{9,8},{10,11... | collective-permute-start | bytes 3145736 | tf_op jit(solution)/shard_map/ppermute | solution.py:476
  121.6 6.7 %collective-permute-start.16 = (bf16[256,2048]{1,0:T(8,128)(2,1)}, bf16[256,2048]{1,0:T(8,128)(2,1)}, u32[]{:S(2)}, u32[]{:S(2)}) collective-permute-start(bf16[256,2048]{1,0:T(8,128)(2,1)} %collective-permute-done.12.refs_4_.refs_11_), channel_id=1, source_target_pairs={{0,1},{1,0},{2,3},{3,2},{4,5},{5,4},{6,7},{7,6},{8,9},{9,8},{10,11... | collective-permute-start | bytes 3145736 | tf_op jit(solution)/shard_map/ppermute | solution.py:476
  123.7 3.0 %copy-start.6 = (bf16[256,2048]{1,0:T(8,128)(2,1)}, bf16[256,2048]{1,0:T(8,128)(2,1)S(1)}, u32[]{:S(2)}) copy-start(bf16[256,2048]{1,0:T(8,128)(2,1)S(1)} %collective-permute-done.13.refs_5_.refs_12_) | copy-start | bytes 3145732
  148.2 54.9 %all-to-all-start.4 = ((bf16[8,320,256]{2,1,0:T(8,128)(2,1)}), bf16[8,320,256]{2,1,0:T(8,128)(2,1)S(1)}, u32[]{:S(2)}, u32[]{:S(2)}) async-start(bf16[8,320,256]{2,1,0:T(8,128)(2,1)} %project_out.2), calls=%async_computation.4 | async-start | bytes 2621440 | tf_op jit(solution)/shard_map/all_to_all | solution.py:463
  160.3 12.2 %collective-permute-start.17 = (bf16[192,256]{1,0:T(8,128)(2,1)}, bf16[192,256]{1,0:T(8,128)(2,1)S(1)}, u32[]{:S(2)}, u32[]{:S(2)}) collective-permute-start(bf16[192,256]{1,0:T(8,128)(2,1)} %get-tuple-element.86), channel_id=1, source_target_pairs={{0,2},{1,3},{2,4},{3,5},{4,6},{5,7},{6,0},{7,1},{8,10},{9,11},{10,... | collective-permute-start | bytes 294920 | tf_op jit(solution)/shard_map/ppermute | solution.py:513
  161.7 12.6 %collective-permute-start.18 = (bf16[192,256]{1,0:T(8,128)(2,1)}, bf16[192,256]{1,0:T(8,128)(2,1)S(1)}, u32[]{:S(2)}, u32[]{:S(2)}) collective-permute-start(bf16[192,256]{1,0:T(8,128)(2,1)} %get-tuple-element.87), channel_id=1, source_target_pairs={{0,6},{1,7},{2,0},{3,1},{4,2},{5,3},{6,4},{7,5},{8,14},{9,15},{10,... | collective-permute-start | bytes 294920 | tf_op jit(solution)/shard_map/ppermute | solution.py:513
  163.0 12.8 %collective-permute-start.19 = (bf16[192,256]{1,0:T(8,128)(2,1)}, bf16[192,256]{1,0:T(8,128)(2,1)S(1)}, u32[]{:S(2)}, u32[]{:S(2)}) collective-permute-start(bf16[192,256]{1,0:T(8,128)(2,1)} %get-tuple-element.88), channel_id=1, source_target_pairs={{0,4},{1,5},{2,6},{3,7},{4,0},{5,1},{6,2},{7,3},{8,12},{9,13},{10,... | collective-permute-start | bytes 294920 | tf_op jit(solution)/shard_map/ppermute | solution.py:513
  164.7 11.1 %collective-permute-start.20 = (bf16[192,256]{1,0:T(8,128)(2,1)}, bf16[192,256]{1,0:T(8,128)(2,1)S(1)}, u32[]{:S(2)}, u32[]{:S(2)}) collective-permute-start(bf16[192,256]{1,0:T(8,128)(2,1)} %get-tuple-element.89), channel_id=1, source_target_pairs={{0,1},{1,0},{2,3},{3,2},{4,5},{5,4},{6,7},{7,6},{8,9},{9,8},{10,11... | collective-permute-start | bytes 294920 | tf_op jit(solution)/shard_map/ppermute | solution.py:513
  165.9 10.8 %collective-permute-start.21 = (bf16[192,256]{1,0:T(8,128)(2,1)}, bf16[192,256]{1,0:T(8,128)(2,1)S(1)}, u32[]{:S(2)}, u32[]{:S(2)}) collective-permute-start(bf16[192,256]{1,0:T(8,128)(2,1)} %get-tuple-element.90), channel_id=1, source_target_pairs={{0,3},{1,2},{2,5},{3,4},{4,7},{5,6},{6,1},{7,0},{8,11},{9,10},{10,... | collective-permute-start | bytes 294920 | tf_op jit(solution)/shard_map/ppermute | solution.py:513
  172.4 8.6 %copy-start.9 = (bf16[192,256]{1,0:T(8,128)(2,1)}, bf16[192,256]{1,0:T(8,128)(2,1)S(1)}, u32[]{:S(2)}) copy-start(bf16[192,256]{1,0:T(8,128)(2,1)S(1)} %collective-permute-done.17.refs_1_) | copy-start | bytes 294916
  172.4 4.3 %collective-permute-start.22 = (bf16[192,256]{1,0:T(8,128)(2,1)}, bf16[192,256]{1,0:T(8,128)(2,1)S(1)}, u32[]{:S(2)}, u32[]{:S(2)}) collective-permute-start(bf16[192,256]{1,0:T(8,128)(2,1)} %get-tuple-element.91), channel_id=1, source_target_pairs={{0,7},{1,6},{2,1},{3,0},{4,3},{5,2},{6,5},{7,4},{8,15},{9,14},{10,... | collective-permute-start | bytes 294920 | tf_op jit(solution)/shard_map/ppermute | solution.py:513
  174.3 6.8 %copy-start.10 = (bf16[192,256]{1,0:T(8,128)(2,1)}, bf16[192,256]{1,0:T(8,128)(2,1)S(1)}, u32[]{:S(2)}) copy-start(bf16[192,256]{1,0:T(8,128)(2,1)S(1)} %collective-permute-done.18.refs_2_) | copy-start | bytes 294916
  174.3 6.8 %collective-permute-start.23 = (bf16[192,256]{1,0:T(8,128)(2,1)}, bf16[192,256]{1,0:T(8,128)(2,1)S(1)}, u32[]{:S(2)}, u32[]{:S(2)}) collective-permute-start(bf16[192,256]{1,0:T(8,128)(2,1)} %get-tuple-element.92), channel_id=1, source_target_pairs={{0,5},{1,4},{2,7},{3,6},{4,1},{5,0},{6,3},{7,2},{8,13},{9,12},{10,... | collective-permute-start | bytes 294920 | tf_op jit(solution)/shard_map/ppermute | solution.py:513
  175.8 5.3 %copy-start.11 = (bf16[192,256]{1,0:T(8,128)(2,1)}, bf16[192,256]{1,0:T(8,128)(2,1)S(1)}, u32[]{:S(2)}) copy-start(bf16[192,256]{1,0:T(8,128)(2,1)S(1)} %collective-permute-done.19.refs_3_) | copy-start | bytes 294916
  175.8 5.2 %copy-start.12 = (bf16[192,256]{1,0:T(8,128)(2,1)}, bf16[192,256]{1,0:T(8,128)(2,1)S(1)}, u32[]{:S(2)}) copy-start(bf16[192,256]{1,0:T(8,128)(2,1)S(1)} %collective-permute-done.20.refs_4_) | copy-start | bytes 294916
  176.7 4.4 %copy-start.13 = (bf16[192,256]{1,0:T(8,128)(2,1)}, bf16[192,256]{1,0:T(8,128)(2,1)S(1)}, u32[]{:S(2)}) copy-start(bf16[192,256]{1,0:T(8,128)(2,1)S(1)} %collective-permute-done.21.refs_5_) | copy-start | bytes 294916
  176.7 4.4 %copy-start.14 = (bf16[192,256]{1,0:T(8,128)(2,1)}, bf16[192,256]{1,0:T(8,128)(2,1)S(1)}, u32[]{:S(2)}) copy-start(bf16[192,256]{1,0:T(8,128)(2,1)S(1)} %collective-permute-done.22.refs_6_) | copy-start | bytes 294916
  181.7 21.3 %copy-start.1 = (s32[8]{0:T(128)S(1)}, s32[8]{0:T(128)}, u32[]{:S(2)}) copy-start(s32[8]{0:T(128)} %pad_add_fusion.3.order) | copy-start | bytes 100
  188.6 5.7 %collective-permute-start.24 = (bf16[192,256]{1,0:T(8,128)(2,1)}, bf16[192,256]{1,0:T(8,128)(2,1)S(1)}, u32[]{:S(2)}, u32[]{:S(2)}) collective-permute-start(bf16[192,256]{1,0:T(8,128)(2,1)} %get-tuple-element.102), channel_id=1, source_target_pairs={{0,2},{1,3},{2,4},{3,5},{4,6},{5,7},{6,0},{7,1},{8,10},{9,11},{10,... | collective-permute-start | bytes 294920 | tf_op jit(solution)/shard_map/ppermute | solution.py:513
  189.9 6.4 %collective-permute-start.25 = (bf16[192,256]{1,0:T(8,128)(2,1)}, bf16[192,256]{1,0:T(8,128)(2,1)S(1)}, u32[]{:S(2)}, u32[]{:S(2)}) collective-permute-start(bf16[192,256]{1,0:T(8,128)(2,1)} %get-tuple-element.103), channel_id=1, source_target_pairs={{0,6},{1,7},{2,0},{3,1},{4,2},{5,3},{6,4},{7,5},{8,14},{9,15},{10,... | collective-permute-start | bytes 294920 | tf_op jit(solution)/shard_map/ppermute | solution.py:513
  191.3 7.4 %collective-permute-start.26 = (bf16[192,256]{1,0:T(8,128)(2,1)}, bf16[192,256]{1,0:T(8,128)(2,1)S(1)}, u32[]{:S(2)}, u32[]{:S(2)}) collective-permute-start(bf16[192,256]{1,0:T(8,128)(2,1)} %get-tuple-element.104), channel_id=1, source_target_pairs={{0,4},{1,5},{2,6},{3,7},{4,0},{5,1},{6,2},{7,3},{8,12},{9,13},{10,... | collective-permute-start | bytes 294920 | tf_op jit(solution)/shard_map/ppermute | solution.py:513
  191.9 6.8 %collective-permute-start.27 = (bf16[192,256]{1,0:T(8,128)(2,1)}, bf16[192,256]{1,0:T(8,128)(2,1)S(1)}, u32[]{:S(2)}, u32[]{:S(2)}) collective-permute-start(bf16[192,256]{1,0:T(8,128)(2,1)} %get-tuple-element.105), channel_id=1, source_target_pairs={{0,1},{1,0},{2,3},{3,2},{4,5},{5,4},{6,7},{7,6},{8,9},{9,8},{10,11... | collective-permute-start | bytes 294920 | tf_op jit(solution)/shard_map/ppermute | solution.py:513
  193.3 6.9 %collective-permute-start.28 = (bf16[192,256]{1,0:T(8,128)(2,1)}, bf16[192,256]{1,0:T(8,128)(2,1)S(1)}, u32[]{:S(2)}, u32[]{:S(2)}) collective-permute-start(bf16[192,256]{1,0:T(8,128)(2,1)} %get-tuple-element.106), channel_id=1, source_target_pairs={{0,3},{1,2},{2,5},{3,4},{4,7},{5,6},{6,1},{7,0},{8,11},{9,10},{10,... | collective-permute-start | bytes 294920 | tf_op jit(solution)/shard_map/ppermute | solution.py:513
  194.3 5.9 %collective-permute-start.29 = (bf16[192,256]{1,0:T(8,128)(2,1)}, bf16[192,256]{1,0:T(8,128)(2,1)S(1)}, u32[]{:S(2)}, u32[]{:S(2)}) collective-permute-start(bf16[192,256]{1,0:T(8,128)(2,1)} %get-tuple-element.107), channel_id=1, source_target_pairs={{0,7},{1,6},{2,1},{3,0},{4,3},{5,2},{6,5},{7,4},{8,15},{9,14},{10,... | collective-permute-start | bytes 294920 | tf_op jit(solution)/shard_map/ppermute | solution.py:513
  196.2 6.8 %collective-permute-start.30 = (bf16[192,256]{1,0:T(8,128)(2,1)}, bf16[192,256]{1,0:T(8,128)(2,1)S(1)}, u32[]{:S(2)}, u32[]{:S(2)}) collective-permute-start(bf16[192,256]{1,0:T(8,128)(2,1)} %get-tuple-element.108), channel_id=1, source_target_pairs={{0,5},{1,4},{2,7},{3,6},{4,1},{5,0},{6,3},{7,2},{8,13},{9,12},{10,... | collective-permute-start | bytes 294920 | tf_op jit(solution)/shard_map/ppermute | solution.py:513
  (5 other events, 5.2 us)

commit v6 on v5

--- a/solution.py
+++ b/solution.py
@@ -12,7 +12,7 @@
 BLOCK = 64
 HOT = 8
 REACH = 2
-FIRST_BLOCKS = 5
+FIRST_BLOCKS = 4
 KV = ("kv_0", "kv_1")
 TP = ("tp_0", "tp_1")
 WIDTH = 256
@@ -29,31 +29,34 @@
     return (values * factor * gain_row).astype(bf16)
 
 
-def share_kernel(rank, tok, out):
+def share_kernel(rank, tok, *outs):
     rows = tok[...].astype(f32)
-    devices = out.shape[0]
+    side, small, _ = outs[0].shape
+    devices = len(outs) * side
     part = BLOCK // devices
-    for k in range(out.shape[1] // 16):
+    for k in range(small // 16):
         parts = []
         for b in range(16 // part):
             first = (k * (16 // part) + b) * BLOCK
             parts.append(rows[first : first + BLOCK].reshape(devices, part, WIDTH))
-        out[:, k * 16 : (k + 1) * 16, :] = jnp.concatenate(parts, axis=1).astype(bf16)
-
-
-def token_shares(rank, tokens, devices):
+        joined = jnp.concatenate(parts, axis=1).astype(bf16)
+        for n, out in enumerate(outs):
+            out[:, k * 16 : (k + 1) * 16, :] = joined[n * side : (n + 1) * side]
+
+
+def token_shares(rank, tokens, long, side):
     length = tokens.shape[0]
+    devices = long * side
     tile = 1024
-    small = tile // devices
     return pl.pallas_call(
         share_kernel,
         grid_spec=pltpu.PrefetchScalarGridSpec(
             num_scalar_prefetch=1,
             grid=(length // tile,),
             in_specs=[pl.BlockSpec((tile, WIDTH), lambda i, rank: (i, rank[0]))],
-            out_specs=pl.BlockSpec((devices, small, WIDTH), lambda i, rank: (0, i, 0)),
-        ),
-        out_shape=jax.ShapeDtypeStruct((devices, length // devices, WIDTH), bf16),
+            out_specs=[pl.BlockSpec((side, tile // devices, WIDTH), lambda i, rank: (0, i, 0))] * long,
+        ),
+        out_shape=[jax.ShapeDtypeStruct((side, length // devices, WIDTH), bf16)] * long,
         compiler_params=pltpu.CompilerParams(vmem_limit_bytes=VMEM_LIMIT),
         cost_estimate=pl.CostEstimate(flops=1 << 20, bytes_accessed=4 << 20, transcendentals=0),
         name="token_shares",
@@ -476,12 +479,11 @@
     return lax.ppermute(piece, TP[1], [(0, 1), (1, 0)])
 
 
-def turned(blocks, here, step, axis):
-    size = lax.axis_size(axis)
-    mine = lax.dynamic_index_in_dim(blocks, (here + step) % size, 0, keepdims=False)
-    if step == 0:
-        return mine
-    return lax.ppermute(mine, axis, [(i, (i + step) % size) for i in range(size)])
+def chosen_of(options, index):
+    result = options[0]
+    for n, option in enumerate(options[1:], 1):
+        result = jnp.where(index == n, option, result)
+    return result
 
 
 def both_cores(parts):
@@ -524,9 +526,11 @@
     query_row = (query_gain * (HEAD_DIM ** (-0.5) * LOG2E))[None, :]
 
     rank = lax.axis_index(TP).astype(jnp.int32).reshape(1)
-    shares = token_shares(rank, tokens, devices)
-    chosen, shares = tied(chosen, shares)
-    shares = exchange(shares, KV)[0]
+    long, side = lax.axis_size(KV[0]), lax.axis_size(KV[1])
+    z, x = lax.axis_index(KV[0]), lax.axis_index(KV[1])
+    columns = token_shares(rank, tokens, long, side)
+    chosen, *columns = tied(chosen, *columns)
+    columns = columns[:1] + [lax.ppermute(columns[n], KV, [(0, n * side)]) for n in range(1, long)]
 
     usable = chosen >= 0
     pick = jnp.where(usable, chosen, 0)
@@ -547,33 +551,27 @@
     toward = piece_order(-1)
     same_order = jnp.arange(ranks, dtype=jnp.int32)
 
-    long, side = lax.axis_size(KV[0]), lax.axis_size(KV[1])
-    z, x = lax.axis_index(KV[0]), lax.axis_index(KV[1])
-    by_row = requests.reshape(long, side, -1)
-    rows_in = [turned(by_row, z, step, KV[0]) for step in range(long)]
-    by_side = jnp.stack(rows_in, axis=1)
-    sides_in = [turned(by_side, x, step, KV[1]) for step in range(side)]
+    asked = exchange(requests, KV)
     pairs = project_kv(tokens, w_key, w_value, key_row).reshape(-1, WIDTH)
-    pairs, *sides_in = tied(pairs, *sides_in)
-    asked = jnp.stack(sides_in, axis=1).reshape(devices, -1)
-    sources = jnp.stack(
-        [((z + long - s) % long) * side + (x + side - t) % side for s in range(long) for t in range(side)]
-    )
-    wheres = sources[None, :] == jnp.arange(devices, dtype=jnp.int32)[:, None]
-    asked = jnp.sum(jnp.where(wheres[:, :, None], asked[None], 0), axis=1).astype(jnp.int32)
     asked_near = asked[:, :REACH].reshape(-1)
     asked_hot = asked[:, HOT:].reshape(-1)
 
     sent = gather_near(asked_near, pairs)
-    sent, shares = tied(sent, shares)
+    sent, *columns = tied(sent, *columns)
+    held = [chosen_of([c[n] for c in columns], z) for n in range(side)]
+    starts = range(0, devices, side)
+    held = held[:1] + [
+        lax.ppermute(held[n], KV, [(i, i + n) for i in starts]) for n in range(1, side)
+    ]
     near = exchange(sent.reshape(devices, -1, WIDTH), KV).reshape(-1, WIDTH)
+    again, sent = tied(tokens, sent)
+    queries = project_q(again, w_query, query_row)
+    queries, *held = tied(queries, *held)
+    shares = chosen_of(held, x)
     parts = [shares] + [along_y(shares, shift) for shift in (1, -1, 2)]
     w_after = along_y(w_out, 1)
     w_before = along_y(w_out, -1)
     w_own = across(w_out)
-    again, sent = tied(tokens, sent)
-    queries = project_q(again, w_query, query_row)
-    queries, *parts = tied(queries, *parts)
     rows_same, rows_other = both_cores(parts)
     sent_hot = project_sent(
         asked_hot, order, rows_same, rows_other, w_key, w_value, key_row, devices

time: 207 us -> 203 us (0.981)
  blocking collectives: 17.9 us -> 0 us
  waiting for transfers between devices: 32.7 us -> 47.5 us
    all_to_all x1 -> x0, blocking collectives: 17.9 us -> none  [exchange(): return lax.all_to_all(pieces, axes, split_axis=0, concat_axis=0, tiled=True)]
    ppermute x6, waiting for transfers between devices: 0.02 us -> 14.2 us  [along_y(): lax.ppermute(piece, TP[0], [(i, (i + shift) % ring) for i in range(ring)])]
    all_to_all x4 -> x5, starting transfers between devices: 22.7 us -> 28.5 us  [exchange(): return lax.all_to_all(pieces, axes, split_axis=0, concat_axis=0, tiled=True)]
    all_to_all x4 -> x5, waiting for transfers between devices: 10.4 us -> 16.2 us  [exchange(): return lax.all_to_all(pieces, axes, split_axis=0, concat_axis=0, tiled=True)]
    ppermute x5, waiting for transfers between devices: 5.32 us -> 0.01 us  [across(): return lax.ppermute(piece, TP[1], [(0, 1), (1, 0)])]
    ppermute x6, starting transfers between devices: 15.9 us -> 10.7 us  [the longest x3 6.81 us: local(): lax.ppermute(columns[n], KV, [(0, n * side)])]
  transfers between devices with their start and end apart: 35 -> 36, of which waited for: 11 -> 14; matrix products, arithmetic and copies ran while one was open for 4% -> 4% of each run, Pallas kernels for 30% -> 31%
where the time goes in v6:
time: 203 us; the launch traced here: 202 us
  Pallas kernels  72.3 us (36%)
  starting transfers between devices  69 us (34%)
  waiting for transfers between devices  47.5 us (23%)
  local copies, waits for them, and re-layouts  7.96 us (4%)
  other arithmetic  4.96 us (2%)
    all_to_all x5, starting transfers between devices, exchange(): return lax.all_to_all(pieces, axes, split_axis=0, concat_axis=0, tiled=True)  28.5 us
    ppermute x14, starting transfers between devices, send_pieces(): got.append(lax.ppermute(pieces[k], TP, pairs) if k else pieces[0])  18.6 us
    pallas_call x2, Pallas kernels, attend(): pl.pallas_call(functools.partial(attention_kernel, first), grid_spec=pltp...  18.5 us
    ppermute x14, waiting for transfers between devices, send_pieces(): got.append(lax.ppermute(pieces[k], TP, pairs) if k else pieces[0])  17 us
    all_to_all x5, waiting for transfers between devices, exchange(): return lax.all_to_all(pieces, axes, split_axis=0, concat_axis=0, tiled=True)  16.2 us
    pallas_call x2, Pallas kernels, project_out(): pl.pallas_call(out_kernel, grid_spec=pltpu.PrefetchScalarGridSpec(num_sca...  15.1 us
    ppermute x6, waiting for transfers between devices, along_y(): lax.ppermute(piece, TP[0], [(i, (i + shift) % ring) for i in range(ring)])  14.2 us
    pallas_call x1, Pallas kernels, project_kv(): pl.pallas_call(kv_kernel, grid=(length // tile,), in_specs=[pl.BlockSpec(...  13.7 us
  transfers between devices with their start and end apart: 36, of which 14 were waited for; matrix products, arithmetic and copies ran while one was open for 4% of the time, Pallas kernels for 31%

profile of v6, /device:TPU:1, one launch (start us, length us, event | category | flops | bytes accessed | tf_op | source)
XLA Modules:
  0.0 202.3 jit_solution(9712957642016217082)
XLA Ops:
  0.0 2.1 %collective-permute-start.10 = (bf16[256,2048]{1,0:T(8,128)(2,1)}, bf16[256,2048]{1,0:T(8,128)(2,1)}, u32[]{:S(2)}, u32[]{:S(2)}) collective-permute-start(bf16[256,2048]{1,0:T(8,128)(2,1)} %refs_8_.1), channel_id=1, source_target_pairs={{0,2},{2,4},{4,6},{6,0},{1,3},{3,5},{5,7},{7,1},{8,10},{10,12},{12... | collective-permute-start | bytes 3145736 | tf_op jit(solution)/shard_map/ppermute | solution.py:475
  2.1 1.4 collective-permute-start.11
  3.6 4.0 %token_shares.1 = (bf16[4,256,256]{2,1,0:T(8,128)(2,1)}, bf16[4,256,256]{2,1,0:T(8,128)(2,1)}, bf16[4,256,256]{2,1,0:T(8,128)(2,1)}, bf16[4,256,256]{2,1,0:T(8,128)(2,1)}) custom-call(s32[1]{0:T(128)} %bitcast.rank, bf16[4096,2048]{1,0:T(8,128)(2,1)} %tok.4), custom_call_target="tpu_custom_call" | custom-call | flops 1048576 | bytes 4194304 | tf_op jit(solution)/shard_map/token_shares/pallas_call | solution.py:51
  9.4 7.6 %all-to-all-start = ((s32[16,1,16]{2,1,0:T(1,128)}), s32[16,1,16]{2,1,0:T(1,128)S(1)}, u32[]{:S(2)}, u32[]{:S(2)}) async-start(s32[16,1,16]{2,1,0:T(1,128)} %bitcast.3), calls=%async_computation | async-start | bytes 16384 | tf_op jit(solution)/shard_map/all_to_all | solution.py:466
  17.0 3.3 %collective-permute-start = (bf16[4,256,256]{2,1,0:T(8,128)(2,1)}, bf16[4,256,256]{2,1,0:T(8,128)(2,1)S(1)}, u32[]{:S(2)}, u32[]{:S(2)}) collective-permute-start(bf16[4,256,256]{2,1,0:T(8,128)(2,1)} %get-tuple-element.68), channel_id=1, source_target_pairs={{0,32},{1,33},{2,34},{3,35},{4,36},{5,37},{6,38},{7,39}} | collective-permute-start | bytes 1572872 | tf_op jit(solution)/shard_map/ppermute | solution.py:533
  20.3 2.2 %collective-permute-start.1 = (bf16[4,256,256]{2,1,0:T(8,128)(2,1)}, bf16[4,256,256]{2,1,0:T(8,128)(2,1)S(1)}, u32[]{:S(2)}, u32[]{:S(2)}) collective-permute-start(bf16[4,256,256]{2,1,0:T(8,128)(2,1)} %get-tuple-element.69), channel_id=1, source_target_pairs={{0,64},{1,65},{2,66},{3,67},{4,68},{5,69},{6,70},{7,71}} | collective-permute-start | bytes 1572872 | tf_op jit(solution)/shard_map/ppermute | solution.py:533
  22.5 1.3 collective-permute-start.2
  24.5 13.7 %project_kv.1 = bf16[64,2,64,256]{3,2,1,0:T(8,128)(2,1)} custom-call(bf16[4096,2048]{1,0:T(8,128)(2,1)} %tok.4, bf16[2048,256]{1,0:T(8,128)(2,1)} %wk.3, bf16[2048,256]{1,0:T(8,128)(2,1)} %wv.3, f32[1,128]{1,0:T(1,128)} %bitcast.48), custom_call_target="tpu_custom_call" | custom-call | flops 8589934592 | bytes 16777216 | tf_op jit(solution)/shard_map/project_kv/pallas_call | solution.py:82
  38.9 4.3 %gather_near.1 = bf16[32,128,256]{2,1,0:T(8,128)(2,1)} custom-call(s32[32]{0:T(128)} %reshape.69.near, bf16[8192,256]{1,0:T(8,128)(2,1)} %bitcast.34), custom_call_target="tpu_custom_call" | custom-call | flops 1048576 | bytes 4194304 | tf_op jit(solution)/shard_map/gather_near/pallas_call | solution.py:150
  43.3 1.3 collective-permute-start.3
  44.7 1.3 collective-permute-start.4
  46.0 1.3 collective-permute-start.5
  47.3 3.7 %all-to-all-start.1 = ((bf16[16,256,256]{2,1,0:T(8,128)(2,1)}), bf16[16,256,256]{2,1,0:T(8,128)(2,1)S(1)}, u32[]{:S(2)}, u32[]{:S(2)}) async-start(bf16[16,256,256]{2,1,0:T(8,128)(2,1)} %bitcast.39), calls=%async_computation.1 | async-start | bytes 4194304 | tf_op jit(solution)/shard_map/all_to_all | solution.py:466
  51.0 10.1 %project_q.1.queries = bf16[4096,256]{1,0:T(8,128)(2,1)} custom-call(bf16[4096,2048]{1,0:T(8,128)(2,1)} %tok.4, bf16[2048,256]{1,0:T(8,128)(2,1)} %wq.1, f32[1,128]{1,0:T(1,128)} %multiply_bitcast_fusion.gain), custom_call_target="tpu_custom_call" | custom-call | flops 4294967296 | bytes 16777216 | tf_op jit(solution)/shard_map/project_q/pallas_call | solution.py:111
  61.2 2.7 %collective-permute-start.7 = (bf16[256,256]{1,0:T(8,128)(2,1)S(1)}, bf16[256,256]{1,0:T(8,128)(2,1)S(1)}, u32[]{:S(2)}, u32[]{:S(2)}) collective-permute-start(bf16[256,256]{1,0:T(8,128)(2,1)S(1)} %select_select_fusion), channel_id=1, source_target_pairs={{0,6},{2,0},{4,2},{6,4},{1,7},{3,1},{5,3},{7,5},{8,14},{10,8},{12,... | collective-permute-start | bytes 393224 | tf_op jit(solution)/shard_map/ppermute | solution.py:475
  64.4 2.1 %collective-permute-done.6 = bf16[256,256]{1,0:T(8,128)(2,1)S(1)} collective-permute-done((bf16[256,256]{1,0:T(8,128)(2,1)S(1)}, bf16[256,256]{1,0:T(8,128)(2,1)S(1)}, u32[]{:S(2)}, u32[]{:S(2)}) %collective-permute-start.6) | collective-permute-done | bytes 131104 | tf_op jit(solution)/shard_map/ppermute | solution.py:475
  67.2 3.4 %collective-permute-done.8 = bf16[256,256]{1,0:T(8,128)(2,1)S(1)} collective-permute-done((bf16[256,256]{1,0:T(8,128)(2,1)S(1)}, bf16[256,256]{1,0:T(8,128)(2,1)S(1)}, u32[]{:S(2)}, u32[]{:S(2)}) %collective-permute-start.8) | collective-permute-done | bytes 131104 | tf_op jit(solution)/shard_map/ppermute | solution.py:475
  70.7 2.6 %collective-permute-start.9 = (bf16[4,256,256]{2,1,0:T(8,128)(2,1)S(1)}, bf16[4,256,256]{2,1,0:T(8,128)(2,1)S(1)}, u32[]{:S(2)}, u32[]{:S(2)}) collective-permute-start(bf16[4,256,256]{2,1,0:T(8,128)(2,1)S(1)} %pad_maximum_fusion.same), channel_id=1, source_target_pairs={{0,1},{1,0},{2,3},{3,2},{4,5},{5,4},{6,7},{7,6},{8,9},{9,8},{10,11... | collective-permute-start | bytes 1572872 | tf_op jit(solution)/shard_map/ppermute | solution.py:479
  76.1 4.8 %project_sent.1 = bf16[16,64,256]{2,1,0:T(8,128)(2,1)} custom-call(s32[128]{0:T(128)} %reshape.68.asked, s32[8]{0:T(128)} %pad_add_fusion.1.order, bf16[4,256,256]{2,1,0:T(8,128)(2,1)} %copy-done.5, bf16[4,256,256]{2,1,0:T(8,128)(2,1)} %copy-done.7, bf16[2048,256]{1,0:T(8,128)(2,1)} %wk.3, bf16[2048,256]{1,0:T(8,128)(2,1)} %wv.3, f32[1,128]{1,0:T(1,128)} %bitcast.49), custom_call_target="tpu_custom_call" | custom-call | flops 536870912 | bytes 8388608 | tf_op jit(solution)/shard_map/project_sent/pallas_call | solution.py:210
  81.9 1.3 select_reduce_fusion
  84.5 6.9 %all-to-all-start.2 = ((bf16[16,64,256]{2,1,0:T(8,128)(2,1)}), bf16[16,64,256]{2,1,0:T(8,128)(2,1)S(1)}, u32[]{:S(2)}, u32[]{:S(2)}) async-start(bf16[16,64,256]{2,1,0:T(8,128)(2,1)} %project_sent.1), calls=%async_computation.2 | async-start | bytes 1048576 | tf_op jit(solution)/shard_map/all_to_all | solution.py:466
  92.3 8.0 %collective-permute-done.12.refs_4_.refs_11_ = bf16[256,2048]{1,0:T(8,128)(2,1)} collective-permute-done((bf16[256,2048]{1,0:T(8,128)(2,1)}, bf16[256,2048]{1,0:T(8,128)(2,1)}, u32[]{:S(2)}, u32[]{:S(2)}) %collective-permute-start.12) | collective-permute-done | bytes 1048608 | tf_op jit(solution)/shard_map/ppermute | solution.py:475
  101.2 1.3 all-to-all-done.2.hot
  103.3 10.1 %attend.2 = bf16[8,256,256]{2,1,0:T(8,128)(2,1)} custom-call(s32[512]{0:T(512)} %reshape.71.at, s32[8]{0:T(128)} %iota.15.where.slot, bf16[4096,256]{1,0:T(8,128)(2,1)} %project_q.1.queries, f32[64,512]{1,0:T(8,128)} %reshape.72.masks, bf16[8192,256]{1,0:T(8,128)(2,1)} %bitcast.35, bf16[4096,256]{1,0:T(8,128)(2,1)} %bitcast.37, bf16[16,64,256]{2,1,0:T(8,128)(2,1)} %copy-done.3), custom_call_target="tpu_custom_call" | custom-call | flops 2147483648 | bytes 10485760 | tf_op jit(solution)/shard_map/attend/pallas_call | solution.py:331
  113.3 5.9 %all-to-all-start.3 = ((bf16[8,256,256]{2,1,0:T(8,128)(2,1)}), bf16[8,256,256]{2,1,0:T(8,128)(2,1)S(1)}, u32[]{:S(2)}, u32[]{:S(2)}) async-start(bf16[8,256,256]{2,1,0:T(8,128)(2,1)} %attend.2), calls=%async_computation.3 | async-start | bytes 2097152 | tf_op jit(solution)/shard_map/all_to_all | solution.py:466
  119.2 14.9 %all-to-all-done.3.refs_0_ = bf16[8,256,256]{2,1,0:T(8,128)(2,1)S(1)} async-done(((bf16[8,256,256]{2,1,0:T(8,128)(2,1)}), bf16[8,256,256]{2,1,0:T(8,128)(2,1)S(1)}, u32[]{:S(2)}, u32[]{:S(2)}) %all-to-all-start.3) | async-done | bytes 1048608 | tf_op jit(solution)/shard_map/all_to_all | solution.py:466
  134.2 1.0 copy-done.4
  135.2 7.5 %project_out.2 = bf16[8,256,256]{2,1,0:T(8,128)(2,1)} custom-call(s32[8]{0:T(128)} %pad_add_fusion.1.order, s32[8]{0:T(128)} %iota.15.where.slot, bf16[8,256,256]{2,1,0:T(8,128)(2,1)} %copy-done.4, bf16[256,2048]{1,0:T(8,128)(2,1)} %refs_8_.1, bf16[256,2048]{1,0:T(8,128)(2,1)} %collective-permute-done.10.refs_2_.refs_9_, ...), custom_call_target="tpu_custom_call" | custom-call | flops 2147483648 | bytes 12582912 | tf_op jit(solution)/shard_map/project_out/pallas_call | solution.py:406
  142.6 4.4 %all-to-all-start.4 = ((bf16[8,256,256]{2,1,0:T(8,128)(2,1)}), bf16[8,256,256]{2,1,0:T(8,128)(2,1)S(1)}, u32[]{:S(2)}, u32[]{:S(2)}) async-start(bf16[8,256,256]{2,1,0:T(8,128)(2,1)} %project_out.2), calls=%async_computation.4 | async-start | bytes 2097152 | tf_op jit(solution)/shard_map/all_to_all | solution.py:466
  147.1 8.4 %attend.3 = (bf16[256,256]{1,0:T(8,128)(2,1)}, bf16[256,256]{1,0:T(8,128)(2,1)}, bf16[256,256]{1,0:T(8,128)(2,1)}, bf16[256,256]{1,0:T(8,128)(2,1)}, bf16[256,25...) custom-call(s32[512]{0:T(512)} %reshape.71.at, ...), custom_call_target="tpu_custom_call" | custom-call | flops 2147483648 | bytes 10485760 | tf_op jit(solution)/shard_map/attend/pallas_call | solution.py:331
  155.4 1.4 collective-permute-start.17
  156.9 1.3 collective-permute-start.18
  158.2 1.7 collective-permute-start.19
  159.9 1.2 collective-permute-start.20
  161.3 4.6 %collective-permute-done.17.refs_1_ = bf16[256,256]{1,0:T(8,128)(2,1)S(1)} collective-permute-done((bf16[256,256]{1,0:T(8,128)(2,1)}, bf16[256,256]{1,0:T(8,128)(2,1)S(1)}, u32[]{:S(2)}, u32[]{:S(2)}) %collective-permute-start.17) | collective-permute-done | bytes 131104 | tf_op jit(solution)/shard_map/ppermute | solution.py:515
  167.8 3.5 %collective-permute-done.21.refs_5_ = bf16[256,256]{1,0:T(8,128)(2,1)S(1)} collective-permute-done((bf16[256,256]{1,0:T(8,128)(2,1)}, bf16[256,256]{1,0:T(8,128)(2,1)S(1)}, u32[]{:S(2)}, u32[]{:S(2)}) %collective-permute-start.21) | collective-permute-done | bytes 131104 | tf_op jit(solution)/shard_map/ppermute | solution.py:515
  172.2 1.5 collective-permute-done.23.refs_7_
  174.3 7.6 %project_out.3 = (bf16[256,256]{1,0:T(8,128)(2,1)}, bf16[256,256]{1,0:T(8,128)(2,1)}, bf16[256,256]{1,0:T(8,128)(2,1)}, bf16[256,256]{1,0:T(8,128)(2,1)}, bf16[2...) custom-call(s32[8]{0:T(128)} %pad_add_fusion.1.order, ...), custom_call_target="tpu_custom_call" | custom-call | flops 2147483648 | bytes 12582912 | tf_op jit(solution)/shard_map/project_out/pallas_call | solution.py:406
  181.9 1.0 collective-permute-start.24
  182.9 2.7 %collective-permute-start.25 = (bf16[256,256]{1,0:T(8,128)(2,1)}, bf16[256,256]{1,0:T(8,128)(2,1)S(1)}, u32[]{:S(2)}, u32[]{:S(2)}) collective-permute-start(bf16[256,256]{1,0:T(8,128)(2,1)} %get-tuple-element.113), channel_id=1, source_target_pairs={{0,6},{1,7},{2,0},{3,1},{4,2},{5,3},{6,4},{7,5},{8,14},{9,15},{10,... | collective-permute-start | bytes 393224 | tf_op jit(solution)/shard_map/ppermute | solution.py:515
  185.6 1.1 collective-permute-start.26
  186.7 1.0 collective-permute-start.27
  187.7 1.0 collective-permute-start.28
  189.2 3.2 %collective-permute-start.29 = (bf16[256,256]{1,0:T(8,128)(2,1)}, bf16[256,256]{1,0:T(8,128)(2,1)S(1)}, u32[]{:S(2)}, u32[]{:S(2)}) collective-permute-start(bf16[256,256]{1,0:T(8,128)(2,1)} %get-tuple-element.117), channel_id=1, source_target_pairs={{0,7},{1,6},{2,1},{3,0},{4,3},{5,2},{6,5},{7,4},{8,15},{9,14},{10,... | collective-permute-start | bytes 393224 | tf_op jit(solution)/shard_map/ppermute | solution.py:515
  192.4 1.5 collective-permute-start.30
  193.9 2.5 %collective-permute-done.28.rest_5_ = bf16[256,256]{1,0:T(8,128)(2,1)S(1)} collective-permute-done((bf16[256,256]{1,0:T(8,128)(2,1)}, bf16[256,256]{1,0:T(8,128)(2,1)S(1)}, u32[]{:S(2)}, u32[]{:S(2)}) %collective-permute-start.28) | collective-permute-done | bytes 131104 | tf_op jit(solution)/shard_map/ppermute | solution.py:515
  196.4 2.9 %collective-permute-done.30.rest_7_ = bf16[256,256]{1,0:T(8,128)(2,1)S(1)} collective-permute-done((bf16[256,256]{1,0:T(8,128)(2,1)}, bf16[256,256]{1,0:T(8,128)(2,1)S(1)}, u32[]{:S(2)}, u32[]{:S(2)}) %collective-permute-start.30) | collective-permute-done | bytes 131104 | tf_op jit(solution)/shard_map/ppermute | solution.py:515
  200.2 1.9 place.1
  (100 shorter events, 17.3 us)
Async XLA Ops:
  0.0 74.0 %collective-permute-start.10 = (bf16[256,2048]{1,0:T(8,128)(2,1)}, bf16[256,2048]{1,0:T(8,128)(2,1)}, u32[]{:S(2)}, u32[]{:S(2)}) collective-permute-start(bf16[256,2048]{1,0:T(8,128)(2,1)} %refs_8_.1), channel_id=1, source_target_pairs={{0,2},{2,4},{4,6},{6,0},{1,3},{3,5},{5,7},{7,1},{8,10},{10,12},{12... | collective-permute-start | bytes 3145736 | tf_op jit(solution)/shard_map/ppermute | solution.py:475
  2.1 89.9 %collective-permute-start.11 = (bf16[256,2048]{1,0:T(8,128)(2,1)}, bf16[256,2048]{1,0:T(8,128)(2,1)}, u32[]{:S(2)}, u32[]{:S(2)}) collective-permute-start(bf16[256,2048]{1,0:T(8,128)(2,1)} %refs_8_.1), channel_id=1, source_target_pairs={{0,6},{2,0},{4,2},{6,4},{1,7},{3,1},{5,3},{7,5},{8,14},{10,8},{12,... | collective-permute-start | bytes 3145736 | tf_op jit(solution)/shard_map/ppermute | solution.py:475
  3.6 4.0 %copy-start.15 = (s32[64,8]{0,1:T(8,128)S(1)}, s32[64,8]{0,1:T(8,128)}, u32[]{:S(2)}) copy-start(s32[64,8]{0,1:T(8,128)} %param.17) | copy-start | bytes 6148
  3.6 20.3 %copy-start.16 = (f32[128]{0:T(128)S(1)}, f32[128]{0:T(128)}, u32[]{:S(2)}) copy-start(f32[128]{0:T(128)} %param.14) | copy-start | bytes 1540
  9.4 28.8 %all-to-all-start = ((s32[16,1,16]{2,1,0:T(1,128)}), s32[16,1,16]{2,1,0:T(1,128)S(1)}, u32[]{:S(2)}, u32[]{:S(2)}) async-start(s32[16,1,16]{2,1,0:T(1,128)} %bitcast.3), calls=%async_computation | async-start | bytes 16384 | tf_op jit(solution)/shard_map/all_to_all | solution.py:466
  17.0 26.2 %collective-permute-start = (bf16[4,256,256]{2,1,0:T(8,128)(2,1)}, bf16[4,256,256]{2,1,0:T(8,128)(2,1)S(1)}, u32[]{:S(2)}, u32[]{:S(2)}) collective-permute-start(bf16[4,256,256]{2,1,0:T(8,128)(2,1)} %get-tuple-element.68), channel_id=1, source_target_pairs={{0,32},{1,33},{2,34},{3,35},{4,36},{5,37},{6,38},{7,39}} | collective-permute-start | bytes 1572872 | tf_op jit(solution)/shard_map/ppermute | solution.py:533
  20.3 22.9 %collective-permute-start.1 = (bf16[4,256,256]{2,1,0:T(8,128)(2,1)}, bf16[4,256,256]{2,1,0:T(8,128)(2,1)S(1)}, u32[]{:S(2)}, u32[]{:S(2)}) collective-permute-start(bf16[4,256,256]{2,1,0:T(8,128)(2,1)} %get-tuple-element.69), channel_id=1, source_target_pairs={{0,64},{1,65},{2,66},{3,67},{4,68},{5,69},{6,70},{7,71}} | collective-permute-start | bytes 1572872 | tf_op jit(solution)/shard_map/ppermute | solution.py:533
  22.5 20.7 %collective-permute-start.2 = (bf16[4,256,256]{2,1,0:T(8,128)(2,1)}, bf16[4,256,256]{2,1,0:T(8,128)(2,1)S(1)}, u32[]{:S(2)}, u32[]{:S(2)}) collective-permute-start(bf16[4,256,256]{2,1,0:T(8,128)(2,1)} %get-tuple-element.70), channel_id=1, source_target_pairs={{0,96},{1,97},{2,98},{3,99},{4,100},{5,101},{6,102},{7,103}} | collective-permute-start | bytes 1572872 | tf_op jit(solution)/shard_map/ppermute | solution.py:533
  38.9 4.4 %copy-start.6 = (bf16[4,256,256]{2,1,0:T(8,128)(2,1)S(1)}, bf16[4,256,256]{2,1,0:T(8,128)(2,1)}, u32[]{:S(2)}) copy-start(bf16[4,256,256]{2,1,0:T(8,128)(2,1)} %get-tuple-element.76) | copy-start | bytes 1572868
  43.3 17.7 %collective-permute-start.3 = (bf16[256,256]{1,0:T(8,128)(2,1)S(1)}, bf16[256,256]{1,0:T(8,128)(2,1)S(1)}, u32[]{:S(2)}, u32[]{:S(2)}) collective-permute-start(bf16[256,256]{1,0:T(8,128)(2,1)S(1)} %get-tuple-element.125), channel_id=1, source_target_pairs={{0,8},{32,40},{64,72},{96,104},{1,9},{33,41},{65,73},{97,105},{2,1... | collective-permute-start | bytes 393224 | tf_op jit(solution)/shard_map/ppermute | solution.py:564
  44.7 16.4 %collective-permute-start.4 = (bf16[256,256]{1,0:T(8,128)(2,1)S(1)}, bf16[256,256]{1,0:T(8,128)(2,1)S(1)}, u32[]{:S(2)}, u32[]{:S(2)}) collective-permute-start(bf16[256,256]{1,0:T(8,128)(2,1)S(1)} %get-tuple-element.124), channel_id=1, source_target_pairs={{0,16},{32,48},{64,80},{96,112},{1,17},{33,49},{65,81},{97,113},{2... | collective-permute-start | bytes 393224 | tf_op jit(solution)/shard_map/ppermute | solution.py:564
  46.0 15.1 %collective-permute-start.5 = (bf16[256,256]{1,0:T(8,128)(2,1)S(1)}, bf16[256,256]{1,0:T(8,128)(2,1)S(1)}, u32[]{:S(2)}, u32[]{:S(2)}) collective-permute-start(bf16[256,256]{1,0:T(8,128)(2,1)S(1)} %get-tuple-element.123), channel_id=1, source_target_pairs={{0,24},{32,56},{64,88},{96,120},{1,25},{33,57},{65,89},{97,121},{2... | collective-permute-start | bytes 393224 | tf_op jit(solution)/shard_map/ppermute | solution.py:564
  47.3 37.2 %all-to-all-start.1 = ((bf16[16,256,256]{2,1,0:T(8,128)(2,1)}), bf16[16,256,256]{2,1,0:T(8,128)(2,1)S(1)}, u32[]{:S(2)}, u32[]{:S(2)}) async-start(bf16[16,256,256]{2,1,0:T(8,128)(2,1)} %bitcast.39), calls=%async_computation.1 | async-start | bytes 4194304 | tf_op jit(solution)/shard_map/all_to_all | solution.py:466
  61.1 5.4 %collective-permute-start.6 = (bf16[256,256]{1,0:T(8,128)(2,1)S(1)}, bf16[256,256]{1,0:T(8,128)(2,1)S(1)}, u32[]{:S(2)}, u32[]{:S(2)}) collective-permute-start(bf16[256,256]{1,0:T(8,128)(2,1)S(1)} %select_select_fusion), channel_id=1, source_target_pairs={{0,2},{2,4},{4,6},{6,0},{1,3},{3,5},{5,7},{7,1},{8,10},{10,12},{12... | collective-permute-start | bytes 393224 | tf_op jit(solution)/shard_map/ppermute | solution.py:475
  61.2 6.0 %collective-permute-start.7 = (bf16[256,256]{1,0:T(8,128)(2,1)S(1)}, bf16[256,256]{1,0:T(8,128)(2,1)S(1)}, u32[]{:S(2)}, u32[]{:S(2)}) collective-permute-start(bf16[256,256]{1,0:T(8,128)(2,1)S(1)} %select_select_fusion), channel_id=1, source_target_pairs={{0,6},{2,0},{4,2},{6,4},{1,7},{3,1},{5,3},{7,5},{8,14},{10,8},{12,... | collective-permute-start | bytes 393224 | tf_op jit(solution)/shard_map/ppermute | solution.py:475
  63.9 6.7 %collective-permute-start.8 = (bf16[256,256]{1,0:T(8,128)(2,1)S(1)}, bf16[256,256]{1,0:T(8,128)(2,1)S(1)}, u32[]{:S(2)}, u32[]{:S(2)}) collective-permute-start(bf16[256,256]{1,0:T(8,128)(2,1)S(1)} %select_select_fusion), channel_id=1, source_target_pairs={{0,4},{2,6},{4,0},{6,2},{1,5},{3,7},{5,1},{7,3},{8,12},{10,14},{12... | collective-permute-start | bytes 393224 | tf_op jit(solution)/shard_map/ppermute | solution.py:475
  70.7 4.6 %copy-start.5 = (bf16[4,256,256]{2,1,0:T(8,128)(2,1)}, bf16[4,256,256]{2,1,0:T(8,128)(2,1)S(1)}, u32[]{:S(2)}) copy-start(bf16[4,256,256]{2,1,0:T(8,128)(2,1)S(1)} %pad_maximum_fusion.same) | copy-start | bytes 1572868
  70.7 4.6 %collective-permute-start.9 = (bf16[4,256,256]{2,1,0:T(8,128)(2,1)S(1)}, bf16[4,256,256]{2,1,0:T(8,128)(2,1)S(1)}, u32[]{:S(2)}, u32[]{:S(2)}) collective-permute-start(bf16[4,256,256]{2,1,0:T(8,128)(2,1)S(1)} %pad_maximum_fusion.same), channel_id=1, source_target_pairs={{0,1},{1,0},{2,3},{3,2},{4,5},{5,4},{6,7},{7,6},{8,9},{9,8},{10,11... | collective-permute-start | bytes 1572872 | tf_op jit(solution)/shard_map/ppermute | solution.py:479
  74.0 26.3 %collective-permute-start.12 = (bf16[256,2048]{1,0:T(8,128)(2,1)}, bf16[256,2048]{1,0:T(8,128)(2,1)}, u32[]{:S(2)}, u32[]{:S(2)}) collective-permute-start(bf16[256,2048]{1,0:T(8,128)(2,1)} %collective-permute-done.10.refs_2_.refs_9_), channel_id=1, source_target_pairs={{0,2},{2,4},{4,6},{6,0},{1,3},{3,5},{5,7},{7,1},{8,10},{10,12},{12... | collective-permute-start | bytes 3145736 | tf_op jit(solution)/shard_map/ppermute | solution.py:475
  84.5 18.0 %copy-start.2 = (bf16[16,256,256]{2,1,0:T(8,128)(2,1)}, bf16[16,256,256]{2,1,0:T(8,128)(2,1)S(1)}, u32[]{:S(2)}) copy-start(bf16[16,256,256]{2,1,0:T(8,128)(2,1)S(1)} %all-to-all-done.1) | copy-start | bytes 6291460
  84.5 18.0 %all-to-all-start.2 = ((bf16[16,64,256]{2,1,0:T(8,128)(2,1)}), bf16[16,64,256]{2,1,0:T(8,128)(2,1)S(1)}, u32[]{:S(2)}, u32[]{:S(2)}) async-start(bf16[16,64,256]{2,1,0:T(8,128)(2,1)} %project_sent.1), calls=%async_computation.2 | async-start | bytes 1048576 | tf_op jit(solution)/shard_map/all_to_all | solution.py:466
  91.4 27.8 %collective-permute-start.13 = (bf16[256,2048]{1,0:T(8,128)(2,1)}, bf16[256,2048]{1,0:T(8,128)(2,1)}, u32[]{:S(2)}, u32[]{:S(2)}) collective-permute-start(bf16[256,2048]{1,0:T(8,128)(2,1)} %refs_8_.1), channel_id=1, source_target_pairs={{0,1},{1,0},{2,3},{3,2},{4,5},{5,4},{6,7},{7,6},{8,9},{9,8},{10,11... | collective-permute-start | bytes 3145736 | tf_op jit(solution)/shard_map/ppermute | solution.py:479
  91.8 27.4 %collective-permute-start.14 = (bf16[256,2048]{1,0:T(8,128)(2,1)}, bf16[256,2048]{1,0:T(8,128)(2,1)}, u32[]{:S(2)}, u32[]{:S(2)}) collective-permute-start(bf16[256,2048]{1,0:T(8,128)(2,1)} %collective-permute-done.10.refs_2_.refs_9_), channel_id=1, source_target_pairs={{0,1},{1,0},{2,3},{3,2},{4,5},{5,4},{6,7},{7,6},{8,9},{9,8},{10,11... | collective-permute-start | bytes 3145736 | tf_op jit(solution)/shard_map/ppermute | solution.py:479
  92.0 27.2 %collective-permute-start.15 = (bf16[256,2048]{1,0:T(8,128)(2,1)}, bf16[256,2048]{1,0:T(8,128)(2,1)}, u32[]{:S(2)}, u32[]{:S(2)}) collective-permute-start(bf16[256,2048]{1,0:T(8,128)(2,1)} %collective-permute-done.11.refs_3_.refs_10_), channel_id=1, source_target_pairs={{0,1},{1,0},{2,3},{3,2},{4,5},{5,4},{6,7},{7,6},{8,9},{9,8},{10,11... | collective-permute-start | bytes 3145736 | tf_op jit(solution)/shard_map/ppermute | solution.py:479
  100.3 18.9 %collective-permute-start.16 = (bf16[256,2048]{1,0:T(8,128)(2,1)}, bf16[256,2048]{1,0:T(8,128)(2,1)}, u32[]{:S(2)}, u32[]{:S(2)}) collective-permute-start(bf16[256,2048]{1,0:T(8,128)(2,1)} %collective-permute-done.12.refs_4_.refs_11_), channel_id=1, source_target_pairs={{0,1},{1,0},{2,3},{3,2},{4,5},{5,4},{6,7},{7,6},{8,9},{9,8},{10,11... | collective-permute-start | bytes 3145736 | tf_op jit(solution)/shard_map/ppermute | solution.py:479
  113.3 20.8 %all-to-all-start.3 = ((bf16[8,256,256]{2,1,0:T(8,128)(2,1)}), bf16[8,256,256]{2,1,0:T(8,128)(2,1)S(1)}, u32[]{:S(2)}, u32[]{:S(2)}) async-start(bf16[8,256,256]{2,1,0:T(8,128)(2,1)} %attend.2), calls=%async_computation.3 | async-start | bytes 2097152 | tf_op jit(solution)/shard_map/all_to_all | solution.py:466
  142.6 56.7 %all-to-all-start.4 = ((bf16[8,256,256]{2,1,0:T(8,128)(2,1)}), bf16[8,256,256]{2,1,0:T(8,128)(2,1)S(1)}, u32[]{:S(2)}, u32[]{:S(2)}) async-start(bf16[8,256,256]{2,1,0:T(8,128)(2,1)} %project_out.2), calls=%async_computation.4 | async-start | bytes 2097152 | tf_op jit(solution)/shard_map/all_to_all | solution.py:466
  155.4 10.4 %collective-permute-start.17 = (bf16[256,256]{1,0:T(8,128)(2,1)}, bf16[256,256]{1,0:T(8,128)(2,1)S(1)}, u32[]{:S(2)}, u32[]{:S(2)}) collective-permute-start(bf16[256,256]{1,0:T(8,128)(2,1)} %get-tuple-element.96), channel_id=1, source_target_pairs={{0,2},{1,3},{2,4},{3,5},{4,6},{5,7},{6,0},{7,1},{8,10},{9,11},{10,... | collective-permute-start | bytes 393224 | tf_op jit(solution)/shard_map/ppermute | solution.py:515
  156.9 9.7 %collective-permute-start.18 = (bf16[256,256]{1,0:T(8,128)(2,1)}, bf16[256,256]{1,0:T(8,128)(2,1)S(1)}, u32[]{:S(2)}, u32[]{:S(2)}) collective-permute-start(bf16[256,256]{1,0:T(8,128)(2,1)} %get-tuple-element.97), channel_id=1, source_target_pairs={{0,6},{1,7},{2,0},{3,1},{4,2},{5,3},{6,4},{7,5},{8,14},{9,15},{10,... | collective-permute-start | bytes 393224 | tf_op jit(solution)/shard_map/ppermute | solution.py:515
  158.2 9.6 %collective-permute-start.19 = (bf16[256,256]{1,0:T(8,128)(2,1)}, bf16[256,256]{1,0:T(8,128)(2,1)S(1)}, u32[]{:S(2)}, u32[]{:S(2)}) collective-permute-start(bf16[256,256]{1,0:T(8,128)(2,1)} %get-tuple-element.98), channel_id=1, source_target_pairs={{0,4},{1,5},{2,6},{3,7},{4,0},{5,1},{6,2},{7,3},{8,12},{9,13},{10,... | collective-permute-start | bytes 393224 | tf_op jit(solution)/shard_map/ppermute | solution.py:515
  159.9 7.9 %collective-permute-start.20 = (bf16[256,256]{1,0:T(8,128)(2,1)}, bf16[256,256]{1,0:T(8,128)(2,1)S(1)}, u32[]{:S(2)}, u32[]{:S(2)}) collective-permute-start(bf16[256,256]{1,0:T(8,128)(2,1)} %get-tuple-element.99), channel_id=1, source_target_pairs={{0,1},{1,0},{2,3},{3,2},{4,5},{5,4},{6,7},{7,6},{8,9},{9,8},{10,11... | collective-permute-start | bytes 393224 | tf_op jit(solution)/shard_map/ppermute | solution.py:515
  161.1 10.1 %collective-permute-start.21 = (bf16[256,256]{1,0:T(8,128)(2,1)}, bf16[256,256]{1,0:T(8,128)(2,1)S(1)}, u32[]{:S(2)}, u32[]{:S(2)}) collective-permute-start(bf16[256,256]{1,0:T(8,128)(2,1)} %get-tuple-element.100), channel_id=1, source_target_pairs={{0,3},{1,2},{2,5},{3,4},{4,7},{5,6},{6,1},{7,0},{8,11},{9,10},{10,... | collective-permute-start | bytes 393224 | tf_op jit(solution)/shard_map/ppermute | solution.py:515
  165.9 7.8 %copy-start.8 = (bf16[256,256]{1,0:T(8,128)(2,1)}, bf16[256,256]{1,0:T(8,128)(2,1)S(1)}, u32[]{:S(2)}) copy-start(bf16[256,256]{1,0:T(8,128)(2,1)S(1)} %collective-permute-done.17.refs_1_) | copy-start | bytes 393220
  165.9 6.3 %collective-permute-start.22 = (bf16[256,256]{1,0:T(8,128)(2,1)}, bf16[256,256]{1,0:T(8,128)(2,1)S(1)}, u32[]{:S(2)}, u32[]{:S(2)}) collective-permute-start(bf16[256,256]{1,0:T(8,128)(2,1)} %get-tuple-element.101), channel_id=1, source_target_pairs={{0,7},{1,6},{2,1},{3,0},{4,3},{5,2},{6,5},{7,4},{8,15},{9,14},{10,... | collective-permute-start | bytes 393224 | tf_op jit(solution)/shard_map/ppermute | solution.py:515
  166.6 7.0 %copy-start.9 = (bf16[256,256]{1,0:T(8,128)(2,1)}, bf16[256,256]{1,0:T(8,128)(2,1)S(1)}, u32[]{:S(2)}) copy-start(bf16[256,256]{1,0:T(8,128)(2,1)S(1)} %collective-permute-done.18.refs_2_) | copy-start | bytes 393220
  166.6 7.0 %collective-permute-start.23 = (bf16[256,256]{1,0:T(8,128)(2,1)}, bf16[256,256]{1,0:T(8,128)(2,1)S(1)}, u32[]{:S(2)}, u32[]{:S(2)}) collective-permute-start(bf16[256,256]{1,0:T(8,128)(2,1)} %get-tuple-element.102), channel_id=1, source_target_pairs={{0,5},{1,4},{2,7},{3,6},{4,1},{5,0},{6,3},{7,2},{8,13},{9,12},{10,... | collective-permute-start | bytes 393224 | tf_op jit(solution)/shard_map/ppermute | solution.py:515
  167.8 5.9 %copy-start.10 = (bf16[256,256]{1,0:T(8,128)(2,1)}, bf16[256,256]{1,0:T(8,128)(2,1)S(1)}, u32[]{:S(2)}) copy-start(bf16[256,256]{1,0:T(8,128)(2,1)S(1)} %collective-permute-done.19.refs_3_) | copy-start | bytes 393220
  167.8 5.9 %copy-start.11 = (bf16[256,256]{1,0:T(8,128)(2,1)}, bf16[256,256]{1,0:T(8,128)(2,1)S(1)}, u32[]{:S(2)}) copy-start(bf16[256,256]{1,0:T(8,128)(2,1)S(1)} %collective-permute-done.20.refs_4_) | copy-start | bytes 393220
  171.2 2.4 %copy-start.12 = (bf16[256,256]{1,0:T(8,128)(2,1)}, bf16[256,256]{1,0:T(8,128)(2,1)S(1)}, u32[]{:S(2)}) copy-start(bf16[256,256]{1,0:T(8,128)(2,1)S(1)} %collective-permute-done.21.refs_5_) | copy-start | bytes 393220
  172.2 1.5 copy-start.13
  174.3 25.0 %copy-start.1 = (s32[8]{0:T(128)S(1)}, s32[8]{0:T(128)}, u32[]{:S(2)}) copy-start(s32[8]{0:T(128)} %pad_add_fusion.1.order) | copy-start | bytes 100
  181.9 7.3 %collective-permute-start.24 = (bf16[256,256]{1,0:T(8,128)(2,1)}, bf16[256,256]{1,0:T(8,128)(2,1)S(1)}, u32[]{:S(2)}, u32[]{:S(2)}) collective-permute-start(bf16[256,256]{1,0:T(8,128)(2,1)} %get-tuple-element.112), channel_id=1, source_target_pairs={{0,2},{1,3},{2,4},{3,5},{4,6},{5,7},{6,0},{7,1},{8,10},{9,11},{10,... | collective-permute-start | bytes 393224 | tf_op jit(solution)/shard_map/ppermute | solution.py:515
  182.9 9.5 %collective-permute-start.25 = (bf16[256,256]{1,0:T(8,128)(2,1)}, bf16[256,256]{1,0:T(8,128)(2,1)S(1)}, u32[]{:S(2)}, u32[]{:S(2)}) collective-permute-start(bf16[256,256]{1,0:T(8,128)(2,1)} %get-tuple-element.113), channel_id=1, source_target_pairs={{0,6},{1,7},{2,0},{3,1},{4,2},{5,3},{6,4},{7,5},{8,14},{9,15},{10,... | collective-permute-start | bytes 393224 | tf_op jit(solution)/shard_map/ppermute | solution.py:515
  185.6 8.2 %collective-permute-start.26 = (bf16[256,256]{1,0:T(8,128)(2,1)}, bf16[256,256]{1,0:T(8,128)(2,1)S(1)}, u32[]{:S(2)}, u32[]{:S(2)}) collective-permute-start(bf16[256,256]{1,0:T(8,128)(2,1)} %get-tuple-element.114), channel_id=1, source_target_pairs={{0,4},{1,5},{2,6},{3,7},{4,0},{5,1},{6,2},{7,3},{8,12},{9,13},{10,... | collective-permute-start | bytes 393224 | tf_op jit(solution)/shard_map/ppermute | solution.py:515
  186.7 7.1 %collective-permute-start.27 = (bf16[256,256]{1,0:T(8,128)(2,1)}, bf16[256,256]{1,0:T(8,128)(2,1)S(1)}, u32[]{:S(2)}, u32[]{:S(2)}) collective-permute-start(bf16[256,256]{1,0:T(8,128)(2,1)} %get-tuple-element.115), channel_id=1, source_target_pairs={{0,1},{1,0},{2,3},{3,2},{4,5},{5,4},{6,7},{7,6},{8,9},{9,8},{10,11... | collective-permute-start | bytes 393224 | tf_op jit(solution)/shard_map/ppermute | solution.py:515
  187.7 8.7 %collective-permute-start.28 = (bf16[256,256]{1,0:T(8,128)(2,1)}, bf16[256,256]{1,0:T(8,128)(2,1)S(1)}, u32[]{:S(2)}, u32[]{:S(2)}) collective-permute-start(bf16[256,256]{1,0:T(8,128)(2,1)} %get-tuple-element.116), channel_id=1, source_target_pairs={{0,3},{1,2},{2,5},{3,4},{4,7},{5,6},{6,1},{7,0},{8,11},{9,10},{10,... | collective-permute-start | bytes 393224 | tf_op jit(solution)/shard_map/ppermute | solution.py:515
  189.2 7.1 %collective-permute-start.29 = (bf16[256,256]{1,0:T(8,128)(2,1)}, bf16[256,256]{1,0:T(8,128)(2,1)S(1)}, u32[]{:S(2)}, u32[]{:S(2)}) collective-permute-start(bf16[256,256]{1,0:T(8,128)(2,1)} %get-tuple-element.117), channel_id=1, source_target_pairs={{0,7},{1,6},{2,1},{3,0},{4,3},{5,2},{6,5},{7,4},{8,15},{9,14},{10,... | collective-permute-start | bytes 393224 | tf_op jit(solution)/shard_map/ppermute | solution.py:515
  192.4 6.9 %collective-permute-start.30 = (bf16[256,256]{1,0:T(8,128)(2,1)}, bf16[256,256]{1,0:T(8,128)(2,1)S(1)}, u32[]{:S(2)}, u32[]{:S(2)}) collective-permute-start(bf16[256,256]{1,0:T(8,128)(2,1)} %get-tuple-element.118), channel_id=1, source_target_pairs={{0,5},{1,4},{2,7},{3,6},{4,1},{5,0},{6,3},{7,2},{8,13},{9,12},{10,... | collective-permute-start | bytes 393224 | tf_op jit(solution)/shard_map/ppermute | solution.py:515
  (5 other events, 4.1 us)

commit v7 on v6

--- a/solution.py
+++ b/solution.py
@@ -570,7 +570,6 @@
     shares = chosen_of(held, x)
     parts = [shares] + [along_y(shares, shift) for shift in (1, -1, 2)]
     w_after = along_y(w_out, 1)
-    w_before = along_y(w_out, -1)
     w_own = across(w_out)
     rows_same, rows_other = both_cores(parts)
     sent_hot = project_sent(
@@ -589,21 +588,20 @@
     at = jnp.where(usable, at, 0).astype(jnp.int32).reshape(-1)
     mask = jnp.repeat(usable.astype(f32), BLOCK, axis=1)
 
-    at, mask, order, toward, same_order, sent_hot = tied(
-        at, mask, order, toward, same_order, sent_hot
-    )
+    order, toward, same_order, sent_hot = tied(order, toward, same_order, sent_hot)
     near, sent_hot = tied(near, sent_hot)
     hot = exchange(sent_hot, KV)
+    w_before = along_y(w_out, -1)
     w_far = along_y(w_after, 1)
-    w_swapped = [across(w_after), across(w_before)]
-    w_swapped.append(across(w_far))
-    weights = [w_out, w_after, w_before, w_far, w_own] + w_swapped
 
     gains = out_gain.reshape(ranks, 1, WIDTH)
     early = (FIRST_BLOCKS * blocks_here) // 8
     first = attend(0, early, False, at, same_order, queries, mask, pairs, near, hot)
     first = exchange(first, TP)
     second = attend(early, blocks_here - early, True, at, toward, queries, mask, pairs, near, hot)
+    *second, w_after, w_before, w_far = tied(*second, w_after, w_before, w_far)
+    w_swapped = [across(w_after), across(w_before), across(w_far)]
+    weights = [w_out, w_after, w_before, w_far, w_own] + w_swapped
     second = send_pieces(second)
     first = project_out(False, order, same_order, first, weights, gains)
     moved = exchange(first, TP)

time: 203 us -> 223 us (1.099)
  waiting for transfers between devices: 47.5 us -> 60.4 us
  starting transfers between devices: 69 us -> 72.5 us
    ppermute x6, waiting for transfers between devices: 14.2 us -> 5.84 us  [along_y(): lax.ppermute(piece, TP[0], [(i, (i + shift) % ring) for i in range(ring)])]
    ppermute x3, waiting for transfers between devices: 0.01 us -> 8.04 us  [local(): lax.ppermute(held[n], KV, [(i, i + n) for i in starts])]
    ppermute x14, waiting for transfers between devices: 17 us -> 23.9 us  [send_pieces(): got.append(lax.ppermute(pieces[k], TP, pairs) if k else pieces[0])]
    all_to_all x5, waiting for transfers between devices: 16.2 us -> 22.5 us  [exchange(): return lax.all_to_all(pieces, axes, split_axis=0, concat_axis=0, tiled=True)]
    ppermute x3, starting transfers between devices: 3.89 us -> 6.62 us  [local(): lax.ppermute(held[n], KV, [(i, i + n) for i in starts])]
    unnamed x34 -> x56, local copies, waits for them, and re-layouts: 4.13 us -> 5.79 us
  transfers between devices with their start and end apart: 36 -> 36, of which waited for: 14 -> 14; matrix products, arithmetic and copies ran while one was open for 4% -> 5% of each run, Pallas kernels for 31% -> 28%
where the time goes in v7:
time: 223 us; the launch traced here: 222 us
  starting transfers between devices  72.5 us (33%)
  Pallas kernels  72.4 us (32%)
  waiting for transfers between devices  60.4 us (27%)
  local copies, waits for them, and re-layouts  9.52 us (4%)
  other arithmetic  7.01 us (3%)
    all_to_all x5, starting transfers between devices, exchange(): return lax.all_to_all(pieces, axes, split_axis=0, concat_axis=0, tiled=True)  27.6 us
    ppermute x14, waiting for transfers between devices, send_pieces(): got.append(lax.ppermute(pieces[k], TP, pairs) if k else pieces[0])  23.9 us
    all_to_all x5, waiting for transfers between devices, exchange(): return lax.all_to_all(pieces, axes, split_axis=0, concat_axis=0, tiled=True)  22.5 us
    ppermute x14, starting transfers between devices, send_pieces(): got.append(lax.ppermute(pieces[k], TP, pairs) if k else pieces[0])  19 us
    pallas_call x2, Pallas kernels, attend(): pl.pallas_call(functools.partial(attention_kernel, first), grid_spec=pltp...  18.5 us
    pallas_call x2, Pallas kernels, project_out(): pl.pallas_call(out_kernel, grid_spec=pltpu.PrefetchScalarGridSpec(num_sca...  15 us
    pallas_call x1, Pallas kernels, project_kv(): pl.pallas_call(kv_kernel, grid=(length // tile,), in_specs=[pl.BlockSpec(...  13.7 us
    pallas_call x1, Pallas kernels, project_q(): pl.pallas_call(q_kernel, grid=(length // tile,), in_specs=[pl.BlockSpec((...  10.1 us
  transfers between devices with their start and end apart: 36, of which 14 were waited for; matrix products, arithmetic and copies ran while one was open for 5% of the time, Pallas kernels for 28%

profile of v7, /device:TPU:1, one launch (start us, length us, event | category | flops | bytes accessed | tf_op | source)
XLA Modules:
  0.0 222.3 jit_solution(3505043784486557831)
XLA Ops:
  0.0 2.1 collective-permute-start.10
  2.1 1.4 collective-permute-start.11
  3.6 4.0 %token_shares.1 = (bf16[4,256,256]{2,1,0:T(8,128)(2,1)}, bf16[4,256,256]{2,1,0:T(8,128)(2,1)}, bf16[4,256,256]{2,1,0:T(8,128)(2,1)}, bf16[4,256,256]{2,1,0:T(8,128)(2,1)}) custom-call(s32[1]{0:T(128)} %bitcast.5.rank, bf16[4096,2048]{1,0:T(8,128)(2,1)} %tok.4), custom_call_target="tpu_custom_call" | custom-call | flops 1048576 | bytes 4194304 | tf_op jit(solution)/shard_map/token_shares/pallas_call | solution.py:51
  9.4 7.6 %all-to-all-start = ((s32[16,1,16]{2,1,0:T(1,128)}), s32[16,1,16]{2,1,0:T(1,128)S(1)}, u32[]{:S(2)}, u32[]{:S(2)}) async-start(s32[16,1,16]{2,1,0:T(1,128)} %bitcast.8), calls=%async_computation | async-start | bytes 16384 | tf_op jit(solution)/shard_map/all_to_all | solution.py:466
  17.0 3.3 %collective-permute-start = (bf16[4,256,256]{2,1,0:T(8,128)(2,1)}, bf16[4,256,256]{2,1,0:T(8,128)(2,1)S(1)}, u32[]{:S(2)}, u32[]{:S(2)}) collective-permute-start(bf16[4,256,256]{2,1,0:T(8,128)(2,1)} %get-tuple-element.77), channel_id=1, source_target_pairs={{0,32},{1,33},{2,34},{3,35},{4,36},{5,37},{6,38},{7,39}} | collective-permute-start | bytes 1572872 | tf_op jit(solution)/shard_map/ppermute | solution.py:533
  20.3 2.2 collective-permute-start.1
  22.5 1.3 collective-permute-start.2
  24.5 13.7 %project_kv.1 = bf16[64,2,64,256]{3,2,1,0:T(8,128)(2,1)} custom-call(bf16[4096,2048]{1,0:T(8,128)(2,1)} %tok.4, bf16[2048,256]{1,0:T(8,128)(2,1)} %wk.3, bf16[2048,256]{1,0:T(8,128)(2,1)} %wv.3, f32[1,128]{1,0:T(1,128)} %bitcast.48), custom_call_target="tpu_custom_call" | custom-call | flops 8589934592 | bytes 16777216 | tf_op jit(solution)/shard_map/project_kv/pallas_call | solution.py:82
  38.8 4.4 %gather_near.1 = bf16[32,128,256]{2,1,0:T(8,128)(2,1)} custom-call(s32[32]{0:T(128)} %reshape.69.near, bf16[8192,256]{1,0:T(8,128)(2,1)} %bitcast.34), custom_call_target="tpu_custom_call" | custom-call | flops 1048576 | bytes 4194304 | tf_op jit(solution)/shard_map/gather_near/pallas_call | solution.py:150
  44.1 3.7 %all-to-all-start.1 = ((bf16[16,256,256]{2,1,0:T(8,128)(2,1)}), bf16[16,256,256]{2,1,0:T(8,128)(2,1)S(1)}, u32[]{:S(2)}, u32[]{:S(2)}) async-start(bf16[16,256,256]{2,1,0:T(8,128)(2,1)} %bitcast.39), calls=%async_computation.1 | async-start | bytes 4194304 | tf_op jit(solution)/shard_map/all_to_all | solution.py:466
  47.9 2.0 select_bitcast_fusion
  49.9 3.1 %collective-permute-start.3 = (bf16[256,256]{1,0:T(8,128)(2,1)}, bf16[256,256]{1,0:T(8,128)(2,1)S(1)}, u32[]{:S(2)}, u32[]{:S(2)}) collective-permute-start(bf16[256,256]{1,0:T(8,128)(2,1)} %get-tuple-element.143), channel_id=1, source_target_pairs={{0,8},{32,40},{64,72},{96,104},{1,9},{33,41},{65,73},{97,105},{2,1... | collective-permute-start | bytes 393224 | tf_op jit(solution)/shard_map/ppermute | solution.py:564
  53.1 2.2 collective-permute-start.4
  55.3 1.3 collective-permute-start.5
  56.6 10.1 %project_q.1.queries = bf16[4096,256]{1,0:T(8,128)(2,1)} custom-call(bf16[4096,2048]{1,0:T(8,128)(2,1)} %tok.4, bf16[2048,256]{1,0:T(8,128)(2,1)} %wq.1, f32[1,128]{1,0:T(1,128)} %multiply_bitcast_fusion.gain), custom_call_target="tpu_custom_call" | custom-call | flops 4294967296 | bytes 16777216 | tf_op jit(solution)/shard_map/project_q/pallas_call | solution.py:111
  66.7 5.3 %collective-permute-done.3 = bf16[256,256]{1,0:T(8,128)(2,1)S(1)} collective-permute-done((bf16[256,256]{1,0:T(8,128)(2,1)}, bf16[256,256]{1,0:T(8,128)(2,1)S(1)}, u32[]{:S(2)}, u32[]{:S(2)}) %collective-permute-start.3) | collective-permute-done | bytes 131104 | tf_op jit(solution)/shard_map/ppermute | solution.py:564
  72.0 2.7 %collective-permute-done.4 = bf16[256,256]{1,0:T(8,128)(2,1)S(1)} collective-permute-done((bf16[256,256]{1,0:T(8,128)(2,1)S(1)}, bf16[256,256]{1,0:T(8,128)(2,1)S(1)}, u32[]{:S(2)}, u32[]{:S(2)}) %collective-permute-start.4) | collective-permute-done | bytes 131104 | tf_op jit(solution)/shard_map/ppermute | solution.py:564
  74.7 1.7 collective-permute-start.8
  78.0 2.1 collective-permute-done.8
  80.6 3.2 %collective-permute-done.6 = bf16[256,256]{1,0:T(8,128)(2,1)S(1)} collective-permute-done((bf16[256,256]{1,0:T(8,128)(2,1)S(1)}, bf16[256,256]{1,0:T(8,128)(2,1)S(1)}, u32[]{:S(2)}, u32[]{:S(2)}) %collective-permute-start.6) | collective-permute-done | bytes 131104 | tf_op jit(solution)/shard_map/ppermute | solution.py:475
  83.9 3.1 %collective-permute-start.9 = (bf16[4,256,256]{2,1,0:T(8,128)(2,1)S(1)}, bf16[4,256,256]{2,1,0:T(8,128)(2,1)S(1)}, u32[]{:S(2)}, u32[]{:S(2)}) collective-permute-start(bf16[4,256,256]{2,1,0:T(8,128)(2,1)S(1)} %pad_maximum_fusion.same), channel_id=1, source_target_pairs={{0,1},{1,0},{2,3},{3,2},{4,5},{5,4},{6,7},{7,6},{8,9},{9,8},{10,11... | collective-permute-start | bytes 1572872 | tf_op jit(solution)/shard_map/ppermute | solution.py:479
  89.9 4.8 %project_sent.1 = bf16[16,64,256]{2,1,0:T(8,128)(2,1)} custom-call(s32[128]{0:T(128)} %reshape.68.asked, s32[8]{0:T(128)} %pad_add_fusion.1.order, bf16[4,256,256]{2,1,0:T(8,128)(2,1)} %copy-done.7, bf16[4,256,256]{2,1,0:T(8,128)(2,1)} %copy-done.11, bf16[2048,256]{1,0:T(8,128)(2,1)} %wk.3, bf16[2048,256]{1,0:T(8,128)(2,1)} %wv.3, f32[1,128]{1,0:T(1,128)} %bitcast.49), custom_call_target="tpu_custom_call" | custom-call | flops 536870912 | bytes 8388608 | tf_op jit(solution)/shard_map/project_sent/pallas_call | solution.py:210
  95.2 7.3 %all-to-all-start.2 = ((bf16[16,64,256]{2,1,0:T(8,128)(2,1)}), bf16[16,64,256]{2,1,0:T(8,128)(2,1)S(1)}, u32[]{:S(2)}, u32[]{:S(2)}) async-start(bf16[16,64,256]{2,1,0:T(8,128)(2,1)} %project_sent.1), calls=%async_computation.2 | async-start | bytes 1048576 | tf_op jit(solution)/shard_map/all_to_all | solution.py:466
  103.2 1.3 select_reduce_fusion
  106.0 7.6 %all-to-all-done.2.hot = bf16[16,64,256]{2,1,0:T(8,128)(2,1)S(1)} async-done(((bf16[16,64,256]{2,1,0:T(8,128)(2,1)}), bf16[16,64,256]{2,1,0:T(8,128)(2,1)S(1)}, u32[]{:S(2)}, u32[]{:S(2)}) %all-to-all-start.2) | async-done | bytes 524320 | tf_op jit(solution)/shard_map/all_to_all | solution.py:466
  114.4 8.4 %attend.3 = (bf16[256,256]{1,0:T(8,128)(2,1)}, bf16[256,256]{1,0:T(8,128)(2,1)}, bf16[256,256]{1,0:T(8,128)(2,1)}, bf16[256,256]{1,0:T(8,128)(2,1)}, bf16[256,25...) custom-call(s32[512]{0:T(512)} %reshape.71.at, ...), custom_call_target="tpu_custom_call" | custom-call | flops 2147483648 | bytes 10485760 | tf_op jit(solution)/shard_map/attend/pallas_call | solution.py:331
  122.8 1.5 collective-permute-start.14
  124.9 10.1 %attend.2 = bf16[8,256,256]{2,1,0:T(8,128)(2,1)} custom-call(s32[512]{0:T(512)} %reshape.71.at, s32[8]{0:T(128)} %iota.15.where.slot, bf16[4096,256]{1,0:T(8,128)(2,1)} %project_q.1.queries, f32[64,512]{1,0:T(8,128)} %reshape.72.masks, bf16[8192,256]{1,0:T(8,128)(2,1)} %bitcast.36, bf16[4096,256]{1,0:T(8,128)(2,1)} %bitcast.38, bf16[16,64,256]{2,1,0:T(8,128)(2,1)} %copy-done.3), custom_call_target="tpu_custom_call" | custom-call | flops 2147483648 | bytes 10485760 | tf_op jit(solution)/shard_map/attend/pallas_call | solution.py:331
  135.0 4.3 %all-to-all-start.3 = ((bf16[8,256,256]{2,1,0:T(8,128)(2,1)}), bf16[8,256,256]{2,1,0:T(8,128)(2,1)S(1)}, u32[]{:S(2)}, u32[]{:S(2)}) async-start(bf16[8,256,256]{2,1,0:T(8,128)(2,1)} %attend.2), calls=%async_computation.3 | async-start | bytes 2097152 | tf_op jit(solution)/shard_map/all_to_all | solution.py:466
  139.4 15.0 %all-to-all-done.3.refs_0_ = bf16[8,256,256]{2,1,0:T(8,128)(2,1)S(1)} async-done(((bf16[8,256,256]{2,1,0:T(8,128)(2,1)}), bf16[8,256,256]{2,1,0:T(8,128)(2,1)S(1)}, u32[]{:S(2)}, u32[]{:S(2)}) %all-to-all-start.3) | async-done | bytes 1048608 | tf_op jit(solution)/shard_map/all_to_all | solution.py:466
  156.0 7.5 %project_out.2 = bf16[8,256,256]{2,1,0:T(8,128)(2,1)} custom-call(s32[8]{0:T(128)} %pad_add_fusion.1.order, s32[8]{0:T(128)} %iota.15.where.slot, bf16[8,256,256]{2,1,0:T(8,128)(2,1)} %copy-done.4, bf16[256,2048]{1,0:T(8,128)(2,1)} %refs_8_.1, bf16[256,2048]{1,0:T(8,128)(2,1)} %collective-permute-done.10.refs_2_.refs_9_, ...), custom_call_target="tpu_custom_call" | custom-call | flops 2147483648 | bytes 12582912 | tf_op jit(solution)/shard_map/project_out/pallas_call | solution.py:406
  163.6 4.6 %all-to-all-start.4 = ((bf16[8,256,256]{2,1,0:T(8,128)(2,1)}), bf16[8,256,256]{2,1,0:T(8,128)(2,1)S(1)}, u32[]{:S(2)}, u32[]{:S(2)}) async-start(bf16[8,256,256]{2,1,0:T(8,128)(2,1)} %project_out.2), calls=%async_computation.4 | async-start | bytes 2097152 | tf_op jit(solution)/shard_map/all_to_all | solution.py:466
  168.2 1.4 collective-permute-start.17
  169.6 1.3 collective-permute-start.18
  170.9 1.7 collective-permute-start.19
  172.6 1.2 collective-permute-start.20
  174.1 11.8 %collective-permute-done.17.refs_1_ = bf16[256,256]{1,0:T(8,128)(2,1)S(1)} collective-permute-done((bf16[256,256]{1,0:T(8,128)(2,1)S(1)}, bf16[256,256]{1,0:T(8,128)(2,1)S(1)}, u32[]{:S(2)}, u32[]{:S(2)}) %collective-permute-start.17) | collective-permute-done | bytes 131104 | tf_op jit(solution)/shard_map/ppermute | solution.py:515
  185.9 1.8 collective-permute-start.22
  187.7 2.3 %collective-permute-start.23 = (bf16[256,256]{1,0:T(8,128)(2,1)S(1)}, bf16[256,256]{1,0:T(8,128)(2,1)S(1)}, u32[]{:S(2)}, u32[]{:S(2)}) collective-permute-start(bf16[256,256]{1,0:T(8,128)(2,1)S(1)} %copy-done.20), channel_id=1, source_target_pairs={{0,5},{1,4},{2,7},{3,6},{4,1},{5,0},{6,3},{7,2},{8,13},{9,12},{10,... | collective-permute-start | bytes 393224 | tf_op jit(solution)/shard_map/ppermute | solution.py:515
  190.0 1.9 collective-permute-done.21.refs_5_
  191.9 2.8 %collective-permute-done.23.refs_7_ = bf16[256,256]{1,0:T(8,128)(2,1)S(1)} collective-permute-done((bf16[256,256]{1,0:T(8,128)(2,1)S(1)}, bf16[256,256]{1,0:T(8,128)(2,1)S(1)}, u32[]{:S(2)}, u32[]{:S(2)}) %collective-permute-start.23) | collective-permute-done | bytes 131104 | tf_op jit(solution)/shard_map/ppermute | solution.py:515
  195.5 7.5 %project_out.3 = (bf16[256,256]{1,0:T(8,128)(2,1)}, bf16[256,256]{1,0:T(8,128)(2,1)}, bf16[256,256]{1,0:T(8,128)(2,1)}, bf16[256,256]{1,0:T(8,128)(2,1)}, bf16[2...) custom-call(s32[8]{0:T(128)} %pad_add_fusion.1.order, ...), custom_call_target="tpu_custom_call" | custom-call | flops 2147483648 | bytes 12582912 | tf_op jit(solution)/shard_map/project_out/pallas_call | solution.py:406
  204.1 1.5 collective-permute-start.25
  209.2 2.5 %collective-permute-start.29 = (bf16[256,256]{1,0:T(8,128)(2,1)}, bf16[256,256]{1,0:T(8,128)(2,1)S(1)}, u32[]{:S(2)}, u32[]{:S(2)}) collective-permute-start(bf16[256,256]{1,0:T(8,128)(2,1)} %get-tuple-element.135), channel_id=1, source_target_pairs={{0,7},{1,6},{2,1},{3,0},{4,3},{5,2},{6,5},{7,4},{8,15},{9,14},{10,... | collective-permute-start | bytes 393224 | tf_op jit(solution)/shard_map/ppermute | solution.py:515
  211.7 1.5 collective-permute-start.30
  213.2 2.9 %collective-permute-done.28.rest_5_ = bf16[256,256]{1,0:T(8,128)(2,1)S(1)} collective-permute-done((bf16[256,256]{1,0:T(8,128)(2,1)}, bf16[256,256]{1,0:T(8,128)(2,1)S(1)}, u32[]{:S(2)}, u32[]{:S(2)}) %collective-permute-start.28) | collective-permute-done | bytes 131104 | tf_op jit(solution)/shard_map/ppermute | solution.py:515
  216.4 3.0 %collective-permute-done.30.rest_7_ = bf16[256,256]{1,0:T(8,128)(2,1)S(1)} collective-permute-done((bf16[256,256]{1,0:T(8,128)(2,1)}, bf16[256,256]{1,0:T(8,128)(2,1)S(1)}, u32[]{:S(2)}, u32[]{:S(2)}) %collective-permute-start.30) | collective-permute-done | bytes 131104 | tf_op jit(solution)/shard_map/ppermute | solution.py:515
  220.3 1.9 place.1
  (122 shorter events, 21.6 us)
Async XLA Ops:
  0.0 87.7 %collective-permute-start.10 = (bf16[256,2048]{1,0:T(8,128)(2,1)}, bf16[256,2048]{1,0:T(8,128)(2,1)}, u32[]{:S(2)}, u32[]{:S(2)}) collective-permute-start(bf16[256,2048]{1,0:T(8,128)(2,1)} %refs_8_.1), channel_id=1, source_target_pairs={{0,2},{2,4},{4,6},{6,0},{1,3},{3,5},{5,7},{7,1},{8,10},{10,12},{12... | collective-permute-start | bytes 3145736 | tf_op jit(solution)/shard_map/ppermute | solution.py:475
  2.1 120.7 %collective-permute-start.11 = (bf16[256,2048]{1,0:T(8,128)(2,1)}, bf16[256,2048]{1,0:T(8,128)(2,1)}, u32[]{:S(2)}, u32[]{:S(2)}) collective-permute-start(bf16[256,2048]{1,0:T(8,128)(2,1)} %refs_8_.1), channel_id=1, source_target_pairs={{0,6},{2,0},{4,2},{6,4},{1,7},{3,1},{5,3},{7,5},{8,14},{10,8},{12,... | collective-permute-start | bytes 3145736 | tf_op jit(solution)/shard_map/ppermute | solution.py:475
  3.6 20.3 %copy-start.27 = (f32[128]{0:T(128)S(1)}, f32[128]{0:T(128)}, u32[]{:S(2)}) copy-start(f32[128]{0:T(128)} %param.14) | copy-start | bytes 1540
  9.4 28.8 %all-to-all-start = ((s32[16,1,16]{2,1,0:T(1,128)}), s32[16,1,16]{2,1,0:T(1,128)S(1)}, u32[]{:S(2)}, u32[]{:S(2)}) async-start(s32[16,1,16]{2,1,0:T(1,128)} %bitcast.8), calls=%async_computation | async-start | bytes 16384 | tf_op jit(solution)/shard_map/all_to_all | solution.py:466
  17.0 26.1 %collective-permute-start = (bf16[4,256,256]{2,1,0:T(8,128)(2,1)}, bf16[4,256,256]{2,1,0:T(8,128)(2,1)S(1)}, u32[]{:S(2)}, u32[]{:S(2)}) collective-permute-start(bf16[4,256,256]{2,1,0:T(8,128)(2,1)} %get-tuple-element.77), channel_id=1, source_target_pairs={{0,32},{1,33},{2,34},{3,35},{4,36},{5,37},{6,38},{7,39}} | collective-permute-start | bytes 1572872 | tf_op jit(solution)/shard_map/ppermute | solution.py:533
  20.3 22.8 %collective-permute-start.1 = (bf16[4,256,256]{2,1,0:T(8,128)(2,1)}, bf16[4,256,256]{2,1,0:T(8,128)(2,1)S(1)}, u32[]{:S(2)}, u32[]{:S(2)}) collective-permute-start(bf16[4,256,256]{2,1,0:T(8,128)(2,1)} %get-tuple-element.78), channel_id=1, source_target_pairs={{0,64},{1,65},{2,66},{3,67},{4,68},{5,69},{6,70},{7,71}} | collective-permute-start | bytes 1572872 | tf_op jit(solution)/shard_map/ppermute | solution.py:533
  22.5 20.7 %collective-permute-start.2 = (bf16[4,256,256]{2,1,0:T(8,128)(2,1)}, bf16[4,256,256]{2,1,0:T(8,128)(2,1)S(1)}, u32[]{:S(2)}, u32[]{:S(2)}) collective-permute-start(bf16[4,256,256]{2,1,0:T(8,128)(2,1)} %get-tuple-element.79), channel_id=1, source_target_pairs={{0,96},{1,97},{2,98},{3,99},{4,100},{5,101},{6,102},{7,103}} | collective-permute-start | bytes 1572872 | tf_op jit(solution)/shard_map/ppermute | solution.py:533
  44.1 51.1 %all-to-all-start.1 = ((bf16[16,256,256]{2,1,0:T(8,128)(2,1)}), bf16[16,256,256]{2,1,0:T(8,128)(2,1)S(1)}, u32[]{:S(2)}, u32[]{:S(2)}) async-start(bf16[16,256,256]{2,1,0:T(8,128)(2,1)} %bitcast.39), calls=%async_computation.1 | async-start | bytes 4194304 | tf_op jit(solution)/shard_map/all_to_all | solution.py:466
  49.9 22.1 %collective-permute-start.3 = (bf16[256,256]{1,0:T(8,128)(2,1)}, bf16[256,256]{1,0:T(8,128)(2,1)S(1)}, u32[]{:S(2)}, u32[]{:S(2)}) collective-permute-start(bf16[256,256]{1,0:T(8,128)(2,1)} %get-tuple-element.143), channel_id=1, source_target_pairs={{0,8},{32,40},{64,72},{96,104},{1,9},{33,41},{65,73},{97,105},{2,1... | collective-permute-start | bytes 393224 | tf_op jit(solution)/shard_map/ppermute | solution.py:564
  53.1 21.6 %collective-permute-start.4 = (bf16[256,256]{1,0:T(8,128)(2,1)S(1)}, bf16[256,256]{1,0:T(8,128)(2,1)S(1)}, u32[]{:S(2)}, u32[]{:S(2)}) collective-permute-start(bf16[256,256]{1,0:T(8,128)(2,1)S(1)} %get-tuple-element.142), channel_id=1, source_target_pairs={{0,16},{32,48},{64,80},{96,112},{1,17},{33,49},{65,81},{97,113},{2... | collective-permute-start | bytes 393224 | tf_op jit(solution)/shard_map/ppermute | solution.py:564
  55.3 19.4 %collective-permute-start.5 = (bf16[256,256]{1,0:T(8,128)(2,1)S(1)}, bf16[256,256]{1,0:T(8,128)(2,1)S(1)}, u32[]{:S(2)}, u32[]{:S(2)}) collective-permute-start(bf16[256,256]{1,0:T(8,128)(2,1)S(1)} %get-tuple-element.141), channel_id=1, source_target_pairs={{0,24},{32,56},{64,88},{96,120},{1,25},{33,57},{65,89},{97,121},{2... | collective-permute-start | bytes 393224 | tf_op jit(solution)/shard_map/ppermute | solution.py:564
  74.7 5.4 %collective-permute-start.8 = (bf16[256,256]{1,0:T(8,128)(2,1)S(1)}, bf16[256,256]{1,0:T(8,128)(2,1)S(1)}, u32[]{:S(2)}, u32[]{:S(2)}) collective-permute-start(bf16[256,256]{1,0:T(8,128)(2,1)S(1)} %select_select_fusion), channel_id=1, source_target_pairs={{0,4},{2,6},{4,0},{6,2},{1,5},{3,7},{5,1},{7,3},{8,12},{10,14},{12... | collective-permute-start | bytes 393224 | tf_op jit(solution)/shard_map/ppermute | solution.py:475
  76.4 4.2 %collective-permute-start.7 = (bf16[256,256]{1,0:T(8,128)(2,1)S(1)}, bf16[256,256]{1,0:T(8,128)(2,1)S(1)}, u32[]{:S(2)}, u32[]{:S(2)}) collective-permute-start(bf16[256,256]{1,0:T(8,128)(2,1)S(1)} %select_select_fusion), channel_id=1, source_target_pairs={{0,6},{2,0},{4,2},{6,4},{1,7},{3,1},{5,3},{7,5},{8,14},{10,8},{12,... | collective-permute-start | bytes 393224 | tf_op jit(solution)/shard_map/ppermute | solution.py:475
  77.2 6.6 %collective-permute-start.6 = (bf16[256,256]{1,0:T(8,128)(2,1)S(1)}, bf16[256,256]{1,0:T(8,128)(2,1)S(1)}, u32[]{:S(2)}, u32[]{:S(2)}) collective-permute-start(bf16[256,256]{1,0:T(8,128)(2,1)S(1)} %select_select_fusion), channel_id=1, source_target_pairs={{0,2},{2,4},{4,6},{6,0},{1,3},{3,5},{5,7},{7,1},{8,10},{10,12},{12... | collective-permute-start | bytes 393224 | tf_op jit(solution)/shard_map/ppermute | solution.py:475
  83.9 5.2 %copy-start.7 = (bf16[4,256,256]{2,1,0:T(8,128)(2,1)}, bf16[4,256,256]{2,1,0:T(8,128)(2,1)S(1)}, u32[]{:S(2)}) copy-start(bf16[4,256,256]{2,1,0:T(8,128)(2,1)S(1)} %pad_maximum_fusion.same) | copy-start | bytes 1572868
  83.9 5.2 %collective-permute-start.9 = (bf16[4,256,256]{2,1,0:T(8,128)(2,1)S(1)}, bf16[4,256,256]{2,1,0:T(8,128)(2,1)S(1)}, u32[]{:S(2)}, u32[]{:S(2)}) collective-permute-start(bf16[4,256,256]{2,1,0:T(8,128)(2,1)S(1)} %pad_maximum_fusion.same), channel_id=1, source_target_pairs={{0,1},{1,0},{2,3},{3,2},{4,5},{5,4},{6,7},{7,6},{8,9},{9,8},{10,11... | collective-permute-start | bytes 1572872 | tf_op jit(solution)/shard_map/ppermute | solution.py:479
  87.7 35.1 %collective-permute-start.12 = (bf16[256,2048]{1,0:T(8,128)(2,1)}, bf16[256,2048]{1,0:T(8,128)(2,1)}, u32[]{:S(2)}, u32[]{:S(2)}) collective-permute-start(bf16[256,2048]{1,0:T(8,128)(2,1)} %collective-permute-done.10.refs_2_.refs_9_), channel_id=1, source_target_pairs={{0,2},{2,4},{4,6},{6,0},{1,3},{3,5},{5,7},{7,1},{8,10},{10,12},{12... | collective-permute-start | bytes 3145736 | tf_op jit(solution)/shard_map/ppermute | solution.py:475
  95.2 18.4 %copy-start.2 = (bf16[16,256,256]{2,1,0:T(8,128)(2,1)}, bf16[16,256,256]{2,1,0:T(8,128)(2,1)S(1)}, u32[]{:S(2)}) copy-start(bf16[16,256,256]{2,1,0:T(8,128)(2,1)S(1)} %all-to-all-done.1) | copy-start | bytes 6291460
  95.2 18.4 %all-to-all-start.2 = ((bf16[16,64,256]{2,1,0:T(8,128)(2,1)}), bf16[16,64,256]{2,1,0:T(8,128)(2,1)S(1)}, u32[]{:S(2)}, u32[]{:S(2)}) async-start(bf16[16,64,256]{2,1,0:T(8,128)(2,1)} %project_sent.1), calls=%async_computation.2 | async-start | bytes 1048576 | tf_op jit(solution)/shard_map/all_to_all | solution.py:466
  102.6 36.8 %collective-permute-start.13 = (bf16[256,2048]{1,0:T(8,128)(2,1)}, bf16[256,2048]{1,0:T(8,128)(2,1)}, u32[]{:S(2)}, u32[]{:S(2)}) collective-permute-start(bf16[256,2048]{1,0:T(8,128)(2,1)} %refs_8_.1), channel_id=1, source_target_pairs={{0,1},{1,0},{2,3},{3,2},{4,5},{5,4},{6,7},{7,6},{8,9},{9,8},{10,11... | collective-permute-start | bytes 3145736 | tf_op jit(solution)/shard_map/ppermute | solution.py:479
  122.8 31.5 %collective-permute-start.14 = (bf16[256,2048]{1,0:T(8,128)(2,1)}, bf16[256,2048]{1,0:T(8,128)(2,1)S(1)}, u32[]{:S(2)}, u32[]{:S(2)}) collective-permute-start(bf16[256,2048]{1,0:T(8,128)(2,1)} %collective-permute-done.10.refs_2_.refs_9_), channel_id=1, source_target_pairs={{0,1},{1,0},{2,3},{3,2},{4,5},{5,4},{6,7},{7,6},{8,9},{9,8},{10,11... | collective-permute-start | bytes 3145736 | tf_op jit(solution)/shard_map/ppermute | solution.py:479
  124.3 30.0 %collective-permute-start.15 = (bf16[256,2048]{1,0:T(8,128)(2,1)}, bf16[256,2048]{1,0:T(8,128)(2,1)S(1)}, u32[]{:S(2)}, u32[]{:S(2)}) collective-permute-start(bf16[256,2048]{1,0:T(8,128)(2,1)} %collective-permute-done.11.refs_3_.refs_10_), channel_id=1, source_target_pairs={{0,1},{1,0},{2,3},{3,2},{4,5},{5,4},{6,7},{7,6},{8,9},{9,8},{10,11... | collective-permute-start | bytes 3145736 | tf_op jit(solution)/shard_map/ppermute | solution.py:479
  124.4 29.9 %collective-permute-start.16 = (bf16[256,2048]{1,0:T(8,128)(2,1)}, bf16[256,2048]{1,0:T(8,128)(2,1)}, u32[]{:S(2)}, u32[]{:S(2)}) collective-permute-start(bf16[256,2048]{1,0:T(8,128)(2,1)} %collective-permute-done.12.refs_4_.refs_11_), channel_id=1, source_target_pairs={{0,1},{1,0},{2,3},{3,2},{4,5},{5,4},{6,7},{7,6},{8,9},{9,8},{10,11... | collective-permute-start | bytes 3145736 | tf_op jit(solution)/shard_map/ppermute | solution.py:479
  135.0 19.3 %all-to-all-start.3 = ((bf16[8,256,256]{2,1,0:T(8,128)(2,1)}), bf16[8,256,256]{2,1,0:T(8,128)(2,1)S(1)}, u32[]{:S(2)}, u32[]{:S(2)}) async-start(bf16[8,256,256]{2,1,0:T(8,128)(2,1)} %attend.2), calls=%async_computation.3 | async-start | bytes 2097152 | tf_op jit(solution)/shard_map/all_to_all | solution.py:466
  163.5 6.1 %copy-start.25 = (bf16[256,256]{1,0:T(8,128)(2,1)S(1)}, bf16[256,256]{1,0:T(8,128)(2,1)}, u32[]{:S(2)}) copy-start(bf16[256,256]{1,0:T(8,128)(2,1)} %get-tuple-element.115) | copy-start | bytes 393220
  163.5 7.4 %copy-start.24 = (bf16[256,256]{1,0:T(8,128)(2,1)S(1)}, bf16[256,256]{1,0:T(8,128)(2,1)}, u32[]{:S(2)}) copy-start(bf16[256,256]{1,0:T(8,128)(2,1)} %get-tuple-element.116) | copy-start | bytes 393220
  163.6 9.0 %copy-start.23 = (bf16[256,256]{1,0:T(8,128)(2,1)S(1)}, bf16[256,256]{1,0:T(8,128)(2,1)}, u32[]{:S(2)}) copy-start(bf16[256,256]{1,0:T(8,128)(2,1)} %get-tuple-element.117) | copy-start | bytes 393220
  163.6 10.3 %copy-start.22 = (bf16[256,256]{1,0:T(8,128)(2,1)S(1)}, bf16[256,256]{1,0:T(8,128)(2,1)}, u32[]{:S(2)}) copy-start(bf16[256,256]{1,0:T(8,128)(2,1)} %get-tuple-element.118) | copy-start | bytes 393220
  163.6 22.3 %copy-start.21 = (bf16[256,256]{1,0:T(8,128)(2,1)S(1)}, bf16[256,256]{1,0:T(8,128)(2,1)}, u32[]{:S(2)}) copy-start(bf16[256,256]{1,0:T(8,128)(2,1)} %get-tuple-element.119) | copy-start | bytes 393220
  163.6 24.1 %copy-start.20 = (bf16[256,256]{1,0:T(8,128)(2,1)S(1)}, bf16[256,256]{1,0:T(8,128)(2,1)}, u32[]{:S(2)}) copy-start(bf16[256,256]{1,0:T(8,128)(2,1)} %get-tuple-element.120) | copy-start | bytes 393220
  163.6 55.7 %all-to-all-start.4 = ((bf16[8,256,256]{2,1,0:T(8,128)(2,1)}), bf16[8,256,256]{2,1,0:T(8,128)(2,1)S(1)}, u32[]{:S(2)}, u32[]{:S(2)}) async-start(bf16[8,256,256]{2,1,0:T(8,128)(2,1)} %project_out.2), calls=%async_computation.4 | async-start | bytes 2097152 | tf_op jit(solution)/shard_map/all_to_all | solution.py:466
  168.2 51.2 %copy-start.1 = (s32[8]{0:T(128)S(1)}, s32[8]{0:T(128)}, u32[]{:S(2)}) copy-start(s32[8]{0:T(128)} %pad_add_fusion.1.order) | copy-start | bytes 100
  168.2 17.7 %collective-permute-start.17 = (bf16[256,256]{1,0:T(8,128)(2,1)S(1)}, bf16[256,256]{1,0:T(8,128)(2,1)S(1)}, u32[]{:S(2)}, u32[]{:S(2)}) collective-permute-start(bf16[256,256]{1,0:T(8,128)(2,1)S(1)} %copy-done.26), channel_id=1, source_target_pairs={{0,2},{1,3},{2,4},{3,5},{4,6},{5,7},{6,0},{7,1},{8,10},{9,11},{10,... | collective-permute-start | bytes 393224 | tf_op jit(solution)/shard_map/ppermute | solution.py:515
  169.6 18.1 %collective-permute-start.18 = (bf16[256,256]{1,0:T(8,128)(2,1)S(1)}, bf16[256,256]{1,0:T(8,128)(2,1)S(1)}, u32[]{:S(2)}, u32[]{:S(2)}) collective-permute-start(bf16[256,256]{1,0:T(8,128)(2,1)S(1)} %copy-done.25), channel_id=1, source_target_pairs={{0,6},{1,7},{2,0},{3,1},{4,2},{5,3},{6,4},{7,5},{8,14},{9,15},{10,... | collective-permute-start | bytes 393224 | tf_op jit(solution)/shard_map/ppermute | solution.py:515
  170.9 19.1 %collective-permute-start.19 = (bf16[256,256]{1,0:T(8,128)(2,1)S(1)}, bf16[256,256]{1,0:T(8,128)(2,1)S(1)}, u32[]{:S(2)}, u32[]{:S(2)}) collective-permute-start(bf16[256,256]{1,0:T(8,128)(2,1)S(1)} %copy-done.24), channel_id=1, source_target_pairs={{0,4},{1,5},{2,6},{3,7},{4,0},{5,1},{6,2},{7,3},{8,12},{9,13},{10,... | collective-permute-start | bytes 393224 | tf_op jit(solution)/shard_map/ppermute | solution.py:515
  172.6 17.4 %collective-permute-start.20 = (bf16[256,256]{1,0:T(8,128)(2,1)S(1)}, bf16[256,256]{1,0:T(8,128)(2,1)S(1)}, u32[]{:S(2)}, u32[]{:S(2)}) collective-permute-start(bf16[256,256]{1,0:T(8,128)(2,1)S(1)} %copy-done.23), channel_id=1, source_target_pairs={{0,1},{1,0},{2,3},{3,2},{4,5},{5,4},{6,7},{7,6},{8,9},{9,8},{10,11... | collective-permute-start | bytes 393224 | tf_op jit(solution)/shard_map/ppermute | solution.py:515
  173.8 18.1 %collective-permute-start.21 = (bf16[256,256]{1,0:T(8,128)(2,1)S(1)}, bf16[256,256]{1,0:T(8,128)(2,1)S(1)}, u32[]{:S(2)}, u32[]{:S(2)}) collective-permute-start(bf16[256,256]{1,0:T(8,128)(2,1)S(1)} %copy-done.22), channel_id=1, source_target_pairs={{0,3},{1,2},{2,5},{3,4},{4,7},{5,6},{6,1},{7,0},{8,11},{9,10},{10,... | collective-permute-start | bytes 393224 | tf_op jit(solution)/shard_map/ppermute | solution.py:515
  185.9 8.9 %copy-start.12 = (bf16[256,256]{1,0:T(8,128)(2,1)}, bf16[256,256]{1,0:T(8,128)(2,1)S(1)}, u32[]{:S(2)}) copy-start(bf16[256,256]{1,0:T(8,128)(2,1)S(1)} %collective-permute-done.17.refs_1_) | copy-start | bytes 393220
  185.9 6.0 %collective-permute-start.22 = (bf16[256,256]{1,0:T(8,128)(2,1)S(1)}, bf16[256,256]{1,0:T(8,128)(2,1)S(1)}, u32[]{:S(2)}, u32[]{:S(2)}) collective-permute-start(bf16[256,256]{1,0:T(8,128)(2,1)S(1)} %copy-done.21), channel_id=1, source_target_pairs={{0,7},{1,6},{2,1},{3,0},{4,3},{5,2},{6,5},{7,4},{8,15},{9,14},{10,... | collective-permute-start | bytes 393224 | tf_op jit(solution)/shard_map/ppermute | solution.py:515
  187.7 7.0 %copy-start.13 = (bf16[256,256]{1,0:T(8,128)(2,1)}, bf16[256,256]{1,0:T(8,128)(2,1)S(1)}, u32[]{:S(2)}) copy-start(bf16[256,256]{1,0:T(8,128)(2,1)S(1)} %collective-permute-done.18.refs_2_) | copy-start | bytes 393220
  187.7 7.0 %collective-permute-start.23 = (bf16[256,256]{1,0:T(8,128)(2,1)S(1)}, bf16[256,256]{1,0:T(8,128)(2,1)S(1)}, u32[]{:S(2)}, u32[]{:S(2)}) collective-permute-start(bf16[256,256]{1,0:T(8,128)(2,1)S(1)} %copy-done.20), channel_id=1, source_target_pairs={{0,5},{1,4},{2,7},{3,6},{4,1},{5,0},{6,3},{7,2},{8,13},{9,12},{10,... | collective-permute-start | bytes 393224 | tf_op jit(solution)/shard_map/ppermute | solution.py:515
  202.9 6.3 %collective-permute-start.24 = (bf16[256,256]{1,0:T(8,128)(2,1)}, bf16[256,256]{1,0:T(8,128)(2,1)S(1)}, u32[]{:S(2)}, u32[]{:S(2)}) collective-permute-start(bf16[256,256]{1,0:T(8,128)(2,1)} %get-tuple-element.130), channel_id=1, source_target_pairs={{0,2},{1,3},{2,4},{3,5},{4,6},{5,7},{6,0},{7,1},{8,10},{9,11},{10,... | collective-permute-start | bytes 393224 | tf_op jit(solution)/shard_map/ppermute | solution.py:515
  204.1 7.6 %collective-permute-start.25 = (bf16[256,256]{1,0:T(8,128)(2,1)}, bf16[256,256]{1,0:T(8,128)(2,1)S(1)}, u32[]{:S(2)}, u32[]{:S(2)}) collective-permute-start(bf16[256,256]{1,0:T(8,128)(2,1)} %get-tuple-element.131), channel_id=1, source_target_pairs={{0,6},{1,7},{2,0},{3,1},{4,2},{5,3},{6,4},{7,5},{8,14},{9,15},{10,... | collective-permute-start | bytes 393224 | tf_op jit(solution)/shard_map/ppermute | solution.py:515
  205.7 7.5 %collective-permute-start.26 = (bf16[256,256]{1,0:T(8,128)(2,1)}, bf16[256,256]{1,0:T(8,128)(2,1)S(1)}, u32[]{:S(2)}, u32[]{:S(2)}) collective-permute-start(bf16[256,256]{1,0:T(8,128)(2,1)} %get-tuple-element.132), channel_id=1, source_target_pairs={{0,4},{1,5},{2,6},{3,7},{4,0},{5,1},{6,2},{7,3},{8,12},{9,13},{10,... | collective-permute-start | bytes 393224 | tf_op jit(solution)/shard_map/ppermute | solution.py:515
  206.4 6.8 %collective-permute-start.27 = (bf16[256,256]{1,0:T(8,128)(2,1)}, bf16[256,256]{1,0:T(8,128)(2,1)S(1)}, u32[]{:S(2)}, u32[]{:S(2)}) collective-permute-start(bf16[256,256]{1,0:T(8,128)(2,1)} %get-tuple-element.133), channel_id=1, source_target_pairs={{0,1},{1,0},{2,3},{3,2},{4,5},{5,4},{6,7},{7,6},{8,9},{9,8},{10,11... | collective-permute-start | bytes 393224 | tf_op jit(solution)/shard_map/ppermute | solution.py:515
  207.0 9.0 %collective-permute-start.28 = (bf16[256,256]{1,0:T(8,128)(2,1)}, bf16[256,256]{1,0:T(8,128)(2,1)S(1)}, u32[]{:S(2)}, u32[]{:S(2)}) collective-permute-start(bf16[256,256]{1,0:T(8,128)(2,1)} %get-tuple-element.134), channel_id=1, source_target_pairs={{0,3},{1,2},{2,5},{3,4},{4,7},{5,6},{6,1},{7,0},{8,11},{9,10},{10,... | collective-permute-start | bytes 393224 | tf_op jit(solution)/shard_map/ppermute | solution.py:515
  209.2 7.2 %collective-permute-start.29 = (bf16[256,256]{1,0:T(8,128)(2,1)}, bf16[256,256]{1,0:T(8,128)(2,1)S(1)}, u32[]{:S(2)}, u32[]{:S(2)}) collective-permute-start(bf16[256,256]{1,0:T(8,128)(2,1)} %get-tuple-element.135), channel_id=1, source_target_pairs={{0,7},{1,6},{2,1},{3,0},{4,3},{5,2},{6,5},{7,4},{8,15},{9,14},{10,... | collective-permute-start | bytes 393224 | tf_op jit(solution)/shard_map/ppermute | solution.py:515
  211.7 7.6 %collective-permute-start.30 = (bf16[256,256]{1,0:T(8,128)(2,1)}, bf16[256,256]{1,0:T(8,128)(2,1)S(1)}, u32[]{:S(2)}, u32[]{:S(2)}) collective-permute-start(bf16[256,256]{1,0:T(8,128)(2,1)} %get-tuple-element.136), channel_id=1, source_target_pairs={{0,5},{1,4},{2,7},{3,6},{4,1},{5,0},{6,3},{7,2},{8,13},{9,12},{10,... | collective-permute-start | bytes 393224 | tf_op jit(solution)/shard_map/ppermute | solution.py:515
  (16 other events, 37.4 us)

commit v8 on v7

--- a/solution.py
+++ b/solution.py
@@ -236,9 +236,10 @@
     devices, hot_rows, _ = hot.shape
     here = pairs.shape[0]
     plain = near.shape[0]
+    used = pl.ds(0, (first + mask.shape[0]) * PAIR * BLOCK)
     copies = [
         pltpu.make_async_copy(hot, raw, sems.at[0]),
-        pltpu.make_async_copy(pairs, table.at[pl.ds(0, here)], sems.at[1]),
+        pltpu.make_async_copy(pairs.at[used], table.at[used], sems.at[1]),
         pltpu.make_async_copy(near, table.at[pl.ds(here, plain)], sems.at[2]),
         pltpu.make_async_copy(queries.at[pl.ds(first * BLOCK, q.shape[0])], q, sems.at[3]),
         pltpu.make_async_copy(masks.at[pl.ds(first, mask.shape[0])], mask, sems.at[4]),
@@ -427,39 +428,50 @@
     return list(outs) if split else outs[0]
 
 
-def place_kernel(order, whole, *rest):
-    count = len(rest) - 2
-    parts, out, sems = rest[:count], rest[count], rest[count + 1]
-    rows = parts[0].shape[0]
-    base = whole.shape[0]
-    copies = [pltpu.make_async_copy(whole, out.at[pl.ds(0, base)], sems.at[count])]
-    for k in range(count):
-        to = pl.multiple_of(base + order[k] * rows, BLOCK)
-        copies.append(pltpu.make_async_copy(parts[k], out.at[pl.ds(to, rows)], sems.at[k]))
+def place_whole_kernel(order, whole, own, out, sems):
+    base, rows = whole.shape[0], own.shape[0]
+    to = pl.multiple_of(base + order[0] * rows, BLOCK)
+    copies = [
+        pltpu.make_async_copy(whole, out.at[pl.ds(0, base)], sems.at[0]),
+        pltpu.make_async_copy(own, out.at[pl.ds(to, rows)], sems.at[1]),
+    ]
     for copy in copies:
         copy.start()
     for copy in copies:
         copy.wait()
 
 
-def place(order, whole, parts):
-    count = len(parts)
-    length = whole.shape[0] + count * parts[0].shape[0]
+def place_parts_kernel(order, filled, *rest):
+    parts, out, sems = rest[:-2], rest[-2], rest[-1]
+    rows = parts[0].shape[0]
+    base = out.shape[0] - (len(parts) + 1) * rows
+    copies = []
+    for k, part in enumerate(parts):
+        to = pl.multiple_of(base + order[k + 1] * rows, BLOCK)
+        copies.append(pltpu.make_async_copy(part, out.at[pl.ds(to, rows)], sems.at[k]))
+    for copy in copies:
+        copy.start()
+    for copy in copies:
+        copy.wait()
+
+
+def place(kernel, length, order, *arrays, aliases=()):
     anywhere = pl.BlockSpec(memory_space=pl.ANY)
     return pl.pallas_call(
-        place_kernel,
+        kernel,
         grid_spec=pltpu.PrefetchScalarGridSpec(
             num_scalar_prefetch=1,
             grid=(1,),
-            in_specs=[anywhere] * (count + 1),
+            in_specs=[anywhere] * len(arrays),
             out_specs=anywhere,
-            scratch_shapes=[pltpu.SemaphoreType.DMA((count + 1,))],
+            scratch_shapes=[pltpu.SemaphoreType.DMA((len(arrays),))],
         ),
         out_shape=jax.ShapeDtypeStruct((length, WIDTH), bf16),
+        input_output_aliases=dict(aliases),
         compiler_params=pltpu.CompilerParams(vmem_limit_bytes=8 << 20),
         cost_estimate=pl.CostEstimate(flops=1 << 20, bytes_accessed=4 << 20, transcendentals=0),
         name="place",
-    )(order, whole, *parts)
+    )(order, *arrays)
 
 
 def exchange(pieces, axes):
@@ -564,13 +576,13 @@
         lax.ppermute(held[n], KV, [(i, i + n) for i in starts]) for n in range(1, side)
     ]
     near = exchange(sent.reshape(devices, -1, WIDTH), KV).reshape(-1, WIDTH)
-    again, sent = tied(tokens, sent)
-    queries = project_q(again, w_query, query_row)
-    queries, *held = tied(queries, *held)
     shares = chosen_of(held, x)
     parts = [shares] + [along_y(shares, shift) for shift in (1, -1, 2)]
     w_after = along_y(w_out, 1)
     w_own = across(w_out)
+    again, sent = tied(tokens, sent)
+    queries = project_q(again, w_query, query_row)
+    queries, *parts = tied(queries, *parts)
     rows_same, rows_other = both_cores(parts)
     sent_hot = project_sent(
         asked_hot, order, rows_same, rows_other, w_key, w_value, key_row, devices
@@ -608,7 +620,8 @@
     second = tied(first, *second)[1:]
     second = project_out(True, order, toward, second, weights, gains)
     second = send_pieces(second)
-    return place(order, moved.reshape(-1, WIDTH), second)
+    filled = place(place_whole_kernel, length, order, moved.reshape(-1, WIDTH), second[0])
+    return place(place_parts_kernel, length, order, filled, *second[1:], aliases={1: 0})
 
 
 def solution(mesh):

time: 223 us -> 225 us (level)
    ppermute x3, waiting for transfers between devices: 8.04 us -> 16.9 us  [local(): lax.ppermute(held[n], KV, [(i, i + n) for i in starts])]
    ppermute x6, waiting for transfers between devices: 5.84 us -> 0.02 us  [along_y(): lax.ppermute(piece, TP[0], [(i, (i + shift) % ring) for i in range(ring)])]
    ppermute x14, waiting for transfers between devices: 23.9 us -> 21.5 us  [send_pieces(): got.append(lax.ppermute(pieces[k], TP, pairs) if k else pieces[0])]
  transfers between devices with their start and end apart: 36 -> 36, of which waited for: 14 -> 11; matrix products, arithmetic and copies ran while one was open for 5% -> 5% of each run, Pallas kernels for 28% -> 28%
where the time goes in v8:
time: 225 us; the launch traced here: 224 us
  starting transfers between devices  73.5 us (33%)
  Pallas kernels  72.9 us (32%)
  waiting for transfers between devices  60.4 us (27%)
  local copies, waits for them, and re-layouts  9.5 us (4%)
  other arithmetic  7.19 us (3%)
    all_to_all x5, starting transfers between devices, exchange(): return lax.all_to_all(pieces, axes, split_axis=0, concat_axis=0, tiled=True)  26.2 us
    all_to_all x5, waiting for transfers between devices, exchange(): return lax.all_to_all(pieces, axes, split_axis=0, concat_axis=0, tiled=True)  22 us
    ppermute x14, waiting for transfers between devices, send_pieces(): got.append(lax.ppermute(pieces[k], TP, pairs) if k else pieces[0])  21.5 us
    ppermute x14, starting transfers between devices, send_pieces(): got.append(lax.ppermute(pieces[k], TP, pairs) if k else pieces[0])  19 us
    pallas_call x2, Pallas kernels, attend(): pl.pallas_call(functools.partial(attention_kernel, first), grid_spec=pltp...  17.9 us
    ppermute x3, waiting for transfers between devices, local(): lax.ppermute(held[n], KV, [(i, i + n) for i in starts])  16.9 us
    pallas_call x2, Pallas kernels, project_out(): pl.pallas_call(out_kernel, grid_spec=pltpu.PrefetchScalarGridSpec(num_sca...  15 us
    pallas_call x1, Pallas kernels, project_kv(): pl.pallas_call(kv_kernel, grid=(length // tile,), in_specs=[pl.BlockSpec(...  13.7 us
  transfers between devices with their start and end apart: 36, of which 11 were waited for; matrix products, arithmetic and copies ran while one was open for 5% of the time, Pallas kernels for 28%

profile of v8, /device:TPU:1, one launch (start us, length us, event | category | flops | bytes accessed | tf_op | source)
XLA Modules:
  0.0 224.2 jit_solution(1961723268245151494)
XLA Ops:
  0.0 2.1 collective-permute-start.10
  2.1 1.4 collective-permute-start.11
  3.6 4.0 %token_shares.1 = (bf16[4,256,256]{2,1,0:T(8,128)(2,1)}, bf16[4,256,256]{2,1,0:T(8,128)(2,1)}, bf16[4,256,256]{2,1,0:T(8,128)(2,1)}, bf16[4,256,256]{2,1,0:T(8,128)(2,1)}) custom-call(s32[1]{0:T(128)} %bitcast.5.rank, bf16[4096,2048]{1,0:T(8,128)(2,1)} %tok.4), custom_call_target="tpu_custom_call" | custom-call | flops 1048576 | bytes 4194304 | tf_op jit(solution)/shard_map/token_shares/pallas_call | solution.py:51
  9.4 7.6 %all-to-all-start = ((s32[16,1,16]{2,1,0:T(1,128)}), s32[16,1,16]{2,1,0:T(1,128)S(1)}, u32[]{:S(2)}, u32[]{:S(2)}) async-start(s32[16,1,16]{2,1,0:T(1,128)} %bitcast.8), calls=%async_computation | async-start | bytes 16384 | tf_op jit(solution)/shard_map/all_to_all | solution.py:478
  17.0 3.3 %collective-permute-start = (bf16[4,256,256]{2,1,0:T(8,128)(2,1)}, bf16[4,256,256]{2,1,0:T(8,128)(2,1)S(1)}, u32[]{:S(2)}, u32[]{:S(2)}) collective-permute-start(bf16[4,256,256]{2,1,0:T(8,128)(2,1)} %get-tuple-element.77), channel_id=1, source_target_pairs={{0,32},{1,33},{2,34},{3,35},{4,36},{5,37},{6,38},{7,39}} | collective-permute-start | bytes 1572872 | tf_op jit(solution)/shard_map/ppermute | solution.py:545
  20.3 2.2 collective-permute-start.1
  22.5 1.3 collective-permute-start.2
  23.9 13.7 %project_kv.1 = bf16[64,2,64,256]{3,2,1,0:T(8,128)(2,1)} custom-call(bf16[4096,2048]{1,0:T(8,128)(2,1)} %tok.4, bf16[2048,256]{1,0:T(8,128)(2,1)} %wk.3, bf16[2048,256]{1,0:T(8,128)(2,1)} %wv.3, f32[1,128]{1,0:T(1,128)} %bitcast.52), custom_call_target="tpu_custom_call" | custom-call | flops 8589934592 | bytes 16777216 | tf_op jit(solution)/shard_map/project_kv/pallas_call | solution.py:82
  38.3 4.4 %gather_near.1 = bf16[32,128,256]{2,1,0:T(8,128)(2,1)} custom-call(s32[32]{0:T(128)} %reshape.69.near, bf16[8192,256]{1,0:T(8,128)(2,1)} %bitcast.38), custom_call_target="tpu_custom_call" | custom-call | flops 1048576 | bytes 4194304 | tf_op jit(solution)/shard_map/gather_near/pallas_call | solution.py:150
  43.7 3.7 %all-to-all-start.1 = ((bf16[16,256,256]{2,1,0:T(8,128)(2,1)}), bf16[16,256,256]{2,1,0:T(8,128)(2,1)S(1)}, u32[]{:S(2)}, u32[]{:S(2)}) async-start(bf16[16,256,256]{2,1,0:T(8,128)(2,1)} %bitcast.43), calls=%async_computation.1 | async-start | bytes 4194304 | tf_op jit(solution)/shard_map/all_to_all | solution.py:478
  47.4 1.3 select_bitcast_fusion
  48.7 4.4 %collective-permute-start.3 = (bf16[256,256]{1,0:T(8,128)(2,1)S(1)}, bf16[256,256]{1,0:T(8,128)(2,1)S(1)}, u32[]{:S(2)}, u32[]{:S(2)}) collective-permute-start(bf16[256,256]{1,0:T(8,128)(2,1)S(1)} %get-tuple-element.143), channel_id=1, source_target_pairs={{0,24},{32,56},{64,88},{96,120},{1,25},{33,57},{65,89},{97,121},{2... | collective-permute-start | bytes 393224 | tf_op jit(solution)/shard_map/ppermute | solution.py:576
  53.1 1.3 collective-permute-start.4
  54.4 1.3 collective-permute-start.5
  56.2 14.7 %collective-permute-done.3 = bf16[256,256]{1,0:T(8,128)(2,1)S(1)} collective-permute-done((bf16[256,256]{1,0:T(8,128)(2,1)S(1)}, bf16[256,256]{1,0:T(8,128)(2,1)S(1)}, u32[]{:S(2)}, u32[]{:S(2)}) %collective-permute-start.3) | collective-permute-done | bytes 131104 | tf_op jit(solution)/shard_map/ppermute | solution.py:576
  71.0 2.2 collective-permute-done.5
  74.3 2.7 %collective-permute-start.7 = (bf16[256,256]{1,0:T(8,128)(2,1)S(1)}, bf16[256,256]{1,0:T(8,128)(2,1)S(1)}, u32[]{:S(2)}, u32[]{:S(2)}) collective-permute-start(bf16[256,256]{1,0:T(8,128)(2,1)S(1)} %fusion.2), channel_id=1, source_target_pairs={{0,6},{2,0},{4,2},{6,4},{1,7},{3,1},{5,3},{7,5},{8,14},{10,8},{12,... | collective-permute-start | bytes 393224 | tf_op jit(solution)/shard_map/ppermute | solution.py:487
  77.4 10.1 %project_q.1.queries = bf16[4096,256]{1,0:T(8,128)(2,1)} custom-call(bf16[4096,2048]{1,0:T(8,128)(2,1)} %tok.4, bf16[2048,256]{1,0:T(8,128)(2,1)} %wq.1, f32[1,128]{1,0:T(1,128)} %multiply_bitcast_fusion.gain), custom_call_target="tpu_custom_call" | custom-call | flops 4294967296 | bytes 16777216 | tf_op jit(solution)/shard_map/project_q/pallas_call | solution.py:111
  87.5 4.3 %collective-permute-start.9 = (bf16[4,256,256]{2,1,0:T(8,128)(2,1)S(1)}, bf16[4,256,256]{2,1,0:T(8,128)(2,1)S(1)}, u32[]{:S(2)}, u32[]{:S(2)}) collective-permute-start(bf16[4,256,256]{2,1,0:T(8,128)(2,1)S(1)} %pad_maximum_fusion.same), channel_id=1, source_target_pairs={{0,1},{1,0},{2,3},{3,2},{4,5},{5,4},{6,7},{7,6},{8,9},{9,8},{10,11... | collective-permute-start | bytes 1572872 | tf_op jit(solution)/shard_map/ppermute | solution.py:491
  95.1 4.8 %project_sent.1 = bf16[16,64,256]{2,1,0:T(8,128)(2,1)} custom-call(s32[128]{0:T(128)} %reshape.68.asked, s32[8]{0:T(128)} %pad_add_fusion.1.order, bf16[4,256,256]{2,1,0:T(8,128)(2,1)} %copy-done.7, bf16[4,256,256]{2,1,0:T(8,128)(2,1)} %copy-done.11, bf16[2048,256]{1,0:T(8,128)(2,1)} %wk.3, bf16[2048,256]{1,0:T(8,128)(2,1)} %wv.3, f32[1,128]{1,0:T(1,128)} %bitcast.53), custom_call_target="tpu_custom_call" | custom-call | flops 536870912 | bytes 8388608 | tf_op jit(solution)/shard_map/project_sent/pallas_call | solution.py:210
  100.4 6.3 %all-to-all-start.2 = ((bf16[16,64,256]{2,1,0:T(8,128)(2,1)}), bf16[16,64,256]{2,1,0:T(8,128)(2,1)S(1)}, u32[]{:S(2)}, u32[]{:S(2)}) async-start(bf16[16,64,256]{2,1,0:T(8,128)(2,1)} %project_sent.1), calls=%async_computation.2 | async-start | bytes 1048576 | tf_op jit(solution)/shard_map/all_to_all | solution.py:478
  107.6 1.3 select_reduce_fusion
  110.5 7.0 %all-to-all-done.2.hot = bf16[16,64,256]{2,1,0:T(8,128)(2,1)S(1)} async-done(((bf16[16,64,256]{2,1,0:T(8,128)(2,1)}), bf16[16,64,256]{2,1,0:T(8,128)(2,1)S(1)}, u32[]{:S(2)}, u32[]{:S(2)}) %all-to-all-start.2) | async-done | bytes 524320 | tf_op jit(solution)/shard_map/all_to_all | solution.py:478
  118.3 8.4 %attend.3 = (bf16[256,256]{1,0:T(8,128)(2,1)}, bf16[256,256]{1,0:T(8,128)(2,1)}, bf16[256,256]{1,0:T(8,128)(2,1)}, bf16[256,256]{1,0:T(8,128)(2,1)}, bf16[256,25...) custom-call(s32[512]{0:T(512)} %reshape.71.at, ...), custom_call_target="tpu_custom_call" | custom-call | flops 2147483648 | bytes 10485760 | tf_op jit(solution)/shard_map/attend/pallas_call | solution.py:332
  126.7 1.8 collective-permute-start.14
  129.0 9.5 %attend.2 = bf16[8,256,256]{2,1,0:T(8,128)(2,1)} custom-call(s32[512]{0:T(512)} %reshape.71.at, s32[8]{0:T(128)} %iota.15.where.slot, bf16[4096,256]{1,0:T(8,128)(2,1)} %project_q.1.queries, f32[64,512]{1,0:T(8,128)} %reshape.72.masks, bf16[8192,256]{1,0:T(8,128)(2,1)} %bitcast.40, bf16[4096,256]{1,0:T(8,128)(2,1)} %bitcast.42, bf16[16,64,256]{2,1,0:T(8,128)(2,1)} %copy-done.3), custom_call_target="tpu_custom_call" | custom-call | flops 2147483648 | bytes 10485760 | tf_op jit(solution)/shard_map/attend/pallas_call | solution.py:332
  138.6 4.0 %all-to-all-start.3 = ((bf16[8,256,256]{2,1,0:T(8,128)(2,1)}), bf16[8,256,256]{2,1,0:T(8,128)(2,1)S(1)}, u32[]{:S(2)}, u32[]{:S(2)}) async-start(bf16[8,256,256]{2,1,0:T(8,128)(2,1)} %attend.2), calls=%async_computation.3 | async-start | bytes 2097152 | tf_op jit(solution)/shard_map/all_to_all | solution.py:478
  142.5 15.0 %all-to-all-done.3.refs_0_ = bf16[8,256,256]{2,1,0:T(8,128)(2,1)S(1)} async-done(((bf16[8,256,256]{2,1,0:T(8,128)(2,1)}), bf16[8,256,256]{2,1,0:T(8,128)(2,1)S(1)}, u32[]{:S(2)}, u32[]{:S(2)}) %all-to-all-start.3) | async-done | bytes 1048608 | tf_op jit(solution)/shard_map/all_to_all | solution.py:478
  159.2 7.5 %project_out.2 = bf16[8,256,256]{2,1,0:T(8,128)(2,1)} custom-call(s32[8]{0:T(128)} %pad_add_fusion.1.order, s32[8]{0:T(128)} %iota.15.where.slot, bf16[8,256,256]{2,1,0:T(8,128)(2,1)} %copy-done.4, bf16[256,2048]{1,0:T(8,128)(2,1)} %refs_8_.1, bf16[256,2048]{1,0:T(8,128)(2,1)} %collective-permute-done.10.refs_2_.refs_9_, ...), custom_call_target="tpu_custom_call" | custom-call | flops 2147483648 | bytes 12582912 | tf_op jit(solution)/shard_map/project_out/pallas_call | solution.py:407
  166.8 4.6 %all-to-all-start.4 = ((bf16[8,256,256]{2,1,0:T(8,128)(2,1)}), bf16[8,256,256]{2,1,0:T(8,128)(2,1)S(1)}, u32[]{:S(2)}, u32[]{:S(2)}) async-start(bf16[8,256,256]{2,1,0:T(8,128)(2,1)} %project_out.2), calls=%async_computation.4 | async-start | bytes 2097152 | tf_op jit(solution)/shard_map/all_to_all | solution.py:478
  171.3 1.4 collective-permute-start.17
  172.8 1.3 collective-permute-start.18
  174.1 1.7 collective-permute-start.19
  175.8 1.2 collective-permute-start.20
  177.3 11.8 %collective-permute-done.17.refs_1_ = bf16[256,256]{1,0:T(8,128)(2,1)S(1)} collective-permute-done((bf16[256,256]{1,0:T(8,128)(2,1)S(1)}, bf16[256,256]{1,0:T(8,128)(2,1)S(1)}, u32[]{:S(2)}, u32[]{:S(2)}) %collective-permute-start.17) | collective-permute-done | bytes 131104 | tf_op jit(solution)/shard_map/ppermute | solution.py:527
  189.1 1.8 collective-permute-start.22
  190.9 2.3 %collective-permute-start.23 = (bf16[256,256]{1,0:T(8,128)(2,1)S(1)}, bf16[256,256]{1,0:T(8,128)(2,1)S(1)}, u32[]{:S(2)}, u32[]{:S(2)}) collective-permute-start(bf16[256,256]{1,0:T(8,128)(2,1)S(1)} %copy-done.20), channel_id=1, source_target_pairs={{0,5},{1,4},{2,7},{3,6},{4,1},{5,0},{6,3},{7,2},{8,13},{9,12},{10,... | collective-permute-start | bytes 393224 | tf_op jit(solution)/shard_map/ppermute | solution.py:527
  193.2 1.9 collective-permute-done.21.refs_5_
  195.1 2.8 %collective-permute-done.23.refs_7_ = bf16[256,256]{1,0:T(8,128)(2,1)S(1)} collective-permute-done((bf16[256,256]{1,0:T(8,128)(2,1)S(1)}, bf16[256,256]{1,0:T(8,128)(2,1)S(1)}, u32[]{:S(2)}, u32[]{:S(2)}) %collective-permute-start.23) | collective-permute-done | bytes 131104 | tf_op jit(solution)/shard_map/ppermute | solution.py:527
  198.6 7.5 %project_out.3 = (bf16[256,256]{1,0:T(8,128)(2,1)}, bf16[256,256]{1,0:T(8,128)(2,1)}, bf16[256,256]{1,0:T(8,128)(2,1)}, bf16[256,256]{1,0:T(8,128)(2,1)}, bf16[2...) custom-call(s32[8]{0:T(128)} %pad_add_fusion.1.order, ...), custom_call_target="tpu_custom_call" | custom-call | flops 2147483648 | bytes 12582912 | tf_op jit(solution)/shard_map/project_out/pallas_call | solution.py:407
  206.1 1.2 collective-permute-start.24
  207.3 1.5 collective-permute-start.25
  211.2 1.2 collective-permute-done.24.rest_0_
  212.4 2.5 %collective-permute-start.29 = (bf16[256,256]{1,0:T(8,128)(2,1)}, bf16[256,256]{1,0:T(8,128)(2,1)S(1)}, u32[]{:S(2)}, u32[]{:S(2)}) collective-permute-start(bf16[256,256]{1,0:T(8,128)(2,1)} %get-tuple-element.135), channel_id=1, source_target_pairs={{0,7},{1,6},{2,1},{3,0},{4,3},{5,2},{6,5},{7,4},{8,15},{9,14},{10,... | collective-permute-start | bytes 393224 | tf_op jit(solution)/shard_map/ppermute | solution.py:527
  214.9 1.5 collective-permute-start.30
  217.2 1.6 place.2.filled
  219.5 3.0 %collective-permute-done.30.rest_6_ = bf16[256,256]{1,0:T(8,128)(2,1)S(1)} collective-permute-done((bf16[256,256]{1,0:T(8,128)(2,1)}, bf16[256,256]{1,0:T(8,128)(2,1)S(1)}, u32[]{:S(2)}, u32[]{:S(2)}) %collective-permute-start.30) | collective-permute-done | bytes 131104 | tf_op jit(solution)/shard_map/ppermute | solution.py:527
  222.5 1.5 place.3
  (123 shorter events, 19.8 us)
Async XLA Ops:
  0.0 92.5 %collective-permute-start.10 = (bf16[256,2048]{1,0:T(8,128)(2,1)}, bf16[256,2048]{1,0:T(8,128)(2,1)}, u32[]{:S(2)}, u32[]{:S(2)}) collective-permute-start(bf16[256,2048]{1,0:T(8,128)(2,1)} %refs_8_.1), channel_id=1, source_target_pairs={{0,2},{2,4},{4,6},{6,0},{1,3},{3,5},{5,7},{7,1},{8,10},{10,12},{12... | collective-permute-start | bytes 3145736 | tf_op jit(solution)/shard_map/ppermute | solution.py:487
  2.1 124.6 %collective-permute-start.11 = (bf16[256,2048]{1,0:T(8,128)(2,1)}, bf16[256,2048]{1,0:T(8,128)(2,1)}, u32[]{:S(2)}, u32[]{:S(2)}) collective-permute-start(bf16[256,2048]{1,0:T(8,128)(2,1)} %refs_8_.1), channel_id=1, source_target_pairs={{0,6},{2,0},{4,2},{6,4},{1,7},{3,1},{5,3},{7,5},{8,14},{10,8},{12,... | collective-permute-start | bytes 3145736 | tf_op jit(solution)/shard_map/ppermute | solution.py:487
  9.4 28.3 %all-to-all-start = ((s32[16,1,16]{2,1,0:T(1,128)}), s32[16,1,16]{2,1,0:T(1,128)S(1)}, u32[]{:S(2)}, u32[]{:S(2)}) async-start(s32[16,1,16]{2,1,0:T(1,128)} %bitcast.8), calls=%async_computation | async-start | bytes 16384 | tf_op jit(solution)/shard_map/all_to_all | solution.py:478
  17.0 25.7 %collective-permute-start = (bf16[4,256,256]{2,1,0:T(8,128)(2,1)}, bf16[4,256,256]{2,1,0:T(8,128)(2,1)S(1)}, u32[]{:S(2)}, u32[]{:S(2)}) collective-permute-start(bf16[4,256,256]{2,1,0:T(8,128)(2,1)} %get-tuple-element.77), channel_id=1, source_target_pairs={{0,32},{1,33},{2,34},{3,35},{4,36},{5,37},{6,38},{7,39}} | collective-permute-start | bytes 1572872 | tf_op jit(solution)/shard_map/ppermute | solution.py:545
  20.3 22.4 %collective-permute-start.1 = (bf16[4,256,256]{2,1,0:T(8,128)(2,1)}, bf16[4,256,256]{2,1,0:T(8,128)(2,1)S(1)}, u32[]{:S(2)}, u32[]{:S(2)}) collective-permute-start(bf16[4,256,256]{2,1,0:T(8,128)(2,1)} %get-tuple-element.78), channel_id=1, source_target_pairs={{0,64},{1,65},{2,66},{3,67},{4,68},{5,69},{6,70},{7,71}} | collective-permute-start | bytes 1572872 | tf_op jit(solution)/shard_map/ppermute | solution.py:545
  22.5 20.2 %collective-permute-start.2 = (bf16[4,256,256]{2,1,0:T(8,128)(2,1)}, bf16[4,256,256]{2,1,0:T(8,128)(2,1)S(1)}, u32[]{:S(2)}, u32[]{:S(2)}) collective-permute-start(bf16[4,256,256]{2,1,0:T(8,128)(2,1)} %get-tuple-element.79), channel_id=1, source_target_pairs={{0,96},{1,97},{2,98},{3,99},{4,100},{5,101},{6,102},{7,103}} | collective-permute-start | bytes 1572872 | tf_op jit(solution)/shard_map/ppermute | solution.py:545
  42.7 13.0 %copy-start.27 = (f32[128]{0:T(128)S(1)}, f32[128]{0:T(128)}, u32[]{:S(2)}) copy-start(f32[128]{0:T(128)} %param.14) | copy-start | bytes 1540
  43.7 56.7 %all-to-all-start.1 = ((bf16[16,256,256]{2,1,0:T(8,128)(2,1)}), bf16[16,256,256]{2,1,0:T(8,128)(2,1)S(1)}, u32[]{:S(2)}, u32[]{:S(2)}) async-start(bf16[16,256,256]{2,1,0:T(8,128)(2,1)} %bitcast.43), calls=%async_computation.1 | async-start | bytes 4194304 | tf_op jit(solution)/shard_map/all_to_all | solution.py:478
  48.7 22.3 %collective-permute-start.3 = (bf16[256,256]{1,0:T(8,128)(2,1)S(1)}, bf16[256,256]{1,0:T(8,128)(2,1)S(1)}, u32[]{:S(2)}, u32[]{:S(2)}) collective-permute-start(bf16[256,256]{1,0:T(8,128)(2,1)S(1)} %get-tuple-element.143), channel_id=1, source_target_pairs={{0,24},{32,56},{64,88},{96,120},{1,25},{33,57},{65,89},{97,121},{2... | collective-permute-start | bytes 393224 | tf_op jit(solution)/shard_map/ppermute | solution.py:576
  53.1 17.9 %collective-permute-start.4 = (bf16[256,256]{1,0:T(8,128)(2,1)S(1)}, bf16[256,256]{1,0:T(8,128)(2,1)S(1)}, u32[]{:S(2)}, u32[]{:S(2)}) collective-permute-start(bf16[256,256]{1,0:T(8,128)(2,1)S(1)} %get-tuple-element.142), channel_id=1, source_target_pairs={{0,16},{32,48},{64,80},{96,112},{1,17},{33,49},{65,81},{97,113},{2... | collective-permute-start | bytes 393224 | tf_op jit(solution)/shard_map/ppermute | solution.py:576
  54.4 18.7 %collective-permute-start.5 = (bf16[256,256]{1,0:T(8,128)(2,1)S(1)}, bf16[256,256]{1,0:T(8,128)(2,1)S(1)}, u32[]{:S(2)}, u32[]{:S(2)}) collective-permute-start(bf16[256,256]{1,0:T(8,128)(2,1)S(1)} %get-tuple-element.141), channel_id=1, source_target_pairs={{0,8},{32,40},{64,72},{96,104},{1,9},{33,41},{65,73},{97,105},{2,1... | collective-permute-start | bytes 393224 | tf_op jit(solution)/shard_map/ppermute | solution.py:576
  74.2 13.3 %collective-permute-start.6 = (bf16[256,256]{1,0:T(8,128)(2,1)S(1)}, bf16[256,256]{1,0:T(8,128)(2,1)S(1)}, u32[]{:S(2)}, u32[]{:S(2)}) collective-permute-start(bf16[256,256]{1,0:T(8,128)(2,1)S(1)} %fusion.2), channel_id=1, source_target_pairs={{0,2},{2,4},{4,6},{6,0},{1,3},{3,5},{5,7},{7,1},{8,10},{10,12},{12... | collective-permute-start | bytes 393224 | tf_op jit(solution)/shard_map/ppermute | solution.py:487
  74.3 13.2 %collective-permute-start.7 = (bf16[256,256]{1,0:T(8,128)(2,1)S(1)}, bf16[256,256]{1,0:T(8,128)(2,1)S(1)}, u32[]{:S(2)}, u32[]{:S(2)}) collective-permute-start(bf16[256,256]{1,0:T(8,128)(2,1)S(1)} %fusion.2), channel_id=1, source_target_pairs={{0,6},{2,0},{4,2},{6,4},{1,7},{3,1},{5,3},{7,5},{8,14},{10,8},{12,... | collective-permute-start | bytes 393224 | tf_op jit(solution)/shard_map/ppermute | solution.py:487
  76.9 10.5 %collective-permute-start.8 = (bf16[256,256]{1,0:T(8,128)(2,1)S(1)}, bf16[256,256]{1,0:T(8,128)(2,1)S(1)}, u32[]{:S(2)}, u32[]{:S(2)}) collective-permute-start(bf16[256,256]{1,0:T(8,128)(2,1)S(1)} %fusion.2), channel_id=1, source_target_pairs={{0,4},{2,6},{4,0},{6,2},{1,5},{3,7},{5,1},{7,3},{8,12},{10,14},{12... | collective-permute-start | bytes 393224 | tf_op jit(solution)/shard_map/ppermute | solution.py:487
  87.5 6.8 %copy-start.7 = (bf16[4,256,256]{2,1,0:T(8,128)(2,1)}, bf16[4,256,256]{2,1,0:T(8,128)(2,1)S(1)}, u32[]{:S(2)}) copy-start(bf16[4,256,256]{2,1,0:T(8,128)(2,1)S(1)} %pad_maximum_fusion.same) | copy-start | bytes 1572868
  87.5 6.7 %collective-permute-start.9 = (bf16[4,256,256]{2,1,0:T(8,128)(2,1)S(1)}, bf16[4,256,256]{2,1,0:T(8,128)(2,1)S(1)}, u32[]{:S(2)}, u32[]{:S(2)}) collective-permute-start(bf16[4,256,256]{2,1,0:T(8,128)(2,1)S(1)} %pad_maximum_fusion.same), channel_id=1, source_target_pairs={{0,1},{1,0},{2,3},{3,2},{4,5},{5,4},{6,7},{7,6},{8,9},{9,8},{10,11... | collective-permute-start | bytes 1572872 | tf_op jit(solution)/shard_map/ppermute | solution.py:491
  92.5 34.3 %collective-permute-start.12 = (bf16[256,2048]{1,0:T(8,128)(2,1)}, bf16[256,2048]{1,0:T(8,128)(2,1)}, u32[]{:S(2)}, u32[]{:S(2)}) collective-permute-start(bf16[256,2048]{1,0:T(8,128)(2,1)} %collective-permute-done.10.refs_2_.refs_9_), channel_id=1, source_target_pairs={{0,2},{2,4},{4,6},{6,0},{1,3},{3,5},{5,7},{7,1},{8,10},{10,12},{12... | collective-permute-start | bytes 3145736 | tf_op jit(solution)/shard_map/ppermute | solution.py:487
  100.4 17.1 %copy-start.2 = (bf16[16,256,256]{2,1,0:T(8,128)(2,1)}, bf16[16,256,256]{2,1,0:T(8,128)(2,1)S(1)}, u32[]{:S(2)}) copy-start(bf16[16,256,256]{2,1,0:T(8,128)(2,1)S(1)} %all-to-all-done.1) | copy-start | bytes 6291460
  100.4 17.1 %all-to-all-start.2 = ((bf16[16,64,256]{2,1,0:T(8,128)(2,1)}), bf16[16,64,256]{2,1,0:T(8,128)(2,1)S(1)}, u32[]{:S(2)}, u32[]{:S(2)}) async-start(bf16[16,64,256]{2,1,0:T(8,128)(2,1)} %project_sent.1), calls=%async_computation.2 | async-start | bytes 1048576 | tf_op jit(solution)/shard_map/all_to_all | solution.py:478
  106.7 35.8 %collective-permute-start.13 = (bf16[256,2048]{1,0:T(8,128)(2,1)}, bf16[256,2048]{1,0:T(8,128)(2,1)}, u32[]{:S(2)}, u32[]{:S(2)}) collective-permute-start(bf16[256,2048]{1,0:T(8,128)(2,1)} %refs_8_.1), channel_id=1, source_target_pairs={{0,1},{1,0},{2,3},{3,2},{4,5},{5,4},{6,7},{7,6},{8,9},{9,8},{10,11... | collective-permute-start | bytes 3145736 | tf_op jit(solution)/shard_map/ppermute | solution.py:491
  126.7 30.8 %collective-permute-start.14 = (bf16[256,2048]{1,0:T(8,128)(2,1)}, bf16[256,2048]{1,0:T(8,128)(2,1)S(1)}, u32[]{:S(2)}, u32[]{:S(2)}) collective-permute-start(bf16[256,2048]{1,0:T(8,128)(2,1)} %collective-permute-done.10.refs_2_.refs_9_), channel_id=1, source_target_pairs={{0,1},{1,0},{2,3},{3,2},{4,5},{5,4},{6,7},{7,6},{8,9},{9,8},{10,11... | collective-permute-start | bytes 3145736 | tf_op jit(solution)/shard_map/ppermute | solution.py:491
  128.5 29.0 %collective-permute-start.15 = (bf16[256,2048]{1,0:T(8,128)(2,1)}, bf16[256,2048]{1,0:T(8,128)(2,1)S(1)}, u32[]{:S(2)}, u32[]{:S(2)}) collective-permute-start(bf16[256,2048]{1,0:T(8,128)(2,1)} %collective-permute-done.11.refs_3_.refs_10_), channel_id=1, source_target_pairs={{0,1},{1,0},{2,3},{3,2},{4,5},{5,4},{6,7},{7,6},{8,9},{9,8},{10,11... | collective-permute-start | bytes 3145736 | tf_op jit(solution)/shard_map/ppermute | solution.py:491
  128.6 28.9 %collective-permute-start.16 = (bf16[256,2048]{1,0:T(8,128)(2,1)}, bf16[256,2048]{1,0:T(8,128)(2,1)}, u32[]{:S(2)}, u32[]{:S(2)}) collective-permute-start(bf16[256,2048]{1,0:T(8,128)(2,1)} %collective-permute-done.12.refs_4_.refs_11_), channel_id=1, source_target_pairs={{0,1},{1,0},{2,3},{3,2},{4,5},{5,4},{6,7},{7,6},{8,9},{9,8},{10,11... | collective-permute-start | bytes 3145736 | tf_op jit(solution)/shard_map/ppermute | solution.py:491
  138.6 18.9 %all-to-all-start.3 = ((bf16[8,256,256]{2,1,0:T(8,128)(2,1)}), bf16[8,256,256]{2,1,0:T(8,128)(2,1)S(1)}, u32[]{:S(2)}, u32[]{:S(2)}) async-start(bf16[8,256,256]{2,1,0:T(8,128)(2,1)} %attend.2), calls=%async_computation.3 | async-start | bytes 2097152 | tf_op jit(solution)/shard_map/all_to_all | solution.py:478
  166.7 6.1 %copy-start.25 = (bf16[256,256]{1,0:T(8,128)(2,1)S(1)}, bf16[256,256]{1,0:T(8,128)(2,1)}, u32[]{:S(2)}) copy-start(bf16[256,256]{1,0:T(8,128)(2,1)} %get-tuple-element.115) | copy-start | bytes 393220
  166.7 7.4 %copy-start.24 = (bf16[256,256]{1,0:T(8,128)(2,1)S(1)}, bf16[256,256]{1,0:T(8,128)(2,1)}, u32[]{:S(2)}) copy-start(bf16[256,256]{1,0:T(8,128)(2,1)} %get-tuple-element.116) | copy-start | bytes 393220
  166.7 9.0 %copy-start.23 = (bf16[256,256]{1,0:T(8,128)(2,1)S(1)}, bf16[256,256]{1,0:T(8,128)(2,1)}, u32[]{:S(2)}) copy-start(bf16[256,256]{1,0:T(8,128)(2,1)} %get-tuple-element.117) | copy-start | bytes 393220
  166.7 10.3 %copy-start.22 = (bf16[256,256]{1,0:T(8,128)(2,1)S(1)}, bf16[256,256]{1,0:T(8,128)(2,1)}, u32[]{:S(2)}) copy-start(bf16[256,256]{1,0:T(8,128)(2,1)} %get-tuple-element.118) | copy-start | bytes 393220
  166.7 22.3 %copy-start.21 = (bf16[256,256]{1,0:T(8,128)(2,1)S(1)}, bf16[256,256]{1,0:T(8,128)(2,1)}, u32[]{:S(2)}) copy-start(bf16[256,256]{1,0:T(8,128)(2,1)} %get-tuple-element.119) | copy-start | bytes 393220
  166.8 24.1 %copy-start.20 = (bf16[256,256]{1,0:T(8,128)(2,1)S(1)}, bf16[256,256]{1,0:T(8,128)(2,1)}, u32[]{:S(2)}) copy-start(bf16[256,256]{1,0:T(8,128)(2,1)} %get-tuple-element.120) | copy-start | bytes 393220
  166.8 49.6 %all-to-all-start.4 = ((bf16[8,256,256]{2,1,0:T(8,128)(2,1)}), bf16[8,256,256]{2,1,0:T(8,128)(2,1)S(1)}, u32[]{:S(2)}, u32[]{:S(2)}) async-start(bf16[8,256,256]{2,1,0:T(8,128)(2,1)} %project_out.2), calls=%async_computation.4 | async-start | bytes 2097152 | tf_op jit(solution)/shard_map/all_to_all | solution.py:478
  171.3 45.0 %copy-start.1 = (s32[8]{0:T(128)S(1)}, s32[8]{0:T(128)}, u32[]{:S(2)}) copy-start(s32[8]{0:T(128)} %pad_add_fusion.1.order) | copy-start | bytes 100
  171.3 17.7 %collective-permute-start.17 = (bf16[256,256]{1,0:T(8,128)(2,1)S(1)}, bf16[256,256]{1,0:T(8,128)(2,1)S(1)}, u32[]{:S(2)}, u32[]{:S(2)}) collective-permute-start(bf16[256,256]{1,0:T(8,128)(2,1)S(1)} %copy-done.26), channel_id=1, source_target_pairs={{0,2},{1,3},{2,4},{3,5},{4,6},{5,7},{6,0},{7,1},{8,10},{9,11},{10,... | collective-permute-start | bytes 393224 | tf_op jit(solution)/shard_map/ppermute | solution.py:527
  172.8 18.1 %collective-permute-start.18 = (bf16[256,256]{1,0:T(8,128)(2,1)S(1)}, bf16[256,256]{1,0:T(8,128)(2,1)S(1)}, u32[]{:S(2)}, u32[]{:S(2)}) collective-permute-start(bf16[256,256]{1,0:T(8,128)(2,1)S(1)} %copy-done.25), channel_id=1, source_target_pairs={{0,6},{1,7},{2,0},{3,1},{4,2},{5,3},{6,4},{7,5},{8,14},{9,15},{10,... | collective-permute-start | bytes 393224 | tf_op jit(solution)/shard_map/ppermute | solution.py:527
  174.1 19.1 %collective-permute-start.19 = (bf16[256,256]{1,0:T(8,128)(2,1)S(1)}, bf16[256,256]{1,0:T(8,128)(2,1)S(1)}, u32[]{:S(2)}, u32[]{:S(2)}) collective-permute-start(bf16[256,256]{1,0:T(8,128)(2,1)S(1)} %copy-done.24), channel_id=1, source_target_pairs={{0,4},{1,5},{2,6},{3,7},{4,0},{5,1},{6,2},{7,3},{8,12},{9,13},{10,... | collective-permute-start | bytes 393224 | tf_op jit(solution)/shard_map/ppermute | solution.py:527
  175.8 17.4 %collective-permute-start.20 = (bf16[256,256]{1,0:T(8,128)(2,1)S(1)}, bf16[256,256]{1,0:T(8,128)(2,1)S(1)}, u32[]{:S(2)}, u32[]{:S(2)}) collective-permute-start(bf16[256,256]{1,0:T(8,128)(2,1)S(1)} %copy-done.23), channel_id=1, source_target_pairs={{0,1},{1,0},{2,3},{3,2},{4,5},{5,4},{6,7},{7,6},{8,9},{9,8},{10,11... | collective-permute-start | bytes 393224 | tf_op jit(solution)/shard_map/ppermute | solution.py:527
  177.0 18.1 %collective-permute-start.21 = (bf16[256,256]{1,0:T(8,128)(2,1)S(1)}, bf16[256,256]{1,0:T(8,128)(2,1)S(1)}, u32[]{:S(2)}, u32[]{:S(2)}) collective-permute-start(bf16[256,256]{1,0:T(8,128)(2,1)S(1)} %copy-done.22), channel_id=1, source_target_pairs={{0,3},{1,2},{2,5},{3,4},{4,7},{5,6},{6,1},{7,0},{8,11},{9,10},{10,... | collective-permute-start | bytes 393224 | tf_op jit(solution)/shard_map/ppermute | solution.py:527
  189.1 8.9 %copy-start.12 = (bf16[256,256]{1,0:T(8,128)(2,1)}, bf16[256,256]{1,0:T(8,128)(2,1)S(1)}, u32[]{:S(2)}) copy-start(bf16[256,256]{1,0:T(8,128)(2,1)S(1)} %collective-permute-done.17.refs_1_) | copy-start | bytes 393220
  189.1 6.0 %collective-permute-start.22 = (bf16[256,256]{1,0:T(8,128)(2,1)S(1)}, bf16[256,256]{1,0:T(8,128)(2,1)S(1)}, u32[]{:S(2)}, u32[]{:S(2)}) collective-permute-start(bf16[256,256]{1,0:T(8,128)(2,1)S(1)} %copy-done.21), channel_id=1, source_target_pairs={{0,7},{1,6},{2,1},{3,0},{4,3},{5,2},{6,5},{7,4},{8,15},{9,14},{10,... | collective-permute-start | bytes 393224 | tf_op jit(solution)/shard_map/ppermute | solution.py:527
  190.9 7.0 %copy-start.13 = (bf16[256,256]{1,0:T(8,128)(2,1)}, bf16[256,256]{1,0:T(8,128)(2,1)S(1)}, u32[]{:S(2)}) copy-start(bf16[256,256]{1,0:T(8,128)(2,1)S(1)} %collective-permute-done.18.refs_2_) | copy-start | bytes 393220
  190.9 7.0 %collective-permute-start.23 = (bf16[256,256]{1,0:T(8,128)(2,1)S(1)}, bf16[256,256]{1,0:T(8,128)(2,1)S(1)}, u32[]{:S(2)}, u32[]{:S(2)}) collective-permute-start(bf16[256,256]{1,0:T(8,128)(2,1)S(1)} %copy-done.20), channel_id=1, source_target_pairs={{0,5},{1,4},{2,7},{3,6},{4,1},{5,0},{6,3},{7,2},{8,13},{9,12},{10,... | collective-permute-start | bytes 393224 | tf_op jit(solution)/shard_map/ppermute | solution.py:527
  206.1 6.3 %collective-permute-start.24 = (bf16[256,256]{1,0:T(8,128)(2,1)}, bf16[256,256]{1,0:T(8,128)(2,1)S(1)}, u32[]{:S(2)}, u32[]{:S(2)}) collective-permute-start(bf16[256,256]{1,0:T(8,128)(2,1)} %get-tuple-element.130), channel_id=1, source_target_pairs={{0,2},{1,3},{2,4},{3,5},{4,6},{5,7},{6,0},{7,1},{8,10},{9,11},{10,... | collective-permute-start | bytes 393224 | tf_op jit(solution)/shard_map/ppermute | solution.py:527
  207.3 7.6 %collective-permute-start.25 = (bf16[256,256]{1,0:T(8,128)(2,1)}, bf16[256,256]{1,0:T(8,128)(2,1)S(1)}, u32[]{:S(2)}, u32[]{:S(2)}) collective-permute-start(bf16[256,256]{1,0:T(8,128)(2,1)} %get-tuple-element.131), channel_id=1, source_target_pairs={{0,6},{1,7},{2,0},{3,1},{4,2},{5,3},{6,4},{7,5},{8,14},{9,15},{10,... | collective-permute-start | bytes 393224 | tf_op jit(solution)/shard_map/ppermute | solution.py:527
  208.9 10.0 %collective-permute-start.26 = (bf16[256,256]{1,0:T(8,128)(2,1)}, bf16[256,256]{1,0:T(8,128)(2,1)S(1)}, u32[]{:S(2)}, u32[]{:S(2)}) collective-permute-start(bf16[256,256]{1,0:T(8,128)(2,1)} %get-tuple-element.132), channel_id=1, source_target_pairs={{0,4},{1,5},{2,6},{3,7},{4,0},{5,1},{6,2},{7,3},{8,12},{9,13},{10,... | collective-permute-start | bytes 393224 | tf_op jit(solution)/shard_map/ppermute | solution.py:527
  209.6 9.3 %collective-permute-start.27 = (bf16[256,256]{1,0:T(8,128)(2,1)}, bf16[256,256]{1,0:T(8,128)(2,1)S(1)}, u32[]{:S(2)}, u32[]{:S(2)}) collective-permute-start(bf16[256,256]{1,0:T(8,128)(2,1)} %get-tuple-element.133), channel_id=1, source_target_pairs={{0,1},{1,0},{2,3},{3,2},{4,5},{5,4},{6,7},{7,6},{8,9},{9,8},{10,11... | collective-permute-start | bytes 393224 | tf_op jit(solution)/shard_map/ppermute | solution.py:527
  210.2 9.0 %collective-permute-start.28 = (bf16[256,256]{1,0:T(8,128)(2,1)}, bf16[256,256]{1,0:T(8,128)(2,1)S(1)}, u32[]{:S(2)}, u32[]{:S(2)}) collective-permute-start(bf16[256,256]{1,0:T(8,128)(2,1)} %get-tuple-element.134), channel_id=1, source_target_pairs={{0,3},{1,2},{2,5},{3,4},{4,7},{5,6},{6,1},{7,0},{8,11},{9,10},{10,... | collective-permute-start | bytes 393224 | tf_op jit(solution)/shard_map/ppermute | solution.py:527
  212.4 7.2 %collective-permute-start.29 = (bf16[256,256]{1,0:T(8,128)(2,1)}, bf16[256,256]{1,0:T(8,128)(2,1)S(1)}, u32[]{:S(2)}, u32[]{:S(2)}) collective-permute-start(bf16[256,256]{1,0:T(8,128)(2,1)} %get-tuple-element.135), channel_id=1, source_target_pairs={{0,7},{1,6},{2,1},{3,0},{4,3},{5,2},{6,5},{7,4},{8,15},{9,14},{10,... | collective-permute-start | bytes 393224 | tf_op jit(solution)/shard_map/ppermute | solution.py:527
  214.9 7.6 %collective-permute-start.30 = (bf16[256,256]{1,0:T(8,128)(2,1)}, bf16[256,256]{1,0:T(8,128)(2,1)S(1)}, u32[]{:S(2)}, u32[]{:S(2)}) collective-permute-start(bf16[256,256]{1,0:T(8,128)(2,1)} %get-tuple-element.136), channel_id=1, source_target_pairs={{0,5},{1,4},{2,7},{3,6},{4,1},{5,0},{6,3},{7,2},{8,13},{9,12},{10,... | collective-permute-start | bytes 393224 | tf_op jit(solution)/shard_map/ppermute | solution.py:527
  (16 other events, 37.4 us)

commit v9 on v8

--- a/solution.py
+++ b/solution.py
@@ -22,6 +22,7 @@
 bf16 = jnp.bfloat16
 f32 = jnp.float32
 VMEM_LIMIT = 60 * 1024 * 1024
+KERNEL_LIMIT = 48 * 1024 * 1024
 
 
 def head_norm(values, gain_row):
@@ -315,7 +316,7 @@
         for n in range(count):
 
             def put(rows, lanes, value, n=n):
-                outs[n][rows, lanes] = value.astype(bf16)
+                outs[n % len(outs)][n // len(outs), rows, lanes] = value.astype(bf16)
 
             piece_of(n, put)
 
@@ -326,8 +327,8 @@
     slots = mask.shape[1] // BLOCK
     rows = length // ranks
     anywhere = pl.BlockSpec(memory_space=pl.ANY)
-    shape = (rows, WIDTH) if split else (ranks, rows, WIDTH)
-    count = ranks if split else 1
+    shape = (2, rows, WIDTH) if split else (ranks, rows, WIDTH)
+    count = ranks // 2 if split else 1
     height = pairs.shape[0] + near.shape[0] + HOT * PAIR * BLOCK
     outs = pl.pallas_call(
         functools.partial(attention_kernel, first),
@@ -364,7 +365,8 @@
     count = order.shape[0]
     n = pl.program_id(0)
     if len(refs) > 2 * count + 4:
-        pieces, refs = refs[:count], refs[count:]
+        pieces = [ref.at[0] for ref in refs[: count // 2]] + list(refs[count // 2 : count])
+        refs = refs[count:]
     else:
         pieces, refs = [refs[0].at[order[k]] for k in range(count)], refs[1:]
     weights, gain, refs = refs[:count], refs[count], refs[count + 1 :]
@@ -409,7 +411,7 @@
         grid_spec=pltpu.PrefetchScalarGridSpec(
             num_scalar_prefetch=2,
             grid=(width // tile,),
-            in_specs=[whole_block(*shape)] * len(pieces)
+            in_specs=[whole_block(*piece.shape) for piece in pieces]
             + [pl.BlockSpec((depth, tile), lambda n, *_: (0, n))] * count
             + [whole_block(*gain.shape)],
             out_specs=[whole_block(*shape)] * len(pieces),
@@ -419,7 +421,7 @@
             ],
         ),
         out_shape=[jax.ShapeDtypeStruct(shape, bf16)] * len(pieces),
-        compiler_params=pltpu.CompilerParams(vmem_limit_bytes=VMEM_LIMIT),
+        compiler_params=pltpu.CompilerParams(vmem_limit_bytes=KERNEL_LIMIT),
         cost_estimate=pl.CostEstimate(
             flops=2 * rows * width * width, bytes_accessed=12 << 20, transcendentals=0
         ),
@@ -512,6 +514,15 @@
     c = lax.axis_index(TP[1])
     rows = jnp.stack([(y + ring + sign * d) % ring for d in OFFSETS])
     return jnp.concatenate([2 * rows + c, 2 * rows + 1 - c]).astype(jnp.int32)
+
+
+def along_ring(pieces):
+    ring = lax.axis_size(TP[0])
+    got = [pieces[0]]
+    for k in range(1, ring):
+        pairs = [(y, (y - OFFSETS[k]) % ring) for y in range(ring)]
+        got.append(lax.ppermute(pieces[k], TP[0], pairs))
+    return got
 
 
 def send_pieces(pieces):
@@ -614,10 +625,11 @@
     *second, w_after, w_before, w_far = tied(*second, w_after, w_before, w_far)
     w_swapped = [across(w_after), across(w_before), across(w_far)]
     weights = [w_out, w_after, w_before, w_far, w_own] + w_swapped
-    second = send_pieces(second)
+    second = along_ring(second)
     first = project_out(False, order, same_order, first, weights, gains)
     moved = exchange(first, TP)
-    second = tied(first, *second)[1:]
+    second = list(tied(first, *second)[1:])
+    second += [across(pair[1]) for pair in second]
     second = project_out(True, order, toward, second, weights, gains)
     second = send_pieces(second)
     filled = place(place_whole_kernel, length, order, moved.reshape(-1, WIDTH), second[0])

time: 225 us -> 230 us (1.022)
  the two profiles are of different devices: /device:TPU:1 before, /device:TPU:9 now
where the time goes in v9:
time: 230 us; the launch traced here: 229 us
  Pallas kernels  102 us (44%)
  starting transfers between devices  72.7 us (32%)
  waiting for transfers between devices  38 us (17%)
  local copies, waits for them, and re-layouts  8.32 us (4%)
  other arithmetic  8 us (3%)
    pallas_call x2, Pallas kernels, place(): pl.pallas_call(kernel, grid_spec=pltpu.PrefetchScalarGridSpec(num_scalar_...  35 us
    all_to_all x5, starting transfers between devices, exchange(): return lax.all_to_all(pieces, axes, split_axis=0, concat_axis=0, tiled=True)  29 us
    ppermute x3, waiting for transfers between devices, local(): lax.ppermute(held[n], KV, [(i, i + n) for i in starts])  18.8 us
    pallas_call x2, Pallas kernels, attend(): pl.pallas_call(functools.partial(attention_kernel, first), grid_spec=pltp...  17.9 us
    all_to_all x5, waiting for transfers between devices, exchange(): return lax.all_to_all(pieces, axes, split_axis=0, concat_axis=0, tiled=True)  17.9 us
    pallas_call x1, Pallas kernels, project_kv(): pl.pallas_call(kv_kernel, grid=(length // tile,), in_specs=[pl.BlockSpec(...  13.7 us
    pallas_call x2, Pallas kernels, project_out(): pl.pallas_call(out_kernel, grid_spec=pltpu.PrefetchScalarGridSpec(num_sca...  11.8 us
    ppermute x7, starting transfers between devices, send_pieces(): got.append(lax.ppermute(pieces[k], TP, pairs) if k else pieces[0])  11.6 us
  transfers between devices with their start and end apart: 36, of which 7 were waited for; matrix products, arithmetic and copies ran while one was open for 6% of the time, Pallas kernels for 44%

profile of v9, /device:TPU:9, one launch (start us, length us, event | category | flops | bytes accessed | tf_op | source)
XLA Modules:
  0.0 229.3 jit_solution(2941207325146701596)
XLA Ops:
  0.0 1.3 collective-permute-start.10
  1.5 4.0 %token_shares.1 = (bf16[4,256,256]{2,1,0:T(8,128)(2,1)}, bf16[4,256,256]{2,1,0:T(8,128)(2,1)}, bf16[4,256,256]{2,1,0:T(8,128)(2,1)}, bf16[4,256,256]{2,1,0:T(8,128)(2,1)}) custom-call(s32[1]{0:T(128)} %bitcast.5.rank, bf16[4096,2048]{1,0:T(8,128)(2,1)} %tok.4), custom_call_target="tpu_custom_call" | custom-call | flops 1048576 | bytes 4194304 | tf_op jit(solution)/shard_map/token_shares/pallas_call | solution.py:52
  7.3 7.6 %all-to-all-start = ((s32[16,1,16]{2,1,0:T(1,128)}), s32[16,1,16]{2,1,0:T(1,128)S(1)}, u32[]{:S(2)}, u32[]{:S(2)}) async-start(s32[16,1,16]{2,1,0:T(1,128)} %bitcast.8), calls=%async_computation | async-start | bytes 16384 | tf_op jit(solution)/shard_map/all_to_all | solution.py:480
  14.9 3.3 %collective-permute-start = (bf16[4,256,256]{2,1,0:T(8,128)(2,1)}, bf16[4,256,256]{2,1,0:T(8,128)(2,1)S(1)}, u32[]{:S(2)}, u32[]{:S(2)}) collective-permute-start(bf16[4,256,256]{2,1,0:T(8,128)(2,1)} %get-tuple-element.65), channel_id=1, source_target_pairs={{0,32},{1,33},{2,34},{3,35},{4,36},{5,37},{6,38},{7,39}} | collective-permute-start | bytes 1572872 | tf_op jit(solution)/shard_map/ppermute | solution.py:556
  18.2 2.2 collective-permute-start.1
  20.4 2.1 collective-permute-start.2
  22.5 13.7 %project_kv.1 = bf16[64,2,64,256]{3,2,1,0:T(8,128)(2,1)} custom-call(bf16[4096,2048]{1,0:T(8,128)(2,1)} %tok.4, bf16[2048,256]{1,0:T(8,128)(2,1)} %wk.3, bf16[2048,256]{1,0:T(8,128)(2,1)} %wv.3, f32[1,128]{1,0:T(1,128)} %bitcast.57), custom_call_target="tpu_custom_call" | custom-call | flops 8589934592 | bytes 16777216 | tf_op jit(solution)/shard_map/project_kv/pallas_call | solution.py:83
  37.0 4.2 %gather_near.1 = bf16[32,128,256]{2,1,0:T(8,128)(2,1)} custom-call(s32[32]{0:T(128)} %reshape.69.near, bf16[8192,256]{1,0:T(8,128)(2,1)} %bitcast.47), custom_call_target="tpu_custom_call" | custom-call | flops 1048576 | bytes 4194304 | tf_op jit(solution)/shard_map/gather_near/pallas_call | solution.py:151
  42.1 4.6 %all-to-all-start.1 = ((bf16[16,256,256]{2,1,0:T(8,128)(2,1)}), bf16[16,256,256]{2,1,0:T(8,128)(2,1)}, u32[]{:S(2)}, u32[]{:S(2)}) async-start(bf16[16,256,256]{2,1,0:T(8,128)(2,1)} %bitcast.50), calls=%async_computation.1 | async-start | bytes 4194304 | tf_op jit(solution)/shard_map/all_to_all | solution.py:480
  46.7 1.3 select_bitcast_fusion
  47.9 4.3 %collective-permute-start.3 = (bf16[256,256]{1,0:T(8,128)(2,1)S(1)}, bf16[256,256]{1,0:T(8,128)(2,1)S(1)}, u32[]{:S(2)}, u32[]{:S(2)}) collective-permute-start(bf16[256,256]{1,0:T(8,128)(2,1)S(1)} %get-tuple-element.119), channel_id=1, source_target_pairs={{0,24},{32,56},{64,88},{96,120},{1,25},{33,57},{65,89},{97,121},{2... | collective-permute-start | bytes 393224 | tf_op jit(solution)/shard_map/ppermute | solution.py:587
  52.3 1.3 collective-permute-start.4
  53.6 1.3 collective-permute-start.5
  55.5 15.0 %collective-permute-done.3 = bf16[256,256]{1,0:T(8,128)(2,1)S(1)} collective-permute-done((bf16[256,256]{1,0:T(8,128)(2,1)S(1)}, bf16[256,256]{1,0:T(8,128)(2,1)S(1)}, u32[]{:S(2)}, u32[]{:S(2)}) %collective-permute-start.3) | collective-permute-done | bytes 131104 | tf_op jit(solution)/shard_map/ppermute | solution.py:587
  70.5 0.9 collective-permute-done.4
  71.4 2.8 %collective-permute-done.5 = bf16[256,256]{1,0:T(8,128)(2,1)S(1)} collective-permute-done((bf16[256,256]{1,0:T(8,128)(2,1)S(1)}, bf16[256,256]{1,0:T(8,128)(2,1)S(1)}, u32[]{:S(2)}, u32[]{:S(2)}) %collective-permute-start.5) | collective-permute-done | bytes 131104 | tf_op jit(solution)/shard_map/ppermute | solution.py:587
  74.3 1.0 fusion.2
  75.3 1.4 collective-permute-start.6
  77.1 1.8 collective-permute-start.8
  78.8 10.1 %project_q.1.queries = bf16[4096,256]{1,0:T(8,128)(2,1)} custom-call(bf16[4096,2048]{1,0:T(8,128)(2,1)} %tok.4, bf16[2048,256]{1,0:T(8,128)(2,1)} %wq.1, f32[1,128]{1,0:T(1,128)} %multiply_bitcast_fusion.gain), custom_call_target="tpu_custom_call" | custom-call | flops 4294967296 | bytes 16777216 | tf_op jit(solution)/shard_map/project_q/pallas_call | solution.py:112
  88.9 0.9 pad_maximum_fusion.same
  89.8 3.4 %collective-permute-start.9 = (bf16[4,256,256]{2,1,0:T(8,128)(2,1)}, bf16[4,256,256]{2,1,0:T(8,128)(2,1)}, u32[]{:S(2)}, u32[]{:S(2)}) collective-permute-start(bf16[4,256,256]{2,1,0:T(8,128)(2,1)} %pad_maximum_fusion.same), channel_id=1, source_target_pairs={{0,1},{1,0},{2,3},{3,2},{4,5},{5,4},{6,7},{7,6},{8,9},{9,8},{10,11... | collective-permute-start | bytes 1572872 | tf_op jit(solution)/shard_map/ppermute | solution.py:493
  93.8 1.9 collective-permute-start.12
  97.2 4.9 %project_sent.1 = bf16[16,64,256]{2,1,0:T(8,128)(2,1)} custom-call(s32[128]{0:T(128)} %reshape.68.asked, s32[8]{0:T(128)} %pad_add_fusion.1.order, bf16[4,256,256]{2,1,0:T(8,128)(2,1)} %pad_maximum_fusion.same, bf16[4,256,256]{2,1,0:T(8,128)(2,1)} %collective-permute-done.9.other, bf16[2048,256]{1,0:T(8,128)(2,1)} %wk.3, bf16[2048,256]{1,0:T(8,128)(2,1)} %wv.3, ...), custom_call_target="tpu_custom_call" | custom-call | flops 536870912 | bytes 8388608 | tf_op jit(solution)/shard_map/project_sent/pallas_call | solution.py:211
  102.6 5.8 %all-to-all-start.2 = ((bf16[16,64,256]{2,1,0:T(8,128)(2,1)}), bf16[16,64,256]{2,1,0:T(8,128)(2,1)}, u32[]{:S(2)}, u32[]{:S(2)}) async-start(bf16[16,64,256]{2,1,0:T(8,128)(2,1)} %project_sent.1), calls=%async_computation.2 | async-start | bytes 1048576 | tf_op jit(solution)/shard_map/all_to_all | solution.py:480
  109.3 1.3 select_reduce_fusion
  112.2 7.1 %all-to-all-done.2.hot = bf16[16,64,256]{2,1,0:T(8,128)(2,1)} async-done(((bf16[16,64,256]{2,1,0:T(8,128)(2,1)}), bf16[16,64,256]{2,1,0:T(8,128)(2,1)}, u32[]{:S(2)}, u32[]{:S(2)}) %all-to-all-start.2) | async-done | bytes 524320 | tf_op jit(solution)/shard_map/all_to_all | solution.py:480
  119.3 8.4 %attend.3 = (bf16[2,256,256]{2,1,0:T(8,128)(2,1)}, bf16[2,256,256]{2,1,0:T(8,128)(2,1)}, bf16[2,256,256]{2,1,0:T(8,128)(2,1)}, bf16[2,256,256]{2,1,0:T(8,128)(2,1)}) custom-call(s32[512]{0:T(512)} %reshape.71.at, s32[8]{0:T(128)} %pad_add_fusion.2.where.slot, bf16[4096,256]{1,0:T(8,128)(2,1)} %project_q.1.queries, f32[64,512]{1,0:T(8,128)} %reshape.72.masks, ...), custom_call_target="tpu_custom_call" | custom-call | flops 2147483648 | bytes 10485760 | tf_op jit(solution)/shard_map/attend/pallas_call | solution.py:333
  127.7 1.7 collective-permute-start.14
  129.9 9.5 %attend.2 = bf16[8,256,256]{2,1,0:T(8,128)(2,1)} custom-call(s32[512]{0:T(512)} %reshape.71.at, s32[8]{0:T(128)} %iota.15.where.slot, bf16[4096,256]{1,0:T(8,128)(2,1)} %project_q.1.queries, f32[64,512]{1,0:T(8,128)} %reshape.72.masks, bf16[8192,256]{1,0:T(8,128)(2,1)} %bitcast.49, bf16[4096,256]{1,0:T(8,128)(2,1)} %bitcast.22.near, ...), custom_call_target="tpu_custom_call" | custom-call | flops 2147483648 | bytes 10485760 | tf_op jit(solution)/shard_map/attend/pallas_call | solution.py:333
  139.5 4.2 %all-to-all-start.3 = ((bf16[8,256,256]{2,1,0:T(8,128)(2,1)}), bf16[8,256,256]{2,1,0:T(8,128)(2,1)}, u32[]{:S(2)}, u32[]{:S(2)}) async-start(bf16[8,256,256]{2,1,0:T(8,128)(2,1)} %attend.2), calls=%async_computation.3 | async-start | bytes 2097152 | tf_op jit(solution)/shard_map/all_to_all | solution.py:480
  145.3 1.2 collective-permute-start.19
  146.5 10.8 %all-to-all-done.3.refs_0_ = bf16[8,256,256]{2,1,0:T(8,128)(2,1)} async-done(((bf16[8,256,256]{2,1,0:T(8,128)(2,1)}), bf16[8,256,256]{2,1,0:T(8,128)(2,1)}, u32[]{:S(2)}, u32[]{:S(2)}) %all-to-all-start.3) | async-done | bytes 1048608 | tf_op jit(solution)/shard_map/all_to_all | solution.py:480
  157.3 5.6 %project_out.2 = bf16[8,256,256]{2,1,0:T(8,128)(2,1)S(1)} custom-call(s32[8]{0:T(128)S(1)} %copy-done.4, s32[8]{0:T(128)S(1)} %copy-done.6, bf16[8,256,256]{2,1,0:T(8,128)(2,1)} %all-to-all-done.3.refs_0_, bf16[256,2048]{1,0:T(8,128)(2,1)S(1)} %copy-done, bf16[256,2048]{1,0:T(8,128)(2,1)S(1)} %collective-permute-done.10.refs_2_.refs_9_, ...), custom_call_target="tpu_custom_call" | custom-call | flops 2147483648 | bytes 12582912 | tf_op jit(solution)/shard_map/project_out/pallas_call | solution.py:409
  162.9 1.0 copy-done.1
  163.8 6.8 %all-to-all-start.4 = ((bf16[8,256,256]{2,1,0:T(8,128)(2,1)}), bf16[8,256,256]{2,1,0:T(8,128)(2,1)}, u32[]{:S(2)}, u32[]{:S(2)}) async-start(bf16[8,256,256]{2,1,0:T(8,128)(2,1)} %copy-done.1), calls=%async_computation.4 | async-start | bytes 2097152 | tf_op jit(solution)/shard_map/all_to_all | solution.py:480
  171.2 0.9 slice_bitcast_fusion.2
  172.3 0.9 slice_bitcast_fusion.1
  173.7 0.9 slice_bitcast_fusion
  174.8 1.2 collective-permute-done.23.refs_7_
  176.1 6.3 %project_out.3 = (bf16[256,256]{1,0:T(8,128)(2,1)S(1)}, bf16[256,256]{1,0:T(8,128)(2,1)S(1)}, bf16[256,256]{1,0:T(8,128)(2,1)S(1)}, bf16[256,256]{1,0:T(8,128)(2...) custom-call(s32[8]{0:T(128)S(1)} %copy-done.4, ...), custom_call_target="tpu_custom_call" | custom-call | flops 2147483648 | bytes 12582912 | tf_op jit(solution)/shard_map/project_out/pallas_call | solution.py:409
  182.3 1.2 collective-permute-start.24
  183.8 1.8 collective-permute-start.26
  185.6 1.0 collective-permute-start.27
  187.3 2.2 collective-permute-start.29
  189.5 4.6 %collective-permute-start.30 = (bf16[256,256]{1,0:T(8,128)(2,1)}, bf16[256,256]{1,0:T(8,128)(2,1)S(1)}, u32[]{:S(2)}, u32[]{:S(2)}) collective-permute-start(bf16[256,256]{1,0:T(8,128)(2,1)} %get-tuple-element.112), channel_id=1, source_target_pairs={{0,5},{1,4},{2,7},{3,6},{4,1},{5,0},{6,3},{7,2},{8,13},{9,12},{10,... | collective-permute-start | bytes 393224 | tf_op jit(solution)/shard_map/ppermute | solution.py:538
  194.1 33.4 %place.2.filled = bf16[4096,256]{1,0:T(8,128)(2,1)} custom-call(s32[8]{0:T(128)S(1)} %copy-done.4, bf16[2048,256]{1,0:T(8,128)(2,1)} %bitcast.24.whole, bf16[256,256]{1,0:T(8,128)(2,1)S(1)} %get-tuple-element.105.own), custom_call_target="tpu_custom_call" | custom-call | flops 1048576 | bytes 4194304 | tf_op jit(solution)/shard_map/place/pallas_call | solution.py:462
  227.6 1.5 place.3
  (93 shorter events, 14.0 us)
Async XLA Ops:
  0.0 93.8 %collective-permute-start.10 = (bf16[256,2048]{1,0:T(8,128)(2,1)}, bf16[256,2048]{1,0:T(8,128)(2,1)S(1)}, u32[]{:S(2)}, u32[]{:S(2)}) collective-permute-start(bf16[256,2048]{1,0:T(8,128)(2,1)} %refs_8_.1), channel_id=1, source_target_pairs={{0,2},{2,4},{4,6},{6,0},{1,3},{3,5},{5,7},{7,1},{8,10},{10,12},{12... | collective-permute-start | bytes 3145736 | tf_op jit(solution)/shard_map/ppermute | solution.py:489
  1.3 126.3 %collective-permute-start.11 = (bf16[256,2048]{1,0:T(8,128)(2,1)}, bf16[256,2048]{1,0:T(8,128)(2,1)S(1)}, u32[]{:S(2)}, u32[]{:S(2)}) collective-permute-start(bf16[256,2048]{1,0:T(8,128)(2,1)} %refs_8_.1), channel_id=1, source_target_pairs={{0,6},{2,0},{4,2},{6,4},{1,7},{3,1},{5,3},{7,5},{8,14},{10,8},{12,... | collective-permute-start | bytes 3145736 | tf_op jit(solution)/shard_map/ppermute | solution.py:489
  1.5 4.0 %copy-start.9 = (s32[64,8]{0,1:T(8,128)S(1)}, s32[64,8]{0,1:T(8,128)}, u32[]{:S(2)}) copy-start(s32[64,8]{0,1:T(8,128)} %param.17) | copy-start | bytes 6148
  7.3 29.1 %all-to-all-start = ((s32[16,1,16]{2,1,0:T(1,128)}), s32[16,1,16]{2,1,0:T(1,128)S(1)}, u32[]{:S(2)}, u32[]{:S(2)}) async-start(s32[16,1,16]{2,1,0:T(1,128)} %bitcast.8), calls=%async_computation | async-start | bytes 16384 | tf_op jit(solution)/shard_map/all_to_all | solution.py:480
  14.9 26.3 %collective-permute-start = (bf16[4,256,256]{2,1,0:T(8,128)(2,1)}, bf16[4,256,256]{2,1,0:T(8,128)(2,1)S(1)}, u32[]{:S(2)}, u32[]{:S(2)}) collective-permute-start(bf16[4,256,256]{2,1,0:T(8,128)(2,1)} %get-tuple-element.65), channel_id=1, source_target_pairs={{0,32},{1,33},{2,34},{3,35},{4,36},{5,37},{6,38},{7,39}} | collective-permute-start | bytes 1572872 | tf_op jit(solution)/shard_map/ppermute | solution.py:556
  18.2 23.1 %collective-permute-start.1 = (bf16[4,256,256]{2,1,0:T(8,128)(2,1)}, bf16[4,256,256]{2,1,0:T(8,128)(2,1)S(1)}, u32[]{:S(2)}, u32[]{:S(2)}) collective-permute-start(bf16[4,256,256]{2,1,0:T(8,128)(2,1)} %get-tuple-element.66), channel_id=1, source_target_pairs={{0,64},{1,65},{2,66},{3,67},{4,68},{5,69},{6,70},{7,71}} | collective-permute-start | bytes 1572872 | tf_op jit(solution)/shard_map/ppermute | solution.py:556
  20.4 20.9 %collective-permute-start.2 = (bf16[4,256,256]{2,1,0:T(8,128)(2,1)}, bf16[4,256,256]{2,1,0:T(8,128)(2,1)}, u32[]{:S(2)}, u32[]{:S(2)}) collective-permute-start(bf16[4,256,256]{2,1,0:T(8,128)(2,1)} %get-tuple-element.67), channel_id=1, source_target_pairs={{0,96},{1,97},{2,98},{3,99},{4,100},{5,101},{6,102},{7,103}} | collective-permute-start | bytes 1572872 | tf_op jit(solution)/shard_map/ppermute | solution.py:556
  41.3 0.8 copy-start.8
  42.1 4.6 %copy-start.7 = (bf16[4,256,256]{2,1,0:T(8,128)(2,1)S(1)}, bf16[4,256,256]{2,1,0:T(8,128)(2,1)}, u32[]{:S(2)}) copy-start(bf16[4,256,256]{2,1,0:T(8,128)(2,1)} %get-tuple-element.73) | copy-start | bytes 1572868
  42.1 12.8 %copy-start.10 = (f32[128]{0:T(128)S(1)}, f32[128]{0:T(128)}, u32[]{:S(2)}) copy-start(f32[128]{0:T(128)} %param.14) | copy-start | bytes 1540
  42.1 60.6 %all-to-all-start.1 = ((bf16[16,256,256]{2,1,0:T(8,128)(2,1)}), bf16[16,256,256]{2,1,0:T(8,128)(2,1)}, u32[]{:S(2)}, u32[]{:S(2)}) async-start(bf16[16,256,256]{2,1,0:T(8,128)(2,1)} %bitcast.50), calls=%async_computation.1 | async-start | bytes 4194304 | tf_op jit(solution)/shard_map/all_to_all | solution.py:480
  47.9 22.6 %collective-permute-start.3 = (bf16[256,256]{1,0:T(8,128)(2,1)S(1)}, bf16[256,256]{1,0:T(8,128)(2,1)S(1)}, u32[]{:S(2)}, u32[]{:S(2)}) collective-permute-start(bf16[256,256]{1,0:T(8,128)(2,1)S(1)} %get-tuple-element.119), channel_id=1, source_target_pairs={{0,24},{32,56},{64,88},{96,120},{1,25},{33,57},{65,89},{97,121},{2... | collective-permute-start | bytes 393224 | tf_op jit(solution)/shard_map/ppermute | solution.py:587
  52.3 19.2 %collective-permute-start.4 = (bf16[256,256]{1,0:T(8,128)(2,1)S(1)}, bf16[256,256]{1,0:T(8,128)(2,1)S(1)}, u32[]{:S(2)}, u32[]{:S(2)}) collective-permute-start(bf16[256,256]{1,0:T(8,128)(2,1)S(1)} %get-tuple-element.118), channel_id=1, source_target_pairs={{0,16},{32,48},{64,80},{96,112},{1,17},{33,49},{65,81},{97,113},{2... | collective-permute-start | bytes 393224 | tf_op jit(solution)/shard_map/ppermute | solution.py:587
  53.6 20.7 %collective-permute-start.5 = (bf16[256,256]{1,0:T(8,128)(2,1)S(1)}, bf16[256,256]{1,0:T(8,128)(2,1)S(1)}, u32[]{:S(2)}, u32[]{:S(2)}) collective-permute-start(bf16[256,256]{1,0:T(8,128)(2,1)S(1)} %get-tuple-element.117), channel_id=1, source_target_pairs={{0,8},{32,40},{64,72},{96,104},{1,9},{33,41},{65,73},{97,105},{2,1... | collective-permute-start | bytes 393224 | tf_op jit(solution)/shard_map/ppermute | solution.py:587
  75.3 13.6 %collective-permute-start.6 = (bf16[256,256]{1,0:T(8,128)(2,1)S(1)}, bf16[256,256]{1,0:T(8,128)(2,1)S(1)}, u32[]{:S(2)}, u32[]{:S(2)}) collective-permute-start(bf16[256,256]{1,0:T(8,128)(2,1)S(1)} %fusion.2), channel_id=1, source_target_pairs={{0,2},{2,4},{4,6},{6,0},{1,3},{3,5},{5,7},{7,1},{8,10},{10,12},{12... | collective-permute-start | bytes 393224 | tf_op jit(solution)/shard_map/ppermute | solution.py:489
  76.7 12.3 %collective-permute-start.7 = (bf16[256,256]{1,0:T(8,128)(2,1)S(1)}, bf16[256,256]{1,0:T(8,128)(2,1)S(1)}, u32[]{:S(2)}, u32[]{:S(2)}) collective-permute-start(bf16[256,256]{1,0:T(8,128)(2,1)S(1)} %fusion.2), channel_id=1, source_target_pairs={{0,6},{2,0},{4,2},{6,4},{1,7},{3,1},{5,3},{7,5},{8,14},{10,8},{12,... | collective-permute-start | bytes 393224 | tf_op jit(solution)/shard_map/ppermute | solution.py:489
  77.1 11.9 %collective-permute-start.8 = (bf16[256,256]{1,0:T(8,128)(2,1)S(1)}, bf16[256,256]{1,0:T(8,128)(2,1)S(1)}, u32[]{:S(2)}, u32[]{:S(2)}) collective-permute-start(bf16[256,256]{1,0:T(8,128)(2,1)S(1)} %fusion.2), channel_id=1, source_target_pairs={{0,4},{2,6},{4,0},{6,2},{1,5},{3,7},{5,1},{7,3},{8,12},{10,14},{12... | collective-permute-start | bytes 393224 | tf_op jit(solution)/shard_map/ppermute | solution.py:489
  89.8 7.4 %collective-permute-start.9 = (bf16[4,256,256]{2,1,0:T(8,128)(2,1)}, bf16[4,256,256]{2,1,0:T(8,128)(2,1)}, u32[]{:S(2)}, u32[]{:S(2)}) collective-permute-start(bf16[4,256,256]{2,1,0:T(8,128)(2,1)} %pad_maximum_fusion.same), channel_id=1, source_target_pairs={{0,1},{1,0},{2,3},{3,2},{4,5},{5,4},{6,7},{7,6},{8,9},{9,8},{10,11... | collective-permute-start | bytes 1572872 | tf_op jit(solution)/shard_map/ppermute | solution.py:493
  93.8 33.8 %collective-permute-start.12 = (bf16[256,2048]{1,0:T(8,128)(2,1)S(1)}, bf16[256,2048]{1,0:T(8,128)(2,1)}, u32[]{:S(2)}, u32[]{:S(2)}) collective-permute-start(bf16[256,2048]{1,0:T(8,128)(2,1)S(1)} %collective-permute-done.10.refs_2_.refs_9_), channel_id=1, source_target_pairs={{0,2},{2,4},{4,6},{6,0},{1,3},{3,5},{5,7},{7,1},{8,10},{10,12},{12... | collective-permute-start | bytes 3145736 | tf_op jit(solution)/shard_map/ppermute | solution.py:489
  97.2 11.2 %copy-start = (bf16[256,2048]{1,0:T(8,128)(2,1)S(1)}, bf16[256,2048]{1,0:T(8,128)(2,1)}, u32[]{:S(2)}) copy-start(bf16[256,2048]{1,0:T(8,128)(2,1)} %refs_8_.1) | copy-start | bytes 3145732
  102.6 16.6 %all-to-all-start.2 = ((bf16[16,64,256]{2,1,0:T(8,128)(2,1)}), bf16[16,64,256]{2,1,0:T(8,128)(2,1)}, u32[]{:S(2)}, u32[]{:S(2)}) async-start(bf16[16,64,256]{2,1,0:T(8,128)(2,1)} %project_sent.1), calls=%async_computation.2 | async-start | bytes 1048576 | tf_op jit(solution)/shard_map/all_to_all | solution.py:480
  108.4 36.0 %collective-permute-start.13 = (bf16[256,2048]{1,0:T(8,128)(2,1)S(1)}, bf16[256,2048]{1,0:T(8,128)(2,1)}, u32[]{:S(2)}, u32[]{:S(2)}) collective-permute-start(bf16[256,2048]{1,0:T(8,128)(2,1)S(1)} %copy-done), channel_id=1, source_target_pairs={{0,1},{1,0},{2,3},{3,2},{4,5},{5,4},{6,7},{7,6},{8,9},{9,8},{10,11... | collective-permute-start | bytes 3145736 | tf_op jit(solution)/shard_map/ppermute | solution.py:493
  127.7 17.6 %collective-permute-start.14 = (bf16[256,2048]{1,0:T(8,128)(2,1)S(1)}, bf16[256,2048]{1,0:T(8,128)(2,1)}, u32[]{:S(2)}, u32[]{:S(2)}) collective-permute-start(bf16[256,2048]{1,0:T(8,128)(2,1)S(1)} %collective-permute-done.10.refs_2_.refs_9_), channel_id=1, source_target_pairs={{0,1},{1,0},{2,3},{3,2},{4,5},{5,4},{6,7},{7,6},{8,9},{9,8},{10,11... | collective-permute-start | bytes 3145736 | tf_op jit(solution)/shard_map/ppermute | solution.py:493
  129.4 27.9 %collective-permute-start.15 = (bf16[256,2048]{1,0:T(8,128)(2,1)S(1)}, bf16[256,2048]{1,0:T(8,128)(2,1)}, u32[]{:S(2)}, u32[]{:S(2)}) collective-permute-start(bf16[256,2048]{1,0:T(8,128)(2,1)S(1)} %collective-permute-done.11.refs_3_.refs_10_), channel_id=1, source_target_pairs={{0,1},{1,0},{2,3},{3,2},{4,5},{5,4},{6,7},{7,6},{8,9},{9,8},{10,11... | collective-permute-start | bytes 3145736 | tf_op jit(solution)/shard_map/ppermute | solution.py:493
  129.5 27.8 %collective-permute-start.16 = (bf16[256,2048]{1,0:T(8,128)(2,1)}, bf16[256,2048]{1,0:T(8,128)(2,1)}, u32[]{:S(2)}, u32[]{:S(2)}) collective-permute-start(bf16[256,2048]{1,0:T(8,128)(2,1)} %collective-permute-done.12.refs_4_.refs_11_), channel_id=1, source_target_pairs={{0,1},{1,0},{2,3},{3,2},{4,5},{5,4},{6,7},{7,6},{8,9},{9,8},{10,11... | collective-permute-start | bytes 3145736 | tf_op jit(solution)/shard_map/ppermute | solution.py:493
  139.5 17.8 %copy-start.3 = (f32[2048]{0:T(1024)S(1)}, f32[2048]{0:T(1024)}, u32[]{:S(2)}) copy-start(f32[2048]{0:T(1024)} %param.16) | copy-start | bytes 24580
  139.5 17.8 %copy-start.4 = (s32[8]{0:T(128)S(1)}, s32[8]{0:T(128)}, u32[]{:S(2)}) copy-start(s32[8]{0:T(128)} %pad_add_fusion.1.order) | copy-start | bytes 100
  139.5 17.8 %copy-start.6 = (s32[8]{0:T(128)S(1)}, s32[8]{0:T(128)}, u32[]{:S(2)}) copy-start(s32[8]{0:T(128)} %iota.15.where.slot) | copy-start | bytes 100
  139.5 17.8 %all-to-all-start.3 = ((bf16[8,256,256]{2,1,0:T(8,128)(2,1)}), bf16[8,256,256]{2,1,0:T(8,128)(2,1)}, u32[]{:S(2)}, u32[]{:S(2)}) async-start(bf16[8,256,256]{2,1,0:T(8,128)(2,1)} %attend.2), calls=%async_computation.3 | async-start | bytes 2097152 | tf_op jit(solution)/shard_map/all_to_all | solution.py:480
  143.7 27.0 %collective-permute-start.17 = (bf16[2,256,256]{2,1,0:T(8,128)(2,1)}, bf16[2,256,256]{2,1,0:T(8,128)(2,1)}, u32[]{:S(2)}, u32[]{:S(2)}) collective-permute-start(bf16[2,256,256]{2,1,0:T(8,128)(2,1)} %get-tuple-element.98), channel_id=1, source_target_pairs={{0,2},{2,4},{4,6},{6,0},{1,3},{3,5},{5,7},{7,1},{8,10},{10,12},{12... | collective-permute-start | bytes 786440 | tf_op jit(solution)/shard_map/ppermute | solution.py:524
  144.4 26.3 %collective-permute-start.18 = (bf16[2,256,256]{2,1,0:T(8,128)(2,1)}, bf16[2,256,256]{2,1,0:T(8,128)(2,1)}, u32[]{:S(2)}, u32[]{:S(2)}) collective-permute-start(bf16[2,256,256]{2,1,0:T(8,128)(2,1)} %get-tuple-element.99), channel_id=1, source_target_pairs={{0,6},{2,0},{4,2},{6,4},{1,7},{3,1},{5,3},{7,5},{8,14},{10,8},{12,... | collective-permute-start | bytes 786440 | tf_op jit(solution)/shard_map/ppermute | solution.py:524
  145.3 25.4 %collective-permute-start.19 = (bf16[2,256,256]{2,1,0:T(8,128)(2,1)}, bf16[2,256,256]{2,1,0:T(8,128)(2,1)}, u32[]{:S(2)}, u32[]{:S(2)}) collective-permute-start(bf16[2,256,256]{2,1,0:T(8,128)(2,1)} %get-tuple-element.100), channel_id=1, source_target_pairs={{0,4},{2,6},{4,0},{6,2},{1,5},{3,7},{5,1},{7,3},{8,12},{10,14},{12... | collective-permute-start | bytes 786440 | tf_op jit(solution)/shard_map/ppermute | solution.py:524
  162.9 1.0 copy-start.1
  163.8 6.9 %copy-start.2 = (bf16[2,256,256]{2,1,0:T(8,128)(2,1)S(1)}, bf16[2,256,256]{2,1,0:T(8,128)(2,1)}, u32[]{:S(2)}) copy-start(bf16[2,256,256]{2,1,0:T(8,128)(2,1)} %get-tuple-element.101.refs_0_) | copy-start | bytes 786436
  163.8 12.2 %copy-start.5 = (s32[8]{0:T(128)S(1)}, s32[8]{0:T(128)}, u32[]{:S(2)}) copy-start(s32[8]{0:T(128)} %pad_add_fusion.2.where.slot) | copy-start | bytes 100
  163.8 30.2 %all-to-all-start.4 = ((bf16[8,256,256]{2,1,0:T(8,128)(2,1)}), bf16[8,256,256]{2,1,0:T(8,128)(2,1)}, u32[]{:S(2)}, u32[]{:S(2)}) async-start(bf16[8,256,256]{2,1,0:T(8,128)(2,1)} %copy-done.1), calls=%async_computation.4 | async-start | bytes 2097152 | tf_op jit(solution)/shard_map/all_to_all | solution.py:480
  170.7 4.1 %collective-permute-start.20 = (bf16[256,256]{1,0:T(8,128)(2,1)S(1)}, bf16[256,256]{1,0:T(8,128)(2,1)S(1)}, u32[]{:S(2)}, u32[]{:S(2)}) collective-permute-start(bf16[256,256]{1,0:T(8,128)(2,1)S(1)} %slice_bitcast_fusion.3), channel_id=1, source_target_pairs={{0,1},{1,0},{2,3},{3,2},{4,5},{5,4},{6,7},{7,6},{8,9},{9,8},{10,11... | collective-permute-start | bytes 393224 | tf_op jit(solution)/shard_map/ppermute | solution.py:493
  172.1 2.7 %collective-permute-start.21 = (bf16[256,256]{1,0:T(8,128)(2,1)S(1)}, bf16[256,256]{1,0:T(8,128)(2,1)S(1)}, u32[]{:S(2)}, u32[]{:S(2)}) collective-permute-start(bf16[256,256]{1,0:T(8,128)(2,1)S(1)} %slice_bitcast_fusion.2), channel_id=1, source_target_pairs={{0,1},{1,0},{2,3},{3,2},{4,5},{5,4},{6,7},{7,6},{8,9},{9,8},{10,11... | collective-permute-start | bytes 393224 | tf_op jit(solution)/shard_map/ppermute | solution.py:493
  173.2 1.6 collective-permute-start.22
  174.6 1.4 collective-permute-start.23
  182.3 4.9 %collective-permute-start.24 = (bf16[256,256]{1,0:T(8,128)(2,1)S(1)}, bf16[256,256]{1,0:T(8,128)(2,1)S(1)}, u32[]{:S(2)}, u32[]{:S(2)}) collective-permute-start(bf16[256,256]{1,0:T(8,128)(2,1)S(1)} %get-tuple-element.106), channel_id=1, source_target_pairs={{0,2},{1,3},{2,4},{3,5},{4,6},{5,7},{6,0},{7,1},{8,10},{9,11},{10,... | collective-permute-start | bytes 393224 | tf_op jit(solution)/shard_map/ppermute | solution.py:538
  183.6 5.9 %collective-permute-start.25 = (bf16[256,256]{1,0:T(8,128)(2,1)S(1)}, bf16[256,256]{1,0:T(8,128)(2,1)S(1)}, u32[]{:S(2)}, u32[]{:S(2)}) collective-permute-start(bf16[256,256]{1,0:T(8,128)(2,1)S(1)} %get-tuple-element.107), channel_id=1, source_target_pairs={{0,6},{1,7},{2,0},{3,1},{4,2},{5,3},{6,4},{7,5},{8,14},{9,15},{10,... | collective-permute-start | bytes 393224 | tf_op jit(solution)/shard_map/ppermute | solution.py:538
  183.8 43.7 %collective-permute-start.26 = (bf16[256,256]{1,0:T(8,128)(2,1)}, bf16[256,256]{1,0:T(8,128)(2,1)S(1)}, u32[]{:S(2)}, u32[]{:S(2)}) collective-permute-start(bf16[256,256]{1,0:T(8,128)(2,1)} %get-tuple-element.108), channel_id=1, source_target_pairs={{0,4},{1,5},{2,6},{3,7},{4,0},{5,1},{6,2},{7,3},{8,12},{9,13},{10,... | collective-permute-start | bytes 393224 | tf_op jit(solution)/shard_map/ppermute | solution.py:538
  185.6 41.9 %collective-permute-start.27 = (bf16[256,256]{1,0:T(8,128)(2,1)}, bf16[256,256]{1,0:T(8,128)(2,1)S(1)}, u32[]{:S(2)}, u32[]{:S(2)}) collective-permute-start(bf16[256,256]{1,0:T(8,128)(2,1)} %get-tuple-element.109), channel_id=1, source_target_pairs={{0,1},{1,0},{2,3},{3,2},{4,5},{5,4},{6,7},{7,6},{8,9},{9,8},{10,11... | collective-permute-start | bytes 393224 | tf_op jit(solution)/shard_map/ppermute | solution.py:538
  186.6 40.9 %collective-permute-start.28 = (bf16[256,256]{1,0:T(8,128)(2,1)}, bf16[256,256]{1,0:T(8,128)(2,1)S(1)}, u32[]{:S(2)}, u32[]{:S(2)}) collective-permute-start(bf16[256,256]{1,0:T(8,128)(2,1)} %get-tuple-element.110), channel_id=1, source_target_pairs={{0,3},{1,2},{2,5},{3,4},{4,7},{5,6},{6,1},{7,0},{8,11},{9,10},{10,... | collective-permute-start | bytes 393224 | tf_op jit(solution)/shard_map/ppermute | solution.py:538
  187.3 40.3 %collective-permute-start.29 = (bf16[256,256]{1,0:T(8,128)(2,1)}, bf16[256,256]{1,0:T(8,128)(2,1)S(1)}, u32[]{:S(2)}, u32[]{:S(2)}) collective-permute-start(bf16[256,256]{1,0:T(8,128)(2,1)} %get-tuple-element.111), channel_id=1, source_target_pairs={{0,7},{1,6},{2,1},{3,0},{4,3},{5,2},{6,5},{7,4},{8,15},{9,14},{10,... | collective-permute-start | bytes 393224 | tf_op jit(solution)/shard_map/ppermute | solution.py:538
  189.5 38.1 %collective-permute-start.30 = (bf16[256,256]{1,0:T(8,128)(2,1)}, bf16[256,256]{1,0:T(8,128)(2,1)S(1)}, u32[]{:S(2)}, u32[]{:S(2)}) collective-permute-start(bf16[256,256]{1,0:T(8,128)(2,1)} %get-tuple-element.112), channel_id=1, source_target_pairs={{0,5},{1,4},{2,7},{3,6},{4,1},{5,0},{6,3},{7,2},{8,13},{9,12},{10,... | collective-permute-start | bytes 393224 | tf_op jit(solution)/shard_map/ppermute | solution.py:538

commit v10 on v8

--- a/solution.py
+++ b/solution.py
@@ -12,7 +12,7 @@
 BLOCK = 64
 HOT = 8
 REACH = 2
-FIRST_BLOCKS = 4
+FIRST_BLOCKS = 3
 KV = ("kv_0", "kv_1")
 TP = ("tp_0", "tp_1")
 WIDTH = 256
@@ -22,6 +22,7 @@
 bf16 = jnp.bfloat16
 f32 = jnp.float32
 VMEM_LIMIT = 60 * 1024 * 1024
+KERNEL_LIMIT = 48 * 1024 * 1024
 
 
 def head_norm(values, gain_row):
@@ -419,7 +420,7 @@
             ],
         ),
         out_shape=[jax.ShapeDtypeStruct(shape, bf16)] * len(pieces),
-        compiler_params=pltpu.CompilerParams(vmem_limit_bytes=VMEM_LIMIT),
+        compiler_params=pltpu.CompilerParams(vmem_limit_bytes=KERNEL_LIMIT),
         cost_estimate=pl.CostEstimate(
             flops=2 * rows * width * width, bytes_accessed=12 << 20, transcendentals=0
         ),

time: 225 us -> 203 us (0.902)
  waiting for transfers between devices: 60.4 us -> 48.7 us
  starting transfers between devices: 73.5 us -> 70.1 us
  local copies, waits for them, and re-layouts: 9.5 us -> 6.39 us
    all_to_all x5, waiting for transfers between devices: 22 us -> 6.99 us  [exchange(): return lax.all_to_all(pieces, axes, split_axis=0, concat_axis=0, tiled=True)]
    unnamed x56 -> x26, local copies, waits for them, and re-layouts: 5.77 us -> 2.53 us
    ppermute x3, waiting for transfers between devices: 16.9 us -> 20.1 us  [local(): lax.ppermute(held[n], KV, [(i, i + n) for i in starts])]
    pallas_call x2, Pallas kernels: 15 us -> 12.7 us  [project_out(): pl.pallas_call(out_kernel, grid_spec=pltpu.PrefetchScalarGridSpec(num_sca...]
  transfers between devices with their start and end apart: 36 -> 36, of which waited for: 11 -> 8; matrix products, arithmetic and copies ran while one was open for 5% -> 4% of each run, Pallas kernels for 28% -> 34%
where the time goes in v10:
time: 203 us; the launch traced here: 202 us
  Pallas kernels  71.2 us (35%)
  starting transfers between devices  70.1 us (35%)
  waiting for transfers between devices  48.7 us (24%)
  local copies, waits for them, and re-layouts  6.39 us (3%)
  other arithmetic  5.02 us (2%)
    all_to_all x5, starting transfers between devices, exchange(): return lax.all_to_all(pieces, axes, split_axis=0, concat_axis=0, tiled=True)  25.6 us
    ppermute x14, waiting for transfers between devices, send_pieces(): got.append(lax.ppermute(pieces[k], TP, pairs) if k else pieces[0])  21.6 us
    ppermute x3, waiting for transfers between devices, local(): lax.ppermute(held[n], KV, [(i, i + n) for i in starts])  20.1 us
    pallas_call x2, Pallas kernels, attend(): pl.pallas_call(functools.partial(attention_kernel, first), grid_spec=pltp...  18.5 us
    ppermute x14, starting transfers between devices, send_pieces(): got.append(lax.ppermute(pieces[k], TP, pairs) if k else pieces[0])  17 us
    pallas_call x1, Pallas kernels, project_kv(): pl.pallas_call(kv_kernel, grid=(length // tile,), in_specs=[pl.BlockSpec(...  13.7 us
    pallas_call x2, Pallas kernels, project_out(): pl.pallas_call(out_kernel, grid_spec=pltpu.PrefetchScalarGridSpec(num_sca...  12.7 us
    pallas_call x1, Pallas kernels, project_q(): pl.pallas_call(q_kernel, grid=(length // tile,), in_specs=[pl.BlockSpec((...  10.1 us
  transfers between devices with their start and end apart: 36, of which 8 were waited for; matrix products, arithmetic and copies ran while one was open for 4% of the time, Pallas kernels for 34%

profile of v10, /device:TPU:1, one launch (start us, length us, event | category | flops | bytes accessed | tf_op | source)
XLA Modules:
  0.0 202.0 jit_solution(1473779030632668144)
XLA Ops:
  0.0 2.1 %collective-permute-start.10 = (bf16[256,2048]{1,0:T(8,128)(2,1)}, bf16[256,2048]{1,0:T(8,128)(2,1)S(1)}, u32[]{:S(2)}, u32[]{:S(2)}) collective-permute-start(bf16[256,2048]{1,0:T(8,128)(2,1)} %refs_8_.1), channel_id=1, source_target_pairs={{0,2},{2,4},{4,6},{6,0},{1,3},{3,5},{5,7},{7,1},{8,10},{10,12},{12... | collective-permute-start | bytes 3145736 | tf_op jit(solution)/shard_map/ppermute | solution.py:488
  2.1 1.4 collective-permute-start.11
  3.6 4.0 %token_shares.1 = (bf16[4,256,256]{2,1,0:T(8,128)(2,1)}, bf16[4,256,256]{2,1,0:T(8,128)(2,1)}, bf16[4,256,256]{2,1,0:T(8,128)(2,1)}, bf16[4,256,256]{2,1,0:T(8,128)(2,1)}) custom-call(s32[1]{0:T(128)} %bitcast.5.rank, bf16[4096,2048]{1,0:T(8,128)(2,1)} %tok.4), custom_call_target="tpu_custom_call" | custom-call | flops 1048576 | bytes 4194304 | tf_op jit(solution)/shard_map/token_shares/pallas_call | solution.py:52
  9.4 7.6 %all-to-all-start = ((s32[16,1,16]{2,1,0:T(1,128)}), s32[16,1,16]{2,1,0:T(1,128)S(1)}, u32[]{:S(2)}, u32[]{:S(2)}) async-start(s32[16,1,16]{2,1,0:T(1,128)} %bitcast.8), calls=%async_computation | async-start | bytes 16384 | tf_op jit(solution)/shard_map/all_to_all | solution.py:479
  17.0 3.3 %collective-permute-start = (bf16[4,256,256]{2,1,0:T(8,128)(2,1)}, bf16[4,256,256]{2,1,0:T(8,128)(2,1)S(1)}, u32[]{:S(2)}, u32[]{:S(2)}) collective-permute-start(bf16[4,256,256]{2,1,0:T(8,128)(2,1)} %get-tuple-element.77), channel_id=1, source_target_pairs={{0,32},{1,33},{2,34},{3,35},{4,36},{5,37},{6,38},{7,39}} | collective-permute-start | bytes 1572872 | tf_op jit(solution)/shard_map/ppermute | solution.py:546
  20.3 2.2 %collective-permute-start.1 = (bf16[4,256,256]{2,1,0:T(8,128)(2,1)}, bf16[4,256,256]{2,1,0:T(8,128)(2,1)S(1)}, u32[]{:S(2)}, u32[]{:S(2)}) collective-permute-start(bf16[4,256,256]{2,1,0:T(8,128)(2,1)} %get-tuple-element.78), channel_id=1, source_target_pairs={{0,64},{1,65},{2,66},{3,67},{4,68},{5,69},{6,70},{7,71}} | collective-permute-start | bytes 1572872 | tf_op jit(solution)/shard_map/ppermute | solution.py:546
  22.5 1.3 collective-permute-start.2
  23.8 13.7 %project_kv.1 = bf16[64,2,64,256]{3,2,1,0:T(8,128)(2,1)} custom-call(bf16[4096,2048]{1,0:T(8,128)(2,1)} %tok.4, bf16[2048,256]{1,0:T(8,128)(2,1)} %wk.3, bf16[2048,256]{1,0:T(8,128)(2,1)} %wv.3, f32[1,128]{1,0:T(1,128)} %bitcast.50), custom_call_target="tpu_custom_call" | custom-call | flops 8589934592 | bytes 16777216 | tf_op jit(solution)/shard_map/project_kv/pallas_call | solution.py:83
  38.3 4.4 %gather_near.1 = bf16[32,128,256]{2,1,0:T(8,128)(2,1)} custom-call(s32[32]{0:T(128)} %reshape.69.near, bf16[8192,256]{1,0:T(8,128)(2,1)} %bitcast.40), custom_call_target="tpu_custom_call" | custom-call | flops 1048576 | bytes 4194304 | tf_op jit(solution)/shard_map/gather_near/pallas_call | solution.py:151
  42.7 4.6 %all-to-all-start.1 = ((bf16[16,256,256]{2,1,0:T(8,128)(2,1)}), bf16[16,256,256]{2,1,0:T(8,128)(2,1)}, u32[]{:S(2)}, u32[]{:S(2)}) async-start(bf16[16,256,256]{2,1,0:T(8,128)(2,1)} %bitcast.43), calls=%async_computation.1 | async-start | bytes 4194304 | tf_op jit(solution)/shard_map/all_to_all | solution.py:479
  47.4 4.3 %collective-permute-start.3 = (bf16[256,256]{1,0:T(8,128)(2,1)S(1)}, bf16[256,256]{1,0:T(8,128)(2,1)S(1)}, u32[]{:S(2)}, u32[]{:S(2)}) collective-permute-start(bf16[256,256]{1,0:T(8,128)(2,1)S(1)} %get-tuple-element.143), channel_id=1, source_target_pairs={{0,24},{32,56},{64,88},{96,120},{1,25},{33,57},{65,89},{97,121},{2... | collective-permute-start | bytes 393224 | tf_op jit(solution)/shard_map/ppermute | solution.py:577
  51.8 1.3 collective-permute-start.4
  53.1 1.3 collective-permute-start.5
  54.9 16.3 %collective-permute-done.3 = bf16[256,256]{1,0:T(8,128)(2,1)S(1)} collective-permute-done((bf16[256,256]{1,0:T(8,128)(2,1)S(1)}, bf16[256,256]{1,0:T(8,128)(2,1)S(1)}, u32[]{:S(2)}, u32[]{:S(2)}) %collective-permute-start.3) | collective-permute-done | bytes 131104 | tf_op jit(solution)/shard_map/ppermute | solution.py:577
  71.2 1.0 collective-permute-done.4
  72.2 2.8 %collective-permute-done.5 = bf16[256,256]{1,0:T(8,128)(2,1)S(1)} collective-permute-done((bf16[256,256]{1,0:T(8,128)(2,1)S(1)}, bf16[256,256]{1,0:T(8,128)(2,1)S(1)}, u32[]{:S(2)}, u32[]{:S(2)}) %collective-permute-start.5) | collective-permute-done | bytes 131104 | tf_op jit(solution)/shard_map/ppermute | solution.py:577
  75.2 2.7 %collective-permute-start.7 = (bf16[256,256]{1,0:T(8,128)(2,1)S(1)}, bf16[256,256]{1,0:T(8,128)(2,1)S(1)}, u32[]{:S(2)}, u32[]{:S(2)}) collective-permute-start(bf16[256,256]{1,0:T(8,128)(2,1)S(1)} %fusion.2), channel_id=1, source_target_pairs={{0,6},{2,0},{4,2},{6,4},{1,7},{3,1},{5,3},{7,5},{8,14},{10,8},{12,... | collective-permute-start | bytes 393224 | tf_op jit(solution)/shard_map/ppermute | solution.py:488
  78.3 10.1 %project_q.1.queries = bf16[4096,256]{1,0:T(8,128)(2,1)} custom-call(bf16[4096,2048]{1,0:T(8,128)(2,1)} %tok.4, bf16[2048,256]{1,0:T(8,128)(2,1)} %wq.1, f32[1,128]{1,0:T(1,128)} %multiply_bitcast_fusion.gain), custom_call_target="tpu_custom_call" | custom-call | flops 4294967296 | bytes 16777216 | tf_op jit(solution)/shard_map/project_q/pallas_call | solution.py:112
  88.4 3.5 %collective-permute-start.9 = (bf16[4,256,256]{2,1,0:T(8,128)(2,1)S(1)}, bf16[4,256,256]{2,1,0:T(8,128)(2,1)S(1)}, u32[]{:S(2)}, u32[]{:S(2)}) collective-permute-start(bf16[4,256,256]{2,1,0:T(8,128)(2,1)S(1)} %pad_maximum_fusion.same), channel_id=1, source_target_pairs={{0,1},{1,0},{2,3},{3,2},{4,5},{5,4},{6,7},{7,6},{8,9},{9,8},{10,11... | collective-permute-start | bytes 1572872 | tf_op jit(solution)/shard_map/ppermute | solution.py:492
  95.2 4.8 %project_sent.1 = bf16[16,64,256]{2,1,0:T(8,128)(2,1)} custom-call(s32[128]{0:T(128)} %reshape.68.asked, s32[8]{0:T(128)} %pad_add_fusion.1.order, bf16[4,256,256]{2,1,0:T(8,128)(2,1)} %copy-done.7, bf16[4,256,256]{2,1,0:T(8,128)(2,1)} %copy-done.9, bf16[2048,256]{1,0:T(8,128)(2,1)} %wk.3, bf16[2048,256]{1,0:T(8,128)(2,1)} %wv.3, f32[1,128]{1,0:T(1,128)} %bitcast.51), custom_call_target="tpu_custom_call" | custom-call | flops 536870912 | bytes 8388608 | tf_op jit(solution)/shard_map/project_sent/pallas_call | solution.py:211
  100.6 5.5 %all-to-all-start.2 = ((bf16[16,64,256]{2,1,0:T(8,128)(2,1)}), bf16[16,64,256]{2,1,0:T(8,128)(2,1)S(1)}, u32[]{:S(2)}, u32[]{:S(2)}) async-start(bf16[16,64,256]{2,1,0:T(8,128)(2,1)} %project_sent.1), calls=%async_computation.2 | async-start | bytes 1048576 | tf_op jit(solution)/shard_map/all_to_all | solution.py:479
  107.0 1.3 select_reduce_fusion
  109.9 7.0 %all-to-all-done.2.hot = bf16[16,64,256]{2,1,0:T(8,128)(2,1)S(1)} async-done(((bf16[16,64,256]{2,1,0:T(8,128)(2,1)}), bf16[16,64,256]{2,1,0:T(8,128)(2,1)S(1)}, u32[]{:S(2)}, u32[]{:S(2)}) %all-to-all-start.2) | async-done | bytes 524320 | tf_op jit(solution)/shard_map/all_to_all | solution.py:479
  117.7 9.9 %attend.3 = (bf16[320,256]{1,0:T(8,128)(2,1)}, bf16[320,256]{1,0:T(8,128)(2,1)}, bf16[320,256]{1,0:T(8,128)(2,1)}, bf16[320,256]{1,0:T(8,128)(2,1)}, bf16[320,25...) custom-call(s32[512]{0:T(512)} %reshape.71.at, ...), custom_call_target="tpu_custom_call" | custom-call | flops 2684354560 | bytes 10485760 | tf_op jit(solution)/shard_map/attend/pallas_call | solution.py:333
  127.7 1.8 collective-permute-start.14
  130.0 8.6 %attend.2 = bf16[8,192,256]{2,1,0:T(8,128)(2,1)} custom-call(s32[512]{0:T(512)} %reshape.71.at, s32[8]{0:T(128)} %iota.15.where.slot, bf16[4096,256]{1,0:T(8,128)(2,1)} %project_q.1.queries, f32[64,512]{1,0:T(8,128)} %reshape.72.masks, bf16[8192,256]{1,0:T(8,128)(2,1)} %bitcast.42, bf16[4096,256]{1,0:T(8,128)(2,1)} %bitcast.22.near, ...), custom_call_target="tpu_custom_call" | custom-call | flops 1610612736 | bytes 10485760 | tf_op jit(solution)/shard_map/attend/pallas_call | solution.py:333
  138.6 4.0 %all-to-all-start.3 = ((bf16[8,192,256]{2,1,0:T(8,128)(2,1)}), bf16[8,192,256]{2,1,0:T(8,128)(2,1)S(1)}, u32[]{:S(2)}, u32[]{:S(2)}) async-start(bf16[8,192,256]{2,1,0:T(8,128)(2,1)} %attend.2), calls=%async_computation.3 | async-start | bytes 1572864 | tf_op jit(solution)/shard_map/all_to_all | solution.py:479
  142.5 1.4 collective-permute-start.17
  144.0 1.3 collective-permute-start.18
  145.2 12.9 %collective-permute-done.17.refs_1_ = bf16[320,256]{1,0:T(8,128)(2,1)S(1)} collective-permute-done((bf16[320,256]{1,0:T(8,128)(2,1)S(1)}, bf16[320,256]{1,0:T(8,128)(2,1)S(1)}, u32[]{:S(2)}, u32[]{:S(2)}) %collective-permute-start.17) | collective-permute-done | bytes 163872 | tf_op jit(solution)/shard_map/ppermute | solution.py:528
  158.6 1.0 collective-permute-start.20
  160.3 2.2 %collective-permute-start.22 = (bf16[320,256]{1,0:T(8,128)(2,1)}, bf16[320,256]{1,0:T(8,128)(2,1)}, u32[]{:S(2)}, u32[]{:S(2)}) collective-permute-start(bf16[320,256]{1,0:T(8,128)(2,1)} %get-tuple-element.119), channel_id=1, source_target_pairs={{0,7},{1,6},{2,1},{3,0},{4,3},{5,2},{6,5},{7,4},{8,15},{9,14},{10,... | collective-permute-start | bytes 491528 | tf_op jit(solution)/shard_map/ppermute | solution.py:528
  162.5 1.3 collective-permute-start.23
  163.9 5.6 %project_out.2 = bf16[8,192,256]{2,1,0:T(8,128)(2,1)} custom-call(s32[8]{0:T(128)S(1)} %copy-done.1, s32[8]{0:T(128)S(1)} %copy-done.3, bf16[8,192,256]{2,1,0:T(8,128)(2,1)S(1)} %all-to-all-done.3.refs_0_, bf16[256,2048]{1,0:T(8,128)(2,1)S(1)} %copy-done, bf16[256,2048]{1,0:T(8,128)(2,1)S(1)} %collective-permute-done.10.refs_2_.refs_9_, ...), custom_call_target="tpu_custom_call" | custom-call | flops 1610612736 | bytes 12582912 | tf_op jit(solution)/shard_map/project_out/pallas_call | solution.py:408
  169.5 3.9 %all-to-all-start.4 = ((bf16[8,192,256]{2,1,0:T(8,128)(2,1)}), bf16[8,192,256]{2,1,0:T(8,128)(2,1)S(1)}, u32[]{:S(2)}, u32[]{:S(2)}) async-start(bf16[8,192,256]{2,1,0:T(8,128)(2,1)} %project_out.2), calls=%async_computation.4 | async-start | bytes 1572864 | tf_op jit(solution)/shard_map/all_to_all | solution.py:479
  173.5 0.9 copy-done.5
  174.4 7.0 %project_out.3 = (bf16[320,256]{1,0:T(8,128)(2,1)S(1)}, bf16[320,256]{1,0:T(8,128)(2,1)S(1)}, bf16[320,256]{1,0:T(8,128)(2,1)S(1)}, bf16[320,256]{1,0:T(8,128)(2...) custom-call(s32[8]{0:T(128)S(1)} %copy-done.1, ...), custom_call_target="tpu_custom_call" | custom-call | flops 2684354560 | bytes 12582912 | tf_op jit(solution)/shard_map/project_out/pallas_call | solution.py:408
  181.4 1.4 collective-permute-start.24
  182.8 1.3 collective-permute-start.25
  184.2 1.7 collective-permute-start.26
  185.8 1.2 collective-permute-start.27
  187.2 2.8 %collective-permute-done.24.rest_0_ = bf16[320,256]{1,0:T(8,128)(2,1)S(1)} collective-permute-done((bf16[320,256]{1,0:T(8,128)(2,1)S(1)}, bf16[320,256]{1,0:T(8,128)(2,1)S(1)}, u32[]{:S(2)}, u32[]{:S(2)}) %collective-permute-start.24) | collective-permute-done | bytes 163872 | tf_op jit(solution)/shard_map/ppermute | solution.py:528
  190.1 1.4 collective-permute-start.29
  191.4 1.5 collective-permute-start.30
  192.9 1.5 place.2.filled
  194.4 3.5 %collective-permute-done.28.rest_4_ = bf16[320,256]{1,0:T(8,128)(2,1)S(1)} collective-permute-done((bf16[320,256]{1,0:T(8,128)(2,1)}, bf16[320,256]{1,0:T(8,128)(2,1)S(1)}, u32[]{:S(2)}, u32[]{:S(2)}) %collective-permute-start.28) | collective-permute-done | bytes 163872 | tf_op jit(solution)/shard_map/ppermute | solution.py:528
  197.9 2.4 %collective-permute-done.30.rest_6_ = bf16[320,256]{1,0:T(8,128)(2,1)S(1)} collective-permute-done((bf16[320,256]{1,0:T(8,128)(2,1)}, bf16[320,256]{1,0:T(8,128)(2,1)S(1)}, u32[]{:S(2)}, u32[]{:S(2)}) %collective-permute-start.30) | collective-permute-done | bytes 163872 | tf_op jit(solution)/shard_map/ppermute | solution.py:528
  200.3 1.6 place.3
  (93 shorter events, 13.1 us)
Async XLA Ops:
  0.0 92.6 %collective-permute-start.10 = (bf16[256,2048]{1,0:T(8,128)(2,1)}, bf16[256,2048]{1,0:T(8,128)(2,1)S(1)}, u32[]{:S(2)}, u32[]{:S(2)}) collective-permute-start(bf16[256,2048]{1,0:T(8,128)(2,1)} %refs_8_.1), channel_id=1, source_target_pairs={{0,2},{2,4},{4,6},{6,0},{1,3},{3,5},{5,7},{7,1},{8,10},{10,12},{12... | collective-permute-start | bytes 3145736 | tf_op jit(solution)/shard_map/ppermute | solution.py:488
  2.1 125.5 %collective-permute-start.11 = (bf16[256,2048]{1,0:T(8,128)(2,1)}, bf16[256,2048]{1,0:T(8,128)(2,1)}, u32[]{:S(2)}, u32[]{:S(2)}) collective-permute-start(bf16[256,2048]{1,0:T(8,128)(2,1)} %refs_8_.1), channel_id=1, source_target_pairs={{0,6},{2,0},{4,2},{6,4},{1,7},{3,1},{5,3},{7,5},{8,14},{10,8},{12,... | collective-permute-start | bytes 3145736 | tf_op jit(solution)/shard_map/ppermute | solution.py:488
  3.6 4.0 %copy-start.10 = (s32[64,8]{0,1:T(8,128)S(1)}, s32[64,8]{0,1:T(8,128)}, u32[]{:S(2)}) copy-start(s32[64,8]{0,1:T(8,128)} %param.17) | copy-start | bytes 6148
  9.4 28.3 %all-to-all-start = ((s32[16,1,16]{2,1,0:T(1,128)}), s32[16,1,16]{2,1,0:T(1,128)S(1)}, u32[]{:S(2)}, u32[]{:S(2)}) async-start(s32[16,1,16]{2,1,0:T(1,128)} %bitcast.8), calls=%async_computation | async-start | bytes 16384 | tf_op jit(solution)/shard_map/all_to_all | solution.py:479
  17.0 25.7 %collective-permute-start = (bf16[4,256,256]{2,1,0:T(8,128)(2,1)}, bf16[4,256,256]{2,1,0:T(8,128)(2,1)S(1)}, u32[]{:S(2)}, u32[]{:S(2)}) collective-permute-start(bf16[4,256,256]{2,1,0:T(8,128)(2,1)} %get-tuple-element.77), channel_id=1, source_target_pairs={{0,32},{1,33},{2,34},{3,35},{4,36},{5,37},{6,38},{7,39}} | collective-permute-start | bytes 1572872 | tf_op jit(solution)/shard_map/ppermute | solution.py:546
  20.3 22.4 %collective-permute-start.1 = (bf16[4,256,256]{2,1,0:T(8,128)(2,1)}, bf16[4,256,256]{2,1,0:T(8,128)(2,1)S(1)}, u32[]{:S(2)}, u32[]{:S(2)}) collective-permute-start(bf16[4,256,256]{2,1,0:T(8,128)(2,1)} %get-tuple-element.78), channel_id=1, source_target_pairs={{0,64},{1,65},{2,66},{3,67},{4,68},{5,69},{6,70},{7,71}} | collective-permute-start | bytes 1572872 | tf_op jit(solution)/shard_map/ppermute | solution.py:546
  22.5 20.2 %collective-permute-start.2 = (bf16[4,256,256]{2,1,0:T(8,128)(2,1)}, bf16[4,256,256]{2,1,0:T(8,128)(2,1)S(1)}, u32[]{:S(2)}, u32[]{:S(2)}) collective-permute-start(bf16[4,256,256]{2,1,0:T(8,128)(2,1)} %get-tuple-element.79), channel_id=1, source_target_pairs={{0,96},{1,97},{2,98},{3,99},{4,100},{5,101},{6,102},{7,103}} | collective-permute-start | bytes 1572872 | tf_op jit(solution)/shard_map/ppermute | solution.py:546
  42.7 4.6 %copy-start.8 = (bf16[4,256,256]{2,1,0:T(8,128)(2,1)S(1)}, bf16[4,256,256]{2,1,0:T(8,128)(2,1)}, u32[]{:S(2)}) copy-start(bf16[4,256,256]{2,1,0:T(8,128)(2,1)} %get-tuple-element.85) | copy-start | bytes 1572868
  42.7 11.6 %copy-start.12 = (f32[128]{0:T(128)S(1)}, f32[128]{0:T(128)}, u32[]{:S(2)}) copy-start(f32[128]{0:T(128)} %param.14) | copy-start | bytes 1540
  42.7 57.8 %all-to-all-start.1 = ((bf16[16,256,256]{2,1,0:T(8,128)(2,1)}), bf16[16,256,256]{2,1,0:T(8,128)(2,1)}, u32[]{:S(2)}, u32[]{:S(2)}) async-start(bf16[16,256,256]{2,1,0:T(8,128)(2,1)} %bitcast.43), calls=%async_computation.1 | async-start | bytes 4194304 | tf_op jit(solution)/shard_map/all_to_all | solution.py:479
  47.4 23.8 %collective-permute-start.3 = (bf16[256,256]{1,0:T(8,128)(2,1)S(1)}, bf16[256,256]{1,0:T(8,128)(2,1)S(1)}, u32[]{:S(2)}, u32[]{:S(2)}) collective-permute-start(bf16[256,256]{1,0:T(8,128)(2,1)S(1)} %get-tuple-element.143), channel_id=1, source_target_pairs={{0,24},{32,56},{64,88},{96,120},{1,25},{33,57},{65,89},{97,121},{2... | collective-permute-start | bytes 393224 | tf_op jit(solution)/shard_map/ppermute | solution.py:577
  51.8 20.4 %collective-permute-start.4 = (bf16[256,256]{1,0:T(8,128)(2,1)S(1)}, bf16[256,256]{1,0:T(8,128)(2,1)S(1)}, u32[]{:S(2)}, u32[]{:S(2)}) collective-permute-start(bf16[256,256]{1,0:T(8,128)(2,1)S(1)} %get-tuple-element.142), channel_id=1, source_target_pairs={{0,16},{32,48},{64,80},{96,112},{1,17},{33,49},{65,81},{97,113},{2... | collective-permute-start | bytes 393224 | tf_op jit(solution)/shard_map/ppermute | solution.py:577
  53.1 22.0 %collective-permute-start.5 = (bf16[256,256]{1,0:T(8,128)(2,1)S(1)}, bf16[256,256]{1,0:T(8,128)(2,1)S(1)}, u32[]{:S(2)}, u32[]{:S(2)}) collective-permute-start(bf16[256,256]{1,0:T(8,128)(2,1)S(1)} %get-tuple-element.141), channel_id=1, source_target_pairs={{0,8},{32,40},{64,72},{96,104},{1,9},{33,41},{65,73},{97,105},{2,1... | collective-permute-start | bytes 393224 | tf_op jit(solution)/shard_map/ppermute | solution.py:577
  75.1 13.3 %collective-permute-start.6 = (bf16[256,256]{1,0:T(8,128)(2,1)S(1)}, bf16[256,256]{1,0:T(8,128)(2,1)S(1)}, u32[]{:S(2)}, u32[]{:S(2)}) collective-permute-start(bf16[256,256]{1,0:T(8,128)(2,1)S(1)} %fusion.2), channel_id=1, source_target_pairs={{0,2},{2,4},{4,6},{6,0},{1,3},{3,5},{5,7},{7,1},{8,10},{10,12},{12... | collective-permute-start | bytes 393224 | tf_op jit(solution)/shard_map/ppermute | solution.py:488
  75.2 13.2 %collective-permute-start.7 = (bf16[256,256]{1,0:T(8,128)(2,1)S(1)}, bf16[256,256]{1,0:T(8,128)(2,1)S(1)}, u32[]{:S(2)}, u32[]{:S(2)}) collective-permute-start(bf16[256,256]{1,0:T(8,128)(2,1)S(1)} %fusion.2), channel_id=1, source_target_pairs={{0,6},{2,0},{4,2},{6,4},{1,7},{3,1},{5,3},{7,5},{8,14},{10,8},{12,... | collective-permute-start | bytes 393224 | tf_op jit(solution)/shard_map/ppermute | solution.py:488
  77.8 10.5 %collective-permute-start.8 = (bf16[256,256]{1,0:T(8,128)(2,1)S(1)}, bf16[256,256]{1,0:T(8,128)(2,1)S(1)}, u32[]{:S(2)}, u32[]{:S(2)}) collective-permute-start(bf16[256,256]{1,0:T(8,128)(2,1)S(1)} %fusion.2), channel_id=1, source_target_pairs={{0,4},{2,6},{4,0},{6,2},{1,5},{3,7},{5,1},{7,3},{8,12},{10,14},{12... | collective-permute-start | bytes 393224 | tf_op jit(solution)/shard_map/ppermute | solution.py:488
  88.4 6.0 %copy-start.7 = (bf16[4,256,256]{2,1,0:T(8,128)(2,1)}, bf16[4,256,256]{2,1,0:T(8,128)(2,1)S(1)}, u32[]{:S(2)}) copy-start(bf16[4,256,256]{2,1,0:T(8,128)(2,1)S(1)} %pad_maximum_fusion.same) | copy-start | bytes 1572868
  88.4 6.0 %collective-permute-start.9 = (bf16[4,256,256]{2,1,0:T(8,128)(2,1)S(1)}, bf16[4,256,256]{2,1,0:T(8,128)(2,1)S(1)}, u32[]{:S(2)}, u32[]{:S(2)}) collective-permute-start(bf16[4,256,256]{2,1,0:T(8,128)(2,1)S(1)} %pad_maximum_fusion.same), channel_id=1, source_target_pairs={{0,1},{1,0},{2,3},{3,2},{4,5},{5,4},{6,7},{7,6},{8,9},{9,8},{10,11... | collective-permute-start | bytes 1572872 | tf_op jit(solution)/shard_map/ppermute | solution.py:492
  92.6 35.0 %collective-permute-start.12 = (bf16[256,2048]{1,0:T(8,128)(2,1)S(1)}, bf16[256,2048]{1,0:T(8,128)(2,1)}, u32[]{:S(2)}, u32[]{:S(2)}) collective-permute-start(bf16[256,2048]{1,0:T(8,128)(2,1)S(1)} %collective-permute-done.10.refs_2_.refs_9_), channel_id=1, source_target_pairs={{0,2},{2,4},{4,6},{6,0},{1,3},{3,5},{5,7},{7,1},{8,10},{10,12},{12... | collective-permute-start | bytes 3145736 | tf_op jit(solution)/shard_map/ppermute | solution.py:488
  94.4 11.7 %copy-start = (bf16[256,2048]{1,0:T(8,128)(2,1)S(1)}, bf16[256,2048]{1,0:T(8,128)(2,1)}, u32[]{:S(2)}) copy-start(bf16[256,2048]{1,0:T(8,128)(2,1)} %refs_8_.1) | copy-start | bytes 3145732
  94.4 0.8 copy-start.9
  100.6 16.3 %all-to-all-start.2 = ((bf16[16,64,256]{2,1,0:T(8,128)(2,1)}), bf16[16,64,256]{2,1,0:T(8,128)(2,1)S(1)}, u32[]{:S(2)}, u32[]{:S(2)}) async-start(bf16[16,64,256]{2,1,0:T(8,128)(2,1)} %project_sent.1), calls=%async_computation.2 | async-start | bytes 1048576 | tf_op jit(solution)/shard_map/all_to_all | solution.py:479
  106.1 37.9 %collective-permute-start.13 = (bf16[256,2048]{1,0:T(8,128)(2,1)S(1)}, bf16[256,2048]{1,0:T(8,128)(2,1)}, u32[]{:S(2)}, u32[]{:S(2)}) collective-permute-start(bf16[256,2048]{1,0:T(8,128)(2,1)S(1)} %copy-done), channel_id=1, source_target_pairs={{0,1},{1,0},{2,3},{3,2},{4,5},{5,4},{6,7},{7,6},{8,9},{9,8},{10,11... | collective-permute-start | bytes 3145736 | tf_op jit(solution)/shard_map/ppermute | solution.py:492
  127.6 14.9 %copy-start.11 = (bf16[320,256]{1,0:T(8,128)(2,1)S(1)}, bf16[320,256]{1,0:T(8,128)(2,1)}, u32[]{:S(2)}) copy-start(bf16[320,256]{1,0:T(8,128)(2,1)} %get-tuple-element.114) | copy-start | bytes 491524
  127.6 36.2 %copy-start.1 = (s32[8]{0:T(128)S(1)}, s32[8]{0:T(128)}, u32[]{:S(2)}) copy-start(s32[8]{0:T(128)} %pad_add_fusion.1.order) | copy-start | bytes 100
  127.6 36.2 %copy-start.2 = (f32[2048]{0:T(1024)S(1)}, f32[2048]{0:T(1024)}, u32[]{:S(2)}) copy-start(f32[2048]{0:T(1024)} %param.16) | copy-start | bytes 24580
  127.7 36.2 %copy-start.3 = (s32[8]{0:T(128)S(1)}, s32[8]{0:T(128)}, u32[]{:S(2)}) copy-start(s32[8]{0:T(128)} %iota.15.where.slot) | copy-start | bytes 100
  127.7 31.9 %collective-permute-start.14 = (bf16[256,2048]{1,0:T(8,128)(2,1)S(1)}, bf16[256,2048]{1,0:T(8,128)(2,1)}, u32[]{:S(2)}, u32[]{:S(2)}) collective-permute-start(bf16[256,2048]{1,0:T(8,128)(2,1)S(1)} %collective-permute-done.10.refs_2_.refs_9_), channel_id=1, source_target_pairs={{0,1},{1,0},{2,3},{3,2},{4,5},{5,4},{6,7},{7,6},{8,9},{9,8},{10,11... | collective-permute-start | bytes 3145736 | tf_op jit(solution)/shard_map/ppermute | solution.py:492
  129.4 30.9 %collective-permute-start.15 = (bf16[256,2048]{1,0:T(8,128)(2,1)}, bf16[256,2048]{1,0:T(8,128)(2,1)}, u32[]{:S(2)}, u32[]{:S(2)}) collective-permute-start(bf16[256,2048]{1,0:T(8,128)(2,1)} %collective-permute-done.11.refs_3_.refs_10_), channel_id=1, source_target_pairs={{0,1},{1,0},{2,3},{3,2},{4,5},{5,4},{6,7},{7,6},{8,9},{9,8},{10,11... | collective-permute-start | bytes 3145736 | tf_op jit(solution)/shard_map/ppermute | solution.py:492
  129.5 33.0 %collective-permute-start.16 = (bf16[256,2048]{1,0:T(8,128)(2,1)}, bf16[256,2048]{1,0:T(8,128)(2,1)}, u32[]{:S(2)}, u32[]{:S(2)}) collective-permute-start(bf16[256,2048]{1,0:T(8,128)(2,1)} %collective-permute-done.12.refs_4_.refs_11_), channel_id=1, source_target_pairs={{0,1},{1,0},{2,3},{3,2},{4,5},{5,4},{6,7},{7,6},{8,9},{9,8},{10,11... | collective-permute-start | bytes 3145736 | tf_op jit(solution)/shard_map/ppermute | solution.py:492
  138.6 25.3 %all-to-all-start.3 = ((bf16[8,192,256]{2,1,0:T(8,128)(2,1)}), bf16[8,192,256]{2,1,0:T(8,128)(2,1)S(1)}, u32[]{:S(2)}, u32[]{:S(2)}) async-start(bf16[8,192,256]{2,1,0:T(8,128)(2,1)} %attend.2), calls=%async_computation.3 | async-start | bytes 1572864 | tf_op jit(solution)/shard_map/all_to_all | solution.py:479
  142.5 15.6 %collective-permute-start.17 = (bf16[320,256]{1,0:T(8,128)(2,1)S(1)}, bf16[320,256]{1,0:T(8,128)(2,1)S(1)}, u32[]{:S(2)}, u32[]{:S(2)}) collective-permute-start(bf16[320,256]{1,0:T(8,128)(2,1)S(1)} %copy-done.11), channel_id=1, source_target_pairs={{0,2},{1,3},{2,4},{3,5},{4,6},{5,7},{6,0},{7,1},{8,10},{9,11},{10,... | collective-permute-start | bytes 491528 | tf_op jit(solution)/shard_map/ppermute | solution.py:528
  144.0 14.6 %collective-permute-start.18 = (bf16[320,256]{1,0:T(8,128)(2,1)}, bf16[320,256]{1,0:T(8,128)(2,1)S(1)}, u32[]{:S(2)}, u32[]{:S(2)}) collective-permute-start(bf16[320,256]{1,0:T(8,128)(2,1)} %get-tuple-element.115), channel_id=1, source_target_pairs={{0,6},{1,7},{2,0},{3,1},{4,2},{5,3},{6,4},{7,5},{8,14},{9,15},{10,... | collective-permute-start | bytes 491528 | tf_op jit(solution)/shard_map/ppermute | solution.py:528
  158.1 15.3 %collective-permute-start.19 = (bf16[320,256]{1,0:T(8,128)(2,1)}, bf16[320,256]{1,0:T(8,128)(2,1)S(1)}, u32[]{:S(2)}, u32[]{:S(2)}) collective-permute-start(bf16[320,256]{1,0:T(8,128)(2,1)} %get-tuple-element.116), channel_id=1, source_target_pairs={{0,4},{1,5},{2,6},{3,7},{4,0},{5,1},{6,2},{7,3},{8,12},{9,13},{10,... | collective-permute-start | bytes 491528 | tf_op jit(solution)/shard_map/ppermute | solution.py:528
  158.6 14.8 %collective-permute-start.20 = (bf16[320,256]{1,0:T(8,128)(2,1)}, bf16[320,256]{1,0:T(8,128)(2,1)}, u32[]{:S(2)}, u32[]{:S(2)}) collective-permute-start(bf16[320,256]{1,0:T(8,128)(2,1)} %get-tuple-element.117), channel_id=1, source_target_pairs={{0,1},{1,0},{2,3},{3,2},{4,5},{5,4},{6,7},{7,6},{8,9},{9,8},{10,11... | collective-permute-start | bytes 491528 | tf_op jit(solution)/shard_map/ppermute | solution.py:528
  159.6 13.9 %collective-permute-start.21 = (bf16[320,256]{1,0:T(8,128)(2,1)}, bf16[320,256]{1,0:T(8,128)(2,1)}, u32[]{:S(2)}, u32[]{:S(2)}) collective-permute-start(bf16[320,256]{1,0:T(8,128)(2,1)} %get-tuple-element.118), channel_id=1, source_target_pairs={{0,3},{1,2},{2,5},{3,4},{4,7},{5,6},{6,1},{7,0},{8,11},{9,10},{10,... | collective-permute-start | bytes 491528 | tf_op jit(solution)/shard_map/ppermute | solution.py:528
  160.3 13.1 %collective-permute-start.22 = (bf16[320,256]{1,0:T(8,128)(2,1)}, bf16[320,256]{1,0:T(8,128)(2,1)}, u32[]{:S(2)}, u32[]{:S(2)}) collective-permute-start(bf16[320,256]{1,0:T(8,128)(2,1)} %get-tuple-element.119), channel_id=1, source_target_pairs={{0,7},{1,6},{2,1},{3,0},{4,3},{5,2},{6,5},{7,4},{8,15},{9,14},{10,... | collective-permute-start | bytes 491528 | tf_op jit(solution)/shard_map/ppermute | solution.py:528
  162.5 10.9 %collective-permute-start.23 = (bf16[320,256]{1,0:T(8,128)(2,1)}, bf16[320,256]{1,0:T(8,128)(2,1)}, u32[]{:S(2)}, u32[]{:S(2)}) collective-permute-start(bf16[320,256]{1,0:T(8,128)(2,1)} %get-tuple-element.120), channel_id=1, source_target_pairs={{0,5},{1,4},{2,7},{3,6},{4,1},{5,0},{6,3},{7,2},{8,13},{9,12},{10,... | collective-permute-start | bytes 491528 | tf_op jit(solution)/shard_map/ppermute | solution.py:528
  163.9 9.6 %copy-start.4 = (s32[8]{0:T(128)S(1)}, s32[8]{0:T(128)}, u32[]{:S(2)}) copy-start(s32[8]{0:T(128)} %pad_add_fusion.2.where.slot) | copy-start | bytes 100
  169.5 23.4 %all-to-all-start.4 = ((bf16[8,192,256]{2,1,0:T(8,128)(2,1)}), bf16[8,192,256]{2,1,0:T(8,128)(2,1)S(1)}, u32[]{:S(2)}, u32[]{:S(2)}) async-start(bf16[8,192,256]{2,1,0:T(8,128)(2,1)} %project_out.2), calls=%async_computation.4 | async-start | bytes 1572864 | tf_op jit(solution)/shard_map/all_to_all | solution.py:479
  173.5 0.9 copy-start.5
  181.4 8.6 %collective-permute-start.24 = (bf16[320,256]{1,0:T(8,128)(2,1)S(1)}, bf16[320,256]{1,0:T(8,128)(2,1)S(1)}, u32[]{:S(2)}, u32[]{:S(2)}) collective-permute-start(bf16[320,256]{1,0:T(8,128)(2,1)S(1)} %get-tuple-element.130), channel_id=1, source_target_pairs={{0,2},{1,3},{2,4},{3,5},{4,6},{5,7},{6,0},{7,1},{8,10},{9,11},{10,... | collective-permute-start | bytes 491528 | tf_op jit(solution)/shard_map/ppermute | solution.py:528
  182.8 8.6 %collective-permute-start.25 = (bf16[320,256]{1,0:T(8,128)(2,1)S(1)}, bf16[320,256]{1,0:T(8,128)(2,1)S(1)}, u32[]{:S(2)}, u32[]{:S(2)}) collective-permute-start(bf16[320,256]{1,0:T(8,128)(2,1)S(1)} %get-tuple-element.131), channel_id=1, source_target_pairs={{0,6},{1,7},{2,0},{3,1},{4,2},{5,3},{6,4},{7,5},{8,14},{9,15},{10,... | collective-permute-start | bytes 491528 | tf_op jit(solution)/shard_map/ppermute | solution.py:528
  184.2 10.2 %collective-permute-start.26 = (bf16[320,256]{1,0:T(8,128)(2,1)}, bf16[320,256]{1,0:T(8,128)(2,1)S(1)}, u32[]{:S(2)}, u32[]{:S(2)}) collective-permute-start(bf16[320,256]{1,0:T(8,128)(2,1)} %get-tuple-element.132), channel_id=1, source_target_pairs={{0,4},{1,5},{2,6},{3,7},{4,0},{5,1},{6,2},{7,3},{8,12},{9,13},{10,... | collective-permute-start | bytes 491528 | tf_op jit(solution)/shard_map/ppermute | solution.py:528
  185.8 8.6 %collective-permute-start.27 = (bf16[320,256]{1,0:T(8,128)(2,1)}, bf16[320,256]{1,0:T(8,128)(2,1)S(1)}, u32[]{:S(2)}, u32[]{:S(2)}) collective-permute-start(bf16[320,256]{1,0:T(8,128)(2,1)} %get-tuple-element.133), channel_id=1, source_target_pairs={{0,1},{1,0},{2,3},{3,2},{4,5},{5,4},{6,7},{7,6},{8,9},{9,8},{10,11... | collective-permute-start | bytes 491528 | tf_op jit(solution)/shard_map/ppermute | solution.py:528
  187.0 10.8 %collective-permute-start.28 = (bf16[320,256]{1,0:T(8,128)(2,1)}, bf16[320,256]{1,0:T(8,128)(2,1)S(1)}, u32[]{:S(2)}, u32[]{:S(2)}) collective-permute-start(bf16[320,256]{1,0:T(8,128)(2,1)} %get-tuple-element.134), channel_id=1, source_target_pairs={{0,3},{1,2},{2,5},{3,4},{4,7},{5,6},{6,1},{7,0},{8,11},{9,10},{10,... | collective-permute-start | bytes 491528 | tf_op jit(solution)/shard_map/ppermute | solution.py:528
  190.1 7.8 %collective-permute-start.29 = (bf16[320,256]{1,0:T(8,128)(2,1)}, bf16[320,256]{1,0:T(8,128)(2,1)S(1)}, u32[]{:S(2)}, u32[]{:S(2)}) collective-permute-start(bf16[320,256]{1,0:T(8,128)(2,1)} %get-tuple-element.135), channel_id=1, source_target_pairs={{0,7},{1,6},{2,1},{3,0},{4,3},{5,2},{6,5},{7,4},{8,15},{9,14},{10,... | collective-permute-start | bytes 491528 | tf_op jit(solution)/shard_map/ppermute | solution.py:528
  191.4 8.8 %collective-permute-start.30 = (bf16[320,256]{1,0:T(8,128)(2,1)}, bf16[320,256]{1,0:T(8,128)(2,1)S(1)}, u32[]{:S(2)}, u32[]{:S(2)}) collective-permute-start(bf16[320,256]{1,0:T(8,128)(2,1)} %get-tuple-element.136), channel_id=1, source_target_pairs={{0,5},{1,4},{2,7},{3,6},{4,1},{5,0},{6,3},{7,2},{8,13},{9,12},{10,... | collective-permute-start | bytes 491528 | tf_op jit(solution)/shard_map/ppermute | solution.py:528
  (1 other events, 0.8 us)

commit v11 on v10

--- a/solution.py
+++ b/solution.py
@@ -12,7 +12,7 @@
 BLOCK = 64
 HOT = 8
 REACH = 2
-FIRST_BLOCKS = 3
+FIRST_BLOCKS = 4
 KV = ("kv_0", "kv_1")
 TP = ("tp_0", "tp_1")
 WIDTH = 256
@@ -48,7 +48,7 @@
 def token_shares(rank, tokens, long, side):
     length = tokens.shape[0]
     devices = long * side
-    tile = 1024
+    tile = 4096
     return pl.pallas_call(
         share_kernel,
         grid_spec=pltpu.PrefetchScalarGridSpec(
@@ -237,15 +237,21 @@
     devices, hot_rows, _ = hot.shape
     here = pairs.shape[0]
     plain = near.shape[0]
-    used = pl.ds(0, (first + mask.shape[0]) * PAIR * BLOCK)
+    count = where.shape[0]
+    whole = len(outs) == 1
+    steps = 2 if whole else 1
+    used = (first + mask.shape[0]) * PAIR * BLOCK // steps
+    owns = []
+    for n in range(steps):
+        span = pl.ds(n * used, used)
+        owns.append(pltpu.make_async_copy(pairs.at[span], table.at[span], sems.at[4 + n]))
     copies = [
         pltpu.make_async_copy(hot, raw, sems.at[0]),
-        pltpu.make_async_copy(pairs.at[used], table.at[used], sems.at[1]),
-        pltpu.make_async_copy(near, table.at[pl.ds(here, plain)], sems.at[2]),
-        pltpu.make_async_copy(queries.at[pl.ds(first * BLOCK, q.shape[0])], q, sems.at[3]),
-        pltpu.make_async_copy(masks.at[pl.ds(first, mask.shape[0])], mask, sems.at[4]),
+        pltpu.make_async_copy(near, table.at[pl.ds(here, plain)], sems.at[1]),
+        pltpu.make_async_copy(queries.at[pl.ds(first * BLOCK, q.shape[0])], q, sems.at[2]),
+        pltpu.make_async_copy(masks.at[pl.ds(first, mask.shape[0])], mask, sems.at[3]),
     ]
-    for copy in copies:
+    for copy in copies + owns:
         copy.start()
     copies[0].wait()
     part = BLOCK // devices
@@ -260,8 +266,6 @@
     for copy in copies[1:]:
         copy.wait()
     slots = mask.shape[1] // BLOCK
-    count = where.shape[0]
-    whole = len(outs) == 1
     per_piece = mask.shape[0] // count
     blank = jnp.zeros((BLOCK, HEAD_DIM), bf16)
 
@@ -302,23 +306,17 @@
             put(to, slice(0, HEAD_DIM), sums[:BLOCK, :HEAD_DIM] * scale[:BLOCK])
             put(to, slice(HEAD_DIM, WIDTH), sums[BLOCK:, HEAD_DIM:] * scale[BLOCK:])
 
-    if whole:
-
-        def one(n, carry):
-            def put(rows, lanes, value):
+    for n in range(count):
+        if n % (count // steps) == 0:
+            owns[n // (count // steps)].wait()
+
+        def put(rows, lanes, value, n=n):
+            if whole:
                 outs[0][n, rows, lanes] = value.astype(bf16)
-
-            piece_of(n, put)
-            return carry
-
-        lax.fori_loop(0, count, one, 0)
-    else:
-        for n in range(count):
-
-            def put(rows, lanes, value, n=n):
+            else:
                 outs[n][rows, lanes] = value.astype(bf16)
 
-            piece_of(n, put)
+        piece_of(n, put)
 
 
 def attend(first, blocks, split, at, where, queries, mask, pairs, near, hot):
@@ -348,7 +346,7 @@
                 pltpu.VMEM((blocks, slots * BLOCK), f32),
                 pltpu.VMEM((height, WIDTH), bf16),
                 pltpu.VMEM(hot.shape, bf16),
-                pltpu.SemaphoreType.DMA((5,)),
+                pltpu.SemaphoreType.DMA((6,)),
             ],
         ),
         out_shape=[jax.ShapeDtypeStruct(shape, bf16)] * count,

time: 203 us -> 217 us (1.069)
  waiting for transfers between devices: 48.7 us -> 64 us
  Pallas kernels: 71.2 us -> 68.5 us
  starting transfers between devices: 70.1 us -> 72.7 us
    all_to_all x5, waiting for transfers between devices: 6.99 us -> 22 us  [exchange(): return lax.all_to_all(pieces, axes, split_axis=0, concat_axis=0, tiled=True)]
  transfers between devices with their start and end apart: 36 -> 36, of which waited for: 8 -> 12; matrix products, arithmetic and copies ran while one was open for 4% -> 4% of each run, Pallas kernels for 34% -> 28%
where the time goes in v11:
time: 217 us; the launch traced here: 216 us
  starting transfers between devices  72.7 us (34%)
  Pallas kernels  68.5 us (32%)
  waiting for transfers between devices  64 us (29%)
  local copies, waits for them, and re-layouts  5.37 us (2%)
  other arithmetic  5.1 us (2%)
    all_to_all x5, starting transfers between devices, exchange(): return lax.all_to_all(pieces, axes, split_axis=0, concat_axis=0, tiled=True)  26.5 us
    all_to_all x5, waiting for transfers between devices, exchange(): return lax.all_to_all(pieces, axes, split_axis=0, concat_axis=0, tiled=True)  22 us
    ppermute x14, waiting for transfers between devices, send_pieces(): got.append(lax.ppermute(pieces[k], TP, pairs) if k else pieces[0])  21.8 us
    ppermute x3, waiting for transfers between devices, local(): lax.ppermute(held[n], KV, [(i, i + n) for i in starts])  20.2 us
    ppermute x14, starting transfers between devices, send_pieces(): got.append(lax.ppermute(pieces[k], TP, pairs) if k else pieces[0])  18.9 us
    pallas_call x2, Pallas kernels, attend(): pl.pallas_call(functools.partial(attention_kernel, first), grid_spec=pltp...  16.4 us
    pallas_call x1, Pallas kernels, project_kv(): pl.pallas_call(kv_kernel, grid=(length // tile,), in_specs=[pl.BlockSpec(...  13.7 us
    pallas_call x2, Pallas kernels, project_out(): pl.pallas_call(out_kernel, grid_spec=pltpu.PrefetchScalarGridSpec(num_sca...  12.4 us
  transfers between devices with their start and end apart: 36, of which 12 were waited for; matrix products, arithmetic and copies ran while one was open for 4% of the time, Pallas kernels for 28%

profile of v11, /device:TPU:1, one launch (start us, length us, event | category | flops | bytes accessed | tf_op | source)
XLA Modules:
  0.0 216.3 jit_solution(1135384283286914151)
XLA Ops:
  0.0 2.1 collective-permute-start.10
  2.1 1.4 collective-permute-start.11
  3.6 3.3 %token_shares.1 = (bf16[4,256,256]{2,1,0:T(8,128)(2,1)}, bf16[4,256,256]{2,1,0:T(8,128)(2,1)}, bf16[4,256,256]{2,1,0:T(8,128)(2,1)}, bf16[4,256,256]{2,1,0:T(8,128)(2,1)}) custom-call(s32[1]{0:T(128)} %bitcast.5.rank, bf16[4096,2048]{1,0:T(8,128)(2,1)} %tok.4), custom_call_target="tpu_custom_call" | custom-call | flops 1048576 | bytes 4194304 | tf_op jit(solution)/shard_map/token_shares/pallas_call | solution.py:52
  8.7 7.6 %all-to-all-start = ((s32[16,1,16]{2,1,0:T(1,128)}), s32[16,1,16]{2,1,0:T(1,128)S(1)}, u32[]{:S(2)}, u32[]{:S(2)}) async-start(s32[16,1,16]{2,1,0:T(1,128)} %bitcast.8), calls=%async_computation | async-start | bytes 16384 | tf_op jit(solution)/shard_map/all_to_all | solution.py:477
  16.3 3.3 %collective-permute-start = (bf16[4,256,256]{2,1,0:T(8,128)(2,1)}, bf16[4,256,256]{2,1,0:T(8,128)(2,1)S(1)}, u32[]{:S(2)}, u32[]{:S(2)}) collective-permute-start(bf16[4,256,256]{2,1,0:T(8,128)(2,1)} %get-tuple-element.77), channel_id=1, source_target_pairs={{0,32},{1,33},{2,34},{3,35},{4,36},{5,37},{6,38},{7,39}} | collective-permute-start | bytes 1572872 | tf_op jit(solution)/shard_map/ppermute | solution.py:544
  19.6 2.2 %collective-permute-start.1 = (bf16[4,256,256]{2,1,0:T(8,128)(2,1)}, bf16[4,256,256]{2,1,0:T(8,128)(2,1)S(1)}, u32[]{:S(2)}, u32[]{:S(2)}) collective-permute-start(bf16[4,256,256]{2,1,0:T(8,128)(2,1)} %get-tuple-element.78), channel_id=1, source_target_pairs={{0,64},{1,65},{2,66},{3,67},{4,68},{5,69},{6,70},{7,71}} | collective-permute-start | bytes 1572872 | tf_op jit(solution)/shard_map/ppermute | solution.py:544
  21.8 1.3 collective-permute-start.2
  23.2 13.7 %project_kv.1 = bf16[64,2,64,256]{3,2,1,0:T(8,128)(2,1)} custom-call(bf16[4096,2048]{1,0:T(8,128)(2,1)} %tok.4, bf16[2048,256]{1,0:T(8,128)(2,1)} %wk.3, bf16[2048,256]{1,0:T(8,128)(2,1)} %wv.3, f32[1,128]{1,0:T(1,128)} %bitcast.50), custom_call_target="tpu_custom_call" | custom-call | flops 8589934592 | bytes 16777216 | tf_op jit(solution)/shard_map/project_kv/pallas_call | solution.py:83
  37.6 4.8 %gather_near.1 = bf16[32,128,256]{2,1,0:T(8,128)(2,1)} custom-call(s32[32]{0:T(128)} %reshape.69.near, bf16[8192,256]{1,0:T(8,128)(2,1)} %bitcast.40), custom_call_target="tpu_custom_call" | custom-call | flops 1048576 | bytes 4194304 | tf_op jit(solution)/shard_map/gather_near/pallas_call | solution.py:151
  42.5 4.6 %all-to-all-start.1 = ((bf16[16,256,256]{2,1,0:T(8,128)(2,1)}), bf16[16,256,256]{2,1,0:T(8,128)(2,1)}, u32[]{:S(2)}, u32[]{:S(2)}) async-start(bf16[16,256,256]{2,1,0:T(8,128)(2,1)} %bitcast.43), calls=%async_computation.1 | async-start | bytes 4194304 | tf_op jit(solution)/shard_map/all_to_all | solution.py:477
  47.2 4.3 %collective-permute-start.3 = (bf16[256,256]{1,0:T(8,128)(2,1)S(1)}, bf16[256,256]{1,0:T(8,128)(2,1)S(1)}, u32[]{:S(2)}, u32[]{:S(2)}) collective-permute-start(bf16[256,256]{1,0:T(8,128)(2,1)S(1)} %get-tuple-element.143), channel_id=1, source_target_pairs={{0,24},{32,56},{64,88},{96,120},{1,25},{33,57},{65,89},{97,121},{2... | collective-permute-start | bytes 393224 | tf_op jit(solution)/shard_map/ppermute | solution.py:575
  51.5 1.3 collective-permute-start.4
  52.8 1.3 collective-permute-start.5
  54.7 16.2 %collective-permute-done.3 = bf16[256,256]{1,0:T(8,128)(2,1)S(1)} collective-permute-done((bf16[256,256]{1,0:T(8,128)(2,1)S(1)}, bf16[256,256]{1,0:T(8,128)(2,1)S(1)}, u32[]{:S(2)}, u32[]{:S(2)}) %collective-permute-start.3) | collective-permute-done | bytes 131104 | tf_op jit(solution)/shard_map/ppermute | solution.py:575
  71.0 1.1 collective-permute-done.4
  72.1 2.8 %collective-permute-done.5 = bf16[256,256]{1,0:T(8,128)(2,1)S(1)} collective-permute-done((bf16[256,256]{1,0:T(8,128)(2,1)S(1)}, bf16[256,256]{1,0:T(8,128)(2,1)S(1)}, u32[]{:S(2)}, u32[]{:S(2)}) %collective-permute-start.5) | collective-permute-done | bytes 131104 | tf_op jit(solution)/shard_map/ppermute | solution.py:575
  75.0 2.7 %collective-permute-start.7 = (bf16[256,256]{1,0:T(8,128)(2,1)S(1)}, bf16[256,256]{1,0:T(8,128)(2,1)S(1)}, u32[]{:S(2)}, u32[]{:S(2)}) collective-permute-start(bf16[256,256]{1,0:T(8,128)(2,1)S(1)} %fusion.2), channel_id=1, source_target_pairs={{0,6},{2,0},{4,2},{6,4},{1,7},{3,1},{5,3},{7,5},{8,14},{10,8},{12,... | collective-permute-start | bytes 393224 | tf_op jit(solution)/shard_map/ppermute | solution.py:486
  77.9 10.1 %project_q.1.queries = bf16[4096,256]{1,0:T(8,128)(2,1)} custom-call(bf16[4096,2048]{1,0:T(8,128)(2,1)} %tok.4, bf16[2048,256]{1,0:T(8,128)(2,1)} %wq.1, f32[1,128]{1,0:T(1,128)} %multiply_bitcast_fusion.gain), custom_call_target="tpu_custom_call" | custom-call | flops 4294967296 | bytes 16777216 | tf_op jit(solution)/shard_map/project_q/pallas_call | solution.py:112
  88.1 3.5 %collective-permute-start.9 = (bf16[4,256,256]{2,1,0:T(8,128)(2,1)S(1)}, bf16[4,256,256]{2,1,0:T(8,128)(2,1)S(1)}, u32[]{:S(2)}, u32[]{:S(2)}) collective-permute-start(bf16[4,256,256]{2,1,0:T(8,128)(2,1)S(1)} %pad_maximum_fusion.same), channel_id=1, source_target_pairs={{0,1},{1,0},{2,3},{3,2},{4,5},{5,4},{6,7},{7,6},{8,9},{9,8},{10,11... | collective-permute-start | bytes 1572872 | tf_op jit(solution)/shard_map/ppermute | solution.py:490
  94.9 4.8 %project_sent.1 = bf16[16,64,256]{2,1,0:T(8,128)(2,1)} custom-call(s32[128]{0:T(128)} %reshape.68.asked, s32[8]{0:T(128)} %pad_add_fusion.1.order, bf16[4,256,256]{2,1,0:T(8,128)(2,1)} %copy-done.7, bf16[4,256,256]{2,1,0:T(8,128)(2,1)} %copy-done.9, bf16[2048,256]{1,0:T(8,128)(2,1)} %wk.3, bf16[2048,256]{1,0:T(8,128)(2,1)} %wv.3, f32[1,128]{1,0:T(1,128)} %bitcast.51), custom_call_target="tpu_custom_call" | custom-call | flops 536870912 | bytes 8388608 | tf_op jit(solution)/shard_map/project_sent/pallas_call | solution.py:211
  100.2 5.8 %all-to-all-start.2 = ((bf16[16,64,256]{2,1,0:T(8,128)(2,1)}), bf16[16,64,256]{2,1,0:T(8,128)(2,1)S(1)}, u32[]{:S(2)}, u32[]{:S(2)}) async-start(bf16[16,64,256]{2,1,0:T(8,128)(2,1)} %project_sent.1), calls=%async_computation.2 | async-start | bytes 1048576 | tf_op jit(solution)/shard_map/all_to_all | solution.py:477
  106.9 1.3 select_reduce_fusion
  109.7 7.1 %all-to-all-done.2.hot = bf16[16,64,256]{2,1,0:T(8,128)(2,1)S(1)} async-done(((bf16[16,64,256]{2,1,0:T(8,128)(2,1)}), bf16[16,64,256]{2,1,0:T(8,128)(2,1)S(1)}, u32[]{:S(2)}, u32[]{:S(2)}) %all-to-all-start.2) | async-done | bytes 524320 | tf_op jit(solution)/shard_map/all_to_all | solution.py:477
  117.6 8.5 %attend.3 = (bf16[256,256]{1,0:T(8,128)(2,1)}, bf16[256,256]{1,0:T(8,128)(2,1)}, bf16[256,256]{1,0:T(8,128)(2,1)}, bf16[256,256]{1,0:T(8,128)(2,1)}, bf16[256,25...) custom-call(s32[512]{0:T(512)} %reshape.71.at, ...), custom_call_target="tpu_custom_call" | custom-call | flops 2147483648 | bytes 10485760 | tf_op jit(solution)/shard_map/attend/pallas_call | solution.py:331
  126.1 1.8 collective-permute-start.14
  128.4 7.9 %attend.2 = bf16[8,256,256]{2,1,0:T(8,128)(2,1)} custom-call(s32[512]{0:T(512)} %reshape.71.at, s32[8]{0:T(128)} %iota.15.where.slot, bf16[4096,256]{1,0:T(8,128)(2,1)} %project_q.1.queries, f32[64,512]{1,0:T(8,128)} %reshape.72.masks, bf16[8192,256]{1,0:T(8,128)(2,1)} %bitcast.42, bf16[4096,256]{1,0:T(8,128)(2,1)} %bitcast.22.near, ...), custom_call_target="tpu_custom_call" | custom-call | flops 2147483648 | bytes 10485760 | tf_op jit(solution)/shard_map/attend/pallas_call | solution.py:331
  136.3 4.0 %all-to-all-start.3 = ((bf16[8,256,256]{2,1,0:T(8,128)(2,1)}), bf16[8,256,256]{2,1,0:T(8,128)(2,1)S(1)}, u32[]{:S(2)}, u32[]{:S(2)}) async-start(bf16[8,256,256]{2,1,0:T(8,128)(2,1)} %attend.2), calls=%async_computation.3 | async-start | bytes 2097152 | tf_op jit(solution)/shard_map/all_to_all | solution.py:477
  140.3 15.0 %all-to-all-done.3.refs_0_ = bf16[8,256,256]{2,1,0:T(8,128)(2,1)S(1)} async-done(((bf16[8,256,256]{2,1,0:T(8,128)(2,1)}), bf16[8,256,256]{2,1,0:T(8,128)(2,1)S(1)}, u32[]{:S(2)}, u32[]{:S(2)}) %all-to-all-start.3) | async-done | bytes 1048608 | tf_op jit(solution)/shard_map/all_to_all | solution.py:477
  155.3 6.3 %project_out.2 = bf16[8,256,256]{2,1,0:T(8,128)(2,1)} custom-call(s32[8]{0:T(128)S(1)} %copy-done.3, s32[8]{0:T(128)S(1)} %copy-done.5, bf16[8,256,256]{2,1,0:T(8,128)(2,1)S(1)} %all-to-all-done.3.refs_0_, bf16[256,2048]{1,0:T(8,128)(2,1)S(1)} %copy-done, bf16[256,2048]{1,0:T(8,128)(2,1)S(1)} %collective-permute-done.10.refs_2_.refs_9_, ...), custom_call_target="tpu_custom_call" | custom-call | flops 2147483648 | bytes 12582912 | tf_op jit(solution)/shard_map/project_out/pallas_call | solution.py:406
  161.6 4.6 %all-to-all-start.4 = ((bf16[8,256,256]{2,1,0:T(8,128)(2,1)}), bf16[8,256,256]{2,1,0:T(8,128)(2,1)S(1)}, u32[]{:S(2)}, u32[]{:S(2)}) async-start(bf16[8,256,256]{2,1,0:T(8,128)(2,1)} %project_out.2), calls=%async_computation.4 | async-start | bytes 2097152 | tf_op jit(solution)/shard_map/all_to_all | solution.py:477
  166.2 1.4 collective-permute-start.17
  167.5 1.3 collective-permute-start.18
  168.8 1.7 collective-permute-start.19
  170.5 1.2 collective-permute-start.20
  171.9 12.0 %collective-permute-done.17.refs_1_ = bf16[256,256]{1,0:T(8,128)(2,1)S(1)} collective-permute-done((bf16[256,256]{1,0:T(8,128)(2,1)}, bf16[256,256]{1,0:T(8,128)(2,1)S(1)}, u32[]{:S(2)}, u32[]{:S(2)}) %collective-permute-start.17) | collective-permute-done | bytes 131104 | tf_op jit(solution)/shard_map/ppermute | solution.py:526
  183.9 1.8 collective-permute-start.22
  185.7 2.3 %collective-permute-start.23 = (bf16[256,256]{1,0:T(8,128)(2,1)S(1)}, bf16[256,256]{1,0:T(8,128)(2,1)S(1)}, u32[]{:S(2)}, u32[]{:S(2)}) collective-permute-start(bf16[256,256]{1,0:T(8,128)(2,1)S(1)} %copy-done.11), channel_id=1, source_target_pairs={{0,5},{1,4},{2,7},{3,6},{4,1},{5,0},{6,3},{7,2},{8,13},{9,12},{10,... | collective-permute-start | bytes 393224 | tf_op jit(solution)/shard_map/ppermute | solution.py:526
  188.0 2.0 collective-permute-done.21.refs_5_
  189.9 2.8 %collective-permute-done.23.refs_7_ = bf16[256,256]{1,0:T(8,128)(2,1)S(1)} collective-permute-done((bf16[256,256]{1,0:T(8,128)(2,1)S(1)}, bf16[256,256]{1,0:T(8,128)(2,1)S(1)}, u32[]{:S(2)}, u32[]{:S(2)}) %collective-permute-start.23) | collective-permute-done | bytes 131104 | tf_op jit(solution)/shard_map/ppermute | solution.py:526
  192.8 6.1 %project_out.3 = (bf16[256,256]{1,0:T(8,128)(2,1)S(1)}, bf16[256,256]{1,0:T(8,128)(2,1)S(1)}, bf16[256,256]{1,0:T(8,128)(2,1)S(1)}, bf16[256,256]{1,0:T(8,128)(2...) custom-call(s32[8]{0:T(128)S(1)} %copy-done.3, ...), custom_call_target="tpu_custom_call" | custom-call | flops 2147483648 | bytes 12582912 | tf_op jit(solution)/shard_map/project_out/pallas_call | solution.py:406
  198.9 1.1 collective-permute-start.24
  200.0 1.5 collective-permute-start.25
  204.9 2.3 %collective-permute-start.29 = (bf16[256,256]{1,0:T(8,128)(2,1)}, bf16[256,256]{1,0:T(8,128)(2,1)S(1)}, u32[]{:S(2)}, u32[]{:S(2)}) collective-permute-start(bf16[256,256]{1,0:T(8,128)(2,1)} %get-tuple-element.135), channel_id=1, source_target_pairs={{0,7},{1,6},{2,1},{3,0},{4,3},{5,2},{6,5},{7,4},{8,15},{9,14},{10,... | collective-permute-start | bytes 393224 | tf_op jit(solution)/shard_map/ppermute | solution.py:526
  207.2 1.7 collective-permute-start.30
  208.9 1.6 place.2.filled
  210.5 1.4 collective-permute-done.28.rest_4_
  212.0 2.6 %collective-permute-done.30.rest_6_ = bf16[256,256]{1,0:T(8,128)(2,1)S(1)} collective-permute-done((bf16[256,256]{1,0:T(8,128)(2,1)S(1)}, bf16[256,256]{1,0:T(8,128)(2,1)S(1)}, u32[]{:S(2)}, u32[]{:S(2)}) %collective-permute-start.30) | collective-permute-done | bytes 131104 | tf_op jit(solution)/shard_map/ppermute | solution.py:526
  214.6 1.5 place.3
  (95 shorter events, 15.0 us)
Async XLA Ops:
  0.0 92.3 %collective-permute-start.10 = (bf16[256,2048]{1,0:T(8,128)(2,1)}, bf16[256,2048]{1,0:T(8,128)(2,1)S(1)}, u32[]{:S(2)}, u32[]{:S(2)}) collective-permute-start(bf16[256,2048]{1,0:T(8,128)(2,1)} %refs_8_.1), channel_id=1, source_target_pairs={{0,2},{2,4},{4,6},{6,0},{1,3},{3,5},{5,7},{7,1},{8,10},{10,12},{12... | collective-permute-start | bytes 3145736 | tf_op jit(solution)/shard_map/ppermute | solution.py:486
  2.1 124.0 %collective-permute-start.11 = (bf16[256,2048]{1,0:T(8,128)(2,1)}, bf16[256,2048]{1,0:T(8,128)(2,1)}, u32[]{:S(2)}, u32[]{:S(2)}) collective-permute-start(bf16[256,2048]{1,0:T(8,128)(2,1)} %refs_8_.1), channel_id=1, source_target_pairs={{0,6},{2,0},{4,2},{6,4},{1,7},{3,1},{5,3},{7,5},{8,14},{10,8},{12,... | collective-permute-start | bytes 3145736 | tf_op jit(solution)/shard_map/ppermute | solution.py:486
  3.6 3.4 %copy-start.10 = (s32[64,8]{0,1:T(8,128)S(1)}, s32[64,8]{0,1:T(8,128)}, u32[]{:S(2)}) copy-start(s32[64,8]{0,1:T(8,128)} %param.17) | copy-start | bytes 6148
  8.7 28.3 %all-to-all-start = ((s32[16,1,16]{2,1,0:T(1,128)}), s32[16,1,16]{2,1,0:T(1,128)S(1)}, u32[]{:S(2)}, u32[]{:S(2)}) async-start(s32[16,1,16]{2,1,0:T(1,128)} %bitcast.8), calls=%async_computation | async-start | bytes 16384 | tf_op jit(solution)/shard_map/all_to_all | solution.py:477
  16.3 26.1 %collective-permute-start = (bf16[4,256,256]{2,1,0:T(8,128)(2,1)}, bf16[4,256,256]{2,1,0:T(8,128)(2,1)S(1)}, u32[]{:S(2)}, u32[]{:S(2)}) collective-permute-start(bf16[4,256,256]{2,1,0:T(8,128)(2,1)} %get-tuple-element.77), channel_id=1, source_target_pairs={{0,32},{1,33},{2,34},{3,35},{4,36},{5,37},{6,38},{7,39}} | collective-permute-start | bytes 1572872 | tf_op jit(solution)/shard_map/ppermute | solution.py:544
  19.6 22.8 %collective-permute-start.1 = (bf16[4,256,256]{2,1,0:T(8,128)(2,1)}, bf16[4,256,256]{2,1,0:T(8,128)(2,1)S(1)}, u32[]{:S(2)}, u32[]{:S(2)}) collective-permute-start(bf16[4,256,256]{2,1,0:T(8,128)(2,1)} %get-tuple-element.78), channel_id=1, source_target_pairs={{0,64},{1,65},{2,66},{3,67},{4,68},{5,69},{6,70},{7,71}} | collective-permute-start | bytes 1572872 | tf_op jit(solution)/shard_map/ppermute | solution.py:544
  21.8 20.6 %collective-permute-start.2 = (bf16[4,256,256]{2,1,0:T(8,128)(2,1)}, bf16[4,256,256]{2,1,0:T(8,128)(2,1)S(1)}, u32[]{:S(2)}, u32[]{:S(2)}) collective-permute-start(bf16[4,256,256]{2,1,0:T(8,128)(2,1)} %get-tuple-element.79), channel_id=1, source_target_pairs={{0,96},{1,97},{2,98},{3,99},{4,100},{5,101},{6,102},{7,103}} | collective-permute-start | bytes 1572872 | tf_op jit(solution)/shard_map/ppermute | solution.py:544
  42.5 4.6 %copy-start.8 = (bf16[4,256,256]{2,1,0:T(8,128)(2,1)S(1)}, bf16[4,256,256]{2,1,0:T(8,128)(2,1)}, u32[]{:S(2)}) copy-start(bf16[4,256,256]{2,1,0:T(8,128)(2,1)} %get-tuple-element.85) | copy-start | bytes 1572868
  42.5 11.6 %copy-start.13 = (f32[128]{0:T(128)S(1)}, f32[128]{0:T(128)}, u32[]{:S(2)}) copy-start(f32[128]{0:T(128)} %param.14) | copy-start | bytes 1540
  42.5 57.7 %all-to-all-start.1 = ((bf16[16,256,256]{2,1,0:T(8,128)(2,1)}), bf16[16,256,256]{2,1,0:T(8,128)(2,1)}, u32[]{:S(2)}, u32[]{:S(2)}) async-start(bf16[16,256,256]{2,1,0:T(8,128)(2,1)} %bitcast.43), calls=%async_computation.1 | async-start | bytes 4194304 | tf_op jit(solution)/shard_map/all_to_all | solution.py:477
  47.2 23.8 %collective-permute-start.3 = (bf16[256,256]{1,0:T(8,128)(2,1)S(1)}, bf16[256,256]{1,0:T(8,128)(2,1)S(1)}, u32[]{:S(2)}, u32[]{:S(2)}) collective-permute-start(bf16[256,256]{1,0:T(8,128)(2,1)S(1)} %get-tuple-element.143), channel_id=1, source_target_pairs={{0,24},{32,56},{64,88},{96,120},{1,25},{33,57},{65,89},{97,121},{2... | collective-permute-start | bytes 393224 | tf_op jit(solution)/shard_map/ppermute | solution.py:575
  51.5 20.6 %collective-permute-start.4 = (bf16[256,256]{1,0:T(8,128)(2,1)S(1)}, bf16[256,256]{1,0:T(8,128)(2,1)S(1)}, u32[]{:S(2)}, u32[]{:S(2)}) collective-permute-start(bf16[256,256]{1,0:T(8,128)(2,1)S(1)} %get-tuple-element.142), channel_id=1, source_target_pairs={{0,16},{32,48},{64,80},{96,112},{1,17},{33,49},{65,81},{97,113},{2... | collective-permute-start | bytes 393224 | tf_op jit(solution)/shard_map/ppermute | solution.py:575
  52.8 22.1 %collective-permute-start.5 = (bf16[256,256]{1,0:T(8,128)(2,1)S(1)}, bf16[256,256]{1,0:T(8,128)(2,1)S(1)}, u32[]{:S(2)}, u32[]{:S(2)}) collective-permute-start(bf16[256,256]{1,0:T(8,128)(2,1)S(1)} %get-tuple-element.141), channel_id=1, source_target_pairs={{0,8},{32,40},{64,72},{96,104},{1,9},{33,41},{65,73},{97,105},{2,1... | collective-permute-start | bytes 393224 | tf_op jit(solution)/shard_map/ppermute | solution.py:575
  75.0 13.1 %collective-permute-start.6 = (bf16[256,256]{1,0:T(8,128)(2,1)S(1)}, bf16[256,256]{1,0:T(8,128)(2,1)S(1)}, u32[]{:S(2)}, u32[]{:S(2)}) collective-permute-start(bf16[256,256]{1,0:T(8,128)(2,1)S(1)} %fusion.2), channel_id=1, source_target_pairs={{0,2},{2,4},{4,6},{6,0},{1,3},{3,5},{5,7},{7,1},{8,10},{10,12},{12... | collective-permute-start | bytes 393224 | tf_op jit(solution)/shard_map/ppermute | solution.py:486
  75.0 13.0 %collective-permute-start.7 = (bf16[256,256]{1,0:T(8,128)(2,1)S(1)}, bf16[256,256]{1,0:T(8,128)(2,1)S(1)}, u32[]{:S(2)}, u32[]{:S(2)}) collective-permute-start(bf16[256,256]{1,0:T(8,128)(2,1)S(1)} %fusion.2), channel_id=1, source_target_pairs={{0,6},{2,0},{4,2},{6,4},{1,7},{3,1},{5,3},{7,5},{8,14},{10,8},{12,... | collective-permute-start | bytes 393224 | tf_op jit(solution)/shard_map/ppermute | solution.py:486
  77.7 10.3 %collective-permute-start.8 = (bf16[256,256]{1,0:T(8,128)(2,1)S(1)}, bf16[256,256]{1,0:T(8,128)(2,1)S(1)}, u32[]{:S(2)}, u32[]{:S(2)}) collective-permute-start(bf16[256,256]{1,0:T(8,128)(2,1)S(1)} %fusion.2), channel_id=1, source_target_pairs={{0,4},{2,6},{4,0},{6,2},{1,5},{3,7},{5,1},{7,3},{8,12},{10,14},{12... | collective-permute-start | bytes 393224 | tf_op jit(solution)/shard_map/ppermute | solution.py:486
  88.1 6.0 %copy-start.7 = (bf16[4,256,256]{2,1,0:T(8,128)(2,1)}, bf16[4,256,256]{2,1,0:T(8,128)(2,1)S(1)}, u32[]{:S(2)}) copy-start(bf16[4,256,256]{2,1,0:T(8,128)(2,1)S(1)} %pad_maximum_fusion.same) | copy-start | bytes 1572868
  88.1 6.0 %collective-permute-start.9 = (bf16[4,256,256]{2,1,0:T(8,128)(2,1)S(1)}, bf16[4,256,256]{2,1,0:T(8,128)(2,1)S(1)}, u32[]{:S(2)}, u32[]{:S(2)}) collective-permute-start(bf16[4,256,256]{2,1,0:T(8,128)(2,1)S(1)} %pad_maximum_fusion.same), channel_id=1, source_target_pairs={{0,1},{1,0},{2,3},{3,2},{4,5},{5,4},{6,7},{7,6},{8,9},{9,8},{10,11... | collective-permute-start | bytes 1572872 | tf_op jit(solution)/shard_map/ppermute | solution.py:490
  92.3 33.8 %collective-permute-start.12 = (bf16[256,2048]{1,0:T(8,128)(2,1)S(1)}, bf16[256,2048]{1,0:T(8,128)(2,1)}, u32[]{:S(2)}, u32[]{:S(2)}) collective-permute-start(bf16[256,2048]{1,0:T(8,128)(2,1)S(1)} %collective-permute-done.10.refs_2_.refs_9_), channel_id=1, source_target_pairs={{0,2},{2,4},{4,6},{6,0},{1,3},{3,5},{5,7},{7,1},{8,10},{10,12},{12... | collective-permute-start | bytes 3145736 | tf_op jit(solution)/shard_map/ppermute | solution.py:486
  94.1 11.9 %copy-start = (bf16[256,2048]{1,0:T(8,128)(2,1)S(1)}, bf16[256,2048]{1,0:T(8,128)(2,1)}, u32[]{:S(2)}) copy-start(bf16[256,2048]{1,0:T(8,128)(2,1)} %refs_8_.1) | copy-start | bytes 3145732
  100.2 16.6 %all-to-all-start.2 = ((bf16[16,64,256]{2,1,0:T(8,128)(2,1)}), bf16[16,64,256]{2,1,0:T(8,128)(2,1)S(1)}, u32[]{:S(2)}, u32[]{:S(2)}) async-start(bf16[16,64,256]{2,1,0:T(8,128)(2,1)} %project_sent.1), calls=%async_computation.2 | async-start | bytes 1048576 | tf_op jit(solution)/shard_map/all_to_all | solution.py:477
  106.0 34.3 %collective-permute-start.13 = (bf16[256,2048]{1,0:T(8,128)(2,1)S(1)}, bf16[256,2048]{1,0:T(8,128)(2,1)}, u32[]{:S(2)}, u32[]{:S(2)}) collective-permute-start(bf16[256,2048]{1,0:T(8,128)(2,1)S(1)} %copy-done), channel_id=1, source_target_pairs={{0,1},{1,0},{2,3},{3,2},{4,5},{5,4},{6,7},{7,6},{8,9},{9,8},{10,11... | collective-permute-start | bytes 3145736 | tf_op jit(solution)/shard_map/ppermute | solution.py:490
  126.1 29.1 %collective-permute-start.14 = (bf16[256,2048]{1,0:T(8,128)(2,1)S(1)}, bf16[256,2048]{1,0:T(8,128)(2,1)}, u32[]{:S(2)}, u32[]{:S(2)}) collective-permute-start(bf16[256,2048]{1,0:T(8,128)(2,1)S(1)} %collective-permute-done.10.refs_2_.refs_9_), channel_id=1, source_target_pairs={{0,1},{1,0},{2,3},{3,2},{4,5},{5,4},{6,7},{7,6},{8,9},{9,8},{10,11... | collective-permute-start | bytes 3145736 | tf_op jit(solution)/shard_map/ppermute | solution.py:490
  127.9 27.4 %collective-permute-start.15 = (bf16[256,2048]{1,0:T(8,128)(2,1)}, bf16[256,2048]{1,0:T(8,128)(2,1)}, u32[]{:S(2)}, u32[]{:S(2)}) collective-permute-start(bf16[256,2048]{1,0:T(8,128)(2,1)} %collective-permute-done.11.refs_3_.refs_10_), channel_id=1, source_target_pairs={{0,1},{1,0},{2,3},{3,2},{4,5},{5,4},{6,7},{7,6},{8,9},{9,8},{10,11... | collective-permute-start | bytes 3145736 | tf_op jit(solution)/shard_map/ppermute | solution.py:490
  128.0 27.3 %collective-permute-start.16 = (bf16[256,2048]{1,0:T(8,128)(2,1)}, bf16[256,2048]{1,0:T(8,128)(2,1)}, u32[]{:S(2)}, u32[]{:S(2)}) collective-permute-start(bf16[256,2048]{1,0:T(8,128)(2,1)} %collective-permute-done.12.refs_4_.refs_11_), channel_id=1, source_target_pairs={{0,1},{1,0},{2,3},{3,2},{4,5},{5,4},{6,7},{7,6},{8,9},{9,8},{10,11... | collective-permute-start | bytes 3145736 | tf_op jit(solution)/shard_map/ppermute | solution.py:490
  136.3 19.0 %copy-start.2 = (f32[2048]{0:T(1024)S(1)}, f32[2048]{0:T(1024)}, u32[]{:S(2)}) copy-start(f32[2048]{0:T(1024)} %param.16) | copy-start | bytes 24580
  136.3 19.0 %copy-start.3 = (s32[8]{0:T(128)S(1)}, s32[8]{0:T(128)}, u32[]{:S(2)}) copy-start(s32[8]{0:T(128)} %pad_add_fusion.1.order) | copy-start | bytes 100
  136.3 19.0 %copy-start.5 = (s32[8]{0:T(128)S(1)}, s32[8]{0:T(128)}, u32[]{:S(2)}) copy-start(s32[8]{0:T(128)} %iota.15.where.slot) | copy-start | bytes 100
  136.3 18.9 %all-to-all-start.3 = ((bf16[8,256,256]{2,1,0:T(8,128)(2,1)}), bf16[8,256,256]{2,1,0:T(8,128)(2,1)S(1)}, u32[]{:S(2)}, u32[]{:S(2)}) async-start(bf16[8,256,256]{2,1,0:T(8,128)(2,1)} %attend.2), calls=%async_computation.3 | async-start | bytes 2097152 | tf_op jit(solution)/shard_map/all_to_all | solution.py:477
  161.5 22.3 %copy-start.12 = (bf16[256,256]{1,0:T(8,128)(2,1)S(1)}, bf16[256,256]{1,0:T(8,128)(2,1)}, u32[]{:S(2)}) copy-start(bf16[256,256]{1,0:T(8,128)(2,1)} %get-tuple-element.119) | copy-start | bytes 393220
  161.6 24.2 %copy-start.11 = (bf16[256,256]{1,0:T(8,128)(2,1)S(1)}, bf16[256,256]{1,0:T(8,128)(2,1)}, u32[]{:S(2)}) copy-start(bf16[256,256]{1,0:T(8,128)(2,1)} %get-tuple-element.120) | copy-start | bytes 393220
  161.6 31.2 %copy-start.1 = (bf16[256,256]{1,0:T(8,128)(2,1)S(1)}, bf16[256,256]{1,0:T(8,128)(2,1)}, u32[]{:S(2)}) copy-start(bf16[256,256]{1,0:T(8,128)(2,1)} %get-tuple-element.121.refs_0_) | copy-start | bytes 393220
  161.6 31.2 %copy-start.4 = (s32[8]{0:T(128)S(1)}, s32[8]{0:T(128)}, u32[]{:S(2)}) copy-start(s32[8]{0:T(128)} %pad_add_fusion.2.where.slot) | copy-start | bytes 100
  161.6 47.3 %all-to-all-start.4 = ((bf16[8,256,256]{2,1,0:T(8,128)(2,1)}), bf16[8,256,256]{2,1,0:T(8,128)(2,1)S(1)}, u32[]{:S(2)}, u32[]{:S(2)}) async-start(bf16[8,256,256]{2,1,0:T(8,128)(2,1)} %project_out.2), calls=%async_computation.4 | async-start | bytes 2097152 | tf_op jit(solution)/shard_map/all_to_all | solution.py:477
  166.2 17.7 %collective-permute-start.17 = (bf16[256,256]{1,0:T(8,128)(2,1)}, bf16[256,256]{1,0:T(8,128)(2,1)S(1)}, u32[]{:S(2)}, u32[]{:S(2)}) collective-permute-start(bf16[256,256]{1,0:T(8,128)(2,1)} %get-tuple-element.114), channel_id=1, source_target_pairs={{0,2},{1,3},{2,4},{3,5},{4,6},{5,7},{6,0},{7,1},{8,10},{9,11},{10,... | collective-permute-start | bytes 393224 | tf_op jit(solution)/shard_map/ppermute | solution.py:526
  167.5 18.2 %collective-permute-start.18 = (bf16[256,256]{1,0:T(8,128)(2,1)}, bf16[256,256]{1,0:T(8,128)(2,1)S(1)}, u32[]{:S(2)}, u32[]{:S(2)}) collective-permute-start(bf16[256,256]{1,0:T(8,128)(2,1)} %get-tuple-element.115), channel_id=1, source_target_pairs={{0,6},{1,7},{2,0},{3,1},{4,2},{5,3},{6,4},{7,5},{8,14},{9,15},{10,... | collective-permute-start | bytes 393224 | tf_op jit(solution)/shard_map/ppermute | solution.py:526
  168.8 19.1 %collective-permute-start.19 = (bf16[256,256]{1,0:T(8,128)(2,1)}, bf16[256,256]{1,0:T(8,128)(2,1)S(1)}, u32[]{:S(2)}, u32[]{:S(2)}) collective-permute-start(bf16[256,256]{1,0:T(8,128)(2,1)} %get-tuple-element.116), channel_id=1, source_target_pairs={{0,4},{1,5},{2,6},{3,7},{4,0},{5,1},{6,2},{7,3},{8,12},{9,13},{10,... | collective-permute-start | bytes 393224 | tf_op jit(solution)/shard_map/ppermute | solution.py:526
  170.5 17.5 %collective-permute-start.20 = (bf16[256,256]{1,0:T(8,128)(2,1)}, bf16[256,256]{1,0:T(8,128)(2,1)S(1)}, u32[]{:S(2)}, u32[]{:S(2)}) collective-permute-start(bf16[256,256]{1,0:T(8,128)(2,1)} %get-tuple-element.117), channel_id=1, source_target_pairs={{0,1},{1,0},{2,3},{3,2},{4,5},{5,4},{6,7},{7,6},{8,9},{9,8},{10,11... | collective-permute-start | bytes 393224 | tf_op jit(solution)/shard_map/ppermute | solution.py:526
  171.7 18.2 %collective-permute-start.21 = (bf16[256,256]{1,0:T(8,128)(2,1)}, bf16[256,256]{1,0:T(8,128)(2,1)S(1)}, u32[]{:S(2)}, u32[]{:S(2)}) collective-permute-start(bf16[256,256]{1,0:T(8,128)(2,1)} %get-tuple-element.118), channel_id=1, source_target_pairs={{0,3},{1,2},{2,5},{3,4},{4,7},{5,6},{6,1},{7,0},{8,11},{9,10},{10,... | collective-permute-start | bytes 393224 | tf_op jit(solution)/shard_map/ppermute | solution.py:526
  183.9 6.1 %collective-permute-start.22 = (bf16[256,256]{1,0:T(8,128)(2,1)S(1)}, bf16[256,256]{1,0:T(8,128)(2,1)S(1)}, u32[]{:S(2)}, u32[]{:S(2)}) collective-permute-start(bf16[256,256]{1,0:T(8,128)(2,1)S(1)} %copy-done.12), channel_id=1, source_target_pairs={{0,7},{1,6},{2,1},{3,0},{4,3},{5,2},{6,5},{7,4},{8,15},{9,14},{10,... | collective-permute-start | bytes 393224 | tf_op jit(solution)/shard_map/ppermute | solution.py:526
  185.7 7.0 %collective-permute-start.23 = (bf16[256,256]{1,0:T(8,128)(2,1)S(1)}, bf16[256,256]{1,0:T(8,128)(2,1)S(1)}, u32[]{:S(2)}, u32[]{:S(2)}) collective-permute-start(bf16[256,256]{1,0:T(8,128)(2,1)S(1)} %copy-done.11), channel_id=1, source_target_pairs={{0,5},{1,4},{2,7},{3,6},{4,1},{5,0},{6,3},{7,2},{8,13},{9,12},{10,... | collective-permute-start | bytes 393224 | tf_op jit(solution)/shard_map/ppermute | solution.py:526
  198.9 6.0 %collective-permute-start.24 = (bf16[256,256]{1,0:T(8,128)(2,1)S(1)}, bf16[256,256]{1,0:T(8,128)(2,1)S(1)}, u32[]{:S(2)}, u32[]{:S(2)}) collective-permute-start(bf16[256,256]{1,0:T(8,128)(2,1)S(1)} %get-tuple-element.130), channel_id=1, source_target_pairs={{0,2},{1,3},{2,4},{3,5},{4,6},{5,7},{6,0},{7,1},{8,10},{9,11},{10,... | collective-permute-start | bytes 393224 | tf_op jit(solution)/shard_map/ppermute | solution.py:526
  200.0 7.2 %collective-permute-start.25 = (bf16[256,256]{1,0:T(8,128)(2,1)S(1)}, bf16[256,256]{1,0:T(8,128)(2,1)S(1)}, u32[]{:S(2)}, u32[]{:S(2)}) collective-permute-start(bf16[256,256]{1,0:T(8,128)(2,1)S(1)} %get-tuple-element.131), channel_id=1, source_target_pairs={{0,6},{1,7},{2,0},{3,1},{4,2},{5,3},{6,4},{7,5},{8,14},{9,15},{10,... | collective-permute-start | bytes 393224 | tf_op jit(solution)/shard_map/ppermute | solution.py:526
  201.5 8.9 %collective-permute-start.26 = (bf16[256,256]{1,0:T(8,128)(2,1)}, bf16[256,256]{1,0:T(8,128)(2,1)S(1)}, u32[]{:S(2)}, u32[]{:S(2)}) collective-permute-start(bf16[256,256]{1,0:T(8,128)(2,1)} %get-tuple-element.132), channel_id=1, source_target_pairs={{0,4},{1,5},{2,6},{3,7},{4,0},{5,1},{6,2},{7,3},{8,12},{9,13},{10,... | collective-permute-start | bytes 393224 | tf_op jit(solution)/shard_map/ppermute | solution.py:526
  202.2 8.2 %collective-permute-start.27 = (bf16[256,256]{1,0:T(8,128)(2,1)}, bf16[256,256]{1,0:T(8,128)(2,1)S(1)}, u32[]{:S(2)}, u32[]{:S(2)}) collective-permute-start(bf16[256,256]{1,0:T(8,128)(2,1)} %get-tuple-element.133), channel_id=1, source_target_pairs={{0,1},{1,0},{2,3},{3,2},{4,5},{5,4},{6,7},{7,6},{8,9},{9,8},{10,11... | collective-permute-start | bytes 393224 | tf_op jit(solution)/shard_map/ppermute | solution.py:526
  202.9 8.9 %collective-permute-start.28 = (bf16[256,256]{1,0:T(8,128)(2,1)}, bf16[256,256]{1,0:T(8,128)(2,1)S(1)}, u32[]{:S(2)}, u32[]{:S(2)}) collective-permute-start(bf16[256,256]{1,0:T(8,128)(2,1)} %get-tuple-element.134), channel_id=1, source_target_pairs={{0,3},{1,2},{2,5},{3,4},{4,7},{5,6},{6,1},{7,0},{8,11},{9,10},{10,... | collective-permute-start | bytes 393224 | tf_op jit(solution)/shard_map/ppermute | solution.py:526
  204.9 7.1 %collective-permute-start.29 = (bf16[256,256]{1,0:T(8,128)(2,1)}, bf16[256,256]{1,0:T(8,128)(2,1)S(1)}, u32[]{:S(2)}, u32[]{:S(2)}) collective-permute-start(bf16[256,256]{1,0:T(8,128)(2,1)} %get-tuple-element.135), channel_id=1, source_target_pairs={{0,7},{1,6},{2,1},{3,0},{4,3},{5,2},{6,5},{7,4},{8,15},{9,14},{10,... | collective-permute-start | bytes 393224 | tf_op jit(solution)/shard_map/ppermute | solution.py:526
  207.2 7.4 %collective-permute-start.30 = (bf16[256,256]{1,0:T(8,128)(2,1)S(1)}, bf16[256,256]{1,0:T(8,128)(2,1)S(1)}, u32[]{:S(2)}, u32[]{:S(2)}) collective-permute-start(bf16[256,256]{1,0:T(8,128)(2,1)S(1)} %get-tuple-element.136), channel_id=1, source_target_pairs={{0,5},{1,4},{2,7},{3,6},{4,1},{5,0},{6,3},{7,2},{8,13},{9,12},{10,... | collective-permute-start | bytes 393224 | tf_op jit(solution)/shard_map/ppermute | solution.py:526
  (2 other events, 1.6 us)
